TPU v7x, 512 devices: a whole 4x8x8 slice. The times are simulated.
512 devices in a mesh: sp: 64 (over z, y), tp: 8 (over x, core).
Axes of the slice: x: 4, y: 8, z: 8, core: 2. Of those that a mesh axis runs over, the one named last changes fastest.
Arguments:
- hidden_in: bfloat16 [32768, 2048], P('sp'), may hold values from -64 to 64
- pre_gain: float32 [2048], replicated, may hold values from 0.1 to 1.9
- query_proj: bfloat16 [2048, 2048], P(None, 'tp'), may hold values from -2 to 2
- key_proj: bfloat16 [2048, 2048], P('sp', 'tp'), may hold values from -2 to 2
- value_proj: bfloat16 [2048, 2048], P('sp', 'tp'), may hold values from -0.125 to 0.125
- out_proj: bfloat16 [2048, 2048], P('tp'), may hold values from -0.125 to 0.125
- post_gain: float32 [2048], replicated, may hold values from 0.1 to 1.9
Outputs:
- layer_out: bfloat16 [32768, 2048], P(('sp', 'tp'))
- log_weight: float32 [32, 32768], P('tp', 'sp')
All inputs are finite; a program needn't handle non-finite values.
Results may differ from a plain program's by a relative error of at most 0.018.
The roundings to bfloat16 on the way count: a program that leaves them out, or rounds other values in their place, can miss the bound.
Values may be sent and summed in bfloat16 or wider, within the bound.
No kernel may reach another device: no remote copies, remote signals or barrier semaphores. Data moves between devices by JAX's collectives and lax.ppermute only.
A program may use at most 64 MiB of HBM per device.

v0:
```python
import jax
import jax.numpy as jnp
from jax import lax
from jax.sharding import PartitionSpec as P

HEAD_DIM = 64
SPAN = 128


EPS = 1e-06
ROPE_BASE = 10000.0
DILATIONS = (1, 4, 16)


def side_by_side(arrays, axis, dim, along):
    widths = [a.shape[along] for a in arrays]
    both = jnp.concatenate(arrays, axis=along)
    whole = lax.all_gather(both, axis, axis=dim, tiled=True)
    return tuple(jnp.split(whole, [sum(widths[:k]) for k in range(1, len(widths))], axis=along))


def passed_along(value, axis, steps):
    count = lax.axis_size(axis)
    first, last = (max(0, -steps), min(count, count - steps))
    return lax.ppermute(value, axis, [(source, source + steps) for source in range(first, last)])


def split_up(x, dim, peers):
    dims = x.shape
    parts = x.reshape(*dims[:dim], peers, dims[dim] // peers, *dims[dim + 1 :])
    return jnp.moveaxis(parts, dim, 0)


def sum_at_owner(x, axis, dim):
    parts = split_up(x, dim, lax.axis_size(axis))
    arrived = lax.all_to_all(parts, axis, split_axis=0, concat_axis=0, tiled=True)
    return arrived.astype(jnp.float32).sum(axis=0)


def rotate(vectors, positions):
    half_dim = vectors.shape[-1] // 2
    frequency = ROPE_BASE ** (-(jnp.arange(half_dim, dtype=jnp.float32) * 2.0 / vectors.shape[-1]))
    angles = positions[:, None] * frequency[None, :]
    cos_part = jnp.cos(angles)[:, None, :]
    sin_part = jnp.sin(angles)[:, None, :]
    front_half = vectors[..., :half_dim]
    back_half = vectors[..., half_dim:]
    return jnp.concatenate(
        [
            front_half * cos_part - back_half * sin_part,
            back_half * cos_part + front_half * sin_part,
        ],
        axis=-1,
    )


def rms_scale(matrix, gain):
    return matrix * lax.rsqrt(jnp.mean(matrix * matrix, axis=-1, keepdims=True) + EPS) * gain


def window_group(queries, buffer, dilation, offset):
    local_rows, head_count, head_depth = queries.shape
    reach_rows = dilation * SPAN
    start_row = buffer.shape[1] - local_rows - reach_rows
    key_rows = buffer[0, start_row:]
    value_rows = buffer[1, start_row:]
    res_len = local_rows // dilation
    block_len = min(SPAN, res_len)
    blocks = res_len // block_len
    query_blocks = queries.reshape(blocks, block_len, dilation, head_count, head_depth)
    key_res = key_rows.reshape(-1, dilation, head_count, head_depth)
    value_res = value_rows.reshape(-1, dilation, head_count, head_depth)
    width_keys = block_len + SPAN
    key_sets = jnp.stack(
        [
            key_res[block_idx * block_len : block_idx * block_len + width_keys]
            for block_idx in range(blocks)
        ]
    )
    value_sets = jnp.stack(
        [
            value_res[block_idx * block_len : block_idx * block_len + width_keys]
            for block_idx in range(blocks)
        ]
    )
    scores = jnp.einsum(
        "bqrhe,bkrhe->brhqk", query_blocks, key_sets, preferred_element_type=jnp.float32
    ) * head_depth ** (-0.5)
    query_idx = jnp.arange(block_len, dtype=jnp.int32)[:, None]
    key_idx = jnp.arange(width_keys, dtype=jnp.int32)[None, :]
    distance = query_idx + SPAN - key_idx
    in_band = (distance >= 0) & (distance <= SPAN)
    key_pos = (
        (
            jnp.arange(blocks, dtype=jnp.int32)[:, None, None, None, None] * block_len
            + jnp.arange(width_keys, dtype=jnp.int32)[None, None, None, None, :]
        )
        * dilation
        + jnp.arange(dilation, dtype=jnp.int32)[None, :, None, None, None]
        + (offset - reach_rows)
    )
    valid = in_band[None, None, None] & (key_pos >= 0)
    scores = jnp.where(valid, scores, -jnp.inf)
    row_max = jnp.max(scores, axis=-1, keepdims=True)
    exp_scores = jnp.exp(scores - row_max)
    denominator = jnp.sum(exp_scores, axis=-1, keepdims=True)
    levels = (row_max + jnp.log(denominator))[..., 0]
    shares = (exp_scores / denominator).astype(jnp.bfloat16)
    outcome = jnp.einsum(
        "brhqk,bkrhe->bqrhe", shares, value_sets, preferred_element_type=jnp.float32
    )
    outcome = outcome.reshape(local_rows, head_count, head_depth)
    levels = levels.transpose(2, 0, 3, 1).reshape(head_count, local_rows)
    return (outcome, levels)


def blend(group_outs, group_levels):
    levels = jnp.stack(group_levels)
    row_max = jnp.max(levels, axis=0)
    log_weight = row_max + jnp.log(jnp.sum(jnp.exp(levels - row_max[None]), axis=0))
    shares = jnp.exp(levels - log_weight[None])
    blended = jnp.sum(shares.transpose(0, 2, 1)[..., None] * jnp.stack(group_outs), axis=0)
    return (blended, log_weight)


def body(hidden_in, pre_gain, query_proj, key_proj, value_proj, out_proj, post_gain):
    local_rows = hidden_in.shape[0]
    local_width = query_proj.shape[1]
    head_count = local_width // HEAD_DIM
    normed = rms_scale(hidden_in.astype(jnp.float32), pre_gain).astype(jnp.bfloat16)
    offset = lax.axis_index("sp") * local_rows
    positions = (offset + jnp.arange(local_rows, dtype=jnp.int32)).astype(jnp.float32)
    queries = rotate(
        jnp.dot(normed, query_proj, preferred_element_type=jnp.float32).reshape(
            local_rows, head_count, HEAD_DIM
        ),
        positions,
    ).astype(jnp.bfloat16)
    pieces = side_by_side((key_proj, value_proj), "sp", 0, 1)
    key_sum = jnp.dot(normed, pieces[0], preferred_element_type=jnp.float32)
    value_sum = jnp.dot(normed, pieces[1], preferred_element_type=jnp.float32)
    key_rows = (
        rotate(key_sum.reshape(local_rows, head_count, HEAD_DIM), positions)
        .astype(jnp.bfloat16)
        .reshape(local_rows, local_width)
    )
    key_value = jnp.stack([key_rows, value_sum.astype(jnp.bfloat16)])
    behind = -(-(16 * SPAN) // local_rows)
    pieces = [key_value]
    current = key_value
    for section in range(behind):
        current = passed_along(current, "sp", 1)
        pieces.insert(0, current)
    buffer = jnp.concatenate(pieces, axis=1)
    buffer = buffer.reshape(2, buffer.shape[1], head_count, HEAD_DIM)
    group_outs = []
    group_levels = []
    for dilation in DILATIONS:
        outcome, levels = window_group(queries, buffer, dilation, offset)
        group_outs.append(outcome)
        group_levels.append(levels)
    blended, log_weight = blend(group_outs, group_levels)
    attended = blended.astype(jnp.bfloat16).reshape(local_rows, local_width)
    summed = sum_at_owner(
        jnp.dot(attended, out_proj, preferred_element_type=jnp.float32).astype(jnp.bfloat16),
        "tp",
        0,
    )
    layer_out = rms_scale(summed, post_gain).astype(jnp.bfloat16)
    return (layer_out, log_weight)


def solution(mesh):
    placed = (P("sp", None), P(), P(None, "tp"), P("sp", "tp"), P("sp", "tp"), P("tp", None), P())
    return jax.shard_map(
        body,
        mesh=mesh,
        in_specs=placed,
        out_specs=(P(("sp", "tp"), None), P("tp", "sp")),
        check_vma=False,
    )
```

profile of v0, /device:TPU:256, one launch (start us, length us, event | category | flops | bytes accessed | tf_op | source)
XLA Modules:
  0.0 262.0 jit_solution(949253217690158348)
XLA Ops:
  7.2 1.5 pad_maximum_fusion.2
  8.8 2.1 fusion
  10.9 0.3 multiply_cosine_fusion
  11.3 2.9 %fusion.73 = f32[512,256]{0,1:T(8,128)} fusion(bf16[2048,256]{1,0:T(8,128)(2,1)} %param.9, bf16[512,2048]{1,0:T(8,128)(2,1)S(1)} %copy-done.3, f32[2048]{0:T(1024)S(1)} %copy-done.37, f32[512]{0:T(512)S(1)} %add_rsqrt_fusion), kind=kOutput, calls=%fused_computation.139 | convolution fusion | flops 541065216 | bytes 3680256 | tf_op jit(solution)/shard_map/dot_general | solution.py:134
  14.2 80.5 %all-gather.2.cloned.1.call-done = bf16[2048,512]{1,0:T(8,128)(2,1)} async-done(((bf16[32,512]{1,0:T(8,128)(2,1)}), bf16[2048,512]{1,0:T(8,128)(2,1)}) %all-gather.2.cloned.1.call-update) | async-done | bytes 2097168 | tf_op jit(solution)/shard_map/all_gather | solution.py:18
  94.7 2.2 fusion.19
  97.2 2.6 fusion.17
  99.9 3.1 %collective-permute-start = (bf16[2,512,256]{2,1,0:T(8,128)(2,1)S(1)}, bf16[2,512,256]{2,1,0:T(8,128)(2,1)S(1)}, u32[]{:S(2)}, u32[]{:S(2)}) collective-permute-start(bf16[2,512,256]{2,1,0:T(8,128)(2,1)S(1)} %pad_maximum_fusion), channel_id=1, source_target_pairs={{0,8},{8,16},{16,24},{24,32},{32,40},{40,48},{48,56},{56,64},{64,7... | collective-permute-start | bytes 1572872 | tf_op jit(solution)/shard_map/ppermute | solution.py:25
  103.1 11.4 %collective-permute-done = bf16[2,512,256]{2,1,0:T(8,128)(2,1)S(1)} collective-permute-done((bf16[2,512,256]{2,1,0:T(8,128)(2,1)S(1)}, bf16[2,512,256]{2,1,0:T(8,128)(2,1)S(1)}, u32[]{:S(2)}, u32[]{:S(2)}) %collective-permute-start) | collective-permute-done | bytes 524320 | tf_op jit(solution)/shard_map/ppermute | solution.py:25
  114.5 1.9 collective-permute-start.1
  116.6 12.4 %collective-permute-done.1 = bf16[2,512,256]{2,1,0:T(8,128)(2,1)S(1)} collective-permute-done((bf16[2,512,256]{2,1,0:T(8,128)(2,1)S(1)}, bf16[2,512,256]{2,1,0:T(8,128)(2,1)S(1)}, u32[]{:S(2)}, u32[]{:S(2)}) %collective-permute-start.1) | collective-permute-done | bytes 524320 | tf_op jit(solution)/shard_map/ppermute | solution.py:25
  128.9 1.9 collective-permute-start.2
  131.0 0.8 broadcast_and_fusion.2
  131.7 11.7 %collective-permute-done.2 = bf16[2,512,256]{2,1,0:T(8,128)(2,1)} collective-permute-done((bf16[2,512,256]{2,1,0:T(8,128)(2,1)S(1)}, bf16[2,512,256]{2,1,0:T(8,128)(2,1)}, u32[]{:S(2)}, u32[]{:S(2)}) %collective-permute-start.2) | collective-permute-done | bytes 524320 | tf_op jit(solution)/shard_map/ppermute | solution.py:25
  143.4 1.9 collective-permute-start.3
  145.4 0.3 copy.57
  145.7 1.0 copy.59
  146.7 0.3 copy.56
  147.0 1.0 copy.58
  147.9 0.9 copy.65
  148.8 0.9 copy.66
  149.8 0.7 copy_bitcast_fusion.1
  150.5 0.7 copy_bitcast_fusion
  151.1 7.0 %collective-permute-done.3 = bf16[2,512,256]{2,1,0:T(8,128)(2,1)} collective-permute-done((bf16[2,512,256]{2,1,0:T(8,128)(2,1)}, bf16[2,512,256]{2,1,0:T(8,128)(2,1)}, u32[]{:S(2)}, u32[]{:S(2)}) %collective-permute-start.3) | collective-permute-done | bytes 524320 | tf_op jit(solution)/shard_map/ppermute | solution.py:25
  158.1 1.9 constant_dynamic-update-slice_fusion.4
  160.0 1.9 constant_dynamic-update-slice_fusion.3
  161.8 0.8 constant_dynamic-update-slice_fusion.2
  162.7 0.9 constant_dynamic-update-slice_fusion.1
  163.6 0.8 constant_dynamic-update-slice_fusion
  164.4 4.4 %copy.55 = bf16[2,2560,256]{1,2,0:T(8,128)(2,1)} copy(bf16[2,2560,256]{2,1,0:T(8,128)(2,1)} %constant_dynamic-update-slice_fusion) | data formatting | bytes 5242880 | tf_op jit(solution)/shard_map/concatenate | solution.py:154
  168.8 3.1 %fusion.76 = (bf16[1,2560,256]{2,1,0:T(8,128)(2,1)S(1)}, bf16[1,2560,256]{2,1,0:T(8,128)(2,1)}) fusion(bf16[2,2560,256]{2,1,0:T(8,128)(2,1)} %constant_dynamic-update-slice_fusion), kind=kLoop, calls=%fused_computation.141 | loop fusion | bytes 5242880 | tf_op jit(solution)/shard_map/slice | solution.py:65
  171.9 1.1 slice_bitcast_fusion.3
  173.0 1.2 fusion.75
  174.1 2.1 reshape.508
  176.2 5.0 %fusion.10 = (f32[16,4,32]{2,1,0:T(4,128)S(1)}, f32[16,4,32,160]{3,2,1,0:T(8,128)S(1)}) fusion(pred[16,32,160]{2,1,0:T(8,128)(4,1)S(1)} %broadcast_and_fusion, bf16[160,16,4,64]{3,2,1,0:T(4,128)(2,1)} %reshape.508, bf16[32,16,4,32]{3,0,2,1:T(8,128)(2,1)} %copy.66, bf16[32,16,4,32]{3,0,2,1:T(8,128)(2,1)} %copy.65), kind=kOutput, calls=%fused_computation.24 | convolution fusion | flops 43448320 | bytes 2973696 | tf_op jit(solution)/shard_map/bqrhe,bkrhe->brhqk/dot_general | solution.py:86
  181.2 0.9 fusion.13
  182.1 0.6 copy-done.17
  182.8 0.7 stack_reshape.27
  183.5 0.7 stack_reshape.30
  184.2 2.4 copy.60
  186.6 2.0 fusion.9
  188.8 0.6 fusion.8
  189.4 0.8 copy-done.6
  190.2 1.6 fusion.11
  191.8 0.6 copy-done.32
  192.4 0.6 add_bitcast_fusion.1
  193.0 0.8 copy.62
  193.8 0.8 stack_reshape.26
  194.6 0.8 stack_reshape.29
  195.3 2.4 copy.73
  197.7 3.9 %convolution_bitcast_fusion = f32[1,128,4,4,64]{1,4,3,2,0:T(8,128)} fusion(bf16[256,4,4,64]{3,1,0,2:T(4,128)(2,1)} %bitcast.115, f32[4,4,128,256]{3,2,1,0:T(8,128)} %copy-done.6, f32[4,4,128]{2,1,0:T(4,128)} %copy-done.32, f32[4,4,128]{2,1,0:T(4,128)} %copy-done.31, pred[4,128,256]{2,1,0:T(8,128)(4,1)} %get-tuple-element.21), kind=kOutput, calls=%fused_computation.29 | convolution fusion | flops 69730304 | bytes 3293184 | tf_op jit(solution)/shard_map/brhqk,bkrhe->bqrhe/dot_general | solution.py:109
  201.8 0.8 convolution_bitcast_fusion.1
  202.6 1.1 copy.72
  203.9 2.4 copy.75
  206.3 2.1 copy.78
  208.4 4.9 %reshape.511 = bf16[160,16,4,64]{3,2,1,0:T(4,128)(2,1)} reshape(bf16[1,2560,256]{2,1,0:T(8,128)(2,1)} %get-tuple-element.13) | data formatting | bytes 2621440 | tf_op jit(solution)/shard_map/reshape.69
  213.3 3.6 %fusion.14 = f32[1,32,16,4,64]{4,1,3,2,0:T(8,128)S(1)} fusion(bf16[160,16,4,64]{3,2,1,0:T(4,128)(2,1)} %reshape.511, f32[16,4,32,160]{3,2,1,0:T(8,128)S(1)} %get-tuple-element.25, f32[16,4,32]{2,1,0:T(4,128)S(1)} %copy-done.18, f32[16,4,32]{2,1,0:T(4,128)S(1)} %copy-done.16, pred[16,32,160]{2,1,0:T(8,128)(4,1)S(1)} %broadcast_and_fusion), kind=kOutput, calls=%fused_computation.28 | convolution fusion | flops 43581440 | bytes 3244032 | tf_op jit(solution)/shard_map/brhqk,bkrhe->bqrhe/dot_general | solution.py:109
  216.9 0.6 copy.77
  217.5 0.5 copy.79
  218.1 3.6 %fusion.7 = bf16[512,4,64]{0,2,1:T(8,128)(2,1)S(1)} fusion(f32[1,512,4,64]{1,0,3,2:T(1,128)S(1)} %copy.79, f32[1,512,4,64]{1,0,3,2:T(1,128)S(1)} %copy-done.2, f32[1,512,4,64]{1,0,3,2:T(1,128)} %bitcast.112, f32[3,512,4]{1,0,2:T(4,128)S(1)} %copy.71), kind=kLoop, calls=%fused_computation.12 | loop fusion | flops 1441792 | bytes 1859584 | tf_op jit(solution)/shard_map/reduce_sum | solution.py:122
  221.7 0.7 convolution_convert_fusion
  222.4 31.3 %all_to_all.5 = bf16[8,64,2048]{2,1,0:T(8,128)(2,1)S(1)} all-to-all(bf16[8,64,2048]{2,1,0:T(8,128)(2,1)S(1)} %bitcast.103), channel_id=1, replica_groups=mesh['sp'=64,'tp'=8] {'tp'}, dimensions={0} | all-to-all | bytes 4194304 | tf_op jit(solution)/shard_map/all_to_all | solution.py:36
  253.7 0.4 convert_reduce_fusion
  254.4 0.8 multiply_convert_fusion
  (103 shorter events, 1.5 us)
Async XLA Ops:
  7.2 214.5 %copy-start = (bf16[256,2048]{1,0:T(8,128)(2,1)S(1)}, bf16[256,2048]{1,0:T(8,128)(2,1)}, u32[]{:S(2)}) copy-start(bf16[256,2048]{1,0:T(8,128)(2,1)} %param.12) | copy-start | bytes 3145732
  7.2 4.1 %copy-start.3 = (bf16[512,2048]{1,0:T(8,128)(2,1)S(1)}, bf16[512,2048]{1,0:T(8,128)(2,1)}, u32[]{:S(2)}) copy-start(bf16[512,2048]{1,0:T(8,128)(2,1)} %param.7) | copy-start | bytes 6291460
  7.2 4.1 %copy-start.37 = (f32[2048]{0:T(1024)S(1)}, f32[2048]{0:T(1024)}, u32[]{:S(2)}) copy-start(f32[2048]{0:T(1024)} %param.8) | copy-start | bytes 24580
  7.2 87.5 %all-gather.2.cloned.1.call-start = ((), (), s32[]{:S(2)}) async-start(), calls=%async_computation.1 | async-start | bytes 2129920 | tf_op jit(solution)/shard_map/all_gather | solution.py:18
  94.7 2.2 copy-start.14
  99.9 14.6 %collective-permute-start = (bf16[2,512,256]{2,1,0:T(8,128)(2,1)S(1)}, bf16[2,512,256]{2,1,0:T(8,128)(2,1)S(1)}, u32[]{:S(2)}, u32[]{:S(2)}) collective-permute-start(bf16[2,512,256]{2,1,0:T(8,128)(2,1)S(1)} %pad_maximum_fusion), channel_id=1, source_target_pairs={{0,8},{8,16},{16,24},{24,32},{32,40},{40,48},{48,56},{56,64},{64,7... | collective-permute-start | bytes 1572872 | tf_op jit(solution)/shard_map/ppermute | solution.py:25
  114.5 30.9 %copy-start.10 = (bf16[2,512,256]{2,1,0:T(8,128)(2,1)}, bf16[2,512,256]{2,1,0:T(8,128)(2,1)S(1)}, u32[]{:S(2)}) copy-start(bf16[2,512,256]{2,1,0:T(8,128)(2,1)S(1)} %collective-permute-done) | copy-start | bytes 1572868
  114.5 14.4 %collective-permute-start.1 = (bf16[2,512,256]{2,1,0:T(8,128)(2,1)S(1)}, bf16[2,512,256]{2,1,0:T(8,128)(2,1)S(1)}, u32[]{:S(2)}, u32[]{:S(2)}) collective-permute-start(bf16[2,512,256]{2,1,0:T(8,128)(2,1)S(1)} %collective-permute-done), channel_id=1, source_target_pairs={{0,8},{8,16},{16,24},{24,32},{32,40},{40,48},{48,56},{56,64},{64,7... | collective-permute-start | bytes 1572872 | tf_op jit(solution)/shard_map/ppermute | solution.py:25
  128.9 16.5 %copy-start.12 = (bf16[2,512,256]{2,1,0:T(8,128)(2,1)}, bf16[2,512,256]{2,1,0:T(8,128)(2,1)S(1)}, u32[]{:S(2)}) copy-start(bf16[2,512,256]{2,1,0:T(8,128)(2,1)S(1)} %collective-permute-done.1) | copy-start | bytes 1572868
  128.9 14.5 %collective-permute-start.2 = (bf16[2,512,256]{2,1,0:T(8,128)(2,1)S(1)}, bf16[2,512,256]{2,1,0:T(8,128)(2,1)}, u32[]{:S(2)}, u32[]{:S(2)}) collective-permute-start(bf16[2,512,256]{2,1,0:T(8,128)(2,1)S(1)} %collective-permute-done.1), channel_id=1, source_target_pairs={{0,8},{8,16},{16,24},{24,32},{32,40},{40,48},{48,56},{56,64},{64,7... | collective-permute-start | bytes 1572872 | tf_op jit(solution)/shard_map/ppermute | solution.py:25
  131.7 57.6 %copy-start.7 = (pred[4,128,256]{2,1,0:T(8,128)(4,1)}, pred[4,128,256]{2,1,0:T(8,128)(4,1)S(1)}, u32[]{:S(2)}) copy-start(pred[4,128,256]{2,1,0:T(8,128)(4,1)S(1)} %get-tuple-element.20) | copy-start | bytes 393220
  143.4 14.7 %collective-permute-start.3 = (bf16[2,512,256]{2,1,0:T(8,128)(2,1)}, bf16[2,512,256]{2,1,0:T(8,128)(2,1)}, u32[]{:S(2)}, u32[]{:S(2)}) collective-permute-start(bf16[2,512,256]{2,1,0:T(8,128)(2,1)} %collective-permute-done.2), channel_id=1, source_target_pairs={{0,8},{8,16},{16,24},{24,32},{32,40},{40,48},{48,56},{56,64},{64,7... | collective-permute-start | bytes 1572872 | tf_op jit(solution)/shard_map/ppermute | solution.py:25
  148.8 13.0 %copy-start.13 = (bf16[2,512,256]{2,1,0:T(8,128)(2,1)S(1)}, bf16[2,512,256]{2,1,0:T(8,128)(2,1)}, u32[]{:S(2)}) copy-start(bf16[2,512,256]{2,1,0:T(8,128)(2,1)} %copy-done.12) | copy-start | bytes 1572868
  149.8 12.9 %copy-start.11 = (bf16[2,512,256]{2,1,0:T(8,128)(2,1)S(1)}, bf16[2,512,256]{2,1,0:T(8,128)(2,1)}, u32[]{:S(2)}) copy-start(bf16[2,512,256]{2,1,0:T(8,128)(2,1)} %copy-done.10) | copy-start | bytes 1572868
  168.8 3.1 %copy-start.1 = (bf16[2,2560,256]{1,2,0:T(8,128)(2,1)S(1)}, bf16[2,2560,256]{1,2,0:T(8,128)(2,1)}, u32[]{:S(2)}) copy-start(bf16[2,2560,256]{1,2,0:T(8,128)(2,1)} %copy.55) | copy-start | bytes 7864324
  181.2 0.9 copy-start.15
  182.1 0.6 copy-start.17
  186.6 2.1 copy-start.23
  186.6 2.1 copy-start.24
  186.6 2.1 copy-start.25
  186.6 2.1 copy-start.26
  186.6 2.1 copy-start.27
  186.6 2.1 copy-start.28
  188.7 1.5 copy-start.6
  188.7 3.1 %copy-start.31 = (f32[4,4,128]{2,1,0:T(4,128)}, f32[4,4,128]{2,1,0:T(4,128)S(1)}, u32[]{:S(2)}) copy-start(f32[4,4,128]{2,1,0:T(4,128)S(1)} %get-tuple-element.26) | copy-start | bytes 24580
  188.7 1.4 copy-start.9
  189.4 2.4 copy-start.4
  191.8 0.6 copy-start.32
  197.7 4.0 %copy-start.5 = (f32[4,4,128,256]{3,2,1,0:T(8,128)S(1)}, f32[4,4,128,256]{3,2,1,0:T(8,128)}, u32[]{:S(2)}) copy-start(f32[4,4,128,256]{3,2,1,0:T(8,128)} %copy-done.4) | copy-start | bytes 6291460
  197.7 4.0 %copy-start.8 = (pred[4,128,256]{2,1,0:T(8,128)(4,1)S(1)}, pred[4,128,256]{2,1,0:T(8,128)(4,1)}, u32[]{:S(2)}) copy-start(pred[4,128,256]{2,1,0:T(8,128)(4,1)} %copy-done.7) | copy-start | bytes 393220
  197.7 4.0 %copy-start.19 = (bf16[1,256,1,4,64]{1,4,3,0,2:T(8,128)(2,1)S(1)}, bf16[1,256,1,4,64]{1,4,3,0,2:T(8,128)(2,1)}, u32[]{:S(2)}) copy-start(bf16[1,256,1,4,64]{1,4,3,0,2:T(8,128)(2,1)} %get-tuple-element.2) | copy-start | bytes 393220
  197.7 4.0 %copy-start.20 = (bf16[1,256,1,4,64]{1,4,3,0,2:T(8,128)(2,1)S(1)}, bf16[1,256,1,4,64]{1,4,3,0,2:T(8,128)(2,1)}, u32[]{:S(2)}) copy-start(bf16[1,256,1,4,64]{1,4,3,0,2:T(8,128)(2,1)} %get-tuple-element.3) | copy-start | bytes 393220
  197.7 4.0 %copy-start.21 = (bf16[1,256,1,4,64]{1,4,3,0,2:T(8,128)(2,1)S(1)}, bf16[1,256,1,4,64]{1,4,3,0,2:T(8,128)(2,1)}, u32[]{:S(2)}) copy-start(bf16[1,256,1,4,64]{1,4,3,0,2:T(8,128)(2,1)} %get-tuple-element.4) | copy-start | bytes 393220
  197.7 4.0 %copy-start.22 = (bf16[1,256,1,4,64]{1,4,3,0,2:T(8,128)(2,1)S(1)}, bf16[1,256,1,4,64]{1,4,3,0,2:T(8,128)(2,1)}, u32[]{:S(2)}) copy-start(bf16[1,256,1,4,64]{1,4,3,0,2:T(8,128)(2,1)} %get-tuple-element.5) | copy-start | bytes 393220
  201.7 2.0 copy-start.33
  201.7 2.0 copy-start.35
  201.7 2.0 copy-start.29
  201.7 2.0 copy-start.30
  203.8 9.5 %copy-start.34 = (f32[4,512]{1,0:T(4,128)}, f32[4,512]{1,0:T(4,128)S(1)}, u32[]{:S(2)}) copy-start(f32[4,512]{1,0:T(4,128)S(1)} %log_add_fusion) | copy-start | bytes 24580
  208.4 4.9 %copy-start.16 = (f32[16,4,32]{2,1,0:T(4,128)S(1)}, f32[16,4,32]{2,1,0:T(4,128)}, u32[]{:S(2)}) copy-start(f32[16,4,32]{2,1,0:T(4,128)} %copy-done.15) | copy-start | bytes 24580
  208.4 4.9 %copy-start.18 = (f32[16,4,32]{2,1,0:T(4,128)S(1)}, f32[16,4,32]{2,1,0:T(4,128)}, u32[]{:S(2)}) copy-start(f32[16,4,32]{2,1,0:T(4,128)} %copy-done.17) | copy-start | bytes 24580
  216.9 1.2 copy-start.2
  253.7 0.7 copy-start.36
Sparse Core Ops, SparseCore 0:
  11.6 82.9 all-gather.1
where the time goes:
time: 263 us; the launch traced here: 262 us
  waiting for transfers between devices  123 us (47%)
  local copies, waits for them, and re-layouts  45.7 us (17%)
  blocking collectives  31.3 us (12%)
  matrix products  24.4 us (9%)
  between operations  14.7 us (6%)
  other arithmetic  14.2 us (5%)
  starting transfers between devices  8.89 us (3%)
    all_gather x1, waiting for transfers between devices, side_by_side(): whole = lax.all_gather(both, axis, axis=dim, tiled=True)  80.5 us
    ppermute x4, waiting for transfers between devices, passed_along(): lax.ppermute(value, axis, [(source, source + steps) for source in range(f...  42.4 us
    all_to_all x1, blocking collectives, sum_at_owner(): lax.all_to_all(parts, axis, split_axis=0, concat_axis=0, tiled=True)  31.3 us
    ppermute x4, starting transfers between devices, passed_along(): lax.ppermute(value, axis, [(source, source + steps) for source in range(f...  8.85 us
    dot_general x3, matrix products, window_group(): jnp.einsum('brhqk,bkrhe->bqrhe', shares, value_sets, preferred_element_ty...  8.3 us
    unnamed x80, local copies, waits for them, and re-layouts  7.71 us
    dot_general x3, matrix products, window_group(): jnp.einsum('bqrhe,bkrhe->brhqk', query_blocks, key_sets, preferred_elemen...  7.62 us
    another operation x4, local copies, waits for them, and re-layouts  7.53 us
  transfers between devices with their start and end apart: 5, of which 5 were waited for; matrix products, arithmetic and copies ran while one was open for 5% of the time, Pallas kernels for 0%

commit v1 on v0

v1 whole, which is shorter than its diff:
```python
import jax
import jax.numpy as jnp
import numpy as np
from jax import lax
from jax.experimental import pallas as pl
from jax.experimental.pallas import tpu as pltpu
from jax.sharding import Mesh
from jax.sharding import PartitionSpec as P

HEAD_DIM = 64
SPAN = 128
EPS = 1e-06
ROPE_BASE = 10000.0
LOW = -1e30
SP = ("zh", "zl", "y")
Z = ("zh", "zl")
TP = ("x", "c")
F32 = jnp.float32
BF16 = jnp.bfloat16


def ring(count, steps):
    return [(i, (i + steps) % count) for i in range(count)]


def natural(i):
    return (i & 31) * 16 + ((i >> 5) & 3) * 4 + (i >> 7)


def to_residue(rows):
    i = lax.broadcasted_iota(jnp.int32, (rows, rows), 0)
    n = lax.broadcasted_iota(jnp.int32, (rows, rows), 1)
    return (natural(i) == n).astype(BF16)


def to_natural(rows):
    i = lax.broadcasted_iota(jnp.int32, (rows, rows), 1)
    n = lax.broadcasted_iota(jnp.int32, (rows, rows), 0)
    return (natural(i) == n).astype(BF16)


def rotated(x, cos, sin):
    width = x.shape[1]
    lane = lax.broadcasted_iota(jnp.int32, x.shape, 1)
    other = jnp.where((lane & 63) < 32, pltpu.roll(x, width - 32, 1), pltpu.roll(x, 32, 1))
    return x * cos + other * sin


def permuted(perm, x):
    return jnp.dot(perm, x, preferred_element_type=F32).astype(BF16)


def query_kernel(hidden_ref, gain_ref, weight_ref, cos_ref, sin_ref, normed_ref, query_ref):
    rows = hidden_ref.shape[0]
    gain = gain_ref[...]

    def step(i, carry):
        part = pl.ds(pl.multiple_of(i * 64, 64), 64)
        x = hidden_ref[part, :].astype(F32)
        scale = lax.rsqrt(jnp.mean(x * x, axis=1, keepdims=True) + EPS)
        normed_ref[part, :] = (x * scale * gain).astype(BF16)
        return carry

    lax.fori_loop(0, rows // 64, step, 0)
    query = jnp.dot(normed_ref[...], weight_ref[...], preferred_element_type=F32)
    query = rotated(query, cos_ref[...], sin_ref[...]).astype(BF16) * 0.125
    query_ref[...] = permuted(to_residue(rows), query)


def key_value_kernel(place_ref, normed_ref, mine_ref, below_ref, above_ref, cos_ref, sin_ref, key_ref, value_ref, weight_ref):
    rows = normed_ref.shape[0]
    width = key_ref.shape[1]
    low = place_ref[0]
    slabs = []
    for k in range(4):
        slabs.append((2 * k + low, mine_ref, k))
    for k in range(2):
        slabs.append((2 * k + 1 - low, below_ref, k))
        slabs.append((2 * (k + 2) + 1 - low, above_ref, k))
    for place, ref, k in slabs:
        weight_ref[pl.ds(pl.multiple_of(place * 256, 256), 256), :] = ref[k]
    normed = normed_ref[...]
    perm = to_residue(rows)
    key = jnp.dot(normed, weight_ref[:, :width], preferred_element_type=F32)
    key = rotated(key, cos_ref[...], sin_ref[...]).astype(BF16)
    key_ref[...] = permuted(perm, key)
    value = jnp.dot(normed, weight_ref[:, width:], preferred_element_type=F32).astype(BF16)
    value_ref[...] = permuted(perm, value)


def near_kernel(q_ref, k0_ref, v0_ref, k1_ref, v1_ref, bias_ref, count_ref, max_ref, sum_ref, acc_ref):
    q = q_ref[...]
    lane = lax.broadcasted_iota(jnp.int32, q.shape, 1) >> 6
    keys = k0_ref.shape[0]
    nt = (((1,), (1,)), ((), ()))
    top = jnp.zeros(q.shape, F32)
    total = jnp.zeros(q.shape, F32)
    acc = jnp.zeros(q.shape, F32)
    for head in range(q.shape[1] // HEAD_DIM):
        mine = lane == head
        qh = jnp.where(mine, q, jnp.zeros_like(q))
        s0 = lax.dot_general(qh, k0_ref[...], nt, preferred_element_type=F32) + bias_ref[0, :, :keys]
        s1 = lax.dot_general(qh, k1_ref[...], nt, preferred_element_type=F32) + bias_ref[0, :, keys:]
        m = jnp.maximum(jnp.max(s0, axis=1, keepdims=True), jnp.max(s1, axis=1, keepdims=True))
        p0 = jnp.exp(s0 - m) * count_ref[0, :, :keys]
        p1 = jnp.exp(s1 - m) * count_ref[0, :, keys:]
        l = jnp.sum(p0, axis=1, keepdims=True) + jnp.sum(p1, axis=1, keepdims=True)
        pv = jnp.dot(p0.astype(BF16), v0_ref[...], preferred_element_type=F32)
        pv = pv + jnp.dot(p1.astype(BF16), v1_ref[...], preferred_element_type=F32)
        top = jnp.where(mine, m, top)
        total = jnp.where(mine, l, total)
        acc = jnp.where(mine, pv, acc)
    max_ref[...] = top
    sum_ref[...] = total
    acc_ref[...] = acc


def far_kernel(place_ref, q_ref, max_ref, sum_ref, acc_ref, k2, v2, k3, v3, k4, v4, out_ref, log_ref, att_ref, lw_ref):
    rows, width = q_ref.shape
    block = place_ref[0]
    nt = (((1,), (1,)), ((), ()))
    qi = lax.broadcasted_iota(jnp.int32, (128, 128), 0)
    ki = lax.broadcasted_iota(jnp.int32, (128, 128), 1)
    same = (qi >> 5) == (ki >> 5)
    biases = []
    for back in (2, 3, 4):
        ok = same & (block >= back)
        if back == 4:
            ok = ok & ((ki & 31) >= (qi & 31))
        biases.append(jnp.where(ok, 0.0, LOW).astype(F32))
    lane = lax.broadcasted_iota(jnp.int32, (128, width), 1) >> 6

    def one(cls, carry):
        part = pl.ds(pl.multiple_of(cls * 128, 128), 128)
        q = q_ref[part, :]
        top, total, acc = max_ref[part, :], sum_ref[part, :], acc_ref[part, :]
        att = jnp.zeros((128, width), F32)
        lw = jnp.zeros((128, width), F32)
        for head in range(width // HEAD_DIM):
            mine = lane == head
            qh = jnp.where(mine, q, jnp.zeros_like(q))
            old = max_ref[part, :][:, head * HEAD_DIM : head * HEAD_DIM + 1]
            scores = []
            m = old
            for k, bias in zip((k2, k3, k4), biases):
                s = lax.dot_general(qh, k[part, :], nt, preferred_element_type=F32) + bias
                m = jnp.maximum(m, jnp.max(s, axis=1, keepdims=True))
                scores.append(s)
            l = jnp.zeros((128, 1), F32)
            pv = jnp.zeros((128, width), F32)
            for s, v in zip(scores, (v2, v3, v4)):
                p = jnp.exp(s - m)
                l = l + jnp.sum(p, axis=1, keepdims=True)
                pv = pv + jnp.dot(p.astype(BF16), v[part, :], preferred_element_type=F32)
            alpha = jnp.exp(top - m)
            whole = total * alpha + l
            att = jnp.where(mine, (acc * alpha + pv) / whole, att)
            lw = jnp.where(mine, m + jnp.log(whole), lw)
        att_ref[part, :] = att.astype(BF16)
        lw_ref[part, :] = lw
        return carry

    lax.fori_loop(0, rows // 128, one, 0)
    perm = to_natural(rows)
    out_ref[...] = permuted(perm, att_ref[...])
    rest = lw_ref[...]
    ordered = jnp.zeros((rows, width), F32)
    for k in range(3):
        piece = rest.astype(BF16)
        rest = rest - piece.astype(F32)
        ordered = ordered + jnp.dot(perm, piece, preferred_element_type=F32)
    flipped = ordered.T
    for head in range(width // HEAD_DIM):
        log_ref[head : head + 1, :] = flipped[head * HEAD_DIM : head * HEAD_DIM + 1, :]


def vmem(count):
    return [pl.BlockSpec(memory_space=pltpu.VMEM)] * count


SMEM = pl.BlockSpec(memory_space=pltpu.SMEM)


def cost(flops, data):
    return pl.CostEstimate(flops=flops, bytes_accessed=data, transcendentals=0)


def tables(offset, rows, width):
    half = HEAD_DIM // 2
    frequency = ROPE_BASE ** (-(jnp.arange(half, dtype=F32) * 2.0 / HEAD_DIM))
    positions = (offset + jnp.arange(rows, dtype=jnp.int32)).astype(F32)
    angles = positions[:, None] * frequency[None, :]
    cos, sin = jnp.cos(angles), jnp.sin(angles)
    heads = width // HEAD_DIM
    return jnp.tile(jnp.concatenate([cos, cos], 1), (1, heads)), jnp.tile(jnp.concatenate([-sin, sin], 1), (1, heads))


def near_masks(rows, block):
    i = jnp.arange(rows, dtype=jnp.int32)
    q = natural(i).reshape(rows // 128, 128, 1)
    k = natural(i)
    k = jnp.concatenate([k, k - rows]).reshape(1, 1, 2 * rows)
    o = q - k
    back = (o >= 0) & ((k >= 0) | (block >= 1))
    count = (o <= SPAN).astype(F32)
    count = count + (((o & 3) == 0) & (o <= 4 * SPAN)).astype(F32)
    count = count + (((o & 15) == 0) & (o <= 16 * SPAN)).astype(F32)
    count = jnp.where(back, count, 0.0)
    return jnp.where(count > 0, 0.0, LOW).astype(F32), count


def body(hidden_in, pre_gain, query_proj, key_proj, value_proj, out_proj, post_gain):
    rows, depth = hidden_in.shape
    width = query_proj.shape[1]
    shape = jax.ShapeDtypeStruct
    block = lax.axis_index(SP)
    low = lax.axis_index("zl")
    core = lax.axis_index("c")

    shard = jnp.concatenate([key_proj, value_proj], axis=1)
    copies = jnp.broadcast_to(shard[None], (32,) + shard.shape)
    mine = lax.all_to_all(copies, ("zh", "y"), split_axis=0, concat_axis=0, tiled=True)
    mine = mine.reshape(4, 256, 2 * width)
    below = lax.ppermute(mine[:2], Z, ring(8, 1))
    above = lax.ppermute(mine[2:], Z, ring(8, -1))

    cos, sin = tables(block * rows, rows, width)
    normed, query = pl.pallas_call(
        query_kernel,
        out_shape=(shape((rows, depth), BF16), shape((rows, width), BF16)),
        in_specs=vmem(5),
        out_specs=tuple(vmem(2)),
        cost_estimate=cost(2 * rows * depth * width, 4 * rows * depth),
        name="query",
    )(hidden_in, pre_gain[None], query_proj, cos, sin)

    key, value = pl.pallas_call(
        key_value_kernel,
        out_shape=(shape((rows, width), BF16),) * 2,
        in_specs=[SMEM] + vmem(6),
        out_specs=tuple(vmem(2)),
        scratch_shapes=[pltpu.VMEM((depth, 2 * width), BF16)],
        cost_estimate=cost(4 * rows * depth * width, 4 * rows * depth),
        name="key_value",
    )(low[None].astype(jnp.int32), normed, mine, below, above, cos, sin)

    forward = [(i, i + 1) for i in range(63)]
    keys, values = [key], [value]
    for back in range(4):
        keys.append(lax.ppermute(keys[-1], SP, forward))
        values.append(lax.ppermute(values[-1], SP, forward))

    bias, count = near_masks(rows, block)
    whole = pl.BlockSpec((rows, width), lambda c: (0, 0))
    piece = pl.BlockSpec((128, width), lambda c: (c, 0))
    mask = pl.BlockSpec((1, 128, 2 * rows), lambda c: (c, 0, 0))
    state = pl.pallas_call(
        near_kernel,
        grid=(rows // 128,),
        out_shape=(shape((rows, width), F32),) * 3,
        in_specs=[piece, whole, whole, whole, whole, mask, mask],
        out_specs=(piece,) * 3,
        cost_estimate=cost(8 * rows * 2 * rows * width, 4 * rows * depth),
        name="near",
    )(query, keys[0], values[0], keys[1], values[1], bias, count)

    attended, log_weight = pl.pallas_call(
        far_kernel,
        out_shape=(shape((rows, width), BF16), shape((width // HEAD_DIM, rows), F32)),
        in_specs=[SMEM] + vmem(10),
        out_specs=tuple(vmem(2)),
        scratch_shapes=[pltpu.VMEM((rows, width), BF16), pltpu.VMEM((rows, width), F32)],
        cost_estimate=cost(8 * rows * 384 * width, 4 * rows * depth),
        name="far",
    )(block[None].astype(jnp.int32), query, *state, keys[2], values[2], keys[3], values[3], keys[4], values[4])

    partial = jnp.dot(attended, out_proj, preferred_element_type=F32).astype(BF16)
    partial = partial.reshape(4, 2, rows // 8, depth)
    kept = lax.dynamic_index_in_dim(partial, core, 1, keepdims=False)
    given = lax.dynamic_index_in_dim(partial, 1 - core, 1, keepdims=False)
    taken = lax.ppermute(given, "c", [(0, 1), (1, 0)])
    pair = (kept.astype(F32) + taken.astype(F32)).astype(BF16)
    arrived = lax.all_to_all(pair, "x", split_axis=0, concat_axis=0, tiled=True)
    summed = arrived.astype(F32).sum(axis=0)
    scale = lax.rsqrt(jnp.mean(summed * summed, axis=-1, keepdims=True) + EPS)
    return (summed * scale * post_gain).astype(BF16), log_weight


def solution(mesh):
    fine = Mesh(np.asarray(mesh.devices).reshape(4, 2, 8, 4, 2), ("zh", "zl", "y", "x", "c"))
    placed = (P(SP, None), P(), P(None, TP), P(SP, TP), P(SP, TP), P(TP, None), P())
    return jax.shard_map(
        body,
        mesh=fine,
        in_specs=placed,
        out_specs=(P(SP + TP, None), P(TP, SP)),
        check_vma=False,
    )
```

time: 263 us -> 174 us (0.66)
  the two profiles are of different devices: /device:TPU:256 before, /device:TPU:24 now
where the time goes in v1:
time: 174 us; the launch traced here: 173 us
  blocking collectives  65.4 us (38%)
  starting transfers between devices  49.7 us (29%)
  Pallas kernels  31.8 us (18%)
  waiting for transfers between devices  10.9 us (6%)
  other arithmetic  7.45 us (4%)
  local copies, waits for them, and re-layouts  5.14 us (3%)
    all_to_all x1, blocking collectives, body(): lax.all_to_all(copies, ('zh', 'y'), split_axis=0, concat_axis=0, tiled=True)  45.9 us
    ppermute x4, starting transfers between devices, body(): keys.append(lax.ppermute(keys[-1], SP, forward))  22.5 us
    all_to_all x1, blocking collectives, body(): arrived = lax.all_to_all(pair, 'x', split_axis=0, concat_axis=0, tiled=True)  19.5 us
    ppermute x4, starting transfers between devices, body(): values.append(lax.ppermute(values[-1], SP, forward))  18.3 us
    pallas_call x1, Pallas kernels, body(): pl.pallas_call(near_kernel, grid=(rows // 128,), out_shape=(shape((rows,...  10.1 us
    pallas_call x1, Pallas kernels, body(): pl.pallas_call(far_kernel, out_shape=(shape((rows, width), BF16), shape((...  9.77 us
    pallas_call x1, Pallas kernels, body(): pl.pallas_call(key_value_kernel, out_shape=(shape((rows, width), BF16),)...  6.45 us
    ppermute x4, waiting for transfers between devices, body(): keys.append(lax.ppermute(keys[-1], SP, forward))  6.28 us
  transfers between devices with their start and end apart: 11, of which 5 were waited for; matrix products, arithmetic and copies ran while one was open for 3% of the time, Pallas kernels for 9%

profile of v1, /device:TPU:24, one launch (start us, length us, event | category | flops | bytes accessed | tf_op | source)
XLA Modules:
  0.0 173.0 jit_solution(12836058750352793223)
XLA Ops:
  0.6 0.0 copy-start
  0.6 0.8 pad_maximum_fusion.2
  1.5 0.1 broadcast_in_dim.32
  1.6 45.9 %all_to_all.10 = bf16[32,32,512]{2,1,0:T(8,128)(2,1)S(1)} all-to-all(bf16[32,32,512]{2,1,0:T(8,128)(2,1)S(1)} %broadcast_in_dim.32), channel_id=1, replica_groups=mesh['zh'=4,'zl'=2,'y'=8,'x'=4,'c'=2] {'zh','y'}, dimensions={0} | all-to-all | bytes 2097152 | tf_op jit(solution)/shard_map/all_to_all | solution.py:222
  47.5 0.0 copy-start.1
  47.5 1.0 fusion.12
  48.5 4.1 %collective-permute-start = (bf16[2,256,512]{2,1,0:T(8,128)(2,1)}, bf16[2,256,512]{2,1,0:T(8,128)(2,1)}, u32[]{:S(2)}, u32[]{:S(2)}) collective-permute-start(bf16[2,256,512]{2,1,0:T(8,128)(2,1)} %bitcast.6), channel_id=1, source_target_pairs={{0,64},{64,128},{128,192},{192,256},{256,320},{320,384},{384,448},... | collective-permute-start | bytes 1572872 | tf_op jit(solution)/shard_map/ppermute | solution.py:224
  52.6 3.0 %collective-permute-start.1 = (bf16[2,256,512]{2,1,0:T(8,128)(2,1)S(1)}, bf16[2,256,512]{2,1,0:T(8,128)(2,1)}, u32[]{:S(2)}, u32[]{:S(2)}) collective-permute-start(bf16[2,256,512]{2,1,0:T(8,128)(2,1)S(1)} %bitcast.21), channel_id=1, source_target_pairs={{0,448},{64,0},{128,64},{192,128},{256,192},{320,256},{384,320},{4... | collective-permute-start | bytes 1572872 | tf_op jit(solution)/shard_map/ppermute | solution.py:225
  55.6 0.3 fusion.6
  56.0 0.1 tile.20
  56.0 1.0 copy.10.sin_ref
  57.0 0.0 copy-done.1
  57.1 1.0 copy.9.cos_ref
  58.1 5.5 %query.1 = (bf16[512,2048]{1,0:T(8,128)(2,1)}, bf16[512,256]{1,0:T(8,128)(2,1)}) custom-call(bf16[512,2048]{1,0:T(8,128)(2,1)} %hidden_ref.1, f32[1,2048]{1,0:T(1,128)} %bitcast.22, bf16[2048,256]{1,0:T(8,128)(2,1)} %weight_ref.1, f32[512,256]{1,0:T(8,128)} %copy.9.cos_ref, f32[512,256]{1,0:T(8,128)} %copy.10.sin_ref), custom_call_target="tpu_custom_call" | custom-call | flops 536870912 | bytes 4194304 | tf_op jit(solution)/shard_map/query/pallas_call | solution.py:228
  63.6 0.0 collective-permute-done.below_ref
  63.6 0.5 collective-permute-done.1.above_ref
  64.1 6.4 %key_value.1 = (bf16[512,256]{1,0:T(8,128)(2,1)}, bf16[512,256]{1,0:T(8,128)(2,1)}) custom-call(s32[1]{0:T(128)} %bitcast.4.place_ref, bf16[512,2048]{1,0:T(8,128)(2,1)} %get-tuple-element.12.normed_ref, bf16[4,256,512]{2,1,0:T(8,128)(2,1)} %bitcast.16, bf16[2,256,512]{2,1,0:T(8,128)(2,1)} %collective-permute-done.below_ref, ...), custom_call_target="tpu_custom_call" | custom-call | flops 1073741824 | bytes 4194304 | tf_op jit(solution)/shard_map/key_value/pallas_call | solution.py:237
  70.6 5.9 %collective-permute-start.2 = (bf16[512,256]{1,0:T(8,128)(2,1)}, bf16[512,256]{1,0:T(8,128)(2,1)S(1)}, u32[]{:S(2)}, u32[]{:S(2)}) collective-permute-start(bf16[512,256]{1,0:T(8,128)(2,1)} %get-tuple-element.13.k0_ref), channel_id=1, source_target_pairs={{0,8},{8,16},{16,24},{24,32},{32,40},{40,48},{48,56},{56,64},{64,7... | collective-permute-start | bytes 786440 | tf_op jit(solution)/shard_map/ppermute | solution.py:250
  76.4 1.9 %collective-permute-start.3 = (bf16[512,256]{1,0:T(8,128)(2,1)}, bf16[512,256]{1,0:T(8,128)(2,1)S(1)}, u32[]{:S(2)}, u32[]{:S(2)}) collective-permute-start(bf16[512,256]{1,0:T(8,128)(2,1)} %get-tuple-element.14.v0_ref), channel_id=1, source_target_pairs={{0,8},{8,16},{16,24},{24,32},{32,40},{40,48},{48,56},{56,64},{64,7... | collective-permute-start | bytes 786440 | tf_op jit(solution)/shard_map/ppermute | solution.py:251
  78.4 5.1 %collective-permute-done.2.k1_ref = bf16[512,256]{1,0:T(8,128)(2,1)S(1)} collective-permute-done((bf16[512,256]{1,0:T(8,128)(2,1)}, bf16[512,256]{1,0:T(8,128)(2,1)S(1)}, u32[]{:S(2)}, u32[]{:S(2)}) %collective-permute-start.2) | collective-permute-done | bytes 262176 | tf_op jit(solution)/shard_map/ppermute | solution.py:250
  83.4 0.0 copy-start.8
  83.4 5.5 %collective-permute-start.4 = (bf16[512,256]{1,0:T(8,128)(2,1)S(1)}, bf16[512,256]{1,0:T(8,128)(2,1)S(1)}, u32[]{:S(2)}, u32[]{:S(2)}) collective-permute-start(bf16[512,256]{1,0:T(8,128)(2,1)S(1)} %collective-permute-done.2.k1_ref), channel_id=1, source_target_pairs={{0,8},{8,16},{16,24},{24,32},{32,40},{40,48},{48,56},{56,64},{64,7... | collective-permute-start | bytes 786440 | tf_op jit(solution)/shard_map/ppermute | solution.py:250
  88.9 0.0 collective-permute-done.3.v1_ref
  88.9 0.0 copy-start.9
  88.9 5.4 %collective-permute-start.5 = (bf16[512,256]{1,0:T(8,128)(2,1)S(1)}, bf16[512,256]{1,0:T(8,128)(2,1)S(1)}, u32[]{:S(2)}, u32[]{:S(2)}) collective-permute-start(bf16[512,256]{1,0:T(8,128)(2,1)S(1)} %collective-permute-done.3.v1_ref), channel_id=1, source_target_pairs={{0,8},{8,16},{16,24},{24,32},{32,40},{40,48},{48,56},{56,64},{64,7... | collective-permute-start | bytes 786440 | tf_op jit(solution)/shard_map/ppermute | solution.py:251
  94.4 1.2 collective-permute-done.4.k2
  95.6 0.0 copy-start.2
  95.6 5.6 %collective-permute-start.6 = (bf16[512,256]{1,0:T(8,128)(2,1)S(1)}, bf16[512,256]{1,0:T(8,128)(2,1)S(1)}, u32[]{:S(2)}, u32[]{:S(2)}) collective-permute-start(bf16[512,256]{1,0:T(8,128)(2,1)S(1)} %collective-permute-done.4.k2), channel_id=1, source_target_pairs={{0,8},{8,16},{16,24},{24,32},{32,40},{40,48},{48,56},{56,64},{64,7... | collective-permute-start | bytes 786440 | tf_op jit(solution)/shard_map/ppermute | solution.py:250
  101.2 0.0 collective-permute-done.5.v2
  101.2 0.0 copy-start.3
  101.2 5.4 %collective-permute-start.7 = (bf16[512,256]{1,0:T(8,128)(2,1)S(1)}, bf16[512,256]{1,0:T(8,128)(2,1)S(1)}, u32[]{:S(2)}, u32[]{:S(2)}) collective-permute-start(bf16[512,256]{1,0:T(8,128)(2,1)S(1)} %collective-permute-done.5.v2), channel_id=1, source_target_pairs={{0,8},{8,16},{16,24},{24,32},{32,40},{40,48},{48,56},{56,64},{64,7... | collective-permute-start | bytes 786440 | tf_op jit(solution)/shard_map/ppermute | solution.py:251
  106.7 0.0 collective-permute-done.6.k3
  106.7 0.0 copy-start.4
  106.7 5.5 %collective-permute-start.8 = (bf16[512,256]{1,0:T(8,128)(2,1)S(1)}, bf16[512,256]{1,0:T(8,128)(2,1)S(1)}, u32[]{:S(2)}, u32[]{:S(2)}) collective-permute-start(bf16[512,256]{1,0:T(8,128)(2,1)S(1)} %collective-permute-done.6.k3), channel_id=1, source_target_pairs={{0,8},{8,16},{16,24},{24,32},{32,40},{40,48},{48,56},{56,64},{64,7... | collective-permute-start | bytes 786440 | tf_op jit(solution)/shard_map/ppermute | solution.py:250
  112.3 1.1 collective-permute-done.7.v3
  113.3 0.0 copy-start.5
  113.3 5.6 %collective-permute-start.9 = (bf16[512,256]{1,0:T(8,128)(2,1)S(1)}, bf16[512,256]{1,0:T(8,128)(2,1)S(1)}, u32[]{:S(2)}, u32[]{:S(2)}) collective-permute-start(bf16[512,256]{1,0:T(8,128)(2,1)S(1)} %collective-permute-done.7.v3), channel_id=1, source_target_pairs={{0,8},{8,16},{16,24},{24,32},{32,40},{40,48},{48,56},{56,64},{64,7... | collective-permute-start | bytes 786440 | tf_op jit(solution)/shard_map/ppermute | solution.py:251
  118.9 3.5 %add_select_fusion = (f32[4,128,1024]{2,1,0:T(8,128)}, f32[4,128,1024]{2,1,0:T(8,128)}) fusion(s32[1024]{0:T(1024)S(1)} %pad_add_fusion, s32[4,128]{1,0:T(4,128)S(1)} %shift-right-arithmetic_add_fusion, pred[1024]{0:T(1024)(128)(4,1)S(1)} %compare_or_fusion), kind=kLoop, calls=%fused_computation.12 | loop fusion | flops 10485760 | bytes 4201472 | tf_op jit(solution)/shard_map/jit(_where)/select_n | solution.py:208
  122.4 0.0 copy-done.8
  122.4 0.0 copy-done.9
  122.4 0.0 copy-done.2
  122.4 0.0 copy-done.3
  122.4 0.0 copy-done.4
  122.4 0.0 copy-done.5
  122.5 10.1 %near.1 = (f32[512,256]{1,0:T(8,128)}, f32[512,256]{1,0:T(8,128)}, f32[512,256]{1,0:T(8,128)}) custom-call(bf16[512,256]{1,0:T(8,128)(2,1)} %get-tuple-element.11.q_ref, bf16[512,256]{1,0:T(8,128)(2,1)} %get-tuple-element.13.k0_ref, bf16[512,256]{1,0:T(8,128)(2,1)} %get-tuple-element.14.v0_ref, bf16[512,256]{1,0:T(8,128)(2,1)} %copy-done.8, ...), custom_call_target="tpu_custom_call" | custom-call | flops 1073741824 | bytes 4194304 | tf_op jit(solution)/shard_map/near/pallas_call | solution.py:257
  132.5 0.0 collective-permute-done.8.k4
  132.5 0.0 copy-start.6
  132.5 0.0 collective-permute-done.9.v4
  132.5 0.0 copy-start.7
  132.5 0.7 copy-done.6
  133.2 0.1 copy-done.7
  133.3 9.8 %far.1 = (bf16[512,256]{1,0:T(8,128)(2,1)}, f32[4,512]{1,0:T(4,128)}) custom-call(s32[1]{0:T(128)} %bitcast.place_ref, bf16[512,256]{1,0:T(8,128)(2,1)} %get-tuple-element.11.q_ref, f32[512,256]{1,0:T(8,128)} %get-tuple-element.15.max_ref, f32[512,256]{1,0:T(8,128)} %get-tuple-element.16.sum_ref, f32[512,256]{1,0:T(8,128)} %get-tuple-element.17.acc_ref, ...), custom_call_target="tpu_custom_call" | custom-call | flops 402653184 | bytes 4194304 | tf_op jit(solution)/shard_map/far/pallas_call | solution.py:267
  143.1 0.0 copy-done
  143.1 1.7 convolution_convert_fusion
  144.8 1.1 dynamic-slice_bitcast_fusion
  145.9 1.9 %collective-permute-start.10 = (bf16[4,64,2048]{2,1,0:T(8,128)(2,1)}, bf16[4,64,2048]{2,1,0:T(8,128)(2,1)}, u32[]{:S(2)}, u32[]{:S(2)}) collective-permute-start(bf16[4,64,2048]{2,1,0:T(8,128)(2,1)} %dynamic-slice_bitcast_fusion), channel_id=1, source_target_pairs={{0,1},{1,0},{2,3},{3,2},{4,5},{5,4},{6,7},{7,6},{8,9},{9,8},{10,11... | collective-permute-start | bytes 3145736 | tf_op jit(solution)/shard_map/ppermute | solution.py:281
  147.8 3.0 %collective-permute-done.10 = bf16[4,64,2048]{2,1,0:T(8,128)(2,1)} collective-permute-done((bf16[4,64,2048]{2,1,0:T(8,128)(2,1)}, bf16[4,64,2048]{2,1,0:T(8,128)(2,1)}, u32[]{:S(2)}, u32[]{:S(2)}) %collective-permute-start.10) | collective-permute-done | bytes 1048608 | tf_op jit(solution)/shard_map/ppermute | solution.py:281
  150.7 1.6 fusion.2
  152.4 0.0 copy-start.10
  152.4 19.5 %all_to_all.11 = bf16[4,64,2048]{2,1,0:T(8,128)(2,1)S(1)} all-to-all(bf16[4,64,2048]{2,1,0:T(8,128)(2,1)S(1)} %fusion.2), channel_id=1, replica_groups=mesh['zh'=4,'zl'=2,'y'=8,'x'=4,'c'=2] {'x'}, dimensions={0} | all-to-all | bytes 2097152 | tf_op jit(solution)/shard_map/all_to_all | solution.py:283
  171.9 0.2 convert_reduce_fusion
  172.0 0.1 multiply_reduce_fusion
  172.2 0.0 copy-done.10
  172.2 0.8 multiply_convert_fusion
  (9 shorter events, 0.1 us)
Async XLA Ops:
  0.6 142.5 %copy-start = (bf16[256,2048]{1,0:T(8,128)(2,1)S(1)}, bf16[256,2048]{1,0:T(8,128)(2,1)}, u32[]{:S(2)}) copy-start(bf16[256,2048]{1,0:T(8,128)(2,1)} %param.12) | copy-start | bytes 3145732
  47.5 9.5 %copy-start.1 = (bf16[32,32,512]{2,1,0:T(8,128)(2,1)}, bf16[32,32,512]{2,1,0:T(8,128)(2,1)S(1)}, u32[]{:S(2)}) copy-start(bf16[32,32,512]{2,1,0:T(8,128)(2,1)S(1)} %all_to_all.10) | copy-start | bytes 3145732
  48.5 15.1 %collective-permute-start = (bf16[2,256,512]{2,1,0:T(8,128)(2,1)}, bf16[2,256,512]{2,1,0:T(8,128)(2,1)}, u32[]{:S(2)}, u32[]{:S(2)}) collective-permute-start(bf16[2,256,512]{2,1,0:T(8,128)(2,1)} %bitcast.6), channel_id=1, source_target_pairs={{0,64},{64,128},{128,192},{192,256},{256,320},{320,384},{384,448},... | collective-permute-start | bytes 1572872 | tf_op jit(solution)/shard_map/ppermute | solution.py:224
  52.6 11.5 %collective-permute-start.1 = (bf16[2,256,512]{2,1,0:T(8,128)(2,1)S(1)}, bf16[2,256,512]{2,1,0:T(8,128)(2,1)}, u32[]{:S(2)}, u32[]{:S(2)}) collective-permute-start(bf16[2,256,512]{2,1,0:T(8,128)(2,1)S(1)} %bitcast.21), channel_id=1, source_target_pairs={{0,448},{64,0},{128,64},{192,128},{256,192},{320,256},{384,320},{4... | collective-permute-start | bytes 1572872 | tf_op jit(solution)/shard_map/ppermute | solution.py:225
  70.6 12.9 %collective-permute-start.2 = (bf16[512,256]{1,0:T(8,128)(2,1)}, bf16[512,256]{1,0:T(8,128)(2,1)S(1)}, u32[]{:S(2)}, u32[]{:S(2)}) collective-permute-start(bf16[512,256]{1,0:T(8,128)(2,1)} %get-tuple-element.13.k0_ref), channel_id=1, source_target_pairs={{0,8},{8,16},{16,24},{24,32},{32,40},{40,48},{48,56},{56,64},{64,7... | collective-permute-start | bytes 786440 | tf_op jit(solution)/shard_map/ppermute | solution.py:250
  76.4 12.5 %collective-permute-start.3 = (bf16[512,256]{1,0:T(8,128)(2,1)}, bf16[512,256]{1,0:T(8,128)(2,1)S(1)}, u32[]{:S(2)}, u32[]{:S(2)}) collective-permute-start(bf16[512,256]{1,0:T(8,128)(2,1)} %get-tuple-element.14.v0_ref), channel_id=1, source_target_pairs={{0,8},{8,16},{16,24},{24,32},{32,40},{40,48},{48,56},{56,64},{64,7... | collective-permute-start | bytes 786440 | tf_op jit(solution)/shard_map/ppermute | solution.py:251
  83.4 39.0 %copy-start.8 = (bf16[512,256]{1,0:T(8,128)(2,1)}, bf16[512,256]{1,0:T(8,128)(2,1)S(1)}, u32[]{:S(2)}) copy-start(bf16[512,256]{1,0:T(8,128)(2,1)S(1)} %collective-permute-done.2.k1_ref) | copy-start | bytes 786436
  83.4 12.2 %collective-permute-start.4 = (bf16[512,256]{1,0:T(8,128)(2,1)S(1)}, bf16[512,256]{1,0:T(8,128)(2,1)S(1)}, u32[]{:S(2)}, u32[]{:S(2)}) collective-permute-start(bf16[512,256]{1,0:T(8,128)(2,1)S(1)} %collective-permute-done.2.k1_ref), channel_id=1, source_target_pairs={{0,8},{8,16},{16,24},{24,32},{32,40},{40,48},{48,56},{56,64},{64,7... | collective-permute-start | bytes 786440 | tf_op jit(solution)/shard_map/ppermute | solution.py:250
  88.9 33.5 %copy-start.9 = (bf16[512,256]{1,0:T(8,128)(2,1)}, bf16[512,256]{1,0:T(8,128)(2,1)S(1)}, u32[]{:S(2)}) copy-start(bf16[512,256]{1,0:T(8,128)(2,1)S(1)} %collective-permute-done.3.v1_ref) | copy-start | bytes 786436
  88.9 12.3 %collective-permute-start.5 = (bf16[512,256]{1,0:T(8,128)(2,1)S(1)}, bf16[512,256]{1,0:T(8,128)(2,1)S(1)}, u32[]{:S(2)}, u32[]{:S(2)}) collective-permute-start(bf16[512,256]{1,0:T(8,128)(2,1)S(1)} %collective-permute-done.3.v1_ref), channel_id=1, source_target_pairs={{0,8},{8,16},{16,24},{24,32},{32,40},{40,48},{48,56},{56,64},{64,7... | collective-permute-start | bytes 786440 | tf_op jit(solution)/shard_map/ppermute | solution.py:251
  95.6 26.8 %copy-start.2 = (bf16[512,256]{1,0:T(8,128)(2,1)}, bf16[512,256]{1,0:T(8,128)(2,1)S(1)}, u32[]{:S(2)}) copy-start(bf16[512,256]{1,0:T(8,128)(2,1)S(1)} %collective-permute-done.4.k2) | copy-start | bytes 786436
  95.6 11.1 %collective-permute-start.6 = (bf16[512,256]{1,0:T(8,128)(2,1)S(1)}, bf16[512,256]{1,0:T(8,128)(2,1)S(1)}, u32[]{:S(2)}, u32[]{:S(2)}) collective-permute-start(bf16[512,256]{1,0:T(8,128)(2,1)S(1)} %collective-permute-done.4.k2), channel_id=1, source_target_pairs={{0,8},{8,16},{16,24},{24,32},{32,40},{40,48},{48,56},{56,64},{64,7... | collective-permute-start | bytes 786440 | tf_op jit(solution)/shard_map/ppermute | solution.py:250
  101.2 21.2 %copy-start.3 = (bf16[512,256]{1,0:T(8,128)(2,1)}, bf16[512,256]{1,0:T(8,128)(2,1)S(1)}, u32[]{:S(2)}) copy-start(bf16[512,256]{1,0:T(8,128)(2,1)S(1)} %collective-permute-done.5.v2) | copy-start | bytes 786436
  101.2 12.1 %collective-permute-start.7 = (bf16[512,256]{1,0:T(8,128)(2,1)S(1)}, bf16[512,256]{1,0:T(8,128)(2,1)S(1)}, u32[]{:S(2)}, u32[]{:S(2)}) collective-permute-start(bf16[512,256]{1,0:T(8,128)(2,1)S(1)} %collective-permute-done.5.v2), channel_id=1, source_target_pairs={{0,8},{8,16},{16,24},{24,32},{32,40},{40,48},{48,56},{56,64},{64,7... | collective-permute-start | bytes 786440 | tf_op jit(solution)/shard_map/ppermute | solution.py:251
  106.7 15.7 %copy-start.4 = (bf16[512,256]{1,0:T(8,128)(2,1)}, bf16[512,256]{1,0:T(8,128)(2,1)S(1)}, u32[]{:S(2)}) copy-start(bf16[512,256]{1,0:T(8,128)(2,1)S(1)} %collective-permute-done.6.k3) | copy-start | bytes 786436
  106.7 25.8 %collective-permute-start.8 = (bf16[512,256]{1,0:T(8,128)(2,1)S(1)}, bf16[512,256]{1,0:T(8,128)(2,1)S(1)}, u32[]{:S(2)}, u32[]{:S(2)}) collective-permute-start(bf16[512,256]{1,0:T(8,128)(2,1)S(1)} %collective-permute-done.6.k3), channel_id=1, source_target_pairs={{0,8},{8,16},{16,24},{24,32},{32,40},{40,48},{48,56},{56,64},{64,7... | collective-permute-start | bytes 786440 | tf_op jit(solution)/shard_map/ppermute | solution.py:250
  113.3 9.1 %copy-start.5 = (bf16[512,256]{1,0:T(8,128)(2,1)}, bf16[512,256]{1,0:T(8,128)(2,1)S(1)}, u32[]{:S(2)}) copy-start(bf16[512,256]{1,0:T(8,128)(2,1)S(1)} %collective-permute-done.7.v3) | copy-start | bytes 786436
  113.3 19.2 %collective-permute-start.9 = (bf16[512,256]{1,0:T(8,128)(2,1)S(1)}, bf16[512,256]{1,0:T(8,128)(2,1)S(1)}, u32[]{:S(2)}, u32[]{:S(2)}) collective-permute-start(bf16[512,256]{1,0:T(8,128)(2,1)S(1)} %collective-permute-done.7.v3), channel_id=1, source_target_pairs={{0,8},{8,16},{16,24},{24,32},{32,40},{40,48},{48,56},{56,64},{64,7... | collective-permute-start | bytes 786440 | tf_op jit(solution)/shard_map/ppermute | solution.py:251
  132.5 0.7 copy-start.6
  132.5 0.8 copy-start.7
  145.9 4.9 %collective-permute-start.10 = (bf16[4,64,2048]{2,1,0:T(8,128)(2,1)}, bf16[4,64,2048]{2,1,0:T(8,128)(2,1)}, u32[]{:S(2)}, u32[]{:S(2)}) collective-permute-start(bf16[4,64,2048]{2,1,0:T(8,128)(2,1)} %dynamic-slice_bitcast_fusion), channel_id=1, source_target_pairs={{0,1},{1,0},{2,3},{3,2},{4,5},{5,4},{6,7},{7,6},{8,9},{9,8},{10,11... | collective-permute-start | bytes 3145736 | tf_op jit(solution)/shard_map/ppermute | solution.py:281
  152.4 19.8 %copy-start.10 = (f32[2048]{0:T(1024)S(1)}, f32[2048]{0:T(1024)}, u32[]{:S(2)}) copy-start(f32[2048]{0:T(1024)} %param.13) | copy-start | bytes 24580

commit v2 on v1

v2 whole, which is shorter than its diff:
```python
import functools

import jax
import jax.numpy as jnp
import numpy as np
from jax import lax
from jax.experimental import pallas as pl
from jax.experimental.pallas import tpu as pltpu
from jax.sharding import Mesh
from jax.sharding import PartitionSpec as P

HEAD_DIM = 64
SPAN = 128
EPS = 1e-06
ROPE_BASE = 10000.0
LOW = -1e30
SP = ("zh", "zl", "y")
Z = ("zh", "zl")
TP = ("x", "c")
F32 = jnp.float32
BF16 = jnp.bfloat16


def ring(count, steps):
    return [(i, (i + steps) % count) for i in range(count)]


def natural(i):
    return (i & 31) * 16 + ((i >> 5) & 3) * 4 + (i >> 7)


def to_residue(rows):
    i = lax.broadcasted_iota(jnp.int32, (rows, rows), 0)
    n = lax.broadcasted_iota(jnp.int32, (rows, rows), 1)
    return (natural(i) == n).astype(BF16)


def to_natural(rows):
    i = lax.broadcasted_iota(jnp.int32, (rows, rows), 1)
    n = lax.broadcasted_iota(jnp.int32, (rows, rows), 0)
    return (natural(i) == n).astype(BF16)


def rotated(x, cos, sin):
    width = x.shape[1]
    lane = lax.broadcasted_iota(jnp.int32, x.shape, 1)
    other = jnp.where((lane & 63) < 32, pltpu.roll(x, width - 32, 1), pltpu.roll(x, 32, 1))
    return x * cos + other * sin


def permuted(perm, x):
    return jnp.dot(perm, x, preferred_element_type=F32).astype(BF16)


def query_kernel(hidden_ref, gain_ref, weight_ref, cos_ref, sin_ref, normed_ref, query_ref):
    rows = hidden_ref.shape[0]
    gain = gain_ref[...]

    def step(i, carry):
        part = pl.ds(pl.multiple_of(i * 64, 64), 64)
        x = hidden_ref[part, :].astype(F32)
        scale = lax.rsqrt(jnp.mean(x * x, axis=1, keepdims=True) + EPS)
        normed_ref[part, :] = (x * scale * gain).astype(BF16)
        return carry

    lax.fori_loop(0, rows // 64, step, 0)
    query = jnp.dot(normed_ref[...], weight_ref[...], preferred_element_type=F32)
    query = rotated(query, cos_ref[...], sin_ref[...]).astype(BF16) * 0.125
    query_ref[...] = permuted(to_residue(rows), query)


def key_value_kernel(place_ref, normed_ref, mine_ref, below_ref, above_ref, cos_ref, sin_ref, key_ref, value_ref, weight_ref):
    rows = normed_ref.shape[0]
    width = key_ref.shape[1]
    low = place_ref[0]
    slabs = []
    for k in range(4):
        slabs.append((2 * k + low, mine_ref, k))
    for k in range(2):
        slabs.append((2 * k + 1 - low, below_ref, k))
        slabs.append((2 * (k + 2) + 1 - low, above_ref, k))
    for place, ref, k in slabs:
        weight_ref[pl.ds(pl.multiple_of(place * 256, 256), 256), :] = ref[k]
    normed = normed_ref[...]
    perm = to_residue(rows)
    key = jnp.dot(normed, weight_ref[:, :width], preferred_element_type=F32)
    key = rotated(key, cos_ref[...], sin_ref[...]).astype(BF16)
    key_ref[...] = permuted(perm, key)
    value = jnp.dot(normed, weight_ref[:, width:], preferred_element_type=F32).astype(BF16)
    value_ref[...] = permuted(perm, value)


NT = (((1,), (1,)), ((), ()))


def stack_heads(q):
    lane = lax.broadcasted_iota(jnp.int32, q.shape, 1) >> 6
    return jnp.concatenate([jnp.where(lane == h, q, jnp.zeros_like(q)) for h in range(q.shape[1] // HEAD_DIM)], axis=0)


def own_heads(stacked):
    rows, width = stacked.shape[0] // 4, stacked.shape[1]
    lane = lax.broadcasted_iota(jnp.int32, (rows, width), 1) >> 6
    out = stacked[:rows]
    for h in range(1, width // HEAD_DIM):
        out = jnp.where(lane == h, stacked[h * rows : (h + 1) * rows], out)
    return out


def near_kernel(place_ref, q_ref, k0_ref, v0_ref, k1_ref, v1_ref, max_ref, sum_ref, acc_ref, s_ref, p_ref, bias_ref, count_ref, stat_ref):
    cls = pl.program_id(0)
    keys, width = k0_ref.shape
    heads = width // HEAD_DIM
    i = lax.broadcasted_iota(jnp.int32, (128, 1), 0)
    qn = (i & 31) * 16 + (i >> 5) * 4 + cls
    kn = natural(lax.broadcasted_iota(jnp.int32, (1, keys), 1))
    seen = (place_ref[0] >= 1).astype(F32)
    for part in range(2):
        o = qn - kn + part * keys
        count = (o <= SPAN).astype(F32)
        count = count + (((o & 3) == 0) & (o <= 4 * SPAN)).astype(F32)
        count = count + ((o & 15) == 0).astype(F32)
        if part == 0:
            count = jnp.where(o >= 0, count, 0.0)
        else:
            count = count * seen
        count_ref[:, part * keys : (part + 1) * keys] = count
        bias_ref[:, part * keys : (part + 1) * keys] = jnp.where(count > 0, 0.0, LOW).astype(F32)
    q4 = stack_heads(q_ref[...])
    s_ref[:, :keys] = lax.dot_general(q4, k0_ref[...], NT, preferred_element_type=F32)
    s_ref[:, keys:] = lax.dot_general(q4, k1_ref[...], NT, preferred_element_type=F32)
    step = 32
    for r in range(0, heads * 128, step):
        mask = slice(r % 128, r % 128 + step)
        s = s_ref[r : r + step, :] + bias_ref[mask, :]
        m = jnp.max(s, axis=1, keepdims=True)
        p = jnp.exp(s - m) * count_ref[mask, :]
        stat_ref[0, r : r + step, :] = jnp.broadcast_to(m, (step, width))
        stat_ref[1, r : r + step, :] = jnp.broadcast_to(jnp.sum(p, axis=1, keepdims=True), (step, width))
        p_ref[r : r + step, :] = p.astype(BF16)
    pv = jnp.dot(p_ref[:, :keys], v0_ref[...], preferred_element_type=F32)
    pv = pv + jnp.dot(p_ref[:, keys:], v1_ref[...], preferred_element_type=F32)
    max_ref[...] = own_heads(stat_ref[0])
    sum_ref[...] = own_heads(stat_ref[1])
    acc_ref[...] = own_heads(pv)


def far_masks(block, backs):
    qi = lax.broadcasted_iota(jnp.int32, (128, 128), 0)
    ki = lax.broadcasted_iota(jnp.int32, (128, 128), 1)
    biases = []
    for back in backs:
        ok = ((qi >> 5) == (ki >> 5)) & (block >= back)
        if back == 4:
            ok = ok & ((ki & 31) >= (qi & 31))
        biases.append(jnp.where(ok, 0.0, LOW).astype(F32))
    return biases


def far_kernel(backs, last, place_ref, q_ref, max_ref, sum_ref, acc_ref, *refs):
    count = len(backs)
    width = q_ref.shape[1]
    heads = width // HEAD_DIM
    sources = [(refs[2 * n], refs[2 * n + 1]) for n in range(count)]
    outs = refs[2 * count :]
    s_ref, p_ref, stat_ref = outs[-3:]
    biases = far_masks(place_ref[0], backs)
    q4 = stack_heads(q_ref[...])
    old = [max_ref[:, h * HEAD_DIM : h * HEAD_DIM + 1] for h in range(heads)]
    for n, (k_ref, _) in enumerate(sources):
        s_ref[:, n * 128 : (n + 1) * 128] = lax.dot_general(q4, k_ref[...], NT, preferred_element_type=F32)
    for h in range(heads):
        part = slice(h * 128, (h + 1) * 128)
        scores = [s_ref[part, n * 128 : (n + 1) * 128] + biases[n] for n in range(count)]
        m = old[h]
        for s in scores:
            m = jnp.maximum(m, jnp.max(s, axis=1, keepdims=True))
        l = jnp.zeros((128, 1), F32)
        for n, s in enumerate(scores):
            p = jnp.exp(s - m)
            l = l + jnp.sum(p, axis=1, keepdims=True)
            p_ref[part, n * 128 : (n + 1) * 128] = p.astype(BF16)
        stat_ref[0, part, :] = jnp.broadcast_to(m, (128, width))
        stat_ref[1, part, :] = jnp.broadcast_to(l, (128, width))
    pv = jnp.dot(p_ref[:, :128], sources[0][1][...], preferred_element_type=F32)
    for n in range(1, count):
        pv = pv + jnp.dot(p_ref[:, n * 128 : (n + 1) * 128], sources[n][1][...], preferred_element_type=F32)
    m = own_heads(stat_ref[0])
    alpha = jnp.exp(max_ref[...] - m)
    total = sum_ref[...] * alpha + own_heads(stat_ref[1])
    acc = acc_ref[...] * alpha + own_heads(pv)
    if last:
        out_ref, log_ref, att_ref = outs[:3]
        cls = pl.program_id(0)
        att_ref[pl.ds(pl.multiple_of(cls * 128, 128), 128), :] = (acc / total).astype(BF16)
        log_ref[...] = m + jnp.log(total)

        @pl.when(cls == pl.num_programs(0) - 1)
        def _():
            out_ref[...] = permuted(to_natural(att_ref.shape[0]), att_ref[...])
    else:
        for ref, value in zip(outs[:3], (m, total, acc)):
            ref[...] = value


def log_kernel(lw_ref, log_ref):
    rows, width = lw_ref.shape
    perm = to_natural(rows)
    rest = lw_ref[...]
    ordered = jnp.zeros((rows, width), F32)
    for _ in range(3):
        piece = rest.astype(BF16)
        rest = rest - piece.astype(F32)
        ordered = ordered + jnp.dot(perm, piece, preferred_element_type=F32)
    flipped = ordered.T
    for head in range(width // HEAD_DIM):
        log_ref[head : head + 1, :] = flipped[head * HEAD_DIM : head * HEAD_DIM + 1, :]


def out_kernel(place_ref, att_ref, mine_ref, other_ref, gain_ref, out_ref, sum_ref):
    x, core = place_ref[0], place_ref[1]
    first = True
    for ref, c in ((mine_ref, core), (other_ref, 1 - core)):
        for n, hop in enumerate((0, 3, 1, 2)):
            group = lax.rem(x + hop, 4) * 2 + c
            part = jnp.dot(att_ref[group], ref[n * 256 : (n + 1) * 256, :], preferred_element_type=F32)
            part = part.astype(BF16).astype(F32)
            if first:
                sum_ref[...] = part
            else:
                sum_ref[...] += part
            first = False
    summed = sum_ref[...]
    scale = lax.rsqrt(jnp.mean(summed * summed, axis=1, keepdims=True) + EPS)
    out_ref[...] = (summed * scale * gain_ref[...]).astype(BF16)


def vmem(count):
    return [pl.BlockSpec(memory_space=pltpu.VMEM)] * count


SMEM = pl.BlockSpec(memory_space=pltpu.SMEM)


def room(mebibytes):
    return pltpu.CompilerParams(vmem_limit_bytes=mebibytes * 1024 * 1024)


def cost(flops, data):
    return pl.CostEstimate(flops=flops, bytes_accessed=data, transcendentals=0)


def tables(offset, rows, width):
    half = HEAD_DIM // 2
    frequency = ROPE_BASE ** (-(jnp.arange(half, dtype=F32) * 2.0 / HEAD_DIM))
    positions = (offset + jnp.arange(rows, dtype=jnp.int32)).astype(F32)
    angles = positions[:, None] * frequency[None, :]
    cos, sin = jnp.cos(angles), jnp.sin(angles)
    heads = width // HEAD_DIM
    return jnp.tile(jnp.concatenate([cos, cos], 1), (1, heads)), jnp.tile(jnp.concatenate([-sin, sin], 1), (1, heads))


def attend_near(block, query, keys, values):
    rows, width = query.shape
    shape = jax.ShapeDtypeStruct
    whole = pl.BlockSpec((rows, width), lambda c: (0, 0))
    piece = pl.BlockSpec((128, width), lambda c: (c, 0))
    return pl.pallas_call(
        near_kernel,
        grid=(rows // 128,),
        out_shape=(shape((rows, width), F32),) * 3,
        in_specs=[SMEM, piece, whole, whole, whole, whole],
        out_specs=(piece,) * 3,
        scratch_shapes=[
            pltpu.VMEM((512, 2 * rows), F32),
            pltpu.VMEM((512, 2 * rows), BF16),
            pltpu.VMEM((128, 2 * rows), F32),
            pltpu.VMEM((128, 2 * rows), F32),
            pltpu.VMEM((2, 512, width), F32),
        ],
        cost_estimate=cost(16 * rows * rows * width, 16 * rows * width),
        compiler_params=room(20),
        name="near",
    )(block, query, keys[0], values[0], keys[1], values[1])


def attend_far(block, query, state, keys, values, backs, last):
    rows, width = query.shape
    shape = jax.ShapeDtypeStruct
    whole = pl.BlockSpec((rows, width), lambda c: (0, 0))
    piece = pl.BlockSpec((128, width), lambda c: (c, 0))
    count = len(backs)
    if last:
        outs = (shape((rows, width), BF16), shape((rows, width), F32))
        specs = (whole, piece)
        scratch = [pltpu.VMEM((rows, width), BF16)]
    else:
        outs = (shape((rows, width), F32),) * 3
        specs = (piece,) * 3
        scratch = []
    scratch = scratch + [
        pltpu.VMEM((512, 128 * count), F32),
        pltpu.VMEM((512, 128 * count), BF16),
        pltpu.VMEM((2, 512, width), F32),
    ]
    sources = []
    for k, v in zip(keys, values):
        sources += [k, v]
    return pl.pallas_call(
        functools.partial(far_kernel, backs, last),
        grid=(rows // 128,),
        out_shape=outs,
        in_specs=[SMEM] + [piece] * (4 + 2 * count),
        out_specs=specs,
        scratch_shapes=scratch,
        cost_estimate=cost(8 * rows * 128 * count * width, 16 * rows * width),
        compiler_params=room(16),
        name="last" if last else "far",
    )(block, query, *state, *sources)


def layer(hidden_in, pre_gain, query_proj, key_proj, value_proj, out_proj, post_gain):
    rows, depth = hidden_in.shape
    width = query_proj.shape[1]
    shape = jax.ShapeDtypeStruct
    sp = lax.axis_index(SP)
    block = sp[None].astype(jnp.int32)
    low = lax.axis_index("zl")
    place = jnp.stack([lax.axis_index("x"), lax.axis_index("c")]).astype(jnp.int32)

    shard = jnp.concatenate([key_proj, value_proj], axis=1)
    copies = jnp.broadcast_to(shard[None], (32,) + shard.shape)
    mine = lax.all_to_all(copies, ("zh", "y"), split_axis=0, concat_axis=0, tiled=True)
    mine = mine.reshape(4, 256, 2 * width)
    below = lax.ppermute(mine[:2], Z, ring(8, 1))
    above = lax.ppermute(mine[2:], Z, ring(8, -1))

    before = lax.ppermute(out_proj, "x", ring(4, 1))
    after = lax.ppermute(out_proj, "x", ring(4, -1))
    upper = lax.ppermute(before[:128], "x", ring(4, 1))
    lower = lax.ppermute(after[128:], "x", ring(4, -1))
    outs = jnp.concatenate([out_proj, before, after, upper, lower], axis=0)
    others = lax.ppermute(outs, "c", [(0, 1), (1, 0)])

    cos, sin = tables(sp * rows, rows, width)
    normed, query = pl.pallas_call(
        query_kernel,
        out_shape=(shape((rows, depth), BF16), shape((rows, width), BF16)),
        in_specs=vmem(5),
        out_specs=tuple(vmem(2)),
        cost_estimate=cost(2 * rows * depth * width, 4 * rows * depth),
        compiler_params=room(16),
    name="query",
    )(hidden_in, pre_gain[None], query_proj, cos, sin)

    key, value = pl.pallas_call(
        key_value_kernel,
        out_shape=(shape((rows, width), BF16),) * 2,
        in_specs=[SMEM] + vmem(6),
        out_specs=tuple(vmem(2)),
        scratch_shapes=[pltpu.VMEM((depth, 2 * width), BF16)],
        cost_estimate=cost(4 * rows * depth * width, 4 * rows * depth),
        compiler_params=room(20),
        name="key_value",
    )(low[None].astype(jnp.int32), normed, mine, below, above, cos, sin)

    forward = [(i, i + 1) for i in range(63)]
    keys, values = [key], [value]
    for _ in range(1, 5):
        keys.append(lax.ppermute(keys[-1], SP, forward))
        values.append(lax.ppermute(values[-1], SP, forward))

    state = attend_near(block, query, keys, values)
    state = attend_far(block, query, state, keys[2:4], values[2:4], (2, 3), False)
    attended, logs = attend_far(block, query, state, keys[4:], values[4:], (4,), True)

    arrived = lax.all_to_all(attended.reshape(8, rows // 8, width), TP, split_axis=0, concat_axis=0, tiled=True)
    log_weight = pl.pallas_call(
        log_kernel,
        out_shape=shape((width // HEAD_DIM, rows), F32),
        in_specs=vmem(1),
        out_specs=vmem(1)[0],
        cost_estimate=cost(6 * rows * rows * width, 4 * rows * width),
        compiler_params=room(12),
    name="log_order",
    )(logs)
    layer_out = pl.pallas_call(
        out_kernel,
        out_shape=shape((rows // 8, depth), BF16),
        in_specs=[SMEM] + vmem(4),
        out_specs=vmem(1)[0],
        scratch_shapes=[pltpu.VMEM((rows // 8, depth), F32)],
        cost_estimate=cost(2 * rows // 8 * depth * depth, 2 * depth * depth),
        compiler_params=room(24),
        name="out",
    )(place, arrived, outs, others, post_gain[None])
    return layer_out, log_weight


def solution(mesh):
    fine = Mesh(np.asarray(mesh.devices).reshape(4, 2, 8, 4, 2), ("zh", "zl", "y", "x", "c"))
    placed = (P(SP, None), P(), P(None, TP), P(SP, TP), P(SP, TP), P(TP, None), P())
    return jax.shard_map(
        layer,
        mesh=fine,
        in_specs=placed,
        out_specs=(P(SP + TP, None), P(TP, SP)),
        check_vma=False,
    )
```

time: 174 us -> 163 us (0.937)
  the two profiles are of different devices: /device:TPU:24 before, /device:TPU:248 now
where the time goes in v2:
time: 163 us; the launch traced here: 162 us
  starting transfers between devices  80.9 us (50%)
  waiting for transfers between devices  37.6 us (23%)
  Pallas kernels  29.3 us (18%)
  local copies, waits for them, and re-layouts  12.5 us (8%)
    ppermute x4, starting transfers between devices, layer(): values.append(lax.ppermute(values[-1], SP, forward))  20.9 us
    ppermute x4, starting transfers between devices, layer(): keys.append(lax.ppermute(keys[-1], SP, forward))  18.8 us
    all_to_all x1, starting transfers between devices, layer(): lax.all_to_all(copies, ('zh', 'y'), split_axis=0, concat_axis=0, tiled=True)  12.8 us
    pallas_call x2, Pallas kernels, attend_far(): pl.pallas_call(functools.partial(far_kernel, backs, last), grid=(rows //...  8.46 us
    ppermute x4, waiting for transfers between devices, layer(): keys.append(lax.ppermute(keys[-1], SP, forward))  7.91 us
    unnamed x12, local copies, waits for them, and re-layouts  6.86 us
    pallas_call x1, Pallas kernels, attend_near(): pl.pallas_call(near_kernel, grid=(rows // 128,), out_shape=(shape((rows,...  6.52 us
    ppermute x1, waiting for transfers between devices, layer(): before = lax.ppermute(out_proj, 'x', ring(4, 1))  6.45 us
  transfers between devices with their start and end apart: 17, of which 10 were waited for; matrix products, arithmetic and copies ran while one was open for 7% of the time, Pallas kernels for 14%

profile of v2, /device:TPU:248, one launch (start us, length us, event | category | flops | bytes accessed | tf_op | source)
XLA Modules:
  0.0 162.4 jit_solution(6358770673162276509)
XLA Ops:
  0.6 3.4 %collective-permute-start.10 = (bf16[256,2048]{1,0:T(8,128)(2,1)}, bf16[256,2048]{1,0:T(8,128)(2,1)S(1)}, u32[]{:S(2)}, u32[]{:S(2)}) collective-permute-start(bf16[256,2048]{1,0:T(8,128)(2,1)} %param.12), channel_id=1, source_target_pairs={{0,2},{2,4},{4,6},{6,0},{1,3},{3,5},{5,7},{7,1},{8,10},{10,12},{12... | collective-permute-start | bytes 3145736 | tf_op jit(solution)/shard_map/ppermute | solution.py:338
  4.0 3.7 %collective-permute-start.11 = (bf16[256,2048]{1,0:T(8,128)(2,1)}, bf16[256,2048]{1,0:T(8,128)(2,1)S(1)}, u32[]{:S(2)}, u32[]{:S(2)}) collective-permute-start(bf16[256,2048]{1,0:T(8,128)(2,1)} %param.12), channel_id=1, source_target_pairs={{0,6},{2,0},{4,2},{6,4},{1,7},{3,1},{5,3},{7,5},{8,14},{10,8},{12,... | collective-permute-start | bytes 3145736 | tf_op jit(solution)/shard_map/ppermute | solution.py:339
  7.7 0.7 pad_maximum_fusion.2
  8.4 1.2 broadcast_in_dim.23
  9.6 12.8 %all-to-all-start = ((bf16[32,32,512]{2,1,0:T(8,128)(2,1)}), bf16[32,32,512]{2,1,0:T(8,128)(2,1)S(1)}, u32[]{:S(2)}, u32[]{:S(2)}) async-start(bf16[32,32,512]{2,1,0:T(8,128)(2,1)} %broadcast_in_dim.23), calls=%async_computation | async-start | bytes 2097152 | tf_op jit(solution)/shard_map/all_to_all | solution.py:333
  22.4 6.5 %collective-permute-done.10 = bf16[256,2048]{1,0:T(8,128)(2,1)S(1)} collective-permute-done((bf16[256,2048]{1,0:T(8,128)(2,1)}, bf16[256,2048]{1,0:T(8,128)(2,1)S(1)}, u32[]{:S(2)}, u32[]{:S(2)}) %collective-permute-start.10) | collective-permute-done | bytes 1048608 | tf_op jit(solution)/shard_map/ppermute | solution.py:338
  28.9 2.2 %collective-permute-start.12 = (bf16[128,2048]{1,0:T(8,128)(2,1)S(1)}, bf16[128,2048]{1,0:T(8,128)(2,1)S(1)}, u32[]{:S(2)}, u32[]{:S(2)}) collective-permute-start(bf16[128,2048]{1,0:T(8,128)(2,1)S(1)} %slice.26), channel_id=1, source_target_pairs={{0,2},{2,4},{4,6},{6,0},{1,3},{3,5},{5,7},{7,1},{8,10},{10,12},{12... | collective-permute-start | bytes 1572872 | tf_op jit(solution)/shard_map/ppermute | solution.py:340
  31.1 2.3 %constant_dynamic-update-slice_fusion.4 = bf16[1024,2048]{1,0:T(8,128)(2,1)} fusion(bf16[256,2048]{1,0:T(8,128)(2,1)} %param.12), kind=kLoop, calls=%fused_computation.10 | loop fusion | bytes 2097152
  33.4 0.0 collective-permute-done.11
  33.5 4.9 %collective-permute-start.13 = (bf16[128,2048]{1,0:T(8,128)(2,1)S(1)}, bf16[128,2048]{1,0:T(8,128)(2,1)S(1)}, u32[]{:S(2)}, u32[]{:S(2)}) collective-permute-start(bf16[128,2048]{1,0:T(8,128)(2,1)S(1)} %slice.27), channel_id=1, source_target_pairs={{0,6},{2,0},{4,2},{6,4},{1,7},{3,1},{5,3},{7,5},{8,14},{10,8},{12,... | collective-permute-start | bytes 1572872 | tf_op jit(solution)/shard_map/ppermute | solution.py:341
  38.4 1.0 constant_dynamic-update-slice_fusion.3
  39.4 1.0 constant_dynamic-update-slice_fusion.2
  40.4 0.0 copy-start.1
  40.4 0.0 copy-start.2
  40.4 4.4 %collective-permute-done.12 = bf16[128,2048]{1,0:T(8,128)(2,1)S(1)} collective-permute-done((bf16[128,2048]{1,0:T(8,128)(2,1)S(1)}, bf16[128,2048]{1,0:T(8,128)(2,1)S(1)}, u32[]{:S(2)}, u32[]{:S(2)}) %collective-permute-start.12) | collective-permute-done | bytes 524320 | tf_op jit(solution)/shard_map/ppermute | solution.py:340
  44.8 0.9 constant_dynamic-update-slice_fusion.1
  45.7 2.7 %collective-permute-done.13 = bf16[128,2048]{1,0:T(8,128)(2,1)S(1)} collective-permute-done((bf16[128,2048]{1,0:T(8,128)(2,1)S(1)}, bf16[128,2048]{1,0:T(8,128)(2,1)S(1)}, u32[]{:S(2)}, u32[]{:S(2)}) %collective-permute-start.13) | collective-permute-done | bytes 524320 | tf_op jit(solution)/shard_map/ppermute | solution.py:341
  48.4 0.9 constant_dynamic-update-slice_fusion.mine_ref
  49.3 1.9 %collective-permute-start.14 = (bf16[1024,2048]{1,0:T(8,128)(2,1)}, bf16[1024,2048]{1,0:T(8,128)(2,1)}, u32[]{:S(2)}, u32[]{:S(2)}) collective-permute-start(bf16[1024,2048]{1,0:T(8,128)(2,1)} %constant_dynamic-update-slice_fusion.mine_ref), channel_id=1, source_target_pairs={{0,1},{1,0},{2,3},{3,2},{4,5},{5,4},{6,7},{7,6},{8,9},{9,8},{10,11... | collective-permute-start | bytes 12582920 | tf_op jit(solution)/shard_map/ppermute | solution.py:343
  51.2 0.0 all-to-all-done
  51.2 1.1 fusion.1
  52.3 5.5 %collective-permute-start = (bf16[2,256,512]{2,1,0:T(8,128)(2,1)}, bf16[2,256,512]{2,1,0:T(8,128)(2,1)}, u32[]{:S(2)}, u32[]{:S(2)}) collective-permute-start(bf16[2,256,512]{2,1,0:T(8,128)(2,1)} %bitcast.8), channel_id=1, source_target_pairs={{0,64},{64,128},{128,192},{192,256},{256,320},{320,384},{384,448},... | collective-permute-start | bytes 1572872 | tf_op jit(solution)/shard_map/ppermute | solution.py:335
  57.8 1.9 %collective-permute-start.1 = (bf16[2,256,512]{2,1,0:T(8,128)(2,1)}, bf16[2,256,512]{2,1,0:T(8,128)(2,1)}, u32[]{:S(2)}, u32[]{:S(2)}) collective-permute-start(bf16[2,256,512]{2,1,0:T(8,128)(2,1)} %bitcast.9), channel_id=1, source_target_pairs={{0,448},{64,0},{128,64},{192,128},{256,192},{320,256},{384,320},{4... | collective-permute-start | bytes 1572872 | tf_op jit(solution)/shard_map/ppermute | solution.py:336
  59.8 0.3 fusion
  60.1 0.1 tile.20
  60.2 0.2 copy.10.sin_ref
  60.4 0.9 tile.8
  61.3 1.2 copy.9.cos_ref
  62.5 0.0 copy-done.1
  62.5 0.0 copy-done.2
  62.5 0.0 copy-start
  62.5 1.6 copy-done
  64.1 2.7 %query.1 = (bf16[512,2048]{1,0:T(8,128)(2,1)S(1)}, bf16[512,256]{1,0:T(8,128)(2,1)S(1)}) custom-call(bf16[512,2048]{1,0:T(8,128)(2,1)S(1)} %copy-done, f32[1,2048]{1,0:T(1,128)S(1)} %bitcast.13, bf16[2048,256]{1,0:T(8,128)(2,1)S(1)} %copy-done.1, f32[512,256]{1,0:T(8,128)S(1)} %copy.9.cos_ref, f32[512,256]{1,0:T(8,128)S(1)} %copy.10.sin_ref), custom_call_target="tpu_custom_call" | custom-call | flops 536870912 | bytes 4194304 | tf_op jit(solution)/shard_map/query/pallas_call | solution.py:346
  66.8 3.2 %collective-permute-done.below_ref = bf16[2,256,512]{2,1,0:T(8,128)(2,1)} collective-permute-done((bf16[2,256,512]{2,1,0:T(8,128)(2,1)}, bf16[2,256,512]{2,1,0:T(8,128)(2,1)}, u32[]{:S(2)}, u32[]{:S(2)}) %collective-permute-start) | collective-permute-done | bytes 524320 | tf_op jit(solution)/shard_map/ppermute | solution.py:335
  70.0 5.3 %collective-permute-done.1.above_ref = bf16[2,256,512]{2,1,0:T(8,128)(2,1)} collective-permute-done((bf16[2,256,512]{2,1,0:T(8,128)(2,1)}, bf16[2,256,512]{2,1,0:T(8,128)(2,1)}, u32[]{:S(2)}, u32[]{:S(2)}) %collective-permute-start.1) | collective-permute-done | bytes 524320 | tf_op jit(solution)/shard_map/ppermute | solution.py:336
  75.3 4.5 %key_value.1 = (bf16[512,256]{1,0:T(8,128)(2,1)S(1)}, bf16[512,256]{1,0:T(8,128)(2,1)S(1)}) custom-call(s32[1]{0:T(128)} %bitcast.6.place_ref, bf16[512,2048]{1,0:T(8,128)(2,1)S(1)} %get-tuple-element.15.normed_ref, bf16[4,256,512]{2,1,0:T(8,128)(2,1)S(1)} %bitcast.12, bf16[2,256,512]{2,1,0:T(8,128)(2,1)} %collective-permute-done.below_ref, ...), custom_call_target="tpu_custom_call" | custom-call | flops 1073741824 | bytes 4194304 | tf_op jit(solution)/shard_map/key_value/pallas_call | solution.py:356
  79.8 1.9 %collective-permute-start.2 = (bf16[512,256]{1,0:T(8,128)(2,1)S(1)}, bf16[512,256]{1,0:T(8,128)(2,1)S(1)}, u32[]{:S(2)}, u32[]{:S(2)}) collective-permute-start(bf16[512,256]{1,0:T(8,128)(2,1)S(1)} %get-tuple-element.16.k0_ref), channel_id=1, source_target_pairs={{0,8},{8,16},{16,24},{24,32},{32,40},{40,48},{48,56},{56,64},{64,7... | collective-permute-start | bytes 786440 | tf_op jit(solution)/shard_map/ppermute | solution.py:370
  81.7 2.9 %collective-permute-start.3 = (bf16[512,256]{1,0:T(8,128)(2,1)S(1)}, bf16[512,256]{1,0:T(8,128)(2,1)S(1)}, u32[]{:S(2)}, u32[]{:S(2)}) collective-permute-start(bf16[512,256]{1,0:T(8,128)(2,1)S(1)} %get-tuple-element.17.v0_ref), channel_id=1, source_target_pairs={{0,8},{8,16},{16,24},{24,32},{32,40},{40,48},{48,56},{56,64},{64,7... | collective-permute-start | bytes 786440 | tf_op jit(solution)/shard_map/ppermute | solution.py:371
  84.7 6.2 %collective-permute-done.2.k1_ref = bf16[512,256]{1,0:T(8,128)(2,1)S(1)} collective-permute-done((bf16[512,256]{1,0:T(8,128)(2,1)S(1)}, bf16[512,256]{1,0:T(8,128)(2,1)S(1)}, u32[]{:S(2)}, u32[]{:S(2)}) %collective-permute-start.2) | collective-permute-done | bytes 262176 | tf_op jit(solution)/shard_map/ppermute | solution.py:370
  90.8 5.2 %collective-permute-start.4 = (bf16[512,256]{1,0:T(8,128)(2,1)S(1)}, bf16[512,256]{1,0:T(8,128)(2,1)S(1)}, u32[]{:S(2)}, u32[]{:S(2)}) collective-permute-start(bf16[512,256]{1,0:T(8,128)(2,1)S(1)} %collective-permute-done.2.k1_ref), channel_id=1, source_target_pairs={{0,8},{8,16},{16,24},{24,32},{32,40},{40,48},{48,56},{56,64},{64,7... | collective-permute-start | bytes 786440 | tf_op jit(solution)/shard_map/ppermute | solution.py:370
  96.1 0.4 collective-permute-done.3.v1_ref
  96.5 3.9 %collective-permute-start.5 = (bf16[512,256]{1,0:T(8,128)(2,1)S(1)}, bf16[512,256]{1,0:T(8,128)(2,1)S(1)}, u32[]{:S(2)}, u32[]{:S(2)}) collective-permute-start(bf16[512,256]{1,0:T(8,128)(2,1)S(1)} %collective-permute-done.3.v1_ref), channel_id=1, source_target_pairs={{0,8},{8,16},{16,24},{24,32},{32,40},{40,48},{48,56},{56,64},{64,7... | collective-permute-start | bytes 786440 | tf_op jit(solution)/shard_map/ppermute | solution.py:371
  100.4 1.7 %collective-permute-done.4.refs_0_ = bf16[512,256]{1,0:T(8,128)(2,1)S(1)} collective-permute-done((bf16[512,256]{1,0:T(8,128)(2,1)S(1)}, bf16[512,256]{1,0:T(8,128)(2,1)S(1)}, u32[]{:S(2)}, u32[]{:S(2)}) %collective-permute-start.4) | collective-permute-done | bytes 262176 | tf_op jit(solution)/shard_map/ppermute | solution.py:370
  102.1 6.3 %collective-permute-start.6 = (bf16[512,256]{1,0:T(8,128)(2,1)S(1)}, bf16[512,256]{1,0:T(8,128)(2,1)S(1)}, u32[]{:S(2)}, u32[]{:S(2)}) collective-permute-start(bf16[512,256]{1,0:T(8,128)(2,1)S(1)} %collective-permute-done.4.refs_0_), channel_id=1, source_target_pairs={{0,8},{8,16},{16,24},{24,32},{32,40},{40,48},{48,56},{56,64},{64,7... | collective-permute-start | bytes 786440 | tf_op jit(solution)/shard_map/ppermute | solution.py:370
  108.4 0.0 collective-permute-done.5.refs_1_
  108.4 6.4 %collective-permute-start.7 = (bf16[512,256]{1,0:T(8,128)(2,1)S(1)}, bf16[512,256]{1,0:T(8,128)(2,1)S(1)}, u32[]{:S(2)}, u32[]{:S(2)}) collective-permute-start(bf16[512,256]{1,0:T(8,128)(2,1)S(1)} %collective-permute-done.5.refs_1_), channel_id=1, source_target_pairs={{0,8},{8,16},{16,24},{24,32},{32,40},{40,48},{48,56},{56,64},{64,7... | collective-permute-start | bytes 786440 | tf_op jit(solution)/shard_map/ppermute | solution.py:371
  114.8 0.0 collective-permute-done.6.refs_2_
  114.8 5.4 %collective-permute-start.8 = (bf16[512,256]{1,0:T(8,128)(2,1)S(1)}, bf16[512,256]{1,0:T(8,128)(2,1)S(1)}, u32[]{:S(2)}, u32[]{:S(2)}) collective-permute-start(bf16[512,256]{1,0:T(8,128)(2,1)S(1)} %collective-permute-done.6.refs_2_), channel_id=1, source_target_pairs={{0,8},{8,16},{16,24},{24,32},{32,40},{40,48},{48,56},{56,64},{64,7... | collective-permute-start | bytes 786440 | tf_op jit(solution)/shard_map/ppermute | solution.py:370
  120.2 1.1 collective-permute-done.7.refs_3_
  121.2 7.7 %collective-permute-start.9 = (bf16[512,256]{1,0:T(8,128)(2,1)S(1)}, bf16[512,256]{1,0:T(8,128)(2,1)S(1)}, u32[]{:S(2)}, u32[]{:S(2)}) collective-permute-start(bf16[512,256]{1,0:T(8,128)(2,1)S(1)} %collective-permute-done.7.refs_3_), channel_id=1, source_target_pairs={{0,8},{8,16},{16,24},{24,32},{32,40},{40,48},{48,56},{56,64},{64,7... | collective-permute-start | bytes 786440 | tf_op jit(solution)/shard_map/ppermute | solution.py:371
  128.9 6.5 %near.1 = (f32[512,256]{1,0:T(8,128)S(1)}, f32[512,256]{1,0:T(8,128)S(1)}, f32[512,256]{1,0:T(8,128)S(1)}) custom-call(s32[1]{0:T(128)} %bitcast.2.place_ref, bf16[512,256]{1,0:T(8,128)(2,1)S(1)} %get-tuple-element.14.q_ref, bf16[512,256]{1,0:T(8,128)(2,1)S(1)} %get-tuple-element.16.k0_ref, bf16[512,256]{1,0:T(8,128)(2,1)S(1)} %get-tuple-element.17.v0_ref, ...), custom_call_target="tpu_custom_call" | custom-call | flops 1073741824 | bytes 2097152 | tf_op jit(solution)/shard_map/near/pallas_call | solution.py:268
  135.5 0.0 copy-start.3
  135.5 4.4 %far.1 = (f32[512,256]{1,0:T(8,128)S(1)}, f32[512,256]{1,0:T(8,128)S(1)}, f32[512,256]{1,0:T(8,128)S(1)}) custom-call(s32[1]{0:T(128)} %bitcast.2.place_ref, bf16[512,256]{1,0:T(8,128)(2,1)S(1)} %get-tuple-element.14.q_ref, f32[512,256]{1,0:T(8,128)S(1)} %get-tuple-element.18.max_ref, f32[512,256]{1,0:T(8,128)S(1)} %get-tuple-element.19.sum_ref, ...), custom_call_target="tpu_custom_call" | custom-call | flops 268435456 | bytes 2097152 | tf_op jit(solution)/shard_map/far/pallas_call | solution.py:309
  139.9 0.0 collective-permute-done.8.refs_0_
  140.0 0.0 collective-permute-done.9.refs_1_
  140.0 4.0 %last.1 = (bf16[512,256]{1,0:T(8,128)(2,1)}, f32[512,256]{1,0:T(8,128)S(1)}) custom-call(s32[1]{0:T(128)} %bitcast.2.place_ref, bf16[512,256]{1,0:T(8,128)(2,1)S(1)} %get-tuple-element.14.q_ref, f32[512,256]{1,0:T(8,128)S(1)} %get-tuple-element.21.max_ref, f32[512,256]{1,0:T(8,128)S(1)} %get-tuple-element.22.sum_ref, ...), custom_call_target="tpu_custom_call" | custom-call | flops 134217728 | bytes 2097152 | tf_op jit(solution)/shard_map/last/pallas_call | solution.py:309
  144.0 5.0 %all-to-all-start.1 = ((bf16[8,64,256]{2,1,0:T(8,128)(2,1)}), bf16[8,64,256]{2,1,0:T(8,128)(2,1)S(1)}, u32[]{:S(2)}, u32[]{:S(2)}) async-start(bf16[8,64,256]{2,1,0:T(8,128)(2,1)} %bitcast.10), calls=%async_computation.1 | async-start | bytes 524288 | tf_op jit(solution)/shard_map/all_to_all | solution.py:377
  149.0 0.1 pad_add_fusion.place_ref
  149.0 1.3 log_order.1
  150.3 6.2 %all-to-all-done.1.att_ref = bf16[8,64,256]{2,1,0:T(8,128)(2,1)S(1)} async-done(((bf16[8,64,256]{2,1,0:T(8,128)(2,1)}), bf16[8,64,256]{2,1,0:T(8,128)(2,1)S(1)}, u32[]{:S(2)}, u32[]{:S(2)}) %all-to-all-start.1) | async-done | bytes 262176 | tf_op jit(solution)/shard_map/all_to_all | solution.py:377
  156.5 0.0 collective-permute-done.14.other_ref
  156.5 0.0 copy-done.3
  156.5 5.9 %out.1 = bf16[64,2048]{1,0:T(8,128)(2,1)} custom-call(s32[2]{0:T(128)S(1)} %pad_add_fusion.place_ref, bf16[8,64,256]{2,1,0:T(8,128)(2,1)S(1)} %all-to-all-done.1.att_ref, bf16[1024,2048]{1,0:T(8,128)(2,1)} %constant_dynamic-update-slice_fusion.mine_ref, bf16[1024,2048]{1,0:T(8,128)(2,1)} %collective-permute-done.14.other_ref, f32[1,2048]{1,0:T(1,128)S(1)} %bitcast.14), custom_call_target="tpu_custom_call" | custom-call | flops 536870912 | bytes 8388608 | tf_op jit(solution)/shard_map/out/pallas_call | solution.py:387
  (5 shorter events, 0.1 us)
Async XLA Ops:
  0.6 28.2 %collective-permute-start.10 = (bf16[256,2048]{1,0:T(8,128)(2,1)}, bf16[256,2048]{1,0:T(8,128)(2,1)S(1)}, u32[]{:S(2)}, u32[]{:S(2)}) collective-permute-start(bf16[256,2048]{1,0:T(8,128)(2,1)} %param.12), channel_id=1, source_target_pairs={{0,2},{2,4},{4,6},{6,0},{1,3},{3,5},{5,7},{7,1},{8,10},{10,12},{12... | collective-permute-start | bytes 3145736 | tf_op jit(solution)/shard_map/ppermute | solution.py:338
  4.0 29.4 %collective-permute-start.11 = (bf16[256,2048]{1,0:T(8,128)(2,1)}, bf16[256,2048]{1,0:T(8,128)(2,1)S(1)}, u32[]{:S(2)}, u32[]{:S(2)}) collective-permute-start(bf16[256,2048]{1,0:T(8,128)(2,1)} %param.12), channel_id=1, source_target_pairs={{0,6},{2,0},{4,2},{6,4},{1,7},{3,1},{5,3},{7,5},{8,14},{10,8},{12,... | collective-permute-start | bytes 3145736 | tf_op jit(solution)/shard_map/ppermute | solution.py:339
  9.6 41.6 %all-to-all-start = ((bf16[32,32,512]{2,1,0:T(8,128)(2,1)}), bf16[32,32,512]{2,1,0:T(8,128)(2,1)S(1)}, u32[]{:S(2)}, u32[]{:S(2)}) async-start(bf16[32,32,512]{2,1,0:T(8,128)(2,1)} %broadcast_in_dim.23), calls=%async_computation | async-start | bytes 2097152 | tf_op jit(solution)/shard_map/all_to_all | solution.py:333
  28.9 15.9 %collective-permute-start.12 = (bf16[128,2048]{1,0:T(8,128)(2,1)S(1)}, bf16[128,2048]{1,0:T(8,128)(2,1)S(1)}, u32[]{:S(2)}, u32[]{:S(2)}) collective-permute-start(bf16[128,2048]{1,0:T(8,128)(2,1)S(1)} %slice.26), channel_id=1, source_target_pairs={{0,2},{2,4},{4,6},{6,0},{1,3},{3,5},{5,7},{7,1},{8,10},{10,12},{12... | collective-permute-start | bytes 1572872 | tf_op jit(solution)/shard_map/ppermute | solution.py:340
  33.5 14.9 %collective-permute-start.13 = (bf16[128,2048]{1,0:T(8,128)(2,1)S(1)}, bf16[128,2048]{1,0:T(8,128)(2,1)S(1)}, u32[]{:S(2)}, u32[]{:S(2)}) collective-permute-start(bf16[128,2048]{1,0:T(8,128)(2,1)S(1)} %slice.27), channel_id=1, source_target_pairs={{0,6},{2,0},{4,2},{6,4},{1,7},{3,1},{5,3},{7,5},{8,14},{10,8},{12,... | collective-permute-start | bytes 1572872 | tf_op jit(solution)/shard_map/ppermute | solution.py:341
  40.4 22.1 %copy-start.1 = (bf16[2048,256]{1,0:T(8,128)(2,1)S(1)}, bf16[2048,256]{1,0:T(8,128)(2,1)}, u32[]{:S(2)}) copy-start(bf16[2048,256]{1,0:T(8,128)(2,1)} %weight_ref.1) | copy-start | bytes 3145732
  40.4 22.1 %copy-start.2 = (f32[2048]{0:T(1024)S(1)}, f32[2048]{0:T(1024)}, u32[]{:S(2)}) copy-start(f32[2048]{0:T(1024)} %param.8) | copy-start | bytes 24580
  49.3 107.2 %collective-permute-start.14 = (bf16[1024,2048]{1,0:T(8,128)(2,1)}, bf16[1024,2048]{1,0:T(8,128)(2,1)}, u32[]{:S(2)}, u32[]{:S(2)}) collective-permute-start(bf16[1024,2048]{1,0:T(8,128)(2,1)} %constant_dynamic-update-slice_fusion.mine_ref), channel_id=1, source_target_pairs={{0,1},{1,0},{2,3},{3,2},{4,5},{5,4},{6,7},{7,6},{8,9},{9,8},{10,11... | collective-permute-start | bytes 12582920 | tf_op jit(solution)/shard_map/ppermute | solution.py:343
  52.3 17.6 %collective-permute-start = (bf16[2,256,512]{2,1,0:T(8,128)(2,1)}, bf16[2,256,512]{2,1,0:T(8,128)(2,1)}, u32[]{:S(2)}, u32[]{:S(2)}) collective-permute-start(bf16[2,256,512]{2,1,0:T(8,128)(2,1)} %bitcast.8), channel_id=1, source_target_pairs={{0,64},{64,128},{128,192},{192,256},{256,320},{320,384},{384,448},... | collective-permute-start | bytes 1572872 | tf_op jit(solution)/shard_map/ppermute | solution.py:335
  57.8 17.5 %collective-permute-start.1 = (bf16[2,256,512]{2,1,0:T(8,128)(2,1)}, bf16[2,256,512]{2,1,0:T(8,128)(2,1)}, u32[]{:S(2)}, u32[]{:S(2)}) collective-permute-start(bf16[2,256,512]{2,1,0:T(8,128)(2,1)} %bitcast.9), channel_id=1, source_target_pairs={{0,448},{64,0},{128,64},{192,128},{256,192},{320,256},{384,320},{4... | collective-permute-start | bytes 1572872 | tf_op jit(solution)/shard_map/ppermute | solution.py:336
  62.5 1.6 copy-start
  79.8 11.1 %collective-permute-start.2 = (bf16[512,256]{1,0:T(8,128)(2,1)S(1)}, bf16[512,256]{1,0:T(8,128)(2,1)S(1)}, u32[]{:S(2)}, u32[]{:S(2)}) collective-permute-start(bf16[512,256]{1,0:T(8,128)(2,1)S(1)} %get-tuple-element.16.k0_ref), channel_id=1, source_target_pairs={{0,8},{8,16},{16,24},{24,32},{32,40},{40,48},{48,56},{56,64},{64,7... | collective-permute-start | bytes 786440 | tf_op jit(solution)/shard_map/ppermute | solution.py:370
  81.7 14.8 %collective-permute-start.3 = (bf16[512,256]{1,0:T(8,128)(2,1)S(1)}, bf16[512,256]{1,0:T(8,128)(2,1)S(1)}, u32[]{:S(2)}, u32[]{:S(2)}) collective-permute-start(bf16[512,256]{1,0:T(8,128)(2,1)S(1)} %get-tuple-element.17.v0_ref), channel_id=1, source_target_pairs={{0,8},{8,16},{16,24},{24,32},{32,40},{40,48},{48,56},{56,64},{64,7... | collective-permute-start | bytes 786440 | tf_op jit(solution)/shard_map/ppermute | solution.py:371
  90.8 11.2 %collective-permute-start.4 = (bf16[512,256]{1,0:T(8,128)(2,1)S(1)}, bf16[512,256]{1,0:T(8,128)(2,1)S(1)}, u32[]{:S(2)}, u32[]{:S(2)}) collective-permute-start(bf16[512,256]{1,0:T(8,128)(2,1)S(1)} %collective-permute-done.2.k1_ref), channel_id=1, source_target_pairs={{0,8},{8,16},{16,24},{24,32},{32,40},{40,48},{48,56},{56,64},{64,7... | collective-permute-start | bytes 786440 | tf_op jit(solution)/shard_map/ppermute | solution.py:370
  96.5 11.9 %collective-permute-start.5 = (bf16[512,256]{1,0:T(8,128)(2,1)S(1)}, bf16[512,256]{1,0:T(8,128)(2,1)S(1)}, u32[]{:S(2)}, u32[]{:S(2)}) collective-permute-start(bf16[512,256]{1,0:T(8,128)(2,1)S(1)} %collective-permute-done.3.v1_ref), channel_id=1, source_target_pairs={{0,8},{8,16},{16,24},{24,32},{32,40},{40,48},{48,56},{56,64},{64,7... | collective-permute-start | bytes 786440 | tf_op jit(solution)/shard_map/ppermute | solution.py:371
  102.1 12.7 %collective-permute-start.6 = (bf16[512,256]{1,0:T(8,128)(2,1)S(1)}, bf16[512,256]{1,0:T(8,128)(2,1)S(1)}, u32[]{:S(2)}, u32[]{:S(2)}) collective-permute-start(bf16[512,256]{1,0:T(8,128)(2,1)S(1)} %collective-permute-done.4.refs_0_), channel_id=1, source_target_pairs={{0,8},{8,16},{16,24},{24,32},{32,40},{40,48},{48,56},{56,64},{64,7... | collective-permute-start | bytes 786440 | tf_op jit(solution)/shard_map/ppermute | solution.py:370
  108.4 12.9 %collective-permute-start.7 = (bf16[512,256]{1,0:T(8,128)(2,1)S(1)}, bf16[512,256]{1,0:T(8,128)(2,1)S(1)}, u32[]{:S(2)}, u32[]{:S(2)}) collective-permute-start(bf16[512,256]{1,0:T(8,128)(2,1)S(1)} %collective-permute-done.5.refs_1_), channel_id=1, source_target_pairs={{0,8},{8,16},{16,24},{24,32},{32,40},{40,48},{48,56},{56,64},{64,7... | collective-permute-start | bytes 786440 | tf_op jit(solution)/shard_map/ppermute | solution.py:371
  114.8 25.2 %collective-permute-start.8 = (bf16[512,256]{1,0:T(8,128)(2,1)S(1)}, bf16[512,256]{1,0:T(8,128)(2,1)S(1)}, u32[]{:S(2)}, u32[]{:S(2)}) collective-permute-start(bf16[512,256]{1,0:T(8,128)(2,1)S(1)} %collective-permute-done.6.refs_2_), channel_id=1, source_target_pairs={{0,8},{8,16},{16,24},{24,32},{32,40},{40,48},{48,56},{56,64},{64,7... | collective-permute-start | bytes 786440 | tf_op jit(solution)/shard_map/ppermute | solution.py:370
  121.2 18.7 %collective-permute-start.9 = (bf16[512,256]{1,0:T(8,128)(2,1)S(1)}, bf16[512,256]{1,0:T(8,128)(2,1)S(1)}, u32[]{:S(2)}, u32[]{:S(2)}) collective-permute-start(bf16[512,256]{1,0:T(8,128)(2,1)S(1)} %collective-permute-done.7.refs_3_), channel_id=1, source_target_pairs={{0,8},{8,16},{16,24},{24,32},{32,40},{40,48},{48,56},{56,64},{64,7... | collective-permute-start | bytes 786440 | tf_op jit(solution)/shard_map/ppermute | solution.py:371
  135.5 21.0 %copy-start.3 = (f32[2048]{0:T(1024)S(1)}, f32[2048]{0:T(1024)}, u32[]{:S(2)}) copy-start(f32[2048]{0:T(1024)} %param.13) | copy-start | bytes 24580
  144.0 12.5 %all-to-all-start.1 = ((bf16[8,64,256]{2,1,0:T(8,128)(2,1)}), bf16[8,64,256]{2,1,0:T(8,128)(2,1)S(1)}, u32[]{:S(2)}, u32[]{:S(2)}) async-start(bf16[8,64,256]{2,1,0:T(8,128)(2,1)} %bitcast.10), calls=%async_computation.1 | async-start | bytes 524288 | tf_op jit(solution)/shard_map/all_to_all | solution.py:377

commit v3 on v2

v3 whole, which is shorter than its diff:
```python
import jax
import jax.numpy as jnp
import numpy as np
from jax import lax
from jax.experimental import pallas as pl
from jax.experimental.pallas import tpu as pltpu
from jax.sharding import Mesh
from jax.sharding import PartitionSpec as P

HEAD_DIM = 64
SPAN = 128
EPS = 1e-06
ROPE_BASE = 10000.0
LOW = -1e30
SP = ("zh", "zl", "y")
Z = ("zh", "zl")
TP = ("x", "c")
F32 = jnp.float32
BF16 = jnp.bfloat16
NT = (((1,), (1,)), ((), ()))
HOPS = (0, 3, 1, 2)


def ring(count, steps):
    return [(i, (i + steps) % count) for i in range(count)]


def natural(i):
    return (i & 31) * 16 + ((i >> 5) & 3) * 4 + (i >> 7)


def to_residue(rows, columns=None):
    i = lax.broadcasted_iota(jnp.int32, (rows, rows), 0)
    if columns is None:
        columns = lax.broadcasted_iota(jnp.int32, (rows, rows), 1)
    return (natural(i) == columns).astype(BF16)


def to_natural(rows):
    i = lax.broadcasted_iota(jnp.int32, (rows, rows), 1)
    n = lax.broadcasted_iota(jnp.int32, (rows, rows), 0)
    return (natural(i) == n).astype(BF16)


def rotated(x, cos, sin):
    width = x.shape[1]
    lane = lax.broadcasted_iota(jnp.int32, x.shape, 1)
    other = jnp.where((lane & 63) < 32, pltpu.roll(x, width - 32, 1), pltpu.roll(x, 32, 1))
    return x * cos + other * sin


def permuted(perm, x):
    return jnp.dot(perm, x, preferred_element_type=F32).astype(BF16)


def normed_rows(x, gain):
    x = x.astype(F32)
    scale = lax.rsqrt(jnp.mean(x * x, axis=1, keepdims=True) + EPS)
    return (x * scale * gain).astype(BF16)


def spread(turn_ref, part):
    cos, sin = turn_ref[0, :, part], turn_ref[1, :, part]
    cos = jnp.concatenate([cos] * 4, axis=0).T
    sin = jnp.concatenate([-sin, sin] * 2, axis=0).T
    return jnp.concatenate([cos, cos], axis=1), jnp.concatenate([sin, sin], axis=1)


def slice_kernel(place_ref, hidden_ref, gain_ref, out_ref):
    out_ref[...] = normed_rows(hidden_ref[...], gain_ref[...])


def query_kernel(hidden_ref, gain_ref, weight_ref, turn_ref, normed_ref, query_ref):
    rows = hidden_ref.shape[0]
    gain = gain_ref[...]

    def step(i, carry):
        part = pl.ds(pl.multiple_of(i * 64, 64), 64)
        normed_ref[part, :] = normed_rows(hidden_ref[part, :], gain)
        return carry

    lax.fori_loop(0, rows // 64, step, 0)
    query = jnp.dot(normed_ref[...], weight_ref[...], preferred_element_type=F32)
    cos, sin = spread(turn_ref, slice(2 * rows, 3 * rows))
    query = rotated(query, cos, sin).astype(BF16) * 0.125
    query_ref[...] = permuted(to_residue(rows), query)


def key_value_kernel(place_ref, normed_ref, mine_ref, below_ref, above_ref, turn_ref, key_ref, value_ref, weight_ref):
    rows = normed_ref.shape[0]
    width = key_ref.shape[1]
    low = place_ref[1]
    slabs = []
    for k in range(4):
        slabs.append((2 * k + low, mine_ref, k))
    for k in range(2):
        slabs.append((2 * k + 1 - low, below_ref, k))
        slabs.append((2 * (k + 2) + 1 - low, above_ref, k))
    for place, ref, k in slabs:
        weight_ref[pl.ds(pl.multiple_of(place * 256, 256), 256), :] = ref[k]
    normed = normed_ref[...]
    perm = to_residue(rows)
    cos, sin = spread(turn_ref, slice(2 * rows, 3 * rows))
    key = jnp.dot(normed, weight_ref[:, :width], preferred_element_type=F32)
    key = rotated(key, cos, sin).astype(BF16)
    key_ref[...] = permuted(perm, key)
    value = jnp.dot(normed, weight_ref[:, width:], preferred_element_type=F32).astype(BF16)
    value_ref[...] = permuted(perm, value)


def far_key_value_kernel(place_ref, mine_ref, other_ref, weight_ref, turn_ref, k4_ref, v4_ref, k3_ref, v3_ref, cos_ref, sin_ref, key_ref, value_ref):
    rows, width = k4_ref.shape
    x, core = place_ref[2], place_ref[3]
    piece = rows // 8
    for n in range(2):
        part = slice(n * rows, (n + 1) * rows)
        cos_ref[part, :], sin_ref[part, :] = spread(turn_ref, part)
    lanes = lax.broadcasted_iota(jnp.int32, (1, rows), 1)
    column = lanes & (piece - 1)
    for half, (ref, c) in enumerate(((mine_ref, core), (other_ref, 1 - core))):
        both = jnp.dot(ref[...], weight_ref[...], preferred_element_type=F32)
        for n, hop in enumerate(HOPS):
            at = (lax.rem(x + hop, 4) * 2 + c) * piece
            lies = (half * 4 + n) * piece
            column = column + jnp.where((lanes >= lies) & (lanes < lies + piece), at, 0)
            for far in range(2):
                source = slice((2 * n + far) * piece, (2 * n + far + 1) * piece)
                table = pl.ds(pl.multiple_of(far * rows + at, piece), piece)
                key = rotated(both[source, :width], cos_ref[table, :], sin_ref[table, :])
                key_ref[far, lies : lies + piece, :] = key.astype(BF16)
                value_ref[far, lies : lies + piece, :] = both[source, width:].astype(BF16)
    perm = to_residue(rows, jnp.broadcast_to(column, (rows, rows)))
    k4_ref[...] = permuted(perm, key_ref[0])
    v4_ref[...] = permuted(perm, value_ref[0])
    k3_ref[...] = permuted(perm, key_ref[1])
    v3_ref[...] = permuted(perm, value_ref[1])


def stack_heads(q):
    lane = lax.broadcasted_iota(jnp.int32, q.shape, 1) >> 6
    return jnp.concatenate([jnp.where(lane == h, q, jnp.zeros_like(q)) for h in range(q.shape[1] // HEAD_DIM)], axis=0)


def own_heads(stacked):
    width = stacked.shape[1]
    heads = width // HEAD_DIM
    rows = stacked.shape[0] // heads
    lane = lax.broadcasted_iota(jnp.int32, (rows, width), 1) >> 6
    out = stacked[:rows]
    for h in range(1, heads):
        out = jnp.where(lane == h, stacked[h * rows : (h + 1) * rows], out)
    return out


def far_bias(block, back):
    qi = lax.broadcasted_iota(jnp.int32, (128, 128), 0)
    ki = lax.broadcasted_iota(jnp.int32, (128, 128), 1)
    ok = ((qi >> 5) == (ki >> 5)) & (block >= back)
    if back == 4:
        ok = ok & ((ki & 31) >= (qi & 31))
    return jnp.where(ok, 0.0, LOW).astype(F32)


def near_kernel(place_ref, q_ref, k0_ref, v0_ref, k1_ref, v1_ref, k3_ref, v3_ref, k4_ref, v4_ref, max_ref, sum_ref, acc_ref, s_ref, p_ref, bias_ref, count_ref, stat_ref, tail_ref):
    cls = pl.program_id(0)
    block = place_ref[0]
    keys, width = k0_ref.shape
    heads = width // HEAD_DIM
    mine = pl.ds(pl.multiple_of(cls * 128, 128), 128)

    @pl.when(cls == 0)
    def _():
        j = lax.broadcasted_iota(jnp.int32, (128, keys), 0)
        i = lax.broadcasted_iota(jnp.int32, (128, keys), 1)
        pick = (i == (j >> 3) * 32 + 24 + (j & 7)).astype(BF16)
        tail_ref[0] = permuted(pick, k1_ref[...])
        tail_ref[1] = permuted(pick, v1_ref[...])
        bias_ref[:, keys + 256 : keys + 384] = far_bias(block, 3)
        bias_ref[:, keys + 384 : keys + 512] = far_bias(block, 4)

    i = lax.broadcasted_iota(jnp.int32, (128, 1), 0)
    qn = (i & 31) * 16 + (i >> 5) * 4 + cls
    seen = block >= 1
    for lies, size in ((0, keys), (keys, 128)):
        k = lax.broadcasted_iota(jnp.int32, (1, size), 1)
        if lies == 0:
            o = qn - natural(k)
        else:
            o = qn - ((k & 31) * 16 + (k >> 5) * 4 + cls) + keys
        count = (o <= SPAN).astype(F32)
        count = count + (((o & 3) == 0) & (o <= 4 * SPAN)).astype(F32)
        count = count + ((o & 15) == 0).astype(F32)
        if lies == 0:
            count = jnp.where(o >= 0, count, 0.0)
        else:
            count = jnp.where(seen, count, 0.0)
        count_ref[:, lies : lies + size] = count
        bias_ref[:, lies : lies + size] = jnp.where(count > 0, 0.0, LOW).astype(F32)
    k = lax.broadcasted_iota(jnp.int32, (1, 128), 1)
    o = qn - ((24 + (k & 7)) * 16 + ((k >> 3) & 3) * 4 + (k >> 5)) + keys
    ok = (o <= SPAN) & ((k >> 5) != cls) & seen
    bias_ref[:, keys + 128 : keys + 256] = jnp.where(ok, 0.0, LOW).astype(F32)

    q4 = stack_heads(q_ref[...])
    s_ref[:, :keys] = lax.dot_general(q4, k0_ref[...], NT, preferred_element_type=F32)
    rest = jnp.concatenate([k1_ref[mine, :], tail_ref[0], k3_ref[mine, :], k4_ref[mine, :]], axis=0)
    s_ref[:, keys:] = lax.dot_general(q4, rest, NT, preferred_element_type=F32)
    step = 32
    for r in range(0, heads * 128, step):
        mask = slice(r % 128, r % 128 + step)
        s = s_ref[r : r + step, :] + bias_ref[mask, :]
        m = jnp.max(s, axis=1, keepdims=True)
        p = jnp.exp(s - m)
        p = jnp.concatenate([p[:, : keys + 128] * count_ref[mask, :], p[:, keys + 128 :]], axis=1)
        stat_ref[0, r : r + step, :] = jnp.broadcast_to(m, (step, width))
        stat_ref[1, r : r + step, :] = jnp.broadcast_to(jnp.sum(p, axis=1, keepdims=True), (step, width))
        p_ref[r : r + step, :] = p.astype(BF16)
    pv = jnp.dot(p_ref[:, :keys], v0_ref[...], preferred_element_type=F32)
    rest = jnp.concatenate([v1_ref[mine, :], tail_ref[1], v3_ref[mine, :], v4_ref[mine, :]], axis=0)
    pv = pv + jnp.dot(p_ref[:, keys:], rest, preferred_element_type=F32)
    max_ref[...] = own_heads(stat_ref[0])
    sum_ref[...] = own_heads(stat_ref[1])
    acc_ref[...] = own_heads(pv)


def last_kernel(place_ref, q_ref, max_ref, sum_ref, acc_ref, k_ref, v_ref, out_ref, log_ref, att_ref, s_ref, p_ref, stat_ref):
    width = q_ref.shape[1]
    heads = width // HEAD_DIM
    bias = far_bias(place_ref[0], 2)
    s_ref[...] = lax.dot_general(stack_heads(q_ref[...]), k_ref[...], NT, preferred_element_type=F32)
    for h in range(heads):
        part = slice(h * 128, (h + 1) * 128)
        s = s_ref[part, :] + bias
        m = jnp.maximum(jnp.max(s, axis=1, keepdims=True), max_ref[:, h * HEAD_DIM : h * HEAD_DIM + 1])
        p = jnp.exp(s - m)
        p_ref[part, :] = p.astype(BF16)
        stat_ref[0, part, :] = jnp.broadcast_to(m, (128, width))
        stat_ref[1, part, :] = jnp.broadcast_to(jnp.sum(p, axis=1, keepdims=True), (128, width))
    pv = jnp.dot(p_ref[...], v_ref[...], preferred_element_type=F32)
    m = own_heads(stat_ref[0])
    alpha = jnp.exp(max_ref[...] - m)
    total = sum_ref[...] * alpha + own_heads(stat_ref[1])
    acc = acc_ref[...] * alpha + own_heads(pv)
    cls = pl.program_id(0)
    att_ref[pl.ds(pl.multiple_of(cls * 128, 128), 128), :] = (acc / total).astype(BF16)
    log_ref[...] = m + jnp.log(total)

    @pl.when(cls == pl.num_programs(0) - 1)
    def _():
        out_ref[...] = permuted(to_natural(att_ref.shape[0]), att_ref[...])


def log_kernel(lw_ref, log_ref):
    rows, width = lw_ref.shape
    perm = to_natural(rows)
    rest = lw_ref[...]
    ordered = jnp.zeros((rows, width), F32)
    for _ in range(3):
        piece = rest.astype(BF16)
        rest = rest - piece.astype(F32)
        ordered = ordered + jnp.dot(perm, piece, preferred_element_type=F32)
    flipped = ordered.T
    for head in range(width // HEAD_DIM):
        log_ref[head : head + 1, :] = flipped[head * HEAD_DIM : head * HEAD_DIM + 1, :]


def out_kernel(place_ref, att_ref, own_ref, before_ref, after_ref, upper_ref, lower_ref, keep_ref, give_ref, sum_ref):
    x, core = place_ref[2], place_ref[3]
    half = own_ref.shape[0] // 2
    rows = keep_ref.shape[0]
    for n, ref in enumerate((own_ref, before_ref, after_ref, None)):
        att = att_ref[lax.rem(x + HOPS[n], 4)]
        if ref is None:
            part = jnp.dot(att[:, :half], upper_ref[...], preferred_element_type=F32)
            part = part + jnp.dot(att[:, half:], lower_ref[...], preferred_element_type=F32)
        else:
            part = jnp.dot(att, ref[...], preferred_element_type=F32)
        part = part.astype(BF16).astype(F32)
        if n == 0:
            sum_ref[...] = part
        else:
            sum_ref[...] += part
    keep_ref[...] = sum_ref[pl.ds(pl.multiple_of(core * rows, rows), rows), :]
    give_ref[...] = sum_ref[pl.ds(pl.multiple_of((1 - core) * rows, rows), rows), :].astype(BF16)


def end_kernel(keep_ref, taken_ref, gain_ref, out_ref):
    summed = keep_ref[...] + taken_ref[...].astype(F32)
    scale = lax.rsqrt(jnp.mean(summed * summed, axis=1, keepdims=True) + EPS)
    out_ref[...] = (summed * scale * gain_ref[...]).astype(BF16)


SMEM = pl.BlockSpec(memory_space=pltpu.SMEM)
VMEM = pl.BlockSpec(memory_space=pltpu.VMEM)


def kernel_call(body, outs, args, flops, limit, scratch=(), **more):
    if "grid_spec" not in more:
        more["scratch_shapes"] = [pltpu.VMEM(s, t) for s, t in scratch]
    if "in_specs" not in more and "grid_spec" not in more:
        more["in_specs"] = [SMEM if a.dtype == jnp.int32 else VMEM for a in args]
        more["out_specs"] = tuple(VMEM for _ in outs)
    data = sum(a.size * a.dtype.itemsize for a in args)
    return pl.pallas_call(
        body,
        out_shape=tuple(jax.ShapeDtypeStruct(s, t) for s, t in outs),
        compiler_params=pltpu.CompilerParams(vmem_limit_bytes=limit * 1024 * 1024),
        cost_estimate=pl.CostEstimate(flops=flops, bytes_accessed=data, transcendentals=0),
        **more,
    )(*args)


def layer(hidden_in, pre_gain, query_proj, key_proj, value_proj, out_proj, post_gain):
    rows, depth = hidden_in.shape
    width = query_proj.shape[1]
    heads = width // HEAD_DIM
    sp, x, core = lax.axis_index(SP), lax.axis_index("x"), lax.axis_index("c")
    place = jnp.stack([sp, lax.axis_index("zl"), x, core]).astype(jnp.int32)
    member = (x * 2 + core)[None].astype(jnp.int32)
    gain = pre_gain[None]
    row = (rows, width)

    shard = jnp.concatenate([key_proj, value_proj], axis=1)
    copies = jnp.broadcast_to(shard[None], (32,) + shard.shape)
    mine = lax.all_to_all(copies, ("zh", "y"), split_axis=0, concat_axis=0, tiled=True)
    mine = mine.reshape(4, 256, 2 * width)
    below = lax.ppermute(mine[:2], Z, ring(8, 1))
    above = lax.ppermute(mine[2:], Z, ring(8, -1))

    piece = rows // 8
    (eighth,) = kernel_call(
        slice_kernel,
        [((piece, depth), BF16)],
        (member, hidden_in, gain),
        10 * piece * depth,
        12,
        grid_spec=pltpu.PrefetchScalarGridSpec(
            num_scalar_prefetch=1,
            grid=(1,),
            in_specs=[pl.BlockSpec((piece, depth), lambda i, t: (t[0], 0)), pl.BlockSpec((1, depth), lambda i, t: (0, 0))],
            out_specs=[pl.BlockSpec((piece, depth), lambda i, t: (0, 0))],
        ),
    )
    fourth = lax.ppermute(eighth, SP, ring(64, 4))
    third = lax.ppermute(fourth, SP, ring(64, -1))
    both = jnp.concatenate([fourth, third], axis=0)
    left = lax.ppermute(both, "x", ring(4, 1))
    right = lax.ppermute(both, "x", ring(4, -1))
    across4 = lax.ppermute(left[:piece], "x", ring(4, 1))
    across3 = lax.ppermute(right[piece:], "x", ring(4, -1))
    far_rows = jnp.concatenate([both, left, right, across4, across3], axis=0)
    far_others = lax.ppermute(far_rows, "c", ring(2, 1))

    before = lax.ppermute(out_proj, "x", ring(4, 1))
    after = lax.ppermute(out_proj, "x", ring(4, -1))
    upper = lax.ppermute(before[: width // 2], "x", ring(4, 1))
    lower = lax.ppermute(after[width // 2 :], "x", ring(4, -1))

    half = HEAD_DIM // 2
    frequency = ROPE_BASE ** (-(jnp.arange(half, dtype=F32) * 2.0 / HEAD_DIM))
    local = jnp.arange(rows, dtype=jnp.int32)
    positions = jnp.concatenate([(sp - 4) * rows + local, (sp - 3) * rows + local, sp * rows + local]).astype(F32)
    angles = positions[None, :] * frequency[:, None]
    turns = jnp.stack([jnp.cos(angles), jnp.sin(angles)])

    normed, query = kernel_call(
        query_kernel, [((rows, depth), BF16), (row, BF16)], (hidden_in, gain, query_proj, turns), 2 * rows * depth * width, 16
    )
    key, value, weights = kernel_call(
        key_value_kernel,
        [(row, BF16), (row, BF16), ((depth, 2 * width), BF16)],
        (place, normed, mine, below, above, turns),
        4 * rows * depth * width,
        20,
    )

    forward = [(i, i + 1) for i in range(63)]
    key1 = lax.ppermute(key, SP, forward)
    value1 = lax.ppermute(value, SP, forward)
    key2 = lax.ppermute(key1, SP, forward)
    value2 = lax.ppermute(value1, SP, forward)

    key4, value4, key3, value3 = kernel_call(
        far_key_value_kernel,
        [(row, BF16)] * 4,
        (place, far_rows, far_others, weights, turns),
        8 * rows * depth * width,
        24,
        [((2 * rows, width), F32), ((2 * rows, width), F32), ((2,) + row, BF16), ((2,) + row, BF16)],
    )

    whole = pl.BlockSpec(row, lambda c: (0, 0))
    part = pl.BlockSpec((128, width), lambda c: (c, 0))
    state = kernel_call(
        near_kernel,
        [(row, F32)] * 3,
        (place, query, key, value, key1, value1, key3, value3, key4, value4),
        16 * rows * rows * width,
        24,
        [((512, 1024), F32), ((512, 1024), BF16), ((128, 1024), F32), ((128, 640), F32), ((2, 512, width), F32), ((2, 128, width), BF16)],
        grid=(rows // 128,),
        in_specs=[SMEM, part] + [whole] * 8,
        out_specs=(part,) * 3,
    )
    attended, logs = kernel_call(
        last_kernel,
        [(row, BF16), (row, F32)],
        (place, query, *state, key2, value2),
        4 * rows * 512 * width,
        16,
        [(row, BF16), ((512, 128), F32), ((512, 128), BF16), ((2, 512, width), F32)],
        grid=(rows // 128,),
        in_specs=[SMEM] + [part] * 6,
        out_specs=(whole, part),
    )

    arrived = lax.all_to_all(attended.reshape(4, rows // 4, width), "x", split_axis=0, concat_axis=0, tiled=True)
    (log_weight,) = kernel_call(log_kernel, [((heads, rows), F32)], (logs,), 6 * rows * rows * width, 12)
    keep, give = kernel_call(
        out_kernel,
        [((piece, depth), F32), ((piece, depth), BF16)],
        (place, arrived, out_proj, before, after, upper, lower),
        2 * rows // 8 * depth * depth,
        20,
        [((2 * piece, depth), F32)],
    )
    taken = lax.ppermute(give, "c", ring(2, 1))
    (layer_out,) = kernel_call(end_kernel, [((piece, depth), BF16)], (keep, taken, post_gain[None]), 10 * piece * depth, 8)
    return layer_out, log_weight


def solution(mesh):
    fine = Mesh(np.asarray(mesh.devices).reshape(4, 2, 8, 4, 2), ("zh", "zl", "y", "x", "c"))
    placed = (P(SP, None), P(), P(None, TP), P(SP, TP), P(SP, TP), P(TP, None), P())
    return jax.shard_map(
        layer,
        mesh=fine,
        in_specs=placed,
        out_specs=(P(SP + TP, None), P(TP, SP)),
        check_vma=False,
    )
```

time: 163 us -> 166 us (1.018)
  the two profiles are of different devices: /device:TPU:248 before, /device:TPU:1 now
where the time goes in v3:
time: 166 us; the launch traced here: 165 us
  starting transfers between devices  85.3 us (51%)
  waiting for transfers between devices  37.9 us (23%)
  Pallas kernels  29 us (17%)
  local copies, waits for them, and re-layouts  10.4 us (6%)
    pallas_call x9, Pallas kernels, kernel_call(): pl.pallas_call(body, out_shape=tuple((jax.ShapeDtypeStruct(s, t) for s, t...  29 us
    ppermute x1, waiting for transfers between devices, layer(): fourth = lax.ppermute(eighth, SP, ring(64, 4))  16.1 us
    ppermute x1, waiting for transfers between devices, layer(): third = lax.ppermute(fourth, SP, ring(64, -1))  8.85 us
    ppermute x1, starting transfers between devices, layer(): fourth = lax.ppermute(eighth, SP, ring(64, 4))  8.27 us
    ppermute x1, starting transfers between devices, layer(): taken = lax.ppermute(give, 'c', ring(2, 1))  8.2 us
    all_to_all x1, starting transfers between devices, layer(): lax.all_to_all(copies, ('zh', 'y'), split_axis=0, concat_axis=0, tiled=True)  7.17 us
    ppermute x1, starting transfers between devices, layer(): value2 = lax.ppermute(value1, SP, forward)  5.6 us
    all_to_all x1, waiting for transfers between devices, layer(): lax.all_to_all(attended.reshape(4, rows // 4, width), 'x', split_axis=0,...  5.46 us
  transfers between devices with their start and end apart: 20, of which 9 were waited for; matrix products, arithmetic and copies ran while one was open for 5% of the time, Pallas kernels for 15%

profile of v3, /device:TPU:1, one launch (start us, length us, event | category | flops | bytes accessed | tf_op | source)
XLA Modules:
  0.0 164.6 jit_solution(13152128988363171054)
XLA Ops:
  0.6 0.0 copy-start
  0.7 1.6 copy-done
  2.2 0.7 copy-done.3
  2.9 0.2 shard_map.88
  3.1 8.3 %collective-permute-start.4 = (bf16[64,2048]{1,0:T(8,128)(2,1)S(1)}, bf16[64,2048]{1,0:T(8,128)(2,1)S(1)}, u32[]{:S(2)}, u32[]{:S(2)}) collective-permute-start(bf16[64,2048]{1,0:T(8,128)(2,1)S(1)} %shard_map.88), channel_id=1, source_target_pairs={{0,32},{8,40},{16,48},{24,56},{32,64},{40,72},{48,80},{56,88},{64,... | collective-permute-start | bytes 786440 | tf_op jit(solution)/shard_map/ppermute | solution.py:344
  11.4 16.1 %collective-permute-done.4 = bf16[64,2048]{1,0:T(8,128)(2,1)S(1)} collective-permute-done((bf16[64,2048]{1,0:T(8,128)(2,1)S(1)}, bf16[64,2048]{1,0:T(8,128)(2,1)S(1)}, u32[]{:S(2)}, u32[]{:S(2)}) %collective-permute-start.4) | collective-permute-done | bytes 262176 | tf_op jit(solution)/shard_map/ppermute | solution.py:344
  27.5 2.9 %collective-permute-start.5 = (bf16[64,2048]{1,0:T(8,128)(2,1)S(1)}, bf16[64,2048]{1,0:T(8,128)(2,1)S(1)}, u32[]{:S(2)}, u32[]{:S(2)}) collective-permute-start(bf16[64,2048]{1,0:T(8,128)(2,1)S(1)} %collective-permute-done.4), channel_id=1, source_target_pairs={{0,504},{8,0},{16,8},{24,16},{32,24},{40,32},{48,40},{56,48},{64,5... | collective-permute-start | bytes 786440 | tf_op jit(solution)/shard_map/ppermute | solution.py:345
  30.5 0.8 constant_dynamic-update-slice_fusion.1
  31.2 8.9 %collective-permute-done.5 = bf16[64,2048]{1,0:T(8,128)(2,1)S(1)} collective-permute-done((bf16[64,2048]{1,0:T(8,128)(2,1)S(1)}, bf16[64,2048]{1,0:T(8,128)(2,1)S(1)}, u32[]{:S(2)}, u32[]{:S(2)}) %collective-permute-start.5) | collective-permute-done | bytes 262176 | tf_op jit(solution)/shard_map/ppermute | solution.py:345
  40.1 0.8 constant_dynamic-update-slice_fusion
  40.9 3.1 %collective-permute-start.6 = (bf16[128,2048]{1,0:T(8,128)(2,1)S(1)}, bf16[128,2048]{1,0:T(8,128)(2,1)S(1)}, u32[]{:S(2)}, u32[]{:S(2)}) collective-permute-start(bf16[128,2048]{1,0:T(8,128)(2,1)S(1)} %get-tuple-element.36), channel_id=1, source_target_pairs={{0,2},{2,4},{4,6},{6,0},{1,3},{3,5},{5,7},{7,1},{8,10},{10,12},{12... | collective-permute-start | bytes 1572872 | tf_op jit(solution)/shard_map/ppermute | solution.py:347
  44.0 3.4 %collective-permute-start.7 = (bf16[128,2048]{1,0:T(8,128)(2,1)S(1)}, bf16[128,2048]{1,0:T(8,128)(2,1)S(1)}, u32[]{:S(2)}, u32[]{:S(2)}) collective-permute-start(bf16[128,2048]{1,0:T(8,128)(2,1)S(1)} %get-tuple-element.36), channel_id=1, source_target_pairs={{0,6},{2,0},{4,2},{6,4},{1,7},{3,1},{5,3},{7,5},{8,14},{10,8},{12,... | collective-permute-start | bytes 1572872 | tf_op jit(solution)/shard_map/ppermute | solution.py:348
  47.4 1.1 broadcast_in_dim.18
  48.5 7.2 %all-to-all-start = ((bf16[32,32,512]{2,1,0:T(8,128)(2,1)}), bf16[32,32,512]{2,1,0:T(8,128)(2,1)S(1)}, u32[]{:S(2)}, u32[]{:S(2)}) async-start(bf16[32,32,512]{2,1,0:T(8,128)(2,1)} %broadcast_in_dim.18), calls=%async_computation | async-start | bytes 2097152 | tf_op jit(solution)/shard_map/all_to_all | solution.py:325
  55.7 0.3 collective-permute-done.6
  56.0 1.9 %collective-permute-start.8 = (bf16[64,2048]{1,0:T(8,128)(2,1)S(1)}, bf16[64,2048]{1,0:T(8,128)(2,1)S(1)}, u32[]{:S(2)}, u32[]{:S(2)}) collective-permute-start(bf16[64,2048]{1,0:T(8,128)(2,1)S(1)} %slice.34), channel_id=1, source_target_pairs={{0,2},{2,4},{4,6},{6,0},{1,3},{3,5},{5,7},{7,1},{8,10},{10,12},{12... | collective-permute-start | bytes 786440 | tf_op jit(solution)/shard_map/ppermute | solution.py:349
  57.9 0.0 collective-permute-done.7
  58.0 4.6 %collective-permute-start.9 = (bf16[64,2048]{1,0:T(8,128)(2,1)S(1)}, bf16[64,2048]{1,0:T(8,128)(2,1)S(1)}, u32[]{:S(2)}, u32[]{:S(2)}) collective-permute-start(bf16[64,2048]{1,0:T(8,128)(2,1)S(1)} %slice.35), channel_id=1, source_target_pairs={{0,6},{2,0},{4,2},{6,4},{1,7},{3,1},{5,3},{7,5},{8,14},{10,8},{12,... | collective-permute-start | bytes 786440 | tf_op jit(solution)/shard_map/ppermute | solution.py:350
  62.5 0.8 constant_dynamic-update-slice_fusion.5
  63.4 0.8 constant_dynamic-update-slice_fusion.4
  64.2 0.4 collective-permute-done.8
  64.6 0.7 constant_dynamic-update-slice_fusion.3
  65.4 0.5 collective-permute-done.9
  65.8 0.7 constant_dynamic-update-slice_fusion.2.mine_ref
  66.6 5.4 %collective-permute-start.10 = (bf16[512,2048]{1,0:T(8,128)(2,1)}, bf16[512,2048]{1,0:T(8,128)(2,1)}, u32[]{:S(2)}, u32[]{:S(2)}) collective-permute-start(bf16[512,2048]{1,0:T(8,128)(2,1)} %constant_dynamic-update-slice_fusion.2.mine_ref), channel_id=1, source_target_pairs={{0,1},{1,0},{2,3},{3,2},{4,5},{5,4},{6,7},{7,6},{8,9},{9,8},{10,11... | collective-permute-start | bytes 6291464 | tf_op jit(solution)/shard_map/ppermute | solution.py:352
  71.9 2.6 %collective-permute-start.13 = (bf16[256,2048]{1,0:T(8,128)(2,1)}, bf16[256,2048]{1,0:T(8,128)(2,1)}, u32[]{:S(2)}, u32[]{:S(2)}) collective-permute-start(bf16[256,2048]{1,0:T(8,128)(2,1)} %own_ref.1), channel_id=1, source_target_pairs={{0,2},{2,4},{4,6},{6,0},{1,3},{3,5},{5,7},{7,1},{8,10},{10,12},{12... | collective-permute-start | bytes 3145736 | tf_op jit(solution)/shard_map/ppermute | solution.py:354
  74.6 4.6 %collective-permute-start.14 = (bf16[256,2048]{1,0:T(8,128)(2,1)}, bf16[256,2048]{1,0:T(8,128)(2,1)}, u32[]{:S(2)}, u32[]{:S(2)}) collective-permute-start(bf16[256,2048]{1,0:T(8,128)(2,1)} %own_ref.1), channel_id=1, source_target_pairs={{0,6},{2,0},{4,2},{6,4},{1,7},{3,1},{5,3},{7,5},{8,14},{10,8},{12,... | collective-permute-start | bytes 3145736 | tf_op jit(solution)/shard_map/ppermute | solution.py:355
  79.3 2.9 %all-to-all-done = bf16[32,32,512]{2,1,0:T(8,128)(2,1)S(1)} async-done(((bf16[32,32,512]{2,1,0:T(8,128)(2,1)}), bf16[32,32,512]{2,1,0:T(8,128)(2,1)S(1)}, u32[]{:S(2)}, u32[]{:S(2)}) %all-to-all-start) | async-done | bytes 1048608 | tf_op jit(solution)/shard_map/all_to_all | solution.py:325
  82.2 0.1 fusion
  82.3 2.7 %collective-permute-start = (bf16[2,256,512]{2,1,0:T(8,128)(2,1)S(1)}, bf16[2,256,512]{2,1,0:T(8,128)(2,1)S(1)}, u32[]{:S(2)}, u32[]{:S(2)}) collective-permute-start(bf16[2,256,512]{2,1,0:T(8,128)(2,1)S(1)} %bitcast.16), channel_id=1, source_target_pairs={{0,64},{64,128},{128,192},{192,256},{256,320},{320,384},{384,448},... | collective-permute-start | bytes 1572872 | tf_op jit(solution)/shard_map/ppermute | solution.py:327
  85.0 4.0 %collective-permute-start.1 = (bf16[2,256,512]{2,1,0:T(8,128)(2,1)S(1)}, bf16[2,256,512]{2,1,0:T(8,128)(2,1)S(1)}, u32[]{:S(2)}, u32[]{:S(2)}) collective-permute-start(bf16[2,256,512]{2,1,0:T(8,128)(2,1)S(1)} %bitcast.15), channel_id=1, source_target_pairs={{0,448},{64,0},{128,64},{192,128},{256,192},{320,256},{384,320},{4... | collective-permute-start | bytes 1572872 | tf_op jit(solution)/shard_map/ppermute | solution.py:328
  88.9 0.8 multiply_cosine_fusion
  89.8 2.7 %shard_map.86 = (bf16[512,2048]{1,0:T(8,128)(2,1)S(1)}, bf16[512,256]{1,0:T(8,128)(2,1)S(1)}) custom-call(bf16[512,2048]{1,0:T(8,128)(2,1)S(1)} %copy-done.1, f32[1,2048]{1,0:T(1,128)S(1)} %bitcast.13, bf16[2048,256]{1,0:T(8,128)(2,1)S(1)} %copy-done.2, f32[2,32,1536]{2,1,0:T(8,128)S(1)} %pad_maximum_fusion.turn_ref), custom_call_target="tpu_custom_call" | custom-call | flops 536870912 | bytes 3547136 | tf_op jit(solution)/shard_map/pallas_call | solution.py:304
  92.5 0.1 pad_add_fusion.place_ref
  92.5 2.5 %collective-permute-done.below_ref = bf16[2,256,512]{2,1,0:T(8,128)(2,1)S(1)} collective-permute-done((bf16[2,256,512]{2,1,0:T(8,128)(2,1)S(1)}, bf16[2,256,512]{2,1,0:T(8,128)(2,1)S(1)}, u32[]{:S(2)}, u32[]{:S(2)}) %collective-permute-start) | collective-permute-done | bytes 524320 | tf_op jit(solution)/shard_map/ppermute | solution.py:327
  95.1 0.8 collective-permute-done.1.above_ref
  95.9 3.9 %shard_map.87 = (bf16[512,256]{1,0:T(8,128)(2,1)S(1)}, bf16[512,256]{1,0:T(8,128)(2,1)S(1)}, bf16[2048,512]{1,0:T(8,128)(2,1)S(1)}) custom-call(s32[4]{0:T(128)S(1)} %pad_add_fusion.place_ref, bf16[512,2048]{1,0:T(8,128)(2,1)S(1)} %get-tuple-element.19.normed_ref, bf16[4,256,512]{2,1,0:T(8,128)(2,1)S(1)} %bitcast.11, ...), custom_call_target="tpu_custom_call" | custom-call | flops 1073741824 | bytes 4587536 | tf_op jit(solution)/shard_map/pallas_call | solution.py:304
  99.7 4.1 %collective-permute-start.2 = (bf16[512,256]{1,0:T(8,128)(2,1)S(1)}, bf16[512,256]{1,0:T(8,128)(2,1)S(1)}, u32[]{:S(2)}, u32[]{:S(2)}) collective-permute-start(bf16[512,256]{1,0:T(8,128)(2,1)S(1)} %get-tuple-element.20.k0_ref), channel_id=1, source_target_pairs={{0,8},{8,16},{16,24},{24,32},{32,40},{40,48},{48,56},{56,64},{64,7... | collective-permute-start | bytes 786440 | tf_op jit(solution)/shard_map/ppermute | solution.py:378
  103.9 5.0 %collective-permute-start.3 = (bf16[512,256]{1,0:T(8,128)(2,1)S(1)}, bf16[512,256]{1,0:T(8,128)(2,1)S(1)}, u32[]{:S(2)}, u32[]{:S(2)}) collective-permute-start(bf16[512,256]{1,0:T(8,128)(2,1)S(1)} %get-tuple-element.21.v0_ref), channel_id=1, source_target_pairs={{0,8},{8,16},{16,24},{24,32},{32,40},{40,48},{48,56},{56,64},{64,7... | collective-permute-start | bytes 786440 | tf_op jit(solution)/shard_map/ppermute | solution.py:379
  108.9 0.0 collective-permute-done.13.before_ref
  108.9 1.1 slice.36
  110.0 1.9 %collective-permute-start.15 = (bf16[128,2048]{1,0:T(8,128)(2,1)S(1)}, bf16[128,2048]{1,0:T(8,128)(2,1)S(1)}, u32[]{:S(2)}, u32[]{:S(2)}) collective-permute-start(bf16[128,2048]{1,0:T(8,128)(2,1)S(1)} %slice.36), channel_id=1, source_target_pairs={{0,2},{2,4},{4,6},{6,0},{1,3},{3,5},{5,7},{7,1},{8,10},{10,12},{12... | collective-permute-start | bytes 1572872 | tf_op jit(solution)/shard_map/ppermute | solution.py:356
  111.9 0.0 collective-permute-done.14.after_ref
  111.9 1.1 slice.37
  113.0 4.6 %collective-permute-start.16 = (bf16[128,2048]{1,0:T(8,128)(2,1)S(1)}, bf16[128,2048]{1,0:T(8,128)(2,1)S(1)}, u32[]{:S(2)}, u32[]{:S(2)}) collective-permute-start(bf16[128,2048]{1,0:T(8,128)(2,1)S(1)} %slice.37), channel_id=1, source_target_pairs={{0,6},{2,0},{4,2},{6,4},{1,7},{3,1},{5,3},{7,5},{8,14},{10,8},{12,... | collective-permute-start | bytes 1572872 | tf_op jit(solution)/shard_map/ppermute | solution.py:357
  117.6 0.0 collective-permute-done.2.k1_ref
  117.6 1.9 %collective-permute-start.11 = (bf16[512,256]{1,0:T(8,128)(2,1)S(1)}, bf16[512,256]{1,0:T(8,128)(2,1)S(1)}, u32[]{:S(2)}, u32[]{:S(2)}) collective-permute-start(bf16[512,256]{1,0:T(8,128)(2,1)S(1)} %collective-permute-done.2.k1_ref), channel_id=1, source_target_pairs={{0,8},{8,16},{16,24},{24,32},{32,40},{40,48},{48,56},{56,64},{64,7... | collective-permute-start | bytes 786440 | tf_op jit(solution)/shard_map/ppermute | solution.py:380
  119.5 0.0 collective-permute-done.3.v1_ref
  119.5 5.6 %collective-permute-start.12 = (bf16[512,256]{1,0:T(8,128)(2,1)S(1)}, bf16[512,256]{1,0:T(8,128)(2,1)S(1)}, u32[]{:S(2)}, u32[]{:S(2)}) collective-permute-start(bf16[512,256]{1,0:T(8,128)(2,1)S(1)} %collective-permute-done.3.v1_ref), channel_id=1, source_target_pairs={{0,8},{8,16},{16,24},{24,32},{32,40},{40,48},{48,56},{56,64},{64,7... | collective-permute-start | bytes 786440 | tf_op jit(solution)/shard_map/ppermute | solution.py:381
  125.1 0.0 collective-permute-done.10.other_ref
  125.1 5.3 %shard_map.89 = (bf16[512,256]{1,0:T(8,128)(2,1)S(1)}, bf16[512,256]{1,0:T(8,128)(2,1)S(1)}, bf16[512,256]{1,0:T(8,128)(2,1)S(1)}, bf16[512,256]{1,0:T(8,128)(2,1)S(1)}) custom-call(s32[4]{0:T(128)S(1)} %pad_add_fusion.place_ref, bf16[512,2048]{1,0:T(8,128)(2,1)} %constant_dynamic-update-slice_fusion.2.mine_ref, ...), custom_call_target="tpu_custom_call" | custom-call | flops 2147483648 | bytes 6684688 | tf_op jit(solution)/shard_map/pallas_call | solution.py:304
  130.4 7.5 %shard_map.90 = (f32[512,256]{1,0:T(8,128)S(1)}, f32[512,256]{1,0:T(8,128)S(1)}, f32[512,256]{1,0:T(8,128)S(1)}) custom-call(s32[4]{0:T(128)S(1)} %pad_add_fusion.place_ref, bf16[512,256]{1,0:T(8,128)(2,1)S(1)} %get-tuple-element.18.q_ref, bf16[512,256]{1,0:T(8,128)(2,1)S(1)} %get-tuple-element.20.k0_ref, bf16[512,256]{1,0:T(8,128)(2,1)S(1)} %get-tuple-element.21.v0_ref, ...), custom_call_target="tpu_custom_call" | custom-call | flops 1073741824 | bytes 2359312 | tf_op jit(solution)/shard_map/pallas_call | solution.py:304
  137.9 0.0 collective-permute-done.11.k_ref
  137.9 0.0 collective-permute-done.12.v_ref
  137.9 4.6 %shard_map.91 = (bf16[512,256]{1,0:T(8,128)(2,1)}, f32[512,256]{1,0:T(8,128)S(1)}) custom-call(s32[4]{0:T(128)S(1)} %pad_add_fusion.place_ref, bf16[512,256]{1,0:T(8,128)(2,1)S(1)} %get-tuple-element.18.q_ref, f32[512,256]{1,0:T(8,128)S(1)} %get-tuple-element.27.max_ref, f32[512,256]{1,0:T(8,128)S(1)} %get-tuple-element.28.sum_ref, ...), custom_call_target="tpu_custom_call" | custom-call | flops 268435456 | bytes 2359312 | tf_op jit(solution)/shard_map/pallas_call | solution.py:304
  142.6 3.4 %all-to-all-start.1 = ((bf16[4,128,256]{2,1,0:T(8,128)(2,1)}), bf16[4,128,256]{2,1,0:T(8,128)(2,1)S(1)}, u32[]{:S(2)}, u32[]{:S(2)}) async-start(bf16[4,128,256]{2,1,0:T(8,128)(2,1)} %bitcast.9), calls=%async_computation.1 | async-start | bytes 524288 | tf_op jit(solution)/shard_map/all_to_all | solution.py:417
  146.0 0.0 copy-start.5
  146.0 0.0 collective-permute-done.15.upper_ref
  146.0 5.5 %all-to-all-done.1.att_ref = bf16[4,128,256]{2,1,0:T(8,128)(2,1)S(1)} async-done(((bf16[4,128,256]{2,1,0:T(8,128)(2,1)}), bf16[4,128,256]{2,1,0:T(8,128)(2,1)S(1)}, u32[]{:S(2)}, u32[]{:S(2)}) %all-to-all-start.1) | async-done | bytes 262176 | tf_op jit(solution)/shard_map/all_to_all | solution.py:417
  151.5 2.8 %shard_map.92 = (f32[64,2048]{1,0:T(8,128)S(1)}, bf16[64,2048]{1,0:T(8,128)(2,1)S(1)}) custom-call(s32[4]{0:T(128)S(1)} %pad_add_fusion.place_ref, bf16[4,128,256]{2,1,0:T(8,128)(2,1)S(1)} %all-to-all-done.1.att_ref, bf16[256,2048]{1,0:T(8,128)(2,1)} %own_ref.1, bf16[256,2048]{1,0:T(8,128)(2,1)} %collective-permute-done.13.before_ref, ...), custom_call_target="tpu_custom_call" | custom-call | flops 536870912 | bytes 4456464 | tf_op jit(solution)/shard_map/pallas_call | solution.py:304
  154.3 8.2 %collective-permute-start.17 = (bf16[64,2048]{1,0:T(8,128)(2,1)S(1)}, bf16[64,2048]{1,0:T(8,128)(2,1)S(1)}, u32[]{:S(2)}, u32[]{:S(2)}) collective-permute-start(bf16[64,2048]{1,0:T(8,128)(2,1)S(1)} %get-tuple-element.32), channel_id=1, source_target_pairs={{0,1},{1,0},{2,3},{3,2},{4,5},{5,4},{6,7},{7,6},{8,9},{9,8},{10,11... | collective-permute-start | bytes 786440 | tf_op jit(solution)/shard_map/ppermute | solution.py:427
  162.5 1.3 shard_map.94
  163.8 0.0 collective-permute-done.17.taken_ref
  163.8 0.9 shard_map.93
  (21 shorter events, 0.1 us)
Async XLA Ops:
  0.6 46.7 %copy-start.6 = (bf16[32,256]{1,0:T(8,128)(2,1)S(1)}, bf16[32,256]{1,0:T(8,128)(2,1)}, u32[]{:S(2)}) copy-start(bf16[32,256]{1,0:T(8,128)(2,1)} %param.11) | copy-start | bytes 49156
  0.6 1.6 copy-start
  2.2 0.7 copy-start.3
  2.9 44.4 %copy-start.7 = (bf16[32,256]{1,0:T(8,128)(2,1)S(1)}, bf16[32,256]{1,0:T(8,128)(2,1)}, u32[]{:S(2)}) copy-start(bf16[32,256]{1,0:T(8,128)(2,1)} %param.10) | copy-start | bytes 49156
  3.1 24.4 %collective-permute-start.4 = (bf16[64,2048]{1,0:T(8,128)(2,1)S(1)}, bf16[64,2048]{1,0:T(8,128)(2,1)S(1)}, u32[]{:S(2)}, u32[]{:S(2)}) collective-permute-start(bf16[64,2048]{1,0:T(8,128)(2,1)S(1)} %shard_map.88), channel_id=1, source_target_pairs={{0,32},{8,40},{16,48},{24,56},{32,64},{40,72},{48,80},{56,88},{64,... | collective-permute-start | bytes 786440 | tf_op jit(solution)/shard_map/ppermute | solution.py:344
  27.5 12.6 %collective-permute-start.5 = (bf16[64,2048]{1,0:T(8,128)(2,1)S(1)}, bf16[64,2048]{1,0:T(8,128)(2,1)S(1)}, u32[]{:S(2)}, u32[]{:S(2)}) collective-permute-start(bf16[64,2048]{1,0:T(8,128)(2,1)S(1)} %collective-permute-done.4), channel_id=1, source_target_pairs={{0,504},{8,0},{16,8},{24,16},{32,24},{40,32},{48,40},{56,48},{64,5... | collective-permute-start | bytes 786440 | tf_op jit(solution)/shard_map/ppermute | solution.py:345
  40.9 15.1 %collective-permute-start.6 = (bf16[128,2048]{1,0:T(8,128)(2,1)S(1)}, bf16[128,2048]{1,0:T(8,128)(2,1)S(1)}, u32[]{:S(2)}, u32[]{:S(2)}) collective-permute-start(bf16[128,2048]{1,0:T(8,128)(2,1)S(1)} %get-tuple-element.36), channel_id=1, source_target_pairs={{0,2},{2,4},{4,6},{6,0},{1,3},{3,5},{5,7},{7,1},{8,10},{10,12},{12... | collective-permute-start | bytes 1572872 | tf_op jit(solution)/shard_map/ppermute | solution.py:347
  44.0 13.9 %collective-permute-start.7 = (bf16[128,2048]{1,0:T(8,128)(2,1)S(1)}, bf16[128,2048]{1,0:T(8,128)(2,1)S(1)}, u32[]{:S(2)}, u32[]{:S(2)}) collective-permute-start(bf16[128,2048]{1,0:T(8,128)(2,1)S(1)} %get-tuple-element.36), channel_id=1, source_target_pairs={{0,6},{2,0},{4,2},{6,4},{1,7},{3,1},{5,3},{7,5},{8,14},{10,8},{12,... | collective-permute-start | bytes 1572872 | tf_op jit(solution)/shard_map/ppermute | solution.py:348
  48.5 33.7 %all-to-all-start = ((bf16[32,32,512]{2,1,0:T(8,128)(2,1)}), bf16[32,32,512]{2,1,0:T(8,128)(2,1)S(1)}, u32[]{:S(2)}, u32[]{:S(2)}) async-start(bf16[32,32,512]{2,1,0:T(8,128)(2,1)} %broadcast_in_dim.18), calls=%async_computation | async-start | bytes 2097152 | tf_op jit(solution)/shard_map/all_to_all | solution.py:325
  56.0 8.6 %collective-permute-start.8 = (bf16[64,2048]{1,0:T(8,128)(2,1)S(1)}, bf16[64,2048]{1,0:T(8,128)(2,1)S(1)}, u32[]{:S(2)}, u32[]{:S(2)}) collective-permute-start(bf16[64,2048]{1,0:T(8,128)(2,1)S(1)} %slice.34), channel_id=1, source_target_pairs={{0,2},{2,4},{4,6},{6,0},{1,3},{3,5},{5,7},{7,1},{8,10},{10,12},{12... | collective-permute-start | bytes 786440 | tf_op jit(solution)/shard_map/ppermute | solution.py:349
  58.0 7.9 %collective-permute-start.9 = (bf16[64,2048]{1,0:T(8,128)(2,1)S(1)}, bf16[64,2048]{1,0:T(8,128)(2,1)S(1)}, u32[]{:S(2)}, u32[]{:S(2)}) collective-permute-start(bf16[64,2048]{1,0:T(8,128)(2,1)S(1)} %slice.35), channel_id=1, source_target_pairs={{0,6},{2,0},{4,2},{6,4},{1,7},{3,1},{5,3},{7,5},{8,14},{10,8},{12,... | collective-permute-start | bytes 786440 | tf_op jit(solution)/shard_map/ppermute | solution.py:350
  64.2 25.5 %copy-start.1 = (bf16[512,2048]{1,0:T(8,128)(2,1)S(1)}, bf16[512,2048]{1,0:T(8,128)(2,1)}, u32[]{:S(2)}) copy-start(bf16[512,2048]{1,0:T(8,128)(2,1)} %hidden_ref.3) | copy-start | bytes 6291460
  64.2 25.5 %copy-start.4 = (f32[2048]{0:T(1024)S(1)}, f32[2048]{0:T(1024)}, u32[]{:S(2)}) copy-start(f32[2048]{0:T(1024)} %param.8) | copy-start | bytes 24580
  66.6 58.6 %collective-permute-start.10 = (bf16[512,2048]{1,0:T(8,128)(2,1)}, bf16[512,2048]{1,0:T(8,128)(2,1)}, u32[]{:S(2)}, u32[]{:S(2)}) collective-permute-start(bf16[512,2048]{1,0:T(8,128)(2,1)} %constant_dynamic-update-slice_fusion.2.mine_ref), channel_id=1, source_target_pairs={{0,1},{1,0},{2,3},{3,2},{4,5},{5,4},{6,7},{7,6},{8,9},{9,8},{10,11... | collective-permute-start | bytes 6291464 | tf_op jit(solution)/shard_map/ppermute | solution.py:352
  71.9 36.9 %collective-permute-start.13 = (bf16[256,2048]{1,0:T(8,128)(2,1)}, bf16[256,2048]{1,0:T(8,128)(2,1)}, u32[]{:S(2)}, u32[]{:S(2)}) collective-permute-start(bf16[256,2048]{1,0:T(8,128)(2,1)} %own_ref.1), channel_id=1, source_target_pairs={{0,2},{2,4},{4,6},{6,0},{1,3},{3,5},{5,7},{7,1},{8,10},{10,12},{12... | collective-permute-start | bytes 3145736 | tf_op jit(solution)/shard_map/ppermute | solution.py:354
  74.6 37.3 %collective-permute-start.14 = (bf16[256,2048]{1,0:T(8,128)(2,1)}, bf16[256,2048]{1,0:T(8,128)(2,1)}, u32[]{:S(2)}, u32[]{:S(2)}) collective-permute-start(bf16[256,2048]{1,0:T(8,128)(2,1)} %own_ref.1), channel_id=1, source_target_pairs={{0,6},{2,0},{4,2},{6,4},{1,7},{3,1},{5,3},{7,5},{8,14},{10,8},{12,... | collective-permute-start | bytes 3145736 | tf_op jit(solution)/shard_map/ppermute | solution.py:355
  82.2 7.6 %copy-start.2 = (bf16[2048,256]{1,0:T(8,128)(2,1)S(1)}, bf16[2048,256]{1,0:T(8,128)(2,1)}, u32[]{:S(2)}) copy-start(bf16[2048,256]{1,0:T(8,128)(2,1)} %weight_ref.1) | copy-start | bytes 3145732
  82.3 12.8 %collective-permute-start = (bf16[2,256,512]{2,1,0:T(8,128)(2,1)S(1)}, bf16[2,256,512]{2,1,0:T(8,128)(2,1)S(1)}, u32[]{:S(2)}, u32[]{:S(2)}) collective-permute-start(bf16[2,256,512]{2,1,0:T(8,128)(2,1)S(1)} %bitcast.16), channel_id=1, source_target_pairs={{0,64},{64,128},{128,192},{192,256},{256,320},{320,384},{384,448},... | collective-permute-start | bytes 1572872 | tf_op jit(solution)/shard_map/ppermute | solution.py:327
  85.0 10.9 %collective-permute-start.1 = (bf16[2,256,512]{2,1,0:T(8,128)(2,1)S(1)}, bf16[2,256,512]{2,1,0:T(8,128)(2,1)S(1)}, u32[]{:S(2)}, u32[]{:S(2)}) collective-permute-start(bf16[2,256,512]{2,1,0:T(8,128)(2,1)S(1)} %bitcast.15), channel_id=1, source_target_pairs={{0,448},{64,0},{128,64},{192,128},{256,192},{320,256},{384,320},{4... | collective-permute-start | bytes 1572872 | tf_op jit(solution)/shard_map/ppermute | solution.py:328
  99.7 17.8 %collective-permute-start.2 = (bf16[512,256]{1,0:T(8,128)(2,1)S(1)}, bf16[512,256]{1,0:T(8,128)(2,1)S(1)}, u32[]{:S(2)}, u32[]{:S(2)}) collective-permute-start(bf16[512,256]{1,0:T(8,128)(2,1)S(1)} %get-tuple-element.20.k0_ref), channel_id=1, source_target_pairs={{0,8},{8,16},{16,24},{24,32},{32,40},{40,48},{48,56},{56,64},{64,7... | collective-permute-start | bytes 786440 | tf_op jit(solution)/shard_map/ppermute | solution.py:378
  103.9 15.7 %collective-permute-start.3 = (bf16[512,256]{1,0:T(8,128)(2,1)S(1)}, bf16[512,256]{1,0:T(8,128)(2,1)S(1)}, u32[]{:S(2)}, u32[]{:S(2)}) collective-permute-start(bf16[512,256]{1,0:T(8,128)(2,1)S(1)} %get-tuple-element.21.v0_ref), channel_id=1, source_target_pairs={{0,8},{8,16},{16,24},{24,32},{32,40},{40,48},{48,56},{56,64},{64,7... | collective-permute-start | bytes 786440 | tf_op jit(solution)/shard_map/ppermute | solution.py:379
  110.0 36.0 %collective-permute-start.15 = (bf16[128,2048]{1,0:T(8,128)(2,1)S(1)}, bf16[128,2048]{1,0:T(8,128)(2,1)S(1)}, u32[]{:S(2)}, u32[]{:S(2)}) collective-permute-start(bf16[128,2048]{1,0:T(8,128)(2,1)S(1)} %slice.36), channel_id=1, source_target_pairs={{0,2},{2,4},{4,6},{6,0},{1,3},{3,5},{5,7},{7,1},{8,10},{10,12},{12... | collective-permute-start | bytes 1572872 | tf_op jit(solution)/shard_map/ppermute | solution.py:356
  113.0 33.0 %collective-permute-start.16 = (bf16[128,2048]{1,0:T(8,128)(2,1)S(1)}, bf16[128,2048]{1,0:T(8,128)(2,1)S(1)}, u32[]{:S(2)}, u32[]{:S(2)}) collective-permute-start(bf16[128,2048]{1,0:T(8,128)(2,1)S(1)} %slice.37), channel_id=1, source_target_pairs={{0,6},{2,0},{4,2},{6,4},{1,7},{3,1},{5,3},{7,5},{8,14},{10,8},{12,... | collective-permute-start | bytes 1572872 | tf_op jit(solution)/shard_map/ppermute | solution.py:357
  117.6 20.3 %collective-permute-start.11 = (bf16[512,256]{1,0:T(8,128)(2,1)S(1)}, bf16[512,256]{1,0:T(8,128)(2,1)S(1)}, u32[]{:S(2)}, u32[]{:S(2)}) collective-permute-start(bf16[512,256]{1,0:T(8,128)(2,1)S(1)} %collective-permute-done.2.k1_ref), channel_id=1, source_target_pairs={{0,8},{8,16},{16,24},{24,32},{32,40},{40,48},{48,56},{56,64},{64,7... | collective-permute-start | bytes 786440 | tf_op jit(solution)/shard_map/ppermute | solution.py:380
  119.5 18.4 %collective-permute-start.12 = (bf16[512,256]{1,0:T(8,128)(2,1)S(1)}, bf16[512,256]{1,0:T(8,128)(2,1)S(1)}, u32[]{:S(2)}, u32[]{:S(2)}) collective-permute-start(bf16[512,256]{1,0:T(8,128)(2,1)S(1)} %collective-permute-done.3.v1_ref), channel_id=1, source_target_pairs={{0,8},{8,16},{16,24},{24,32},{32,40},{40,48},{48,56},{56,64},{64,7... | collective-permute-start | bytes 786440 | tf_op jit(solution)/shard_map/ppermute | solution.py:381
  142.6 8.9 %all-to-all-start.1 = ((bf16[4,128,256]{2,1,0:T(8,128)(2,1)}), bf16[4,128,256]{2,1,0:T(8,128)(2,1)S(1)}, u32[]{:S(2)}, u32[]{:S(2)}) async-start(bf16[4,128,256]{2,1,0:T(8,128)(2,1)} %bitcast.9), calls=%async_computation.1 | async-start | bytes 524288 | tf_op jit(solution)/shard_map/all_to_all | solution.py:417
  146.0 17.8 %copy-start.5 = (f32[2048]{0:T(1024)S(1)}, f32[2048]{0:T(1024)}, u32[]{:S(2)}) copy-start(f32[2048]{0:T(1024)} %param.13) | copy-start | bytes 24580
  154.3 9.5 %collective-permute-start.17 = (bf16[64,2048]{1,0:T(8,128)(2,1)S(1)}, bf16[64,2048]{1,0:T(8,128)(2,1)S(1)}, u32[]{:S(2)}, u32[]{:S(2)}) collective-permute-start(bf16[64,2048]{1,0:T(8,128)(2,1)S(1)} %get-tuple-element.32), channel_id=1, source_target_pairs={{0,1},{1,0},{2,3},{3,2},{4,5},{5,4},{6,7},{7,6},{8,9},{9,8},{10,11... | collective-permute-start | bytes 786440 | tf_op jit(solution)/shard_map/ppermute | solution.py:427

commit v4 on v3

--- a/solution.py
+++ b/solution.py
@@ -1,3 +1,5 @@
+import functools
+
 import jax
 import jax.numpy as jnp
 import numpy as np
@@ -81,14 +83,22 @@
 
     lax.fori_loop(0, rows // 64, step, 0)
     query = jnp.dot(normed_ref[...], weight_ref[...], preferred_element_type=F32)
-    cos, sin = spread(turn_ref, slice(2 * rows, 3 * rows))
+    cos, sin = spread(turn_ref, slice(rows, 2 * rows))
     query = rotated(query, cos, sin).astype(BF16) * 0.125
     query_ref[...] = permuted(to_residue(rows), query)
 
 
+def project(normed, weight_ref, cos, sin, key_ref, value_ref):
+    rows, width = key_ref.shape
+    perm = to_residue(rows)
+    key = jnp.dot(normed, weight_ref[:, :width], preferred_element_type=F32)
+    key_ref[...] = permuted(perm, rotated(key, cos, sin).astype(BF16))
+    value = jnp.dot(normed, weight_ref[:, width:], preferred_element_type=F32).astype(BF16)
+    value_ref[...] = permuted(perm, value)
+
+
 def key_value_kernel(place_ref, normed_ref, mine_ref, below_ref, above_ref, turn_ref, key_ref, value_ref, weight_ref):
     rows = normed_ref.shape[0]
-    width = key_ref.shape[1]
     low = place_ref[1]
     slabs = []
     for k in range(4):
@@ -98,42 +108,11 @@
         slabs.append((2 * (k + 2) + 1 - low, above_ref, k))
     for place, ref, k in slabs:
         weight_ref[pl.ds(pl.multiple_of(place * 256, 256), 256), :] = ref[k]
-    normed = normed_ref[...]
-    perm = to_residue(rows)
-    cos, sin = spread(turn_ref, slice(2 * rows, 3 * rows))
-    key = jnp.dot(normed, weight_ref[:, :width], preferred_element_type=F32)
-    key = rotated(key, cos, sin).astype(BF16)
-    key_ref[...] = permuted(perm, key)
-    value = jnp.dot(normed, weight_ref[:, width:], preferred_element_type=F32).astype(BF16)
-    value_ref[...] = permuted(perm, value)
-
-
-def far_key_value_kernel(place_ref, mine_ref, other_ref, weight_ref, turn_ref, k4_ref, v4_ref, k3_ref, v3_ref, cos_ref, sin_ref, key_ref, value_ref):
-    rows, width = k4_ref.shape
-    x, core = place_ref[2], place_ref[3]
-    piece = rows // 8
-    for n in range(2):
-        part = slice(n * rows, (n + 1) * rows)
-        cos_ref[part, :], sin_ref[part, :] = spread(turn_ref, part)
-    lanes = lax.broadcasted_iota(jnp.int32, (1, rows), 1)
-    column = lanes & (piece - 1)
-    for half, (ref, c) in enumerate(((mine_ref, core), (other_ref, 1 - core))):
-        both = jnp.dot(ref[...], weight_ref[...], preferred_element_type=F32)
-        for n, hop in enumerate(HOPS):
-            at = (lax.rem(x + hop, 4) * 2 + c) * piece
-            lies = (half * 4 + n) * piece
-            column = column + jnp.where((lanes >= lies) & (lanes < lies + piece), at, 0)
-            for far in range(2):
-                source = slice((2 * n + far) * piece, (2 * n + far + 1) * piece)
-                table = pl.ds(pl.multiple_of(far * rows + at, piece), piece)
-                key = rotated(both[source, :width], cos_ref[table, :], sin_ref[table, :])
-                key_ref[far, lies : lies + piece, :] = key.astype(BF16)
-                value_ref[far, lies : lies + piece, :] = both[source, width:].astype(BF16)
-    perm = to_residue(rows, jnp.broadcast_to(column, (rows, rows)))
-    k4_ref[...] = permuted(perm, key_ref[0])
-    v4_ref[...] = permuted(perm, value_ref[0])
-    k3_ref[...] = permuted(perm, key_ref[1])
-    v3_ref[...] = permuted(perm, value_ref[1])
+    project(normed_ref[...], weight_ref, *spread(turn_ref, slice(rows, 2 * rows)), key_ref, value_ref)
+
+
+def far_key_value_kernel(normed_ref, weight_ref, turn_ref, key_ref, value_ref):
+    project(normed_ref[...], weight_ref, *spread(turn_ref, slice(0, normed_ref.shape[0])), key_ref, value_ref)
 
 
 def stack_heads(q):
@@ -161,7 +140,7 @@
     return jnp.where(ok, 0.0, LOW).astype(F32)
 
 
-def near_kernel(place_ref, q_ref, k0_ref, v0_ref, k1_ref, v1_ref, k3_ref, v3_ref, k4_ref, v4_ref, max_ref, sum_ref, acc_ref, s_ref, p_ref, bias_ref, count_ref, stat_ref, tail_ref):
+def near_kernel(place_ref, q_ref, k0_ref, v0_ref, k1_ref, v1_ref, max_ref, sum_ref, acc_ref, s_ref, p_ref, bias_ref, count_ref, stat_ref, tail_ref):
     cls = pl.program_id(0)
     block = place_ref[0]
     keys, width = k0_ref.shape
@@ -175,8 +154,6 @@
         pick = (i == (j >> 3) * 32 + 24 + (j & 7)).astype(BF16)
         tail_ref[0] = permuted(pick, k1_ref[...])
         tail_ref[1] = permuted(pick, v1_ref[...])
-        bias_ref[:, keys + 256 : keys + 384] = far_bias(block, 3)
-        bias_ref[:, keys + 384 : keys + 512] = far_bias(block, 4)
 
     i = lax.broadcasted_iota(jnp.int32, (128, 1), 0)
     qn = (i & 31) * 16 + (i >> 5) * 4 + cls
@@ -199,12 +176,12 @@
     k = lax.broadcasted_iota(jnp.int32, (1, 128), 1)
     o = qn - ((24 + (k & 7)) * 16 + ((k >> 3) & 3) * 4 + (k >> 5)) + keys
     ok = (o <= SPAN) & ((k >> 5) != cls) & seen
-    bias_ref[:, keys + 128 : keys + 256] = jnp.where(ok, 0.0, LOW).astype(F32)
-
-    q4 = stack_heads(q_ref[...])
-    s_ref[:, :keys] = lax.dot_general(q4, k0_ref[...], NT, preferred_element_type=F32)
-    rest = jnp.concatenate([k1_ref[mine, :], tail_ref[0], k3_ref[mine, :], k4_ref[mine, :]], axis=0)
-    s_ref[:, keys:] = lax.dot_general(q4, rest, NT, preferred_element_type=F32)
+    bias_ref[:, keys + 128 :] = jnp.where(ok, 0.0, LOW).astype(F32)
+
+    stacked = stack_heads(q_ref[...])
+    s_ref[:, :keys] = lax.dot_general(stacked, k0_ref[...], NT, preferred_element_type=F32)
+    rest = jnp.concatenate([k1_ref[mine, :], tail_ref[0]], axis=0)
+    s_ref[:, keys:] = lax.dot_general(stacked, rest, NT, preferred_element_type=F32)
     step = 32
     for r in range(0, heads * 128, step):
         mask = slice(r % 128, r % 128 + step)
@@ -216,38 +193,48 @@
         stat_ref[1, r : r + step, :] = jnp.broadcast_to(jnp.sum(p, axis=1, keepdims=True), (step, width))
         p_ref[r : r + step, :] = p.astype(BF16)
     pv = jnp.dot(p_ref[:, :keys], v0_ref[...], preferred_element_type=F32)
-    rest = jnp.concatenate([v1_ref[mine, :], tail_ref[1], v3_ref[mine, :], v4_ref[mine, :]], axis=0)
+    rest = jnp.concatenate([v1_ref[mine, :], tail_ref[1]], axis=0)
     pv = pv + jnp.dot(p_ref[:, keys:], rest, preferred_element_type=F32)
     max_ref[...] = own_heads(stat_ref[0])
     sum_ref[...] = own_heads(stat_ref[1])
     acc_ref[...] = own_heads(pv)
 
 
-def last_kernel(place_ref, q_ref, max_ref, sum_ref, acc_ref, k_ref, v_ref, out_ref, log_ref, att_ref, s_ref, p_ref, stat_ref):
+def far_kernel(backs, last, place_ref, q_ref, max_ref, sum_ref, acc_ref, *refs):
     width = q_ref.shape[1]
     heads = width // HEAD_DIM
-    bias = far_bias(place_ref[0], 2)
-    s_ref[...] = lax.dot_general(stack_heads(q_ref[...]), k_ref[...], NT, preferred_element_type=F32)
+    count = len(backs)
+    sources, outs = refs[: 2 * count], refs[2 * count :]
+    p_ref, stat_ref = outs[-2:]
+    bias = jnp.concatenate([far_bias(place_ref[0], back) for back in backs], axis=1)
+    key = jnp.concatenate([ref[...] for ref in sources[0::2]], axis=0)
+    value = jnp.concatenate([ref[...] for ref in sources[1::2]], axis=0)
+    scores = lax.dot_general(stack_heads(q_ref[...]), key, NT, preferred_element_type=F32)
     for h in range(heads):
         part = slice(h * 128, (h + 1) * 128)
-        s = s_ref[part, :] + bias
+        s = scores[part] + bias
         m = jnp.maximum(jnp.max(s, axis=1, keepdims=True), max_ref[:, h * HEAD_DIM : h * HEAD_DIM + 1])
         p = jnp.exp(s - m)
         p_ref[part, :] = p.astype(BF16)
         stat_ref[0, part, :] = jnp.broadcast_to(m, (128, width))
         stat_ref[1, part, :] = jnp.broadcast_to(jnp.sum(p, axis=1, keepdims=True), (128, width))
-    pv = jnp.dot(p_ref[...], v_ref[...], preferred_element_type=F32)
+    pv = jnp.dot(p_ref[...], value, preferred_element_type=F32)
     m = own_heads(stat_ref[0])
     alpha = jnp.exp(max_ref[...] - m)
     total = sum_ref[...] * alpha + own_heads(stat_ref[1])
     acc = acc_ref[...] * alpha + own_heads(pv)
-    cls = pl.program_id(0)
-    att_ref[pl.ds(pl.multiple_of(cls * 128, 128), 128), :] = (acc / total).astype(BF16)
-    log_ref[...] = m + jnp.log(total)
-
-    @pl.when(cls == pl.num_programs(0) - 1)
-    def _():
-        out_ref[...] = permuted(to_natural(att_ref.shape[0]), att_ref[...])
+    if last:
+        cls = pl.program_id(0)
+        out_ref, log_ref, att_ref = outs[:3]
+        att_ref[pl.ds(pl.multiple_of(cls * 128, 128), 128), :] = (acc / total).astype(BF16)
+        log_ref[...] = m + jnp.log(total)
+
+        @pl.when(cls == pl.num_programs(0) - 1)
+        def _():
+            out_ref[...] = permuted(to_natural(att_ref.shape[0]), att_ref[...])
+    else:
+        for ref, value in zip(outs[:3], (m, total, acc)):
+            ref[...] = value
 
 
 def log_kernel(lw_ref, log_ref):
@@ -310,10 +297,16 @@
     )(*args)
 
 
+def spread_to(value, axis, count):
+    copies = jnp.broadcast_to(value[None], (count,) + value.shape)
+    return lax.all_to_all(copies, axis, split_axis=0, concat_axis=0, tiled=True)
+
+
 def layer(hidden_in, pre_gain, query_proj, key_proj, value_proj, out_proj, post_gain):
     rows, depth = hidden_in.shape
     width = query_proj.shape[1]
     heads = width // HEAD_DIM
+    piece = rows // 8
     sp, x, core = lax.axis_index(SP), lax.axis_index("x"), lax.axis_index("c")
     place = jnp.stack([sp, lax.axis_index("zl"), x, core]).astype(jnp.int32)
     member = (x * 2 + core)[None].astype(jnp.int32)
@@ -321,13 +314,10 @@
     row = (rows, width)
 
     shard = jnp.concatenate([key_proj, value_proj], axis=1)
-    copies = jnp.broadcast_to(shard[None], (32,) + shard.shape)
-    mine = lax.all_to_all(copies, ("zh", "y"), split_axis=0, concat_axis=0, tiled=True)
-    mine = mine.reshape(4, 256, 2 * width)
+    mine = spread_to(shard, ("zh", "y"), 32).reshape(4, 256, 2 * width)
     below = lax.ppermute(mine[:2], Z, ring(8, 1))
     above = lax.ppermute(mine[2:], Z, ring(8, -1))
 
-    piece = rows // 8
     (eighth,) = kernel_call(
         slice_kernel,
         [((piece, depth), BF16)],
@@ -342,24 +332,17 @@
         ),
     )
     fourth = lax.ppermute(eighth, SP, ring(64, 4))
-    third = lax.ppermute(fourth, SP, ring(64, -1))
-    both = jnp.concatenate([fourth, third], axis=0)
-    left = lax.ppermute(both, "x", ring(4, 1))
-    right = lax.ppermute(both, "x", ring(4, -1))
-    across4 = lax.ppermute(left[:piece], "x", ring(4, 1))
-    across3 = lax.ppermute(right[piece:], "x", ring(4, -1))
-    far_rows = jnp.concatenate([both, left, right, across4, across3], axis=0)
-    far_others = lax.ppermute(far_rows, "c", ring(2, 1))
+    far_rows = spread_to(fourth, TP, 8).reshape(rows, depth)
 
     before = lax.ppermute(out_proj, "x", ring(4, 1))
     after = lax.ppermute(out_proj, "x", ring(4, -1))
     upper = lax.ppermute(before[: width // 2], "x", ring(4, 1))
     lower = lax.ppermute(after[width // 2 :], "x", ring(4, -1))
 
-    half = HEAD_DIM // 2
-    frequency = ROPE_BASE ** (-(jnp.arange(half, dtype=F32) * 2.0 / HEAD_DIM))
+    quarter = HEAD_DIM // 2
+    frequency = ROPE_BASE ** (-(jnp.arange(quarter, dtype=F32) * 2.0 / HEAD_DIM))
     local = jnp.arange(rows, dtype=jnp.int32)
-    positions = jnp.concatenate([(sp - 4) * rows + local, (sp - 3) * rows + local, sp * rows + local]).astype(F32)
+    positions = jnp.concatenate([(sp - 4) * rows + local, sp * rows + local]).astype(F32)
     angles = positions[None, :] * frequency[:, None]
     turns = jnp.stack([jnp.cos(angles), jnp.sin(angles)])
 
@@ -373,20 +356,13 @@
         4 * rows * depth * width,
         20,
     )
-
     forward = [(i, i + 1) for i in range(63)]
-    key1 = lax.ppermute(key, SP, forward)
-    value1 = lax.ppermute(value, SP, forward)
-    key2 = lax.ppermute(key1, SP, forward)
-    value2 = lax.ppermute(value1, SP, forward)
-
-    key4, value4, key3, value3 = kernel_call(
-        far_key_value_kernel,
-        [(row, BF16)] * 4,
-        (place, far_rows, far_others, weights, turns),
-        8 * rows * depth * width,
-        24,
-        [((2 * rows, width), F32), ((2 * rows, width), F32), ((2,) + row, BF16), ((2,) + row, BF16)],
+    keys, values = [key], [value]
+    for _ in range(1, 4):
+        keys.append(lax.ppermute(keys[-1], SP, forward))
+        values.append(lax.ppermute(values[-1], SP, forward))
+    key4, value4 = kernel_call(
+        far_key_value_kernel, [(row, BF16)] * 2, (far_rows, weights, turns), 4 * rows * depth * width, 16
     )
 
     whole = pl.BlockSpec(row, lambda c: (0, 0))
@@ -394,25 +370,29 @@
     state = kernel_call(
         near_kernel,
         [(row, F32)] * 3,
-        (place, query, key, value, key1, value1, key3, value3, key4, value4),
+        (place, query, keys[0], values[0], keys[1], values[1]),
         16 * rows * rows * width,
-        24,
-        [((512, 1024), F32), ((512, 1024), BF16), ((128, 1024), F32), ((128, 640), F32), ((2, 512, width), F32), ((2, 128, width), BF16)],
+        20,
+        [((512, 768), F32), ((512, 768), BF16), ((128, 768), F32), ((128, 640), F32), ((2, 512, width), F32), ((2, 128, width), BF16)],
         grid=(rows // 128,),
-        in_specs=[SMEM, part] + [whole] * 8,
+        in_specs=[SMEM, part] + [whole] * 4,
         out_specs=(part,) * 3,
     )
-    attended, logs = kernel_call(
-        last_kernel,
-        [(row, BF16), (row, F32)],
-        (place, query, *state, key2, value2),
-        4 * rows * 512 * width,
-        16,
-        [(row, BF16), ((512, 128), F32), ((512, 128), BF16), ((2, 512, width), F32)],
-        grid=(rows // 128,),
-        in_specs=[SMEM] + [part] * 6,
-        out_specs=(whole, part),
-    )
+    sources = {2: (keys[2], values[2]), 3: (keys[3], values[3]), 4: (key4, value4)}
+    for backs in ((2, 4), (3,)):
+        last = backs == (3,)
+        state = kernel_call(
+            functools.partial(far_kernel, backs, last),
+            [(row, BF16), (row, F32)] if last else [(row, F32)] * 3,
+            (place, query, *state, *(array for back in backs for array in sources[back])),
+            4 * rows * 512 * width * len(backs),
+            16,
+            ([(row, BF16)] if last else []) + [((512, 128 * len(backs)), BF16), ((2, 512, width), F32)],
+            grid=(rows // 128,),
+            in_specs=[SMEM] + [part] * (4 + 2 * len(backs)),
+            out_specs=(whole, part) if last else (part,) * 3,
+        )
+    attended, logs = state
 
     arrived = lax.all_to_all(attended.reshape(4, rows // 4, width), "x", split_axis=0, concat_axis=0, tiled=True)
     (log_weight,) = kernel_call(log_kernel, [((heads, rows), F32)], (logs,), 6 * rows * rows * width, 12)

time: 166 us -> 173 us (1.042)
  waiting for transfers between devices: 37.9 us -> 46.4 us
  starting transfers between devices: 85.3 us -> 82.4 us
  Pallas kernels: 29 us -> 31.8 us
    ppermute x1, waiting for transfers between devices: 16.1 us -> 32.2 us  [layer(): fourth = lax.ppermute(eighth, SP, ring(64, 4))]
    all_to_all x1 -> x2, starting transfers between devices: 7.17 us -> 22 us  [spread_to(): return lax.all_to_all(copies, axis, split_axis=0, concat_axis=0, tiled=True)]
    ppermute x10 -> x6, starting transfers between devices: 37.9 us -> 25.4 us  [the longest x3 16.1 us: layer(): keys.append(lax.ppermute(keys[-1], SP, forward))]
    ppermute x10 -> x6, waiting for transfers between devices: 10 us -> 0.93 us  [the longest x3 0.72 us: layer(): values.append(lax.ppermute(values[-1], SP, forward))]
    unnamed x20 -> x22, local copies, waits for them, and re-layouts: 5.44 us -> 2.17 us
    ppermute x1, starting transfers between devices: 8.2 us -> 4.97 us  [layer(): taken = lax.ppermute(give, 'c', ring(2, 1))]
    ppermute x1, waiting for transfers between devices: 2.55 us -> 5.48 us  [layer(): below = lax.ppermute(mine[:2], Z, ring(8, 1))]
    all_to_all x1 -> x2, waiting for transfers between devices: 2.93 us -> 0.01 us  [spread_to(): return lax.all_to_all(copies, axis, split_axis=0, concat_axis=0, tiled=True)]
  transfers between devices with their start and end apart: 20 -> 17, of which waited for: 9 -> 7; matrix products, arithmetic and copies ran while one was open for 5% -> 3% of each run, Pallas kernels for 15% -> 16%
where the time goes in v4:
time: 173 us; the launch traced here: 172 us
  starting transfers between devices  82.4 us (48%)
  waiting for transfers between devices  46.4 us (27%)
  Pallas kernels  31.8 us (18%)
  local copies, waits for them, and re-layouts  8.79 us (5%)
    ppermute x1, waiting for transfers between devices, layer(): fourth = lax.ppermute(eighth, SP, ring(64, 4))  32.2 us
    pallas_call x10, Pallas kernels, kernel_call(): pl.pallas_call(body, out_shape=tuple((jax.ShapeDtypeStruct(s, t) for s, t...  31.8 us
    all_to_all x2, starting transfers between devices, spread_to(): return lax.all_to_all(copies, axis, split_axis=0, concat_axis=0, tiled=True)  22 us
    ppermute x3, starting transfers between devices, layer(): keys.append(lax.ppermute(keys[-1], SP, forward))  16.1 us
    ppermute x3, starting transfers between devices, layer(): values.append(lax.ppermute(values[-1], SP, forward))  9.33 us
    ppermute x1, starting transfers between devices, layer(): fourth = lax.ppermute(eighth, SP, ring(64, 4))  7.05 us
    ppermute x1, waiting for transfers between devices, layer(): below = lax.ppermute(mine[:2], Z, ring(8, 1))  5.48 us
    all_to_all x1, waiting for transfers between devices, layer(): lax.all_to_all(attended.reshape(4, rows // 4, width), 'x', split_axis=0,...  5.46 us
  transfers between devices with their start and end apart: 17, of which 7 were waited for; matrix products, arithmetic and copies ran while one was open for 3% of the time, Pallas kernels for 16%

profile of v4, /device:TPU:1, one launch (start us, length us, event | category | flops | bytes accessed | tf_op | source)
XLA Modules:
  0.0 171.9 jit_solution(16132893853549834936)
XLA Ops:
  0.6 0.0 copy-start.5
  0.6 0.0 copy-start
  0.7 0.9 pad_maximum_fusion.1
  1.5 1.1 broadcast_in_dim.11
  2.6 16.5 %all-to-all-start = ((bf16[32,32,512]{2,1,0:T(8,128)(2,1)}), bf16[32,32,512]{2,1,0:T(8,128)(2,1)S(1)}, u32[]{:S(2)}, u32[]{:S(2)}) async-start(bf16[32,32,512]{2,1,0:T(8,128)(2,1)} %broadcast_in_dim.11), calls=%async_computation | async-start | bytes 2097152 | tf_op jit(solution)/shard_map/all_to_all | solution.py:302
  19.1 0.0 copy-done.5
  19.2 0.0 copy-done
  19.2 0.2 shard_map.89
  19.3 7.0 %collective-permute-start.6 = (bf16[64,2048]{1,0:T(8,128)(2,1)S(1)}, bf16[64,2048]{1,0:T(8,128)(2,1)S(1)}, u32[]{:S(2)}, u32[]{:S(2)}) collective-permute-start(bf16[64,2048]{1,0:T(8,128)(2,1)S(1)} %shard_map.89), channel_id=1, source_target_pairs={{0,32},{8,40},{16,48},{24,56},{32,64},{40,72},{48,80},{56,88},{64,... | collective-permute-start | bytes 786440 | tf_op jit(solution)/shard_map/ppermute | solution.py:334
  26.4 32.2 %collective-permute-done.6 = bf16[64,2048]{1,0:T(8,128)(2,1)S(1)} collective-permute-done((bf16[64,2048]{1,0:T(8,128)(2,1)S(1)}, bf16[64,2048]{1,0:T(8,128)(2,1)S(1)}, u32[]{:S(2)}, u32[]{:S(2)}) %collective-permute-start.6) | collective-permute-done | bytes 262176 | tf_op jit(solution)/shard_map/ppermute | solution.py:334
  58.5 0.0 all-to-all-done
  58.5 1.6 broadcast_in_dim.26
  60.1 5.5 %all-to-all-start.1 = ((bf16[8,64,2048]{2,1,0:T(8,128)(2,1)}), bf16[8,64,2048]{2,1,0:T(8,128)(2,1)}, u32[]{:S(2)}, u32[]{:S(2)}) async-start(bf16[8,64,2048]{2,1,0:T(8,128)(2,1)} %broadcast_in_dim.26), calls=%async_computation.1 | async-start | bytes 4194304 | tf_op jit(solution)/shard_map/all_to_all | solution.py:302
  65.7 3.3 %collective-permute-start.9 = (bf16[256,2048]{1,0:T(8,128)(2,1)}, bf16[256,2048]{1,0:T(8,128)(2,1)}, u32[]{:S(2)}, u32[]{:S(2)}) collective-permute-start(bf16[256,2048]{1,0:T(8,128)(2,1)} %own_ref.1), channel_id=1, source_target_pairs={{0,2},{2,4},{4,6},{6,0},{1,3},{3,5},{5,7},{7,1},{8,10},{10,12},{12... | collective-permute-start | bytes 3145736 | tf_op jit(solution)/shard_map/ppermute | solution.py:337
  68.9 3.2 %collective-permute-start.10 = (bf16[256,2048]{1,0:T(8,128)(2,1)}, bf16[256,2048]{1,0:T(8,128)(2,1)}, u32[]{:S(2)}, u32[]{:S(2)}) collective-permute-start(bf16[256,2048]{1,0:T(8,128)(2,1)} %own_ref.1), channel_id=1, source_target_pairs={{0,6},{2,0},{4,2},{6,4},{1,7},{3,1},{5,3},{7,5},{8,14},{10,8},{12,... | collective-permute-start | bytes 3145736 | tf_op jit(solution)/shard_map/ppermute | solution.py:338
  72.2 0.0 copy-start.4
  72.2 0.1 fusion
  72.3 2.1 %collective-permute-start = (bf16[2,256,512]{2,1,0:T(8,128)(2,1)S(1)}, bf16[2,256,512]{2,1,0:T(8,128)(2,1)S(1)}, u32[]{:S(2)}, u32[]{:S(2)}) collective-permute-start(bf16[2,256,512]{2,1,0:T(8,128)(2,1)S(1)} %bitcast.17), channel_id=1, source_target_pairs={{0,64},{64,128},{128,192},{192,256},{256,320},{320,384},{384,448},... | collective-permute-start | bytes 1572872 | tf_op jit(solution)/shard_map/ppermute | solution.py:318
  74.4 4.6 %collective-permute-start.1 = (bf16[2,256,512]{2,1,0:T(8,128)(2,1)S(1)}, bf16[2,256,512]{2,1,0:T(8,128)(2,1)S(1)}, u32[]{:S(2)}, u32[]{:S(2)}) collective-permute-start(bf16[2,256,512]{2,1,0:T(8,128)(2,1)S(1)} %bitcast.16), channel_id=1, source_target_pairs={{0,448},{64,0},{128,64},{192,128},{256,192},{320,256},{384,320},{4... | collective-permute-start | bytes 1572872 | tf_op jit(solution)/shard_map/ppermute | solution.py:319
  79.0 0.5 multiply_cosine_fusion
  79.5 2.7 %shard_map.86 = (bf16[512,2048]{1,0:T(8,128)(2,1)S(1)}, bf16[512,256]{1,0:T(8,128)(2,1)S(1)}) custom-call(bf16[512,2048]{1,0:T(8,128)(2,1)S(1)} %copy-done, f32[1,2048]{1,0:T(1,128)S(1)} %bitcast.14, bf16[2048,256]{1,0:T(8,128)(2,1)S(1)} %copy-done.4, f32[2,32,1024]{2,1,0:T(8,128)S(1)} %pad_maximum_fusion.turn_ref), custom_call_target="tpu_custom_call" | custom-call | flops 536870912 | bytes 3416064 | tf_op jit(solution)/shard_map/pallas_call | solution.py:291
  82.2 0.0 copy-start.2
  82.2 0.7 copy-done.2
  82.9 0.1 pad_add_fusion.place_ref
  83.0 5.5 %collective-permute-done.below_ref = bf16[2,256,512]{2,1,0:T(8,128)(2,1)S(1)} collective-permute-done((bf16[2,256,512]{2,1,0:T(8,128)(2,1)S(1)}, bf16[2,256,512]{2,1,0:T(8,128)(2,1)S(1)}, u32[]{:S(2)}, u32[]{:S(2)}) %collective-permute-start) | collective-permute-done | bytes 524320 | tf_op jit(solution)/shard_map/ppermute | solution.py:318
  88.5 0.8 collective-permute-done.1.above_ref
  89.3 3.9 %shard_map.87 = (bf16[512,256]{1,0:T(8,128)(2,1)S(1)}, bf16[512,256]{1,0:T(8,128)(2,1)S(1)}, bf16[2048,512]{1,0:T(8,128)(2,1)S(1)}) custom-call(s32[4]{0:T(128)S(1)} %pad_add_fusion.place_ref, bf16[512,2048]{1,0:T(8,128)(2,1)S(1)} %get-tuple-element.20.normed_ref, bf16[4,256,512]{2,1,0:T(8,128)(2,1)S(1)} %bitcast.12, ...), custom_call_target="tpu_custom_call" | custom-call | flops 1073741824 | bytes 4456464 | tf_op jit(solution)/shard_map/pallas_call | solution.py:291
  93.2 5.2 %collective-permute-start.2 = (bf16[512,256]{1,0:T(8,128)(2,1)S(1)}, bf16[512,256]{1,0:T(8,128)(2,1)S(1)}, u32[]{:S(2)}, u32[]{:S(2)}) collective-permute-start(bf16[512,256]{1,0:T(8,128)(2,1)S(1)} %get-tuple-element.21.k0_ref), channel_id=1, source_target_pairs={{0,8},{8,16},{16,24},{24,32},{32,40},{40,48},{48,56},{56,64},{64,7... | collective-permute-start | bytes 786440 | tf_op jit(solution)/shard_map/ppermute | solution.py:362
  98.4 0.7 copy-done.7
  99.1 2.2 %collective-permute-start.3 = (bf16[512,256]{1,0:T(8,128)(2,1)S(1)}, bf16[512,256]{1,0:T(8,128)(2,1)S(1)}, u32[]{:S(2)}, u32[]{:S(2)}) collective-permute-start(bf16[512,256]{1,0:T(8,128)(2,1)S(1)} %get-tuple-element.22.v0_ref), channel_id=1, source_target_pairs={{0,8},{8,16},{16,24},{24,32},{32,40},{40,48},{48,56},{56,64},{64,7... | collective-permute-start | bytes 786440 | tf_op jit(solution)/shard_map/ppermute | solution.py:363
  101.3 0.7 copy-done.9
  102.0 0.2 collective-permute-done.2.k1_ref
  102.3 4.9 %collective-permute-start.4 = (bf16[512,256]{1,0:T(8,128)(2,1)S(1)}, bf16[512,256]{1,0:T(8,128)(2,1)}, u32[]{:S(2)}, u32[]{:S(2)}) collective-permute-start(bf16[512,256]{1,0:T(8,128)(2,1)S(1)} %collective-permute-done.2.k1_ref), channel_id=1, source_target_pairs={{0,8},{8,16},{16,24},{24,32},{32,40},{40,48},{48,56},{56,64},{64,7... | collective-permute-start | bytes 786440 | tf_op jit(solution)/shard_map/ppermute | solution.py:362
  107.2 0.7 collective-permute-done.3.v1_ref
  107.9 4.9 %collective-permute-start.5 = (bf16[512,256]{1,0:T(8,128)(2,1)S(1)}, bf16[512,256]{1,0:T(8,128)(2,1)}, u32[]{:S(2)}, u32[]{:S(2)}) collective-permute-start(bf16[512,256]{1,0:T(8,128)(2,1)S(1)} %collective-permute-done.3.v1_ref), channel_id=1, source_target_pairs={{0,8},{8,16},{16,24},{24,32},{32,40},{40,48},{48,56},{56,64},{64,7... | collective-permute-start | bytes 786440 | tf_op jit(solution)/shard_map/ppermute | solution.py:363
  112.8 1.6 collective-permute-done.9.before_ref
  114.3 1.9 %slice.26 = bf16[128,2048]{1,0:T(8,128)(2,1)} slice(bf16[256,2048]{1,0:T(8,128)(2,1)} %collective-permute-done.9.before_ref), slice={[0:128], [0:2048]} | slice | bytes 1048576 | tf_op jit(solution)/shard_map/slice | solution.py:339
  116.3 1.9 %collective-permute-start.11 = (bf16[128,2048]{1,0:T(8,128)(2,1)}, bf16[128,2048]{1,0:T(8,128)(2,1)}, u32[]{:S(2)}, u32[]{:S(2)}) collective-permute-start(bf16[128,2048]{1,0:T(8,128)(2,1)} %slice.26), channel_id=1, source_target_pairs={{0,2},{2,4},{4,6},{6,0},{1,3},{3,5},{5,7},{7,1},{8,10},{10,12},{12... | collective-permute-start | bytes 1572872 | tf_op jit(solution)/shard_map/ppermute | solution.py:339
  118.2 0.0 collective-permute-done.10.after_ref
  118.2 1.9 %slice.27 = bf16[128,2048]{1,0:T(8,128)(2,1)} slice(bf16[256,2048]{1,0:T(8,128)(2,1)} %collective-permute-done.10.after_ref), slice={[128:256], [0:2048]} | slice | bytes 1048576 | tf_op jit(solution)/shard_map/slice | solution.py:340
  120.1 4.6 %collective-permute-start.12 = (bf16[128,2048]{1,0:T(8,128)(2,1)}, bf16[128,2048]{1,0:T(8,128)(2,1)}, u32[]{:S(2)}, u32[]{:S(2)}) collective-permute-start(bf16[128,2048]{1,0:T(8,128)(2,1)} %slice.27), channel_id=1, source_target_pairs={{0,6},{2,0},{4,2},{6,4},{1,7},{3,1},{5,3},{7,5},{8,14},{10,8},{12,... | collective-permute-start | bytes 1572872 | tf_op jit(solution)/shard_map/ppermute | solution.py:340
  124.7 0.0 collective-permute-done.4.refs_0_
  124.7 5.9 %collective-permute-start.7 = (bf16[512,256]{1,0:T(8,128)(2,1)}, bf16[512,256]{1,0:T(8,128)(2,1)}, u32[]{:S(2)}, u32[]{:S(2)}) collective-permute-start(bf16[512,256]{1,0:T(8,128)(2,1)} %collective-permute-done.4.refs_0_), channel_id=1, source_target_pairs={{0,8},{8,16},{16,24},{24,32},{32,40},{40,48},{48,56},{56,64},{64,7... | collective-permute-start | bytes 786440 | tf_op jit(solution)/shard_map/ppermute | solution.py:362
  130.6 0.0 collective-permute-done.5.refs_1_
  130.6 2.2 %collective-permute-start.8 = (bf16[512,256]{1,0:T(8,128)(2,1)}, bf16[512,256]{1,0:T(8,128)(2,1)}, u32[]{:S(2)}, u32[]{:S(2)}) collective-permute-start(bf16[512,256]{1,0:T(8,128)(2,1)} %collective-permute-done.5.refs_1_), channel_id=1, source_target_pairs={{0,8},{8,16},{16,24},{24,32},{32,40},{40,48},{48,56},{56,64},{64,7... | collective-permute-start | bytes 786440 | tf_op jit(solution)/shard_map/ppermute | solution.py:363
  132.9 0.0 all-to-all-done.1
  132.9 4.8 %shard_map.90 = (bf16[512,256]{1,0:T(8,128)(2,1)S(1)}, bf16[512,256]{1,0:T(8,128)(2,1)S(1)}) custom-call(bf16[512,2048]{1,0:T(8,128)(2,1)} %bitcast.9.normed_ref, bf16[2048,512]{1,0:T(8,128)(2,1)S(1)} %get-tuple-element.26.weight_ref, f32[2,32,1024]{2,1,0:T(8,128)S(1)} %pad_maximum_fusion.turn_ref), custom_call_target="tpu_custom_call" | custom-call | flops 1073741824 | bytes 4456448 | tf_op jit(solution)/shard_map/pallas_call | solution.py:291
  137.8 5.9 %shard_map.88 = (f32[512,256]{1,0:T(8,128)S(1)}, f32[512,256]{1,0:T(8,128)S(1)}, f32[512,256]{1,0:T(8,128)S(1)}) custom-call(s32[4]{0:T(128)S(1)} %pad_add_fusion.place_ref, bf16[512,256]{1,0:T(8,128)(2,1)S(1)} %copy-done.3, bf16[512,256]{1,0:T(8,128)(2,1)S(1)} %copy-done.8, bf16[512,256]{1,0:T(8,128)(2,1)S(1)} %copy-done.10, ...), custom_call_target="tpu_custom_call" | custom-call | flops 1073741824 | bytes 1310736 | tf_op jit(solution)/shard_map/pallas_call | solution.py:291
  143.6 4.3 %shard_map.91 = (f32[512,256]{1,0:T(8,128)S(1)}, f32[512,256]{1,0:T(8,128)S(1)}, f32[512,256]{1,0:T(8,128)S(1)}) custom-call(s32[4]{0:T(128)S(1)} %pad_add_fusion.place_ref, bf16[512,256]{1,0:T(8,128)(2,1)S(1)} %copy-done.3, f32[512,256]{1,0:T(8,128)S(1)} %get-tuple-element.23.max_ref, f32[512,256]{1,0:T(8,128)S(1)} %get-tuple-element.24.sum_ref, ...), custom_call_target="tpu_custom_call" | custom-call | flops 536870912 | bytes 2883600 | tf_op jit(solution)/shard_map/pallas_call | solution.py:291
  147.9 0.0 copy-start.1
  147.9 0.0 collective-permute-done.7.refs_0_
  147.9 0.0 collective-permute-done.8.refs_1_
  147.9 5.2 %shard_map.92 = (bf16[512,256]{1,0:T(8,128)(2,1)}, f32[512,256]{1,0:T(8,128)S(1)}) custom-call(s32[4]{0:T(128)S(1)} %pad_add_fusion.place_ref, bf16[512,256]{1,0:T(8,128)(2,1)S(1)} %copy-done.3, f32[512,256]{1,0:T(8,128)S(1)} %get-tuple-element.29.max_ref, f32[512,256]{1,0:T(8,128)S(1)} %get-tuple-element.30.sum_ref, ...), custom_call_target="tpu_custom_call" | custom-call | flops 268435456 | bytes 2359312 | tf_op jit(solution)/shard_map/pallas_call | solution.py:291
  153.1 3.4 %all-to-all-start.2 = ((bf16[4,128,256]{2,1,0:T(8,128)(2,1)}), bf16[4,128,256]{2,1,0:T(8,128)(2,1)S(1)}, u32[]{:S(2)}, u32[]{:S(2)}) async-start(bf16[4,128,256]{2,1,0:T(8,128)(2,1)} %bitcast.10), calls=%async_computation.2 | async-start | bytes 524288 | tf_op jit(solution)/shard_map/all_to_all | solution.py:397
  156.5 0.0 copy-start.6
  156.5 0.0 collective-permute-done.11.upper_ref
  156.5 0.0 collective-permute-done.12.lower_ref
  156.6 5.5 %all-to-all-done.2.att_ref = bf16[4,128,256]{2,1,0:T(8,128)(2,1)S(1)} async-done(((bf16[4,128,256]{2,1,0:T(8,128)(2,1)}), bf16[4,128,256]{2,1,0:T(8,128)(2,1)S(1)}, u32[]{:S(2)}, u32[]{:S(2)}) %all-to-all-start.2) | async-done | bytes 262176 | tf_op jit(solution)/shard_map/all_to_all | solution.py:397
  162.0 2.8 %shard_map.93 = (f32[64,2048]{1,0:T(8,128)S(1)}, bf16[64,2048]{1,0:T(8,128)(2,1)S(1)}) custom-call(s32[4]{0:T(128)S(1)} %pad_add_fusion.place_ref, bf16[4,128,256]{2,1,0:T(8,128)(2,1)S(1)} %all-to-all-done.2.att_ref, bf16[256,2048]{1,0:T(8,128)(2,1)S(1)} %copy-done.1, bf16[256,2048]{1,0:T(8,128)(2,1)} %collective-permute-done.9.before_ref, ...), custom_call_target="tpu_custom_call" | custom-call | flops 536870912 | bytes 4456464 | tf_op jit(solution)/shard_map/pallas_call | solution.py:291
  164.8 5.0 %collective-permute-start.13 = (bf16[64,2048]{1,0:T(8,128)(2,1)S(1)}, bf16[64,2048]{1,0:T(8,128)(2,1)S(1)}, u32[]{:S(2)}, u32[]{:S(2)}) collective-permute-start(bf16[64,2048]{1,0:T(8,128)(2,1)S(1)} %get-tuple-element.34), channel_id=1, source_target_pairs={{0,1},{1,0},{2,3},{3,2},{4,5},{5,4},{6,7},{7,6},{8,9},{9,8},{10,11... | collective-permute-start | bytes 786440 | tf_op jit(solution)/shard_map/ppermute | solution.py:407
  169.8 1.3 shard_map.95
  171.1 0.0 collective-permute-done.13.taken_ref
  171.1 0.0 copy-done.6
  171.1 0.9 shard_map.94
  (14 shorter events, 0.1 us)
Async XLA Ops:
  0.6 18.5 %copy-start.5 = (f32[2048]{0:T(1024)S(1)}, f32[2048]{0:T(1024)}, u32[]{:S(2)}) copy-start(f32[2048]{0:T(1024)} %param.8) | copy-start | bytes 24580
  0.6 18.5 %copy-start = (bf16[512,2048]{1,0:T(8,128)(2,1)S(1)}, bf16[512,2048]{1,0:T(8,128)(2,1)}, u32[]{:S(2)}) copy-start(bf16[512,2048]{1,0:T(8,128)(2,1)} %hidden_ref.3) | copy-start | bytes 6291460
  2.6 55.9 %all-to-all-start = ((bf16[32,32,512]{2,1,0:T(8,128)(2,1)}), bf16[32,32,512]{2,1,0:T(8,128)(2,1)S(1)}, u32[]{:S(2)}, u32[]{:S(2)}) async-start(bf16[32,32,512]{2,1,0:T(8,128)(2,1)} %broadcast_in_dim.11), calls=%async_computation | async-start | bytes 2097152 | tf_op jit(solution)/shard_map/all_to_all | solution.py:302
  19.3 39.2 %collective-permute-start.6 = (bf16[64,2048]{1,0:T(8,128)(2,1)S(1)}, bf16[64,2048]{1,0:T(8,128)(2,1)S(1)}, u32[]{:S(2)}, u32[]{:S(2)}) collective-permute-start(bf16[64,2048]{1,0:T(8,128)(2,1)S(1)} %shard_map.89), channel_id=1, source_target_pairs={{0,32},{8,40},{16,48},{24,56},{32,64},{40,72},{48,80},{56,88},{64,... | collective-permute-start | bytes 786440 | tf_op jit(solution)/shard_map/ppermute | solution.py:334
  60.1 72.7 %all-to-all-start.1 = ((bf16[8,64,2048]{2,1,0:T(8,128)(2,1)}), bf16[8,64,2048]{2,1,0:T(8,128)(2,1)}, u32[]{:S(2)}, u32[]{:S(2)}) async-start(bf16[8,64,2048]{2,1,0:T(8,128)(2,1)} %broadcast_in_dim.26), calls=%async_computation.1 | async-start | bytes 4194304 | tf_op jit(solution)/shard_map/all_to_all | solution.py:302
  65.7 48.7 %collective-permute-start.9 = (bf16[256,2048]{1,0:T(8,128)(2,1)}, bf16[256,2048]{1,0:T(8,128)(2,1)}, u32[]{:S(2)}, u32[]{:S(2)}) collective-permute-start(bf16[256,2048]{1,0:T(8,128)(2,1)} %own_ref.1), channel_id=1, source_target_pairs={{0,2},{2,4},{4,6},{6,0},{1,3},{3,5},{5,7},{7,1},{8,10},{10,12},{12... | collective-permute-start | bytes 3145736 | tf_op jit(solution)/shard_map/ppermute | solution.py:337
  68.9 49.3 %collective-permute-start.10 = (bf16[256,2048]{1,0:T(8,128)(2,1)}, bf16[256,2048]{1,0:T(8,128)(2,1)}, u32[]{:S(2)}, u32[]{:S(2)}) collective-permute-start(bf16[256,2048]{1,0:T(8,128)(2,1)} %own_ref.1), channel_id=1, source_target_pairs={{0,6},{2,0},{4,2},{6,4},{1,7},{3,1},{5,3},{7,5},{8,14},{10,8},{12,... | collective-permute-start | bytes 3145736 | tf_op jit(solution)/shard_map/ppermute | solution.py:338
  72.2 7.3 %copy-start.4 = (bf16[2048,256]{1,0:T(8,128)(2,1)S(1)}, bf16[2048,256]{1,0:T(8,128)(2,1)}, u32[]{:S(2)}) copy-start(bf16[2048,256]{1,0:T(8,128)(2,1)} %weight_ref.1) | copy-start | bytes 3145732
  72.3 16.2 %collective-permute-start = (bf16[2,256,512]{2,1,0:T(8,128)(2,1)S(1)}, bf16[2,256,512]{2,1,0:T(8,128)(2,1)S(1)}, u32[]{:S(2)}, u32[]{:S(2)}) collective-permute-start(bf16[2,256,512]{2,1,0:T(8,128)(2,1)S(1)} %bitcast.17), channel_id=1, source_target_pairs={{0,64},{64,128},{128,192},{192,256},{256,320},{320,384},{384,448},... | collective-permute-start | bytes 1572872 | tf_op jit(solution)/shard_map/ppermute | solution.py:318
  74.4 14.9 %collective-permute-start.1 = (bf16[2,256,512]{2,1,0:T(8,128)(2,1)S(1)}, bf16[2,256,512]{2,1,0:T(8,128)(2,1)S(1)}, u32[]{:S(2)}, u32[]{:S(2)}) collective-permute-start(bf16[2,256,512]{2,1,0:T(8,128)(2,1)S(1)} %bitcast.16), channel_id=1, source_target_pairs={{0,448},{64,0},{128,64},{192,128},{256,192},{320,256},{384,320},{4... | collective-permute-start | bytes 1572872 | tf_op jit(solution)/shard_map/ppermute | solution.py:319
  82.2 0.7 copy-start.2
  93.2 9.1 %collective-permute-start.2 = (bf16[512,256]{1,0:T(8,128)(2,1)S(1)}, bf16[512,256]{1,0:T(8,128)(2,1)S(1)}, u32[]{:S(2)}, u32[]{:S(2)}) collective-permute-start(bf16[512,256]{1,0:T(8,128)(2,1)S(1)} %get-tuple-element.21.k0_ref), channel_id=1, source_target_pairs={{0,8},{8,16},{16,24},{24,32},{32,40},{40,48},{48,56},{56,64},{64,7... | collective-permute-start | bytes 786440 | tf_op jit(solution)/shard_map/ppermute | solution.py:362
  98.4 0.7 copy-start.7
  99.1 8.7 %collective-permute-start.3 = (bf16[512,256]{1,0:T(8,128)(2,1)S(1)}, bf16[512,256]{1,0:T(8,128)(2,1)S(1)}, u32[]{:S(2)}, u32[]{:S(2)}) collective-permute-start(bf16[512,256]{1,0:T(8,128)(2,1)S(1)} %get-tuple-element.22.v0_ref), channel_id=1, source_target_pairs={{0,8},{8,16},{16,24},{24,32},{32,40},{40,48},{48,56},{56,64},{64,7... | collective-permute-start | bytes 786440 | tf_op jit(solution)/shard_map/ppermute | solution.py:363
  101.3 0.7 copy-start.9
  102.3 22.5 %collective-permute-start.4 = (bf16[512,256]{1,0:T(8,128)(2,1)S(1)}, bf16[512,256]{1,0:T(8,128)(2,1)}, u32[]{:S(2)}, u32[]{:S(2)}) collective-permute-start(bf16[512,256]{1,0:T(8,128)(2,1)S(1)} %collective-permute-done.2.k1_ref), channel_id=1, source_target_pairs={{0,8},{8,16},{16,24},{24,32},{32,40},{40,48},{48,56},{56,64},{64,7... | collective-permute-start | bytes 786440 | tf_op jit(solution)/shard_map/ppermute | solution.py:362
  107.9 22.8 %collective-permute-start.5 = (bf16[512,256]{1,0:T(8,128)(2,1)S(1)}, bf16[512,256]{1,0:T(8,128)(2,1)}, u32[]{:S(2)}, u32[]{:S(2)}) collective-permute-start(bf16[512,256]{1,0:T(8,128)(2,1)S(1)} %collective-permute-done.3.v1_ref), channel_id=1, source_target_pairs={{0,8},{8,16},{16,24},{24,32},{32,40},{40,48},{48,56},{56,64},{64,7... | collective-permute-start | bytes 786440 | tf_op jit(solution)/shard_map/ppermute | solution.py:363
  116.3 40.3 %collective-permute-start.11 = (bf16[128,2048]{1,0:T(8,128)(2,1)}, bf16[128,2048]{1,0:T(8,128)(2,1)}, u32[]{:S(2)}, u32[]{:S(2)}) collective-permute-start(bf16[128,2048]{1,0:T(8,128)(2,1)} %slice.26), channel_id=1, source_target_pairs={{0,2},{2,4},{4,6},{6,0},{1,3},{3,5},{5,7},{7,1},{8,10},{10,12},{12... | collective-permute-start | bytes 1572872 | tf_op jit(solution)/shard_map/ppermute | solution.py:339
  120.1 36.4 %collective-permute-start.12 = (bf16[128,2048]{1,0:T(8,128)(2,1)}, bf16[128,2048]{1,0:T(8,128)(2,1)}, u32[]{:S(2)}, u32[]{:S(2)}) collective-permute-start(bf16[128,2048]{1,0:T(8,128)(2,1)} %slice.27), channel_id=1, source_target_pairs={{0,6},{2,0},{4,2},{6,4},{1,7},{3,1},{5,3},{7,5},{8,14},{10,8},{12,... | collective-permute-start | bytes 1572872 | tf_op jit(solution)/shard_map/ppermute | solution.py:340
  124.7 23.2 %collective-permute-start.7 = (bf16[512,256]{1,0:T(8,128)(2,1)}, bf16[512,256]{1,0:T(8,128)(2,1)}, u32[]{:S(2)}, u32[]{:S(2)}) collective-permute-start(bf16[512,256]{1,0:T(8,128)(2,1)} %collective-permute-done.4.refs_0_), channel_id=1, source_target_pairs={{0,8},{8,16},{16,24},{24,32},{32,40},{40,48},{48,56},{56,64},{64,7... | collective-permute-start | bytes 786440 | tf_op jit(solution)/shard_map/ppermute | solution.py:362
  130.6 17.3 %collective-permute-start.8 = (bf16[512,256]{1,0:T(8,128)(2,1)}, bf16[512,256]{1,0:T(8,128)(2,1)}, u32[]{:S(2)}, u32[]{:S(2)}) collective-permute-start(bf16[512,256]{1,0:T(8,128)(2,1)} %collective-permute-done.5.refs_1_), channel_id=1, source_target_pairs={{0,8},{8,16},{16,24},{24,32},{32,40},{40,48},{48,56},{56,64},{64,7... | collective-permute-start | bytes 786440 | tf_op jit(solution)/shard_map/ppermute | solution.py:363
  132.9 4.9 %copy-start.3 = (bf16[512,256]{1,0:T(8,128)(2,1)S(1)}, bf16[512,256]{1,0:T(8,128)(2,1)}, u32[]{:S(2)}) copy-start(bf16[512,256]{1,0:T(8,128)(2,1)} %copy-done.2) | copy-start | bytes 786436
  132.9 4.9 %copy-start.8 = (bf16[512,256]{1,0:T(8,128)(2,1)S(1)}, bf16[512,256]{1,0:T(8,128)(2,1)}, u32[]{:S(2)}) copy-start(bf16[512,256]{1,0:T(8,128)(2,1)} %copy-done.7) | copy-start | bytes 786436
  132.9 4.9 %copy-start.10 = (bf16[512,256]{1,0:T(8,128)(2,1)S(1)}, bf16[512,256]{1,0:T(8,128)(2,1)}, u32[]{:S(2)}) copy-start(bf16[512,256]{1,0:T(8,128)(2,1)} %copy-done.9) | copy-start | bytes 786436
  147.9 14.1 %copy-start.1 = (bf16[256,2048]{1,0:T(8,128)(2,1)S(1)}, bf16[256,2048]{1,0:T(8,128)(2,1)}, u32[]{:S(2)}) copy-start(bf16[256,2048]{1,0:T(8,128)(2,1)} %own_ref.1) | copy-start | bytes 3145732
  153.1 8.9 %all-to-all-start.2 = ((bf16[4,128,256]{2,1,0:T(8,128)(2,1)}), bf16[4,128,256]{2,1,0:T(8,128)(2,1)S(1)}, u32[]{:S(2)}, u32[]{:S(2)}) async-start(bf16[4,128,256]{2,1,0:T(8,128)(2,1)} %bitcast.10), calls=%async_computation.2 | async-start | bytes 524288 | tf_op jit(solution)/shard_map/all_to_all | solution.py:397
  156.5 14.5 %copy-start.6 = (f32[2048]{0:T(1024)S(1)}, f32[2048]{0:T(1024)}, u32[]{:S(2)}) copy-start(f32[2048]{0:T(1024)} %param.13) | copy-start | bytes 24580
  164.8 6.2 %collective-permute-start.13 = (bf16[64,2048]{1,0:T(8,128)(2,1)S(1)}, bf16[64,2048]{1,0:T(8,128)(2,1)S(1)}, u32[]{:S(2)}, u32[]{:S(2)}) collective-permute-start(bf16[64,2048]{1,0:T(8,128)(2,1)S(1)} %get-tuple-element.34), channel_id=1, source_target_pairs={{0,1},{1,0},{2,3},{3,2},{4,5},{5,4},{6,7},{7,6},{8,9},{9,8},{10,11... | collective-permute-start | bytes 786440 | tf_op jit(solution)/shard_map/ppermute | solution.py:407

commit v5 on v4

--- a/solution.py
+++ b/solution.py
@@ -140,11 +140,62 @@
     return jnp.where(ok, 0.0, LOW).astype(F32)
 
 
-def near_kernel(place_ref, q_ref, k0_ref, v0_ref, k1_ref, v1_ref, max_ref, sum_ref, acc_ref, s_ref, p_ref, bias_ref, count_ref, stat_ref, tail_ref):
+def times_seen(o):
+    count = (o <= SPAN).astype(F32)
+    count = count + (((o & 3) == 0) & (o <= 4 * SPAN)).astype(F32)
+    return count + ((o & 15) == 0).astype(F32)
+
+
+def query_places(cls):
+    i = lax.broadcasted_iota(jnp.int32, (128, 1), 0)
+    return (i & 31) * 16 + (i >> 5) * 4 + cls
+
+
+def own_kernel(q_ref, k_ref, v_ref, max_ref, sum_ref, acc_ref, s_ref, p_ref, bias_ref, count_ref, stat_ref):
+    keys, width = k_ref.shape
+    heads = width // HEAD_DIM
+    o = query_places(pl.program_id(0)) - natural(lax.broadcasted_iota(jnp.int32, (1, keys), 1))
+    count = jnp.where(o >= 0, times_seen(o), 0.0)
+    count_ref[...] = count
+    bias_ref[...] = jnp.where(count > 0, 0.0, LOW).astype(F32)
+    s_ref[...] = lax.dot_general(stack_heads(q_ref[...]), k_ref[...], NT, preferred_element_type=F32)
+    step = 32
+    for r in range(0, heads * 128, step):
+        mask = slice(r % 128, r % 128 + step)
+        s = s_ref[r : r + step, :] + bias_ref[mask, :]
+        m = jnp.max(s, axis=1, keepdims=True)
+        p = jnp.exp(s - m) * count_ref[mask, :]
+        stat_ref[0, r : r + step, :] = jnp.broadcast_to(m, (step, width))
+        stat_ref[1, r : r + step, :] = jnp.broadcast_to(jnp.sum(p, axis=1, keepdims=True), (step, width))
+        p_ref[r : r + step, :] = p.astype(BF16)
+    pv = jnp.dot(p_ref[...], v_ref[...], preferred_element_type=F32)
+    max_ref[...] = own_heads(stat_ref[0])
+    sum_ref[...] = own_heads(stat_ref[1])
+    acc_ref[...] = own_heads(pv)
+
+
+def merged(scores, bias, count, value, max_ref, sum_ref, acc_ref, p_ref, stat_ref):
+    width = max_ref.shape[1]
+    for h in range(width // HEAD_DIM):
+        part = slice(h * 128, (h + 1) * 128)
+        s = scores[part] + bias
+        m = jnp.maximum(jnp.max(s, axis=1, keepdims=True), max_ref[:, h * HEAD_DIM : h * HEAD_DIM + 1])
+        p = jnp.exp(s - m)
+        if count is not None:
+            p = p * count
+        p_ref[part, :] = p.astype(BF16)
+        stat_ref[0, part, :] = jnp.broadcast_to(m, (128, width))
+        stat_ref[1, part, :] = jnp.broadcast_to(jnp.sum(p, axis=1, keepdims=True), (128, width))
+    pv = jnp.dot(p_ref[...], value, preferred_element_type=F32)
+    m = own_heads(stat_ref[0])
+    alpha = jnp.exp(max_ref[...] - m)
+    total = sum_ref[...] * alpha + own_heads(stat_ref[1])
+    return m, total, acc_ref[...] * alpha + own_heads(pv)
+
+
+def before_kernel(place_ref, q_ref, max_ref, sum_ref, acc_ref, k_ref, v_ref, new_max, new_sum, new_acc, p_ref, stat_ref, tail_ref):
     cls = pl.program_id(0)
-    block = place_ref[0]
-    keys, width = k0_ref.shape
-    heads = width // HEAD_DIM
+    keys = k_ref.shape[0]
     mine = pl.ds(pl.multiple_of(cls * 128, 128), 128)
 
     @pl.when(cls == 0)
@@ -152,57 +203,26 @@
         j = lax.broadcasted_iota(jnp.int32, (128, keys), 0)
         i = lax.broadcasted_iota(jnp.int32, (128, keys), 1)
         pick = (i == (j >> 3) * 32 + 24 + (j & 7)).astype(BF16)
-        tail_ref[0] = permuted(pick, k1_ref[...])
-        tail_ref[1] = permuted(pick, v1_ref[...])
-
-    i = lax.broadcasted_iota(jnp.int32, (128, 1), 0)
-    qn = (i & 31) * 16 + (i >> 5) * 4 + cls
-    seen = block >= 1
-    for lies, size in ((0, keys), (keys, 128)):
-        k = lax.broadcasted_iota(jnp.int32, (1, size), 1)
-        if lies == 0:
-            o = qn - natural(k)
-        else:
-            o = qn - ((k & 31) * 16 + (k >> 5) * 4 + cls) + keys
-        count = (o <= SPAN).astype(F32)
-        count = count + (((o & 3) == 0) & (o <= 4 * SPAN)).astype(F32)
-        count = count + ((o & 15) == 0).astype(F32)
-        if lies == 0:
-            count = jnp.where(o >= 0, count, 0.0)
-        else:
-            count = jnp.where(seen, count, 0.0)
-        count_ref[:, lies : lies + size] = count
-        bias_ref[:, lies : lies + size] = jnp.where(count > 0, 0.0, LOW).astype(F32)
+        tail_ref[0] = permuted(pick, k_ref[...])
+        tail_ref[1] = permuted(pick, v_ref[...])
+
+    seen = place_ref[0] >= 1
+    qn = query_places(cls)
     k = lax.broadcasted_iota(jnp.int32, (1, 128), 1)
-    o = qn - ((24 + (k & 7)) * 16 + ((k >> 3) & 3) * 4 + (k >> 5)) + keys
-    ok = (o <= SPAN) & ((k >> 5) != cls) & seen
-    bias_ref[:, keys + 128 :] = jnp.where(ok, 0.0, LOW).astype(F32)
-
-    stacked = stack_heads(q_ref[...])
-    s_ref[:, :keys] = lax.dot_general(stacked, k0_ref[...], NT, preferred_element_type=F32)
-    rest = jnp.concatenate([k1_ref[mine, :], tail_ref[0]], axis=0)
-    s_ref[:, keys:] = lax.dot_general(stacked, rest, NT, preferred_element_type=F32)
-    step = 32
-    for r in range(0, heads * 128, step):
-        mask = slice(r % 128, r % 128 + step)
-        s = s_ref[r : r + step, :] + bias_ref[mask, :]
-        m = jnp.max(s, axis=1, keepdims=True)
-        p = jnp.exp(s - m)
-        p = jnp.concatenate([p[:, : keys + 128] * count_ref[mask, :], p[:, keys + 128 :]], axis=1)
-        stat_ref[0, r : r + step, :] = jnp.broadcast_to(m, (step, width))
-        stat_ref[1, r : r + step, :] = jnp.broadcast_to(jnp.sum(p, axis=1, keepdims=True), (step, width))
-        p_ref[r : r + step, :] = p.astype(BF16)
-    pv = jnp.dot(p_ref[:, :keys], v0_ref[...], preferred_element_type=F32)
-    rest = jnp.concatenate([v1_ref[mine, :], tail_ref[1]], axis=0)
-    pv = pv + jnp.dot(p_ref[:, keys:], rest, preferred_element_type=F32)
-    max_ref[...] = own_heads(stat_ref[0])
-    sum_ref[...] = own_heads(stat_ref[1])
-    acc_ref[...] = own_heads(pv)
+    same = times_seen(qn - ((k & 31) * 16 + (k >> 5) * 4 + cls) + keys)
+    last = qn - ((24 + (k & 7)) * 16 + ((k >> 3) & 3) * 4 + (k >> 5)) + keys
+    last = ((last <= SPAN) & ((k >> 5) != cls)).astype(F32)
+    count = jnp.where(seen, jnp.concatenate([same, last], axis=1), 0.0)
+    bias = jnp.where(count > 0, 0.0, LOW).astype(F32)
+    key = jnp.concatenate([k_ref[mine, :], tail_ref[0]], axis=0)
+    value = jnp.concatenate([v_ref[mine, :], tail_ref[1]], axis=0)
+    scores = lax.dot_general(stack_heads(q_ref[...]), key, NT, preferred_element_type=F32)
+    state = merged(scores, bias, count, value, max_ref, sum_ref, acc_ref, p_ref, stat_ref)
+    for ref, part in zip((new_max, new_sum, new_acc), state):
+        ref[...] = part
 
 
 def far_kernel(backs, last, place_ref, q_ref, max_ref, sum_ref, acc_ref, *refs):
-    width = q_ref.shape[1]
-    heads = width // HEAD_DIM
     count = len(backs)
     sources, outs = refs[: 2 * count], refs[2 * count :]
     p_ref, stat_ref = outs[-2:]
@@ -210,19 +230,7 @@
     key = jnp.concatenate([ref[...] for ref in sources[0::2]], axis=0)
     value = jnp.concatenate([ref[...] for ref in sources[1::2]], axis=0)
     scores = lax.dot_general(stack_heads(q_ref[...]), key, NT, preferred_element_type=F32)
-    for h in range(heads):
-        part = slice(h * 128, (h + 1) * 128)
-        s = scores[part] + bias
-        m = jnp.maximum(jnp.max(s, axis=1, keepdims=True), max_ref[:, h * HEAD_DIM : h * HEAD_DIM + 1])
-        p = jnp.exp(s - m)
-        p_ref[part, :] = p.astype(BF16)
-        stat_ref[0, part, :] = jnp.broadcast_to(m, (128, width))
-        stat_ref[1, part, :] = jnp.broadcast_to(jnp.sum(p, axis=1, keepdims=True), (128, width))
-    pv = jnp.dot(p_ref[...], value, preferred_element_type=F32)
-    m = own_heads(stat_ref[0])
-    alpha = jnp.exp(max_ref[...] - m)
-    total = sum_ref[...] * alpha + own_heads(stat_ref[1])
-    acc = acc_ref[...] * alpha + own_heads(pv)
+    m, total, acc = merged(scores, bias, None, value, max_ref, sum_ref, acc_ref, p_ref, stat_ref)
     if last:
         cls = pl.program_id(0)
         out_ref, log_ref, att_ref = outs[:3]
@@ -233,8 +241,8 @@
         def _():
             out_ref[...] = permuted(to_natural(att_ref.shape[0]), att_ref[...])
     else:
-        for ref, value in zip(outs[:3], (m, total, acc)):
-            ref[...] = value
+        for ref, part in zip(outs[:3], (m, total, acc)):
+            ref[...] = part
 
 
 def log_kernel(lw_ref, log_ref):
@@ -251,17 +259,11 @@
         log_ref[head : head + 1, :] = flipped[head * HEAD_DIM : head * HEAD_DIM + 1, :]
 
 
-def out_kernel(place_ref, att_ref, own_ref, before_ref, after_ref, upper_ref, lower_ref, keep_ref, give_ref, sum_ref):
+def out_kernel(place_ref, att_ref, own_ref, before_ref, after_ref, across_ref, keep_ref, give_ref, sum_ref):
     x, core = place_ref[2], place_ref[3]
-    half = own_ref.shape[0] // 2
     rows = keep_ref.shape[0]
-    for n, ref in enumerate((own_ref, before_ref, after_ref, None)):
-        att = att_ref[lax.rem(x + HOPS[n], 4)]
-        if ref is None:
-            part = jnp.dot(att[:, :half], upper_ref[...], preferred_element_type=F32)
-            part = part + jnp.dot(att[:, half:], lower_ref[...], preferred_element_type=F32)
-        else:
-            part = jnp.dot(att, ref[...], preferred_element_type=F32)
+    for n, ref in enumerate((own_ref, before_ref, after_ref, across_ref)):
+        part = jnp.dot(att_ref[lax.rem(x + HOPS[n], 4)], ref[...], preferred_element_type=F32)
         part = part.astype(BF16).astype(F32)
         if n == 0:
             sum_ref[...] = part
@@ -336,8 +338,7 @@
 
     before = lax.ppermute(out_proj, "x", ring(4, 1))
     after = lax.ppermute(out_proj, "x", ring(4, -1))
-    upper = lax.ppermute(before[: width // 2], "x", ring(4, 1))
-    lower = lax.ppermute(after[width // 2 :], "x", ring(4, -1))
+    across = lax.ppermute(out_proj, "x", ring(4, 2))
 
     quarter = HEAD_DIM // 2
     frequency = ROPE_BASE ** (-(jnp.arange(quarter, dtype=F32) * 2.0 / HEAD_DIM))
@@ -347,14 +348,14 @@
     turns = jnp.stack([jnp.cos(angles), jnp.sin(angles)])
 
     normed, query = kernel_call(
-        query_kernel, [((rows, depth), BF16), (row, BF16)], (hidden_in, gain, query_proj, turns), 2 * rows * depth * width, 16
+        query_kernel, [((rows, depth), BF16), (row, BF16)], (hidden_in, gain, query_proj, turns), 2 * rows * depth * width, 12
     )
     key, value, weights = kernel_call(
         key_value_kernel,
         [(row, BF16), (row, BF16), ((depth, 2 * width), BF16)],
         (place, normed, mine, below, above, turns),
         4 * rows * depth * width,
-        20,
+        12,
     )
     forward = [(i, i + 1) for i in range(63)]
     keys, values = [key], [value]
@@ -362,20 +363,32 @@
         keys.append(lax.ppermute(keys[-1], SP, forward))
         values.append(lax.ppermute(values[-1], SP, forward))
     key4, value4 = kernel_call(
-        far_key_value_kernel, [(row, BF16)] * 2, (far_rows, weights, turns), 4 * rows * depth * width, 16
+        far_key_value_kernel, [(row, BF16)] * 2, (far_rows, weights, turns), 4 * rows * depth * width, 10
     )
 
     whole = pl.BlockSpec(row, lambda c: (0, 0))
     part = pl.BlockSpec((128, width), lambda c: (c, 0))
+    pair = ((512, 256), BF16), ((2, 512, width), F32)
     state = kernel_call(
-        near_kernel,
+        own_kernel,
         [(row, F32)] * 3,
-        (place, query, keys[0], values[0], keys[1], values[1]),
-        16 * rows * rows * width,
-        20,
-        [((512, 768), F32), ((512, 768), BF16), ((128, 768), F32), ((128, 640), F32), ((2, 512, width), F32), ((2, 128, width), BF16)],
+        (query, keys[0], values[0]),
+        8 * rows * rows * width,
+        10,
+        [((512, 512), F32), ((512, 512), BF16), ((128, 512), F32), ((128, 512), F32), ((2, 512, width), F32)],
         grid=(rows // 128,),
-        in_specs=[SMEM, part] + [whole] * 4,
+        in_specs=[part, whole, whole],
+        out_specs=(part,) * 3,
+    )
+    state = kernel_call(
+        before_kernel,
+        [(row, F32)] * 3,
+        (place, query, *state, keys[1], values[1]),
+        4 * rows * rows * width,
+        10,
+        [*pair, ((2, 128, width), BF16)],
+        grid=(rows // 128,),
+        in_specs=[SMEM] + [part] * 4 + [whole, whole],
         out_specs=(part,) * 3,
     )
     sources = {2: (keys[2], values[2]), 3: (keys[3], values[3]), 4: (key4, value4)}
@@ -386,7 +399,7 @@
             [(row, BF16), (row, F32)] if last else [(row, F32)] * 3,
             (place, query, *state, *(array for back in backs for array in sources[back])),
             4 * rows * 512 * width * len(backs),
-            16,
+            10,
             ([(row, BF16)] if last else []) + [((512, 128 * len(backs)), BF16), ((2, 512, width), F32)],
             grid=(rows // 128,),
             in_specs=[SMEM] + [part] * (4 + 2 * len(backs)),
@@ -395,13 +408,13 @@
     attended, logs = state
 
     arrived = lax.all_to_all(attended.reshape(4, rows // 4, width), "x", split_axis=0, concat_axis=0, tiled=True)
-    (log_weight,) = kernel_call(log_kernel, [((heads, rows), F32)], (logs,), 6 * rows * rows * width, 12)
+    (log_weight,) = kernel_call(log_kernel, [((heads, rows), F32)], (logs,), 6 * rows * rows * width, 8)
     keep, give = kernel_call(
         out_kernel,
         [((piece, depth), F32), ((piece, depth), BF16)],
-        (place, arrived, out_proj, before, after, upper, lower),
+        (place, arrived, out_proj, before, after, across),
         2 * rows // 8 * depth * depth,
-        20,
+        12,
         [((2 * piece, depth), F32)],
     )
     taken = lax.ppermute(give, "c", ring(2, 1))

time: 173 us -> 173 us (level)
  local copies, waits for them, and re-layouts: 8.79 us -> 5.11 us
  starting transfers between devices: 82.4 us -> 85.2 us
    ppermute x1, starting transfers between devices: 4.97 us -> 9.38 us  [layer(): taken = lax.ppermute(give, 'c', ring(2, 1))]
    ppermute x2 -> x1, starting transfers between devices: 6.47 us -> 2.49 us  [layer(): across = lax.ppermute(out_proj, 'x', ring(4, 2))]
    slice x2 -> x0, local copies, waits for them, and re-layouts: 3.86 us -> none  [the longest x1 1.94 us: layer(): upper = lax.ppermute(before[:width // 2], 'x', ring(4, 1))]
    ppermute x3, starting transfers between devices: 9.33 us -> 12 us  [layer(): values.append(lax.ppermute(values[-1], SP, forward))]
    pallas_call x10 -> x11, Pallas kernels: 31.8 us -> 33.5 us  [kernel_call(): pl.pallas_call(body, out_shape=tuple((jax.ShapeDtypeStruct(s, t) for s, t...]
  transfers between devices with their start and end apart: 17 -> 16, of which waited for: 7 -> 6; matrix products, arithmetic and copies ran while one was open for 3% -> 0% of each run, Pallas kernels for 16% -> 17%
where the time goes in v5:
time: 173 us; the launch traced here: 172 us
  starting transfers between devices  85.2 us (49%)
  waiting for transfers between devices  45.8 us (26%)
  Pallas kernels  33.5 us (19%)
  local copies, waits for them, and re-layouts  5.11 us (3%)
    pallas_call x11, Pallas kernels, kernel_call(): pl.pallas_call(body, out_shape=tuple((jax.ShapeDtypeStruct(s, t) for s, t...  33.5 us
    ppermute x1, waiting for transfers between devices, layer(): fourth = lax.ppermute(eighth, SP, ring(64, 4))  32.2 us
    all_to_all x2, starting transfers between devices, spread_to(): return lax.all_to_all(copies, axis, split_axis=0, concat_axis=0, tiled=True)  22 us
    ppermute x3, starting transfers between devices, layer(): keys.append(lax.ppermute(keys[-1], SP, forward))  15.1 us
    ppermute x3, starting transfers between devices, layer(): values.append(lax.ppermute(values[-1], SP, forward))  12 us
    ppermute x1, starting transfers between devices, layer(): taken = lax.ppermute(give, 'c', ring(2, 1))  9.38 us
    ppermute x1, starting transfers between devices, layer(): fourth = lax.ppermute(eighth, SP, ring(64, 4))  7.05 us
    ppermute x1, waiting for transfers between devices, layer(): below = lax.ppermute(mine[:2], Z, ring(8, 1))  5.57 us
  transfers between devices with their start and end apart: 16, of which 6 were waited for; matrix products, arithmetic and copies ran while one was open for 0% of the time, Pallas kernels for 17%

profile of v5, /device:TPU:1, one launch (start us, length us, event | category | flops | bytes accessed | tf_op | source)
XLA Modules:
  0.0 172.2 jit_solution(975764612366605634)
XLA Ops:
  0.6 0.0 copy-start.11
  0.6 0.0 copy-start
  0.7 0.9 pad_maximum_fusion.1
  1.5 1.1 broadcast_in_dim.11
  2.7 16.5 %all-to-all-start = ((bf16[32,32,512]{2,1,0:T(8,128)(2,1)}), bf16[32,32,512]{2,1,0:T(8,128)(2,1)S(1)}, u32[]{:S(2)}, u32[]{:S(2)}) async-start(bf16[32,32,512]{2,1,0:T(8,128)(2,1)} %broadcast_in_dim.11), calls=%async_computation | async-start | bytes 2097152 | tf_op jit(solution)/shard_map/all_to_all | solution.py:304
  19.2 0.0 copy-done.11
  19.2 0.0 copy-done
  19.2 0.2 shard_map.90
  19.4 7.0 %collective-permute-start.6 = (bf16[64,2048]{1,0:T(8,128)(2,1)S(1)}, bf16[64,2048]{1,0:T(8,128)(2,1)S(1)}, u32[]{:S(2)}, u32[]{:S(2)}) collective-permute-start(bf16[64,2048]{1,0:T(8,128)(2,1)S(1)} %shard_map.90), channel_id=1, source_target_pairs={{0,32},{8,40},{16,48},{24,56},{32,64},{40,72},{48,80},{56,88},{64,... | collective-permute-start | bytes 786440 | tf_op jit(solution)/shard_map/ppermute | solution.py:336
  26.4 32.2 %collective-permute-done.6 = bf16[64,2048]{1,0:T(8,128)(2,1)S(1)} collective-permute-done((bf16[64,2048]{1,0:T(8,128)(2,1)S(1)}, bf16[64,2048]{1,0:T(8,128)(2,1)S(1)}, u32[]{:S(2)}, u32[]{:S(2)}) %collective-permute-start.6) | collective-permute-done | bytes 262176 | tf_op jit(solution)/shard_map/ppermute | solution.py:336
  58.6 0.0 all-to-all-done
  58.6 1.6 broadcast_in_dim.26
  60.2 5.5 %all-to-all-start.1 = ((bf16[8,64,2048]{2,1,0:T(8,128)(2,1)}), bf16[8,64,2048]{2,1,0:T(8,128)(2,1)}, u32[]{:S(2)}, u32[]{:S(2)}) async-start(bf16[8,64,2048]{2,1,0:T(8,128)(2,1)} %broadcast_in_dim.26), calls=%async_computation.1 | async-start | bytes 4194304 | tf_op jit(solution)/shard_map/all_to_all | solution.py:304
  65.7 4.5 %collective-permute-start.10 = (bf16[256,2048]{1,0:T(8,128)(2,1)}, bf16[256,2048]{1,0:T(8,128)(2,1)}, u32[]{:S(2)}, u32[]{:S(2)}) collective-permute-start(bf16[256,2048]{1,0:T(8,128)(2,1)} %own_ref.1), channel_id=1, source_target_pairs={{0,6},{2,0},{4,2},{6,4},{1,7},{3,1},{5,3},{7,5},{8,14},{10,8},{12,... | collective-permute-start | bytes 3145736 | tf_op jit(solution)/shard_map/ppermute | solution.py:340
  70.2 2.5 %collective-permute-start.11 = (bf16[256,2048]{1,0:T(8,128)(2,1)}, bf16[256,2048]{1,0:T(8,128)(2,1)}, u32[]{:S(2)}, u32[]{:S(2)}) collective-permute-start(bf16[256,2048]{1,0:T(8,128)(2,1)} %own_ref.1), channel_id=1, source_target_pairs={{0,4},{2,6},{4,0},{6,2},{1,5},{3,7},{5,1},{7,3},{8,12},{10,14},{12... | collective-permute-start | bytes 3145736 | tf_op jit(solution)/shard_map/ppermute | solution.py:341
  72.7 2.5 %collective-permute-start.9 = (bf16[256,2048]{1,0:T(8,128)(2,1)}, bf16[256,2048]{1,0:T(8,128)(2,1)}, u32[]{:S(2)}, u32[]{:S(2)}) collective-permute-start(bf16[256,2048]{1,0:T(8,128)(2,1)} %own_ref.1), channel_id=1, source_target_pairs={{0,2},{2,4},{4,6},{6,0},{1,3},{3,5},{5,7},{7,1},{8,10},{10,12},{12... | collective-permute-start | bytes 3145736 | tf_op jit(solution)/shard_map/ppermute | solution.py:339
  75.2 0.0 copy-start.4
  75.2 0.1 fusion
  75.3 2.1 %collective-permute-start = (bf16[2,256,512]{2,1,0:T(8,128)(2,1)S(1)}, bf16[2,256,512]{2,1,0:T(8,128)(2,1)S(1)}, u32[]{:S(2)}, u32[]{:S(2)}) collective-permute-start(bf16[2,256,512]{2,1,0:T(8,128)(2,1)S(1)} %bitcast.17), channel_id=1, source_target_pairs={{0,64},{64,128},{128,192},{192,256},{256,320},{320,384},{384,448},... | collective-permute-start | bytes 1572872 | tf_op jit(solution)/shard_map/ppermute | solution.py:320
  77.4 4.6 %collective-permute-start.1 = (bf16[2,256,512]{2,1,0:T(8,128)(2,1)S(1)}, bf16[2,256,512]{2,1,0:T(8,128)(2,1)S(1)}, u32[]{:S(2)}, u32[]{:S(2)}) collective-permute-start(bf16[2,256,512]{2,1,0:T(8,128)(2,1)S(1)} %bitcast.16), channel_id=1, source_target_pairs={{0,448},{64,0},{128,64},{192,128},{256,192},{320,256},{384,320},{4... | collective-permute-start | bytes 1572872 | tf_op jit(solution)/shard_map/ppermute | solution.py:321
  82.0 0.5 multiply_cosine_fusion
  82.5 2.7 %shard_map.86 = (bf16[512,2048]{1,0:T(8,128)(2,1)S(1)}, bf16[512,256]{1,0:T(8,128)(2,1)S(1)}) custom-call(bf16[512,2048]{1,0:T(8,128)(2,1)S(1)} %copy-done, f32[1,2048]{1,0:T(1,128)S(1)} %bitcast.14, bf16[2048,256]{1,0:T(8,128)(2,1)S(1)} %copy-done.4, f32[2,32,1024]{2,1,0:T(8,128)S(1)} %pad_maximum_fusion.turn_ref), custom_call_target="tpu_custom_call" | custom-call | flops 536870912 | bytes 3416064 | tf_op jit(solution)/shard_map/pallas_call | solution.py:293
  85.2 0.0 copy-start.1
  85.2 0.1 pad_add_fusion.place_ref
  85.3 5.6 %collective-permute-done.below_ref = bf16[2,256,512]{2,1,0:T(8,128)(2,1)S(1)} collective-permute-done((bf16[2,256,512]{2,1,0:T(8,128)(2,1)S(1)}, bf16[2,256,512]{2,1,0:T(8,128)(2,1)S(1)}, u32[]{:S(2)}, u32[]{:S(2)}) %collective-permute-start) | collective-permute-done | bytes 524320 | tf_op jit(solution)/shard_map/ppermute | solution.py:320
  90.9 0.8 collective-permute-done.1.above_ref
  91.7 3.9 %shard_map.87 = (bf16[512,256]{1,0:T(8,128)(2,1)S(1)}, bf16[512,256]{1,0:T(8,128)(2,1)S(1)}, bf16[2048,512]{1,0:T(8,128)(2,1)S(1)}) custom-call(s32[4]{0:T(128)S(1)} %pad_add_fusion.place_ref, bf16[512,2048]{1,0:T(8,128)(2,1)S(1)} %get-tuple-element.23.normed_ref, bf16[4,256,512]{2,1,0:T(8,128)(2,1)S(1)} %bitcast.12, ...), custom_call_target="tpu_custom_call" | custom-call | flops 1073741824 | bytes 4456464 | tf_op jit(solution)/shard_map/pallas_call | solution.py:293
  95.6 5.2 %collective-permute-start.2 = (bf16[512,256]{1,0:T(8,128)(2,1)S(1)}, bf16[512,256]{1,0:T(8,128)(2,1)S(1)}, u32[]{:S(2)}, u32[]{:S(2)}) collective-permute-start(bf16[512,256]{1,0:T(8,128)(2,1)S(1)} %get-tuple-element.24.k_ref), channel_id=1, source_target_pairs={{0,8},{8,16},{16,24},{24,32},{32,40},{40,48},{48,56},{56,64},{64,7... | collective-permute-start | bytes 786440 | tf_op jit(solution)/shard_map/ppermute | solution.py:363
  100.8 2.2 %collective-permute-start.3 = (bf16[512,256]{1,0:T(8,128)(2,1)S(1)}, bf16[512,256]{1,0:T(8,128)(2,1)S(1)}, u32[]{:S(2)}, u32[]{:S(2)}) collective-permute-start(bf16[512,256]{1,0:T(8,128)(2,1)S(1)} %get-tuple-element.25.v_ref), channel_id=1, source_target_pairs={{0,8},{8,16},{16,24},{24,32},{32,40},{40,48},{48,56},{56,64},{64,7... | collective-permute-start | bytes 786440 | tf_op jit(solution)/shard_map/ppermute | solution.py:364
  103.0 1.1 collective-permute-done.2.k_ref
  104.1 5.0 %collective-permute-start.4 = (bf16[512,256]{1,0:T(8,128)(2,1)S(1)}, bf16[512,256]{1,0:T(8,128)(2,1)}, u32[]{:S(2)}, u32[]{:S(2)}) collective-permute-start(bf16[512,256]{1,0:T(8,128)(2,1)S(1)} %collective-permute-done.2.k_ref), channel_id=1, source_target_pairs={{0,8},{8,16},{16,24},{24,32},{32,40},{40,48},{48,56},{56,64},{64,7... | collective-permute-start | bytes 786440 | tf_op jit(solution)/shard_map/ppermute | solution.py:363
  109.1 0.7 copy-done.7
  109.8 0.0 collective-permute-done.3.v_ref
  109.8 4.8 %collective-permute-start.5 = (bf16[512,256]{1,0:T(8,128)(2,1)S(1)}, bf16[512,256]{1,0:T(8,128)(2,1)}, u32[]{:S(2)}, u32[]{:S(2)}) collective-permute-start(bf16[512,256]{1,0:T(8,128)(2,1)S(1)} %collective-permute-done.3.v_ref), channel_id=1, source_target_pairs={{0,8},{8,16},{16,24},{24,32},{32,40},{40,48},{48,56},{56,64},{64,7... | collective-permute-start | bytes 786440 | tf_op jit(solution)/shard_map/ppermute | solution.py:364
  114.6 0.7 copy-done.9
  115.3 0.0 collective-permute-done.4.refs_0_
  115.3 4.9 %collective-permute-start.7 = (bf16[512,256]{1,0:T(8,128)(2,1)}, bf16[512,256]{1,0:T(8,128)(2,1)}, u32[]{:S(2)}, u32[]{:S(2)}) collective-permute-start(bf16[512,256]{1,0:T(8,128)(2,1)} %collective-permute-done.4.refs_0_), channel_id=1, source_target_pairs={{0,8},{8,16},{16,24},{24,32},{32,40},{40,48},{48,56},{56,64},{64,7... | collective-permute-start | bytes 786440 | tf_op jit(solution)/shard_map/ppermute | solution.py:363
  120.2 0.7 collective-permute-done.5.refs_1_
  120.9 4.9 %collective-permute-start.8 = (bf16[512,256]{1,0:T(8,128)(2,1)}, bf16[512,256]{1,0:T(8,128)(2,1)}, u32[]{:S(2)}, u32[]{:S(2)}) collective-permute-start(bf16[512,256]{1,0:T(8,128)(2,1)} %collective-permute-done.5.refs_1_), channel_id=1, source_target_pairs={{0,8},{8,16},{16,24},{24,32},{32,40},{40,48},{48,56},{56,64},{64,7... | collective-permute-start | bytes 786440 | tf_op jit(solution)/shard_map/ppermute | solution.py:364
  125.8 3.5 %shard_map.88 = (f32[512,256]{1,0:T(8,128)S(1)}, f32[512,256]{1,0:T(8,128)S(1)}, f32[512,256]{1,0:T(8,128)S(1)}) custom-call(bf16[512,256]{1,0:T(8,128)(2,1)S(1)} %get-tuple-element.22.q_ref, bf16[512,256]{1,0:T(8,128)(2,1)S(1)} %get-tuple-element.24.k_ref, bf16[512,256]{1,0:T(8,128)(2,1)S(1)} %get-tuple-element.25.v_ref), custom_call_target="tpu_custom_call" | custom-call | flops 536870912 | bytes 786432 | tf_op jit(solution)/shard_map/pallas_call | solution.py:293
  129.4 0.8 copy-done.5
  130.2 0.0 all-to-all-done.1
  130.2 4.9 %shard_map.91 = (bf16[512,256]{1,0:T(8,128)(2,1)S(1)}, bf16[512,256]{1,0:T(8,128)(2,1)S(1)}) custom-call(bf16[512,2048]{1,0:T(8,128)(2,1)} %bitcast.9.normed_ref, bf16[2048,512]{1,0:T(8,128)(2,1)S(1)} %get-tuple-element.32.weight_ref, f32[2,32,1024]{2,1,0:T(8,128)S(1)} %pad_maximum_fusion.turn_ref), custom_call_target="tpu_custom_call" | custom-call | flops 1073741824 | bytes 4456448 | tf_op jit(solution)/shard_map/pallas_call | solution.py:293
  135.1 0.0 copy-done.2
  135.1 0.0 copy-done.6
  135.1 0.0 copy-done.8
  135.1 0.0 copy-done.10
  135.1 4.1 %shard_map.89 = (f32[512,256]{1,0:T(8,128)S(1)}, f32[512,256]{1,0:T(8,128)S(1)}, f32[512,256]{1,0:T(8,128)S(1)}) custom-call(s32[4]{0:T(128)S(1)} %pad_add_fusion.place_ref, bf16[512,256]{1,0:T(8,128)(2,1)S(1)} %copy-done.2, f32[512,256]{1,0:T(8,128)S(1)} %get-tuple-element.26.max_ref, f32[512,256]{1,0:T(8,128)S(1)} %get-tuple-element.27.sum_ref, ...), custom_call_target="tpu_custom_call" | custom-call | flops 268435456 | bytes 2359312 | tf_op jit(solution)/shard_map/pallas_call | solution.py:293
  139.3 4.3 %shard_map.92 = (f32[512,256]{1,0:T(8,128)S(1)}, f32[512,256]{1,0:T(8,128)S(1)}, f32[512,256]{1,0:T(8,128)S(1)}) custom-call(s32[4]{0:T(128)S(1)} %pad_add_fusion.place_ref, bf16[512,256]{1,0:T(8,128)(2,1)S(1)} %copy-done.2, f32[512,256]{1,0:T(8,128)S(1)} %get-tuple-element.29.max_ref, f32[512,256]{1,0:T(8,128)S(1)} %get-tuple-element.30.sum_ref, ...), custom_call_target="tpu_custom_call" | custom-call | flops 536870912 | bytes 2883600 | tf_op jit(solution)/shard_map/pallas_call | solution.py:293
  143.5 0.0 copy-start.3
  143.6 0.0 collective-permute-done.7.refs_0_
  143.6 0.0 collective-permute-done.8.refs_1_
  143.6 5.2 %shard_map.93 = (bf16[512,256]{1,0:T(8,128)(2,1)}, f32[512,256]{1,0:T(8,128)S(1)}) custom-call(s32[4]{0:T(128)S(1)} %pad_add_fusion.place_ref, bf16[512,256]{1,0:T(8,128)(2,1)S(1)} %copy-done.2, f32[512,256]{1,0:T(8,128)S(1)} %get-tuple-element.35.max_ref, f32[512,256]{1,0:T(8,128)S(1)} %get-tuple-element.36.sum_ref, ...), custom_call_target="tpu_custom_call" | custom-call | flops 268435456 | bytes 2359312 | tf_op jit(solution)/shard_map/pallas_call | solution.py:293
  148.8 3.7 %all-to-all-start.2 = ((bf16[4,128,256]{2,1,0:T(8,128)(2,1)}), bf16[4,128,256]{2,1,0:T(8,128)(2,1)S(1)}, u32[]{:S(2)}, u32[]{:S(2)}) async-start(bf16[4,128,256]{2,1,0:T(8,128)(2,1)} %bitcast.10), calls=%async_computation.2 | async-start | bytes 524288 | tf_op jit(solution)/shard_map/all_to_all | solution.py:410
  152.4 0.0 collective-permute-done.10.after_ref
  152.4 0.0 collective-permute-done.11.across_ref
  152.4 0.0 collective-permute-done.9.before_ref
  152.4 5.5 %all-to-all-done.2.att_ref = bf16[4,128,256]{2,1,0:T(8,128)(2,1)S(1)} async-done(((bf16[4,128,256]{2,1,0:T(8,128)(2,1)}), bf16[4,128,256]{2,1,0:T(8,128)(2,1)S(1)}, u32[]{:S(2)}, u32[]{:S(2)}) %all-to-all-start.2) | async-done | bytes 262176 | tf_op jit(solution)/shard_map/all_to_all | solution.py:410
  157.9 2.7 %shard_map.94 = (f32[64,2048]{1,0:T(8,128)S(1)}, bf16[64,2048]{1,0:T(8,128)(2,1)S(1)}) custom-call(s32[4]{0:T(128)S(1)} %pad_add_fusion.place_ref, bf16[4,128,256]{2,1,0:T(8,128)(2,1)S(1)} %all-to-all-done.2.att_ref, bf16[256,2048]{1,0:T(8,128)(2,1)S(1)} %copy-done.3, bf16[256,2048]{1,0:T(8,128)(2,1)} %collective-permute-done.9.before_ref, ...), custom_call_target="tpu_custom_call" | custom-call | flops 536870912 | bytes 4456464 | tf_op jit(solution)/shard_map/pallas_call | solution.py:293
  160.6 9.4 %collective-permute-start.12 = (bf16[64,2048]{1,0:T(8,128)(2,1)S(1)}, bf16[64,2048]{1,0:T(8,128)(2,1)S(1)}, u32[]{:S(2)}, u32[]{:S(2)}) collective-permute-start(bf16[64,2048]{1,0:T(8,128)(2,1)S(1)} %get-tuple-element.40), channel_id=1, source_target_pairs={{0,1},{1,0},{2,3},{3,2},{4,5},{5,4},{6,7},{7,6},{8,9},{9,8},{10,11... | collective-permute-start | bytes 786440 | tf_op jit(solution)/shard_map/ppermute | solution.py:420
  170.0 1.3 shard_map.96
  171.3 0.0 collective-permute-done.12.taken_ref
  171.3 0.0 copy-done.12
  171.3 0.9 shard_map.95
  (15 shorter events, 0.1 us)
Async XLA Ops:
  0.6 18.5 %copy-start.11 = (f32[2048]{0:T(1024)S(1)}, f32[2048]{0:T(1024)}, u32[]{:S(2)}) copy-start(f32[2048]{0:T(1024)} %param.8) | copy-start | bytes 24580
  0.6 18.5 %copy-start = (bf16[512,2048]{1,0:T(8,128)(2,1)S(1)}, bf16[512,2048]{1,0:T(8,128)(2,1)}, u32[]{:S(2)}) copy-start(bf16[512,2048]{1,0:T(8,128)(2,1)} %hidden_ref.3) | copy-start | bytes 6291460
  2.7 55.9 %all-to-all-start = ((bf16[32,32,512]{2,1,0:T(8,128)(2,1)}), bf16[32,32,512]{2,1,0:T(8,128)(2,1)S(1)}, u32[]{:S(2)}, u32[]{:S(2)}) async-start(bf16[32,32,512]{2,1,0:T(8,128)(2,1)} %broadcast_in_dim.11), calls=%async_computation | async-start | bytes 2097152 | tf_op jit(solution)/shard_map/all_to_all | solution.py:304
  19.4 39.2 %collective-permute-start.6 = (bf16[64,2048]{1,0:T(8,128)(2,1)S(1)}, bf16[64,2048]{1,0:T(8,128)(2,1)S(1)}, u32[]{:S(2)}, u32[]{:S(2)}) collective-permute-start(bf16[64,2048]{1,0:T(8,128)(2,1)S(1)} %shard_map.90), channel_id=1, source_target_pairs={{0,32},{8,40},{16,48},{24,56},{32,64},{40,72},{48,80},{56,88},{64,... | collective-permute-start | bytes 786440 | tf_op jit(solution)/shard_map/ppermute | solution.py:336
  60.2 70.0 %all-to-all-start.1 = ((bf16[8,64,2048]{2,1,0:T(8,128)(2,1)}), bf16[8,64,2048]{2,1,0:T(8,128)(2,1)}, u32[]{:S(2)}, u32[]{:S(2)}) async-start(bf16[8,64,2048]{2,1,0:T(8,128)(2,1)} %broadcast_in_dim.26), calls=%async_computation.1 | async-start | bytes 4194304 | tf_op jit(solution)/shard_map/all_to_all | solution.py:304
  65.7 86.7 %collective-permute-start.10 = (bf16[256,2048]{1,0:T(8,128)(2,1)}, bf16[256,2048]{1,0:T(8,128)(2,1)}, u32[]{:S(2)}, u32[]{:S(2)}) collective-permute-start(bf16[256,2048]{1,0:T(8,128)(2,1)} %own_ref.1), channel_id=1, source_target_pairs={{0,6},{2,0},{4,2},{6,4},{1,7},{3,1},{5,3},{7,5},{8,14},{10,8},{12,... | collective-permute-start | bytes 3145736 | tf_op jit(solution)/shard_map/ppermute | solution.py:340
  70.2 82.3 %collective-permute-start.11 = (bf16[256,2048]{1,0:T(8,128)(2,1)}, bf16[256,2048]{1,0:T(8,128)(2,1)}, u32[]{:S(2)}, u32[]{:S(2)}) collective-permute-start(bf16[256,2048]{1,0:T(8,128)(2,1)} %own_ref.1), channel_id=1, source_target_pairs={{0,4},{2,6},{4,0},{6,2},{1,5},{3,7},{5,1},{7,3},{8,12},{10,14},{12... | collective-permute-start | bytes 3145736 | tf_op jit(solution)/shard_map/ppermute | solution.py:341
  72.7 79.8 %collective-permute-start.9 = (bf16[256,2048]{1,0:T(8,128)(2,1)}, bf16[256,2048]{1,0:T(8,128)(2,1)}, u32[]{:S(2)}, u32[]{:S(2)}) collective-permute-start(bf16[256,2048]{1,0:T(8,128)(2,1)} %own_ref.1), channel_id=1, source_target_pairs={{0,2},{2,4},{4,6},{6,0},{1,3},{3,5},{5,7},{7,1},{8,10},{10,12},{12... | collective-permute-start | bytes 3145736 | tf_op jit(solution)/shard_map/ppermute | solution.py:339
  75.2 7.4 %copy-start.4 = (bf16[2048,256]{1,0:T(8,128)(2,1)S(1)}, bf16[2048,256]{1,0:T(8,128)(2,1)}, u32[]{:S(2)}) copy-start(bf16[2048,256]{1,0:T(8,128)(2,1)} %weight_ref.1) | copy-start | bytes 3145732
  75.3 15.6 %collective-permute-start = (bf16[2,256,512]{2,1,0:T(8,128)(2,1)S(1)}, bf16[2,256,512]{2,1,0:T(8,128)(2,1)S(1)}, u32[]{:S(2)}, u32[]{:S(2)}) collective-permute-start(bf16[2,256,512]{2,1,0:T(8,128)(2,1)S(1)} %bitcast.17), channel_id=1, source_target_pairs={{0,64},{64,128},{128,192},{192,256},{256,320},{320,384},{384,448},... | collective-permute-start | bytes 1572872 | tf_op jit(solution)/shard_map/ppermute | solution.py:320
  77.4 14.3 %collective-permute-start.1 = (bf16[2,256,512]{2,1,0:T(8,128)(2,1)S(1)}, bf16[2,256,512]{2,1,0:T(8,128)(2,1)S(1)}, u32[]{:S(2)}, u32[]{:S(2)}) collective-permute-start(bf16[2,256,512]{2,1,0:T(8,128)(2,1)S(1)} %bitcast.16), channel_id=1, source_target_pairs={{0,448},{64,0},{128,64},{192,128},{256,192},{320,256},{384,320},{4... | collective-permute-start | bytes 1572872 | tf_op jit(solution)/shard_map/ppermute | solution.py:321
  85.2 40.6 %copy-start.1 = (bf16[512,256]{1,0:T(8,128)(2,1)}, bf16[512,256]{1,0:T(8,128)(2,1)S(1)}, u32[]{:S(2)}) copy-start(bf16[512,256]{1,0:T(8,128)(2,1)S(1)} %get-tuple-element.22.q_ref) | copy-start | bytes 786436
  95.6 8.5 %collective-permute-start.2 = (bf16[512,256]{1,0:T(8,128)(2,1)S(1)}, bf16[512,256]{1,0:T(8,128)(2,1)S(1)}, u32[]{:S(2)}, u32[]{:S(2)}) collective-permute-start(bf16[512,256]{1,0:T(8,128)(2,1)S(1)} %get-tuple-element.24.k_ref), channel_id=1, source_target_pairs={{0,8},{8,16},{16,24},{24,32},{32,40},{40,48},{48,56},{56,64},{64,7... | collective-permute-start | bytes 786440 | tf_op jit(solution)/shard_map/ppermute | solution.py:363
  100.8 8.9 %collective-permute-start.3 = (bf16[512,256]{1,0:T(8,128)(2,1)S(1)}, bf16[512,256]{1,0:T(8,128)(2,1)S(1)}, u32[]{:S(2)}, u32[]{:S(2)}) collective-permute-start(bf16[512,256]{1,0:T(8,128)(2,1)S(1)} %get-tuple-element.25.v_ref), channel_id=1, source_target_pairs={{0,8},{8,16},{16,24},{24,32},{32,40},{40,48},{48,56},{56,64},{64,7... | collective-permute-start | bytes 786440 | tf_op jit(solution)/shard_map/ppermute | solution.py:364
  104.1 11.2 %collective-permute-start.4 = (bf16[512,256]{1,0:T(8,128)(2,1)S(1)}, bf16[512,256]{1,0:T(8,128)(2,1)}, u32[]{:S(2)}, u32[]{:S(2)}) collective-permute-start(bf16[512,256]{1,0:T(8,128)(2,1)S(1)} %collective-permute-done.2.k_ref), channel_id=1, source_target_pairs={{0,8},{8,16},{16,24},{24,32},{32,40},{40,48},{48,56},{56,64},{64,7... | collective-permute-start | bytes 786440 | tf_op jit(solution)/shard_map/ppermute | solution.py:363
  109.0 0.7 copy-start.7
  109.8 11.2 %collective-permute-start.5 = (bf16[512,256]{1,0:T(8,128)(2,1)S(1)}, bf16[512,256]{1,0:T(8,128)(2,1)}, u32[]{:S(2)}, u32[]{:S(2)}) collective-permute-start(bf16[512,256]{1,0:T(8,128)(2,1)S(1)} %collective-permute-done.3.v_ref), channel_id=1, source_target_pairs={{0,8},{8,16},{16,24},{24,32},{32,40},{40,48},{48,56},{56,64},{64,7... | collective-permute-start | bytes 786440 | tf_op jit(solution)/shard_map/ppermute | solution.py:364
  114.6 0.7 copy-start.9
  115.3 28.2 %collective-permute-start.7 = (bf16[512,256]{1,0:T(8,128)(2,1)}, bf16[512,256]{1,0:T(8,128)(2,1)}, u32[]{:S(2)}, u32[]{:S(2)}) collective-permute-start(bf16[512,256]{1,0:T(8,128)(2,1)} %collective-permute-done.4.refs_0_), channel_id=1, source_target_pairs={{0,8},{8,16},{16,24},{24,32},{32,40},{40,48},{48,56},{56,64},{64,7... | collective-permute-start | bytes 786440 | tf_op jit(solution)/shard_map/ppermute | solution.py:363
  120.9 22.7 %collective-permute-start.8 = (bf16[512,256]{1,0:T(8,128)(2,1)}, bf16[512,256]{1,0:T(8,128)(2,1)}, u32[]{:S(2)}, u32[]{:S(2)}) collective-permute-start(bf16[512,256]{1,0:T(8,128)(2,1)} %collective-permute-done.5.refs_1_), channel_id=1, source_target_pairs={{0,8},{8,16},{16,24},{24,32},{32,40},{40,48},{48,56},{56,64},{64,7... | collective-permute-start | bytes 786440 | tf_op jit(solution)/shard_map/ppermute | solution.py:364
  129.3 0.9 copy-start.5
  130.2 4.9 %copy-start.2 = (bf16[512,256]{1,0:T(8,128)(2,1)S(1)}, bf16[512,256]{1,0:T(8,128)(2,1)}, u32[]{:S(2)}) copy-start(bf16[512,256]{1,0:T(8,128)(2,1)} %copy-done.1) | copy-start | bytes 786436
  130.2 4.9 %copy-start.6 = (f32[512,256]{1,0:T(8,128)S(1)}, f32[512,256]{1,0:T(8,128)}, u32[]{:S(2)}) copy-start(f32[512,256]{1,0:T(8,128)} %copy-done.5) | copy-start | bytes 1572868
  130.2 4.9 %copy-start.8 = (bf16[512,256]{1,0:T(8,128)(2,1)S(1)}, bf16[512,256]{1,0:T(8,128)(2,1)}, u32[]{:S(2)}) copy-start(bf16[512,256]{1,0:T(8,128)(2,1)} %copy-done.7) | copy-start | bytes 786436
  130.2 4.9 %copy-start.10 = (bf16[512,256]{1,0:T(8,128)(2,1)S(1)}, bf16[512,256]{1,0:T(8,128)(2,1)}, u32[]{:S(2)}) copy-start(bf16[512,256]{1,0:T(8,128)(2,1)} %copy-done.9) | copy-start | bytes 786436
  143.5 14.4 %copy-start.3 = (bf16[256,2048]{1,0:T(8,128)(2,1)S(1)}, bf16[256,2048]{1,0:T(8,128)(2,1)}, u32[]{:S(2)}) copy-start(bf16[256,2048]{1,0:T(8,128)(2,1)} %own_ref.1) | copy-start | bytes 3145732
  148.8 9.2 %all-to-all-start.2 = ((bf16[4,128,256]{2,1,0:T(8,128)(2,1)}), bf16[4,128,256]{2,1,0:T(8,128)(2,1)S(1)}, u32[]{:S(2)}, u32[]{:S(2)}) async-start(bf16[4,128,256]{2,1,0:T(8,128)(2,1)} %bitcast.10), calls=%async_computation.2 | async-start | bytes 524288 | tf_op jit(solution)/shard_map/all_to_all | solution.py:410
  152.4 18.9 %copy-start.12 = (f32[2048]{0:T(1024)S(1)}, f32[2048]{0:T(1024)}, u32[]{:S(2)}) copy-start(f32[2048]{0:T(1024)} %param.13) | copy-start | bytes 24580
  160.6 10.7 %collective-permute-start.12 = (bf16[64,2048]{1,0:T(8,128)(2,1)S(1)}, bf16[64,2048]{1,0:T(8,128)(2,1)S(1)}, u32[]{:S(2)}, u32[]{:S(2)}) collective-permute-start(bf16[64,2048]{1,0:T(8,128)(2,1)S(1)} %get-tuple-element.40), channel_id=1, source_target_pairs={{0,1},{1,0},{2,3},{3,2},{4,5},{5,4},{6,7},{7,6},{8,9},{9,8},{10,11... | collective-permute-start | bytes 786440 | tf_op jit(solution)/shard_map/ppermute | solution.py:420

commit v6 on v5

--- a/solution.py
+++ b/solution.py
@@ -88,31 +88,41 @@
     query_ref[...] = permuted(to_residue(rows), query)
 
 
-def project(normed, weight_ref, cos, sin, key_ref, value_ref):
+def project(normed_ref, turn_ref, weight_ref, key_ref, value_ref, both_ref):
     rows, width = key_ref.shape
-    perm = to_residue(rows)
-    key = jnp.dot(normed, weight_ref[:, :width], preferred_element_type=F32)
-    key_ref[...] = permuted(perm, rotated(key, cos, sin).astype(BF16))
-    value = jnp.dot(normed, weight_ref[:, width:], preferred_element_type=F32).astype(BF16)
-    value_ref[...] = permuted(perm, value)
-
-
-def key_value_kernel(place_ref, normed_ref, mine_ref, below_ref, above_ref, turn_ref, key_ref, value_ref, weight_ref):
-    rows = normed_ref.shape[0]
-    low = place_ref[1]
-    slabs = []
-    for k in range(4):
-        slabs.append((2 * k + low, mine_ref, k))
-    for k in range(2):
-        slabs.append((2 * k + 1 - low, below_ref, k))
-        slabs.append((2 * (k + 2) + 1 - low, above_ref, k))
-    for place, ref, k in slabs:
-        weight_ref[pl.ds(pl.multiple_of(place * 256, 256), 256), :] = ref[k]
-    project(normed_ref[...], weight_ref, *spread(turn_ref, slice(rows, 2 * rows)), key_ref, value_ref)
-
-
-def far_key_value_kernel(normed_ref, weight_ref, turn_ref, key_ref, value_ref):
-    project(normed_ref[...], weight_ref, *spread(turn_ref, slice(0, normed_ref.shape[0])), key_ref, value_ref)
+    block = normed_ref.shape[0]
+    n = pl.program_id(0)
+    cos, sin = spread(turn_ref, slice(0, block))
+    both = jnp.dot(normed_ref[...], weight_ref[...], preferred_element_type=F32)
+    part = pl.ds(pl.multiple_of(n * block, block), block)
+    both_ref[part, :width] = rotated(both[:, :width], cos, sin).astype(BF16)
+    both_ref[part, width:] = both[:, width:].astype(BF16)
+
+    @pl.when(n == pl.num_programs(0) - 1)
+    def _():
+        ordered = permuted(to_residue(rows), both_ref[...])
+        key_ref[...] = ordered[:, :width]
+        value_ref[...] = ordered[:, width:]
+
+
+def key_value_kernel(place_ref, normed_ref, turn_ref, mine_ref, below_ref, above_ref, key_ref, value_ref, weight_ref, both_ref):
+    @pl.when(pl.program_id(0) == 0)
+    def _():
+        low = place_ref[1]
+        slabs = []
+        for k in range(4):
+            slabs.append((2 * k + low, mine_ref, k))
+        for k in range(2):
+            slabs.append((2 * k + 1 - low, below_ref, k))
+            slabs.append((2 * (k + 2) + 1 - low, above_ref, k))
+        for place, ref, k in slabs:
+            weight_ref[pl.ds(pl.multiple_of(place * 256, 256), 256), :] = ref[k]
+
+    project(normed_ref, turn_ref, weight_ref, key_ref, value_ref, both_ref)
+
+
+def far_key_value_kernel(normed_ref, turn_ref, weight_ref, key_ref, value_ref, both_ref):
+    project(normed_ref, turn_ref, weight_ref, key_ref, value_ref, both_ref)
 
 
 def stack_heads(q):
@@ -151,7 +161,23 @@
     return (i & 31) * 16 + (i >> 5) * 4 + cls
 
 
-def own_kernel(q_ref, k_ref, v_ref, max_ref, sum_ref, acc_ref, s_ref, p_ref, bias_ref, count_ref, stat_ref):
+def statistics(tops, sums):
+    lane = lax.broadcasted_iota(jnp.int32, (tops[0].shape[0], 128), 1)
+    out = jnp.zeros(lane.shape, F32)
+    for n, column in enumerate(tops + sums):
+        out = jnp.where(lane == n, column, out)
+    return out
+
+
+def by_head(columns, width):
+    lane = lax.broadcasted_iota(jnp.int32, (columns[0].shape[0], width), 1) >> 6
+    out = jnp.broadcast_to(columns[0], lane.shape)
+    for h in range(1, len(columns)):
+        out = jnp.where(lane == h, columns[h], out)
+    return out
+
+
+def own_kernel(q_ref, k_ref, v_ref, stat_ref, acc_ref, s_ref, p_ref, bias_ref, count_ref, raw_ref):
     keys, width = k_ref.shape
     heads = width // HEAD_DIM
     o = query_places(pl.program_id(0)) - natural(lax.broadcasted_iota(jnp.int32, (1, keys), 1))
@@ -165,35 +191,36 @@
         s = s_ref[r : r + step, :] + bias_ref[mask, :]
         m = jnp.max(s, axis=1, keepdims=True)
         p = jnp.exp(s - m) * count_ref[mask, :]
-        stat_ref[0, r : r + step, :] = jnp.broadcast_to(m, (step, width))
-        stat_ref[1, r : r + step, :] = jnp.broadcast_to(jnp.sum(p, axis=1, keepdims=True), (step, width))
+        raw_ref[0, r : r + step, :] = jnp.broadcast_to(m, (step, 128))
+        raw_ref[1, r : r + step, :] = jnp.broadcast_to(jnp.sum(p, axis=1, keepdims=True), (step, 128))
         p_ref[r : r + step, :] = p.astype(BF16)
-    pv = jnp.dot(p_ref[...], v_ref[...], preferred_element_type=F32)
-    max_ref[...] = own_heads(stat_ref[0])
-    sum_ref[...] = own_heads(stat_ref[1])
-    acc_ref[...] = own_heads(pv)
-
-
-def merged(scores, bias, count, value, max_ref, sum_ref, acc_ref, p_ref, stat_ref):
-    width = max_ref.shape[1]
-    for h in range(width // HEAD_DIM):
-        part = slice(h * 128, (h + 1) * 128)
-        s = scores[part] + bias
-        m = jnp.maximum(jnp.max(s, axis=1, keepdims=True), max_ref[:, h * HEAD_DIM : h * HEAD_DIM + 1])
+    columns = [[raw_ref[n, h * 128 : (h + 1) * 128, :] for h in range(heads)] for n in range(2)]
+    stat_ref[...] = statistics(*columns)
+    acc_ref[...] = own_heads(jnp.dot(p_ref[...], v_ref[...], preferred_element_type=F32))
+
+
+def merged(q, key, value, bias, count, stat, acc):
+    width = q.shape[1]
+    heads = width // HEAD_DIM
+    scores = lax.dot_general(stack_heads(q), key, NT, preferred_element_type=F32)
+    tops, sums, shares, scales = [], [], [], []
+    for h in range(heads):
+        s = scores[h * 128 : (h + 1) * 128] + bias
+        old = stat[:, h : h + 1]
+        m = jnp.maximum(jnp.max(s, axis=1, keepdims=True), old)
         p = jnp.exp(s - m)
         if count is not None:
             p = p * count
-        p_ref[part, :] = p.astype(BF16)
-        stat_ref[0, part, :] = jnp.broadcast_to(m, (128, width))
-        stat_ref[1, part, :] = jnp.broadcast_to(jnp.sum(p, axis=1, keepdims=True), (128, width))
-    pv = jnp.dot(p_ref[...], value, preferred_element_type=F32)
-    m = own_heads(stat_ref[0])
-    alpha = jnp.exp(max_ref[...] - m)
-    total = sum_ref[...] * alpha + own_heads(stat_ref[1])
-    return m, total, acc_ref[...] * alpha + own_heads(pv)
-
-
-def before_kernel(place_ref, q_ref, max_ref, sum_ref, acc_ref, k_ref, v_ref, new_max, new_sum, new_acc, p_ref, stat_ref, tail_ref):
+        scale = jnp.exp(old - m)
+        tops.append(m)
+        sums.append(stat[:, heads + h : heads + h + 1] * scale + jnp.sum(p, axis=1, keepdims=True))
+        scales.append(scale)
+        shares.append(p.astype(BF16))
+    pv = own_heads(jnp.dot(jnp.concatenate(shares, axis=0), value, preferred_element_type=F32))
+    return tops, sums, acc * by_head(scales, width) + pv
+
+
+def before_kernel(place_ref, q_ref, stat_ref, acc_ref, k_ref, v_ref, new_stat, new_acc, tail_ref):
     cls = pl.program_id(0)
     keys = k_ref.shape[0]
     mine = pl.ds(pl.multiple_of(cls * 128, 128), 128)
@@ -216,59 +243,56 @@
     bias = jnp.where(count > 0, 0.0, LOW).astype(F32)
     key = jnp.concatenate([k_ref[mine, :], tail_ref[0]], axis=0)
     value = jnp.concatenate([v_ref[mine, :], tail_ref[1]], axis=0)
-    scores = lax.dot_general(stack_heads(q_ref[...]), key, NT, preferred_element_type=F32)
-    state = merged(scores, bias, count, value, max_ref, sum_ref, acc_ref, p_ref, stat_ref)
-    for ref, part in zip((new_max, new_sum, new_acc), state):
-        ref[...] = part
-
-
-def far_kernel(backs, last, place_ref, q_ref, max_ref, sum_ref, acc_ref, *refs):
-    count = len(backs)
-    sources, outs = refs[: 2 * count], refs[2 * count :]
-    p_ref, stat_ref = outs[-2:]
+    tops, sums, acc = merged(q_ref[...], key, value, bias, count, stat_ref[...], acc_ref[...])
+    new_stat[...] = statistics(tops, sums)
+    new_acc[...] = acc
+
+
+def far_kernel(backs, place_ref, q_ref, stat_ref, acc_ref, *refs):
+    sources, (new_stat, new_acc) = refs[:-2], refs[-2:]
     bias = jnp.concatenate([far_bias(place_ref[0], back) for back in backs], axis=1)
     key = jnp.concatenate([ref[...] for ref in sources[0::2]], axis=0)
     value = jnp.concatenate([ref[...] for ref in sources[1::2]], axis=0)
-    scores = lax.dot_general(stack_heads(q_ref[...]), key, NT, preferred_element_type=F32)
-    m, total, acc = merged(scores, bias, None, value, max_ref, sum_ref, acc_ref, p_ref, stat_ref)
-    if last:
-        cls = pl.program_id(0)
-        out_ref, log_ref, att_ref = outs[:3]
-        att_ref[pl.ds(pl.multiple_of(cls * 128, 128), 128), :] = (acc / total).astype(BF16)
-        log_ref[...] = m + jnp.log(total)
-
-        @pl.when(cls == pl.num_programs(0) - 1)
-        def _():
-            out_ref[...] = permuted(to_natural(att_ref.shape[0]), att_ref[...])
-    else:
-        for ref, part in zip(outs[:3], (m, total, acc)):
-            ref[...] = part
-
-
-def log_kernel(lw_ref, log_ref):
-    rows, width = lw_ref.shape
+    tops, sums, acc = merged(q_ref[...], key, value, bias, None, stat_ref[...], acc_ref[...])
+    new_stat[...] = statistics(tops, sums)
+    new_acc[...] = acc
+
+
+def last_kernel(back, place_ref, q_ref, stat_ref, acc_ref, k_ref, v_ref, out_ref, new_stat):
+    rows, width = q_ref.shape
+    bias = far_bias(place_ref[0], back)
+    done = []
+    for cls in range(rows // 128):
+        part = slice(cls * 128, (cls + 1) * 128)
+        tops, sums, acc = merged(q_ref[part, :], k_ref[part, :], v_ref[part, :], bias, None, stat_ref[part, :], acc_ref[part, :])
+        new_stat[part, :] = statistics(tops, sums)
+        done.append((acc / by_head(sums, width)).astype(BF16))
+    out_ref[...] = permuted(to_natural(rows), jnp.concatenate(done, axis=0))
+
+
+def log_kernel(stat_ref, log_ref):
+    rows = stat_ref.shape[0]
+    heads = log_ref.shape[0]
     perm = to_natural(rows)
-    rest = lw_ref[...]
-    ordered = jnp.zeros((rows, width), F32)
+    rest = stat_ref[...]
+    ordered = jnp.zeros(rest.shape, F32)
     for _ in range(3):
         piece = rest.astype(BF16)
         rest = rest - piece.astype(F32)
         ordered = ordered + jnp.dot(perm, piece, preferred_element_type=F32)
     flipped = ordered.T
-    for head in range(width // HEAD_DIM):
-        log_ref[head : head + 1, :] = flipped[head * HEAD_DIM : head * HEAD_DIM + 1, :]
+    log_ref[...] = flipped[:heads] + jnp.log(flipped[heads : 2 * heads])
 
 
 def out_kernel(place_ref, att_ref, own_ref, before_ref, after_ref, across_ref, keep_ref, give_ref, sum_ref):
     x, core = place_ref[2], place_ref[3]
     rows = keep_ref.shape[0]
+    total = None
     for n, ref in enumerate((own_ref, before_ref, after_ref, across_ref)):
         part = jnp.dot(att_ref[lax.rem(x + HOPS[n], 4)], ref[...], preferred_element_type=F32)
         part = part.astype(BF16).astype(F32)
-        if n == 0:
-            sum_ref[...] = part
-        else:
-            sum_ref[...] += part
+        total = part if total is None else total + part
+    sum_ref[...] = total
     keep_ref[...] = sum_ref[pl.ds(pl.multiple_of(core * rows, rows), rows), :]
     give_ref[...] = sum_ref[pl.ds(pl.multiple_of((1 - core) * rows, rows), rows), :].astype(BF16)
 
@@ -315,8 +339,9 @@
     gain = pre_gain[None]
     row = (rows, width)
 
-    shard = jnp.concatenate([key_proj, value_proj], axis=1)
-    mine = spread_to(shard, ("zh", "y"), 32).reshape(4, 256, 2 * width)
+    copies = [jnp.broadcast_to(shard[None], (32,) + shard.shape) for shard in (key_proj, value_proj)]
+    mine = lax.all_to_all(jnp.concatenate(copies, axis=2), ("zh", "y"), split_axis=0, concat_axis=0, tiled=True)
+    mine = mine.reshape(4, 256, 2 * width)
     below = lax.ppermute(mine[:2], Z, ring(8, 1))
     above = lax.ppermute(mine[2:], Z, ring(8, -1))
 
@@ -350,12 +375,27 @@
     normed, query = kernel_call(
         query_kernel, [((rows, depth), BF16), (row, BF16)], (hidden_in, gain, query_proj, turns), 2 * rows * depth * width, 12
     )
+    block_rows = rows // 4
+    row_part = pl.BlockSpec((block_rows, depth), lambda n: (n, 0))
+    whole = pl.BlockSpec(row, lambda c: (0, 0))
+    weight_spec = pl.BlockSpec((depth, 2 * width), lambda n: (0, 0))
     key, value, weights = kernel_call(
         key_value_kernel,
         [(row, BF16), (row, BF16), ((depth, 2 * width), BF16)],
-        (place, normed, mine, below, above, turns),
+        (place, normed, turns, mine, below, above),
         4 * rows * depth * width,
-        12,
+        14,
+        [((rows, 2 * width), BF16)],
+        grid=(4,),
+        in_specs=[
+            SMEM,
+            row_part,
+            pl.BlockSpec((2, HEAD_DIM // 2, block_rows), lambda n: (0, 0, 4 + n)),
+            pl.BlockSpec((4, 256, 2 * width), lambda n: (0, 0, 0)),
+            pl.BlockSpec((2, 256, 2 * width), lambda n: (0, 0, 0)),
+            pl.BlockSpec((2, 256, 2 * width), lambda n: (0, 0, 0)),
+        ],
+        out_specs=(whole, whole, weight_spec),
     )
     forward = [(i, i + 1) for i in range(63)]
     keys, values = [key], [value]
@@ -363,59 +403,74 @@
         keys.append(lax.ppermute(keys[-1], SP, forward))
         values.append(lax.ppermute(values[-1], SP, forward))
     key4, value4 = kernel_call(
-        far_key_value_kernel, [(row, BF16)] * 2, (far_rows, weights, turns), 4 * rows * depth * width, 10
-    )
-
-    whole = pl.BlockSpec(row, lambda c: (0, 0))
+        far_key_value_kernel,
+        [(row, BF16)] * 2,
+        (far_rows, turns, weights),
+        4 * rows * depth * width,
+        14,
+        [((rows, 2 * width), BF16)],
+        grid=(4,),
+        in_specs=[row_part, pl.BlockSpec((2, HEAD_DIM // 2, block_rows), lambda n: (0, 0, n)), weight_spec],
+        out_specs=(whole, whole),
+    )
+
     part = pl.BlockSpec((128, width), lambda c: (c, 0))
-    pair = ((512, 256), BF16), ((2, 512, width), F32)
+    stat_part = pl.BlockSpec((128, 128), lambda c: (c, 0))
+    outs = [((rows, 128), F32), (row, F32)]
     state = kernel_call(
         own_kernel,
-        [(row, F32)] * 3,
+        outs,
         (query, keys[0], values[0]),
         8 * rows * rows * width,
         10,
-        [((512, 512), F32), ((512, 512), BF16), ((128, 512), F32), ((128, 512), F32), ((2, 512, width), F32)],
+        [((512, 512), F32), ((512, 512), BF16), ((128, 512), F32), ((128, 512), F32), ((2, 512, 128), F32)],
         grid=(rows // 128,),
         in_specs=[part, whole, whole],
-        out_specs=(part,) * 3,
+        out_specs=(stat_part, part),
     )
     state = kernel_call(
         before_kernel,
-        [(row, F32)] * 3,
+        outs,
         (place, query, *state, keys[1], values[1]),
         4 * rows * rows * width,
         10,
-        [*pair, ((2, 128, width), BF16)],
+        [((2, 128, width), BF16)],
         grid=(rows // 128,),
-        in_specs=[SMEM] + [part] * 4 + [whole, whole],
-        out_specs=(part,) * 3,
-    )
-    sources = {2: (keys[2], values[2]), 3: (keys[3], values[3]), 4: (key4, value4)}
-    for backs in ((2, 4), (3,)):
-        last = backs == (3,)
-        state = kernel_call(
-            functools.partial(far_kernel, backs, last),
-            [(row, BF16), (row, F32)] if last else [(row, F32)] * 3,
-            (place, query, *state, *(array for back in backs for array in sources[back])),
-            4 * rows * 512 * width * len(backs),
-            10,
-            ([(row, BF16)] if last else []) + [((512, 128 * len(backs)), BF16), ((2, 512, width), F32)],
-            grid=(rows // 128,),
-            in_specs=[SMEM] + [part] * (4 + 2 * len(backs)),
-            out_specs=(whole, part) if last else (part,) * 3,
-        )
-    attended, logs = state
+        in_specs=[SMEM, part, stat_part, part, whole, whole],
+        out_specs=(stat_part, part),
+    )
+    state = kernel_call(
+        functools.partial(far_kernel, (2, 4)),
+        outs,
+        (place, query, *state, keys[2], values[2], key4, value4),
+        4 * rows * 1024 * width,
+        10,
+        grid=(rows // 128,),
+        in_specs=[SMEM, part, stat_part] + [part] * 5,
+        out_specs=(stat_part, part),
+    )
+    attended, logs = kernel_call(
+        functools.partial(last_kernel, 3),
+        [(row, BF16), ((rows, 128), F32)],
+        (place, query, *state, keys[3], values[3]),
+        4 * rows * 512 * width,
+        12,
+    )
 
     arrived = lax.all_to_all(attended.reshape(4, rows // 4, width), "x", split_axis=0, concat_axis=0, tiled=True)
     (log_weight,) = kernel_call(log_kernel, [((heads, rows), F32)], (logs,), 6 * rows * rows * width, 8)
+    columns = depth // 4
+    piece_spec = pl.BlockSpec((piece, columns), lambda n: (0, n))
     keep, give = kernel_call(
         out_kernel,
         [((piece, depth), F32), ((piece, depth), BF16)],
         (place, arrived, out_proj, before, after, across),
         2 * rows // 8 * depth * depth,
         12,
-        [((2 * piece, depth), F32)],
+        [((2 * piece, columns), F32)],
+        grid=(4,),
+        in_specs=[SMEM, pl.BlockSpec((4, rows // 4, width), lambda n: (0, 0, 0))] + [pl.BlockSpec((width, columns), lambda n: (0, n))] * 4,
+        out_specs=(piece_spec, piece_spec),
     )
     taken = lax.ppermute(give, "c", ring(2, 1))
     (layer_out,) = kernel_call(end_kernel, [((piece, depth), BF16)], (keep, taken, post_gain[None]), 10 * piece * depth, 8)

time: 173 us -> 182 us (1.052)
  Pallas kernels: 33.5 us -> 42.1 us
    all_to_all x0 -> x1, starting transfers between devices: none -> 16.5 us  [layer(): lax.all_to_all(jnp.concatenate(copies, axis=2), ('zh', 'y'), split_axis=0...]
    all_to_all x2 -> x1, starting transfers between devices: 22 us -> 5.53 us  [spread_to(): return lax.all_to_all(copies, axis, split_axis=0, concat_axis=0, tiled=True)]
    pallas_call x11, Pallas kernels: 33.5 us -> 42.1 us  [kernel_call(): pl.pallas_call(body, out_shape=tuple((jax.ShapeDtypeStruct(s, t) for s, t...]
  transfers between devices with their start and end apart: 16 -> 16, of which waited for: 6 -> 8; matrix products, arithmetic and copies ran while one was open for 0% -> 0% of each run, Pallas kernels for 17% -> 21%
where the time goes in v6:
time: 182 us; the launch traced here: 181 us
  starting transfers between devices  85.3 us (47%)
  waiting for transfers between devices  47.1 us (26%)
  Pallas kernels  42.1 us (23%)
  local copies, waits for them, and re-layouts  3.99 us (2%)
    pallas_call x11, Pallas kernels, kernel_call(): pl.pallas_call(body, out_shape=tuple((jax.ShapeDtypeStruct(s, t) for s, t...  42.1 us
    ppermute x1, waiting for transfers between devices, layer(): fourth = lax.ppermute(eighth, SP, ring(64, 4))  32.2 us
    all_to_all x1, starting transfers between devices, layer(): lax.all_to_all(jnp.concatenate(copies, axis=2), ('zh', 'y'), split_axis=0...  16.5 us
    ppermute x3, starting transfers between devices, layer(): keys.append(lax.ppermute(keys[-1], SP, forward))  15.1 us
    ppermute x3, starting transfers between devices, layer(): values.append(lax.ppermute(values[-1], SP, forward))  12.1 us
    ppermute x1, starting transfers between devices, layer(): taken = lax.ppermute(give, 'c', ring(2, 1))  9.39 us
    ppermute x1, starting transfers between devices, layer(): fourth = lax.ppermute(eighth, SP, ring(64, 4))  7.05 us
    ppermute x1, waiting for transfers between devices, layer(): below = lax.ppermute(mine[:2], Z, ring(8, 1))  5.58 us
  transfers between devices with their start and end apart: 16, of which 8 were waited for; matrix products, arithmetic and copies ran while one was open for 0% of the time, Pallas kernels for 21%

profile of v6, /device:TPU:1, one launch (start us, length us, event | category | flops | bytes accessed | tf_op | source)
XLA Modules:
  0.0 181.2 jit_solution(10666558390076533483)
XLA Ops:
  0.6 0.8 broadcast_in_dim.13
  1.4 0.8 broadcast_in_dim.14
  2.2 0.0 copy-start
  2.2 0.0 copy-start.7
  2.2 1.1 pad_maximum_fusion
  3.3 16.5 %all-to-all-start = ((bf16[32,32,512]{2,1,0:T(8,128)(2,1)}), bf16[32,32,512]{2,1,0:T(8,128)(2,1)S(1)}, u32[]{:S(2)}, u32[]{:S(2)}) async-start(bf16[32,32,512]{2,1,0:T(8,128)(2,1)} %pad_maximum_fusion), calls=%async_computation | async-start | bytes 2097152 | tf_op jit(solution)/shard_map/all_to_all | solution.py:343
  19.8 0.0 copy-done
  19.8 0.0 copy-done.7
  19.8 0.2 shard_map.90
  20.0 7.0 %collective-permute-start.6 = (bf16[64,2048]{1,0:T(8,128)(2,1)S(1)}, bf16[64,2048]{1,0:T(8,128)(2,1)S(1)}, u32[]{:S(2)}, u32[]{:S(2)}) collective-permute-start(bf16[64,2048]{1,0:T(8,128)(2,1)S(1)} %shard_map.90), channel_id=1, source_target_pairs={{0,32},{8,40},{16,48},{24,56},{32,64},{40,72},{48,80},{56,88},{64,... | collective-permute-start | bytes 786440 | tf_op jit(solution)/shard_map/ppermute | solution.py:361
  27.0 32.2 %collective-permute-done.6 = bf16[64,2048]{1,0:T(8,128)(2,1)S(1)} collective-permute-done((bf16[64,2048]{1,0:T(8,128)(2,1)S(1)}, bf16[64,2048]{1,0:T(8,128)(2,1)S(1)}, u32[]{:S(2)}, u32[]{:S(2)}) %collective-permute-start.6) | collective-permute-done | bytes 262176 | tf_op jit(solution)/shard_map/ppermute | solution.py:361
  59.2 0.0 all-to-all-done
  59.2 1.6 broadcast_in_dim.16
  60.8 5.5 %all-to-all-start.1 = ((bf16[8,64,2048]{2,1,0:T(8,128)(2,1)}), bf16[8,64,2048]{2,1,0:T(8,128)(2,1)}, u32[]{:S(2)}, u32[]{:S(2)}) async-start(bf16[8,64,2048]{2,1,0:T(8,128)(2,1)} %broadcast_in_dim.16), calls=%async_computation.1 | async-start | bytes 4194304 | tf_op jit(solution)/shard_map/all_to_all | solution.py:328
  66.3 4.5 %collective-permute-start.10 = (bf16[256,2048]{1,0:T(8,128)(2,1)}, bf16[256,2048]{1,0:T(8,128)(2,1)}, u32[]{:S(2)}, u32[]{:S(2)}) collective-permute-start(bf16[256,2048]{1,0:T(8,128)(2,1)} %own_ref.1), channel_id=1, source_target_pairs={{0,6},{2,0},{4,2},{6,4},{1,7},{3,1},{5,3},{7,5},{8,14},{10,8},{12,... | collective-permute-start | bytes 3145736 | tf_op jit(solution)/shard_map/ppermute | solution.py:365
  70.8 2.5 %collective-permute-start.11 = (bf16[256,2048]{1,0:T(8,128)(2,1)}, bf16[256,2048]{1,0:T(8,128)(2,1)}, u32[]{:S(2)}, u32[]{:S(2)}) collective-permute-start(bf16[256,2048]{1,0:T(8,128)(2,1)} %own_ref.1), channel_id=1, source_target_pairs={{0,4},{2,6},{4,0},{6,2},{1,5},{3,7},{5,1},{7,3},{8,12},{10,14},{12... | collective-permute-start | bytes 3145736 | tf_op jit(solution)/shard_map/ppermute | solution.py:366
  73.3 2.5 %collective-permute-start.9 = (bf16[256,2048]{1,0:T(8,128)(2,1)}, bf16[256,2048]{1,0:T(8,128)(2,1)}, u32[]{:S(2)}, u32[]{:S(2)}) collective-permute-start(bf16[256,2048]{1,0:T(8,128)(2,1)} %own_ref.1), channel_id=1, source_target_pairs={{0,2},{2,4},{4,6},{6,0},{1,3},{3,5},{5,7},{7,1},{8,10},{10,12},{12... | collective-permute-start | bytes 3145736 | tf_op jit(solution)/shard_map/ppermute | solution.py:364
  75.8 0.0 copy-start.4
  75.8 0.1 fusion
  75.9 2.1 %collective-permute-start = (bf16[2,256,512]{2,1,0:T(8,128)(2,1)S(1)}, bf16[2,256,512]{2,1,0:T(8,128)(2,1)S(1)}, u32[]{:S(2)}, u32[]{:S(2)}) collective-permute-start(bf16[2,256,512]{2,1,0:T(8,128)(2,1)S(1)} %bitcast.17), channel_id=1, source_target_pairs={{0,64},{64,128},{128,192},{192,256},{256,320},{320,384},{384,448},... | collective-permute-start | bytes 1572872 | tf_op jit(solution)/shard_map/ppermute | solution.py:345
  78.0 4.6 %collective-permute-start.1 = (bf16[2,256,512]{2,1,0:T(8,128)(2,1)S(1)}, bf16[2,256,512]{2,1,0:T(8,128)(2,1)S(1)}, u32[]{:S(2)}, u32[]{:S(2)}) collective-permute-start(bf16[2,256,512]{2,1,0:T(8,128)(2,1)S(1)} %bitcast.16), channel_id=1, source_target_pairs={{0,448},{64,0},{128,64},{192,128},{256,192},{320,256},{384,320},{4... | collective-permute-start | bytes 1572872 | tf_op jit(solution)/shard_map/ppermute | solution.py:346
  82.6 0.5 multiply_cosine_fusion
  83.1 0.0 copy-done.4
  83.2 2.7 %shard_map.86 = (bf16[512,2048]{1,0:T(8,128)(2,1)S(1)}, bf16[512,256]{1,0:T(8,128)(2,1)S(1)}) custom-call(bf16[512,2048]{1,0:T(8,128)(2,1)S(1)} %copy-done, f32[1,2048]{1,0:T(1,128)S(1)} %bitcast.14, bf16[2048,256]{1,0:T(8,128)(2,1)S(1)} %copy-done.4, f32[2,32,1024]{2,1,0:T(8,128)S(1)} %pad_maximum_fusion.1.turn_ref), custom_call_target="tpu_custom_call" | custom-call | flops 536870912 | bytes 3416064 | tf_op jit(solution)/shard_map/pallas_call | solution.py:317
  85.8 0.0 copy-start.1
  85.9 0.1 pad_add_fusion.place_ref
  85.9 5.6 %collective-permute-done.below_ref = bf16[2,256,512]{2,1,0:T(8,128)(2,1)S(1)} collective-permute-done((bf16[2,256,512]{2,1,0:T(8,128)(2,1)S(1)}, bf16[2,256,512]{2,1,0:T(8,128)(2,1)S(1)}, u32[]{:S(2)}, u32[]{:S(2)}) %collective-permute-start) | collective-permute-done | bytes 524320 | tf_op jit(solution)/shard_map/ppermute | solution.py:345
  91.5 0.8 collective-permute-done.1.above_ref
  92.3 3.6 %shard_map.87 = (bf16[512,256]{1,0:T(8,128)(2,1)S(1)}, bf16[512,256]{1,0:T(8,128)(2,1)S(1)}, bf16[2048,512]{1,0:T(8,128)(2,1)S(1)}) custom-call(s32[4]{0:T(128)S(1)} %pad_add_fusion.place_ref, bf16[512,2048]{1,0:T(8,128)(2,1)S(1)} %get-tuple-element.20.normed_ref, f32[2,32,1024]{2,1,0:T(8,128)S(1)} %pad_maximum_fusion.1.turn_ref, ...), custom_call_target="tpu_custom_call" | custom-call | flops 1073741824 | bytes 4456464 | tf_op jit(solution)/shard_map/pallas_call | solution.py:317
  95.9 5.2 %collective-permute-start.2 = (bf16[512,256]{1,0:T(8,128)(2,1)S(1)}, bf16[512,256]{1,0:T(8,128)(2,1)S(1)}, u32[]{:S(2)}, u32[]{:S(2)}) collective-permute-start(bf16[512,256]{1,0:T(8,128)(2,1)S(1)} %get-tuple-element.21.k_ref), channel_id=1, source_target_pairs={{0,8},{8,16},{16,24},{24,32},{32,40},{40,48},{48,56},{56,64},{64,7... | collective-permute-start | bytes 786440 | tf_op jit(solution)/shard_map/ppermute | solution.py:403
  101.1 2.2 %collective-permute-start.3 = (bf16[512,256]{1,0:T(8,128)(2,1)S(1)}, bf16[512,256]{1,0:T(8,128)(2,1)S(1)}, u32[]{:S(2)}, u32[]{:S(2)}) collective-permute-start(bf16[512,256]{1,0:T(8,128)(2,1)S(1)} %get-tuple-element.22.v_ref), channel_id=1, source_target_pairs={{0,8},{8,16},{16,24},{24,32},{32,40},{40,48},{48,56},{56,64},{64,7... | collective-permute-start | bytes 786440 | tf_op jit(solution)/shard_map/ppermute | solution.py:404
  103.4 1.1 collective-permute-done.2.k_ref
  104.4 4.9 %collective-permute-start.4 = (bf16[512,256]{1,0:T(8,128)(2,1)S(1)}, bf16[512,256]{1,0:T(8,128)(2,1)}, u32[]{:S(2)}, u32[]{:S(2)}) collective-permute-start(bf16[512,256]{1,0:T(8,128)(2,1)S(1)} %collective-permute-done.2.k_ref), channel_id=1, source_target_pairs={{0,8},{8,16},{16,24},{24,32},{32,40},{40,48},{48,56},{56,64},{64,7... | collective-permute-start | bytes 786440 | tf_op jit(solution)/shard_map/ppermute | solution.py:403
  109.3 0.7 collective-permute-done.3.v_ref
  110.0 5.0 %collective-permute-start.5 = (bf16[512,256]{1,0:T(8,128)(2,1)S(1)}, bf16[512,256]{1,0:T(8,128)(2,1)}, u32[]{:S(2)}, u32[]{:S(2)}) collective-permute-start(bf16[512,256]{1,0:T(8,128)(2,1)S(1)} %collective-permute-done.3.v_ref), channel_id=1, source_target_pairs={{0,8},{8,16},{16,24},{24,32},{32,40},{40,48},{48,56},{56,64},{64,7... | collective-permute-start | bytes 786440 | tf_op jit(solution)/shard_map/ppermute | solution.py:404
  115.0 0.7 collective-permute-done.4.refs_0_
  115.6 4.9 %collective-permute-start.7 = (bf16[512,256]{1,0:T(8,128)(2,1)}, bf16[512,256]{1,0:T(8,128)(2,1)}, u32[]{:S(2)}, u32[]{:S(2)}) collective-permute-start(bf16[512,256]{1,0:T(8,128)(2,1)} %collective-permute-done.4.refs_0_), channel_id=1, source_target_pairs={{0,8},{8,16},{16,24},{24,32},{32,40},{40,48},{48,56},{56,64},{64,7... | collective-permute-start | bytes 786440 | tf_op jit(solution)/shard_map/ppermute | solution.py:403
  120.6 0.7 collective-permute-done.5.refs_1_
  121.2 4.9 %collective-permute-start.8 = (bf16[512,256]{1,0:T(8,128)(2,1)}, bf16[512,256]{1,0:T(8,128)(2,1)}, u32[]{:S(2)}, u32[]{:S(2)}) collective-permute-start(bf16[512,256]{1,0:T(8,128)(2,1)} %collective-permute-done.5.refs_1_), channel_id=1, source_target_pairs={{0,8},{8,16},{16,24},{24,32},{32,40},{40,48},{48,56},{56,64},{64,7... | collective-permute-start | bytes 786440 | tf_op jit(solution)/shard_map/ppermute | solution.py:404
  126.2 0.0 copy-done.1
  126.2 3.5 %shard_map.88 = (f32[512,128]{1,0:T(8,128)S(1)}, f32[512,256]{1,0:T(8,128)S(1)}) custom-call(bf16[512,256]{1,0:T(8,128)(2,1)S(1)} %get-tuple-element.19.q_ref, bf16[512,256]{1,0:T(8,128)(2,1)S(1)} %get-tuple-element.21.k_ref, bf16[512,256]{1,0:T(8,128)(2,1)S(1)} %get-tuple-element.22.v_ref), custom_call_target="tpu_custom_call" | custom-call | flops 536870912 | bytes 786432 | tf_op jit(solution)/shard_map/pallas_call | solution.py:317
  129.6 0.0 copy-start.5
  129.6 0.7 copy-done.5
  130.4 0.0 all-to-all-done.1
  130.4 4.5 %shard_map.91 = (bf16[512,256]{1,0:T(8,128)(2,1)S(1)}, bf16[512,256]{1,0:T(8,128)(2,1)S(1)}) custom-call(bf16[512,2048]{1,0:T(8,128)(2,1)} %bitcast.9.normed_ref, f32[2,32,1024]{2,1,0:T(8,128)S(1)} %pad_maximum_fusion.1.turn_ref, bf16[2048,512]{1,0:T(8,128)(2,1)S(1)} %get-tuple-element.27.weight_ref), custom_call_target="tpu_custom_call" | custom-call | flops 1073741824 | bytes 4456448 | tf_op jit(solution)/shard_map/pallas_call | solution.py:317
  134.8 0.0 copy-done.2
  134.8 0.0 copy-done.6
  134.9 7.4 %shard_map.89 = (f32[512,128]{1,0:T(8,128)S(1)}, f32[512,256]{1,0:T(8,128)S(1)}) custom-call(s32[4]{0:T(128)S(1)} %pad_add_fusion.place_ref, bf16[512,256]{1,0:T(8,128)(2,1)S(1)} %copy-done.2, f32[512,128]{1,0:T(8,128)S(1)} %copy-done.6, f32[512,256]{1,0:T(8,128)S(1)} %get-tuple-element.24.acc_ref, bf16[512,256]{1,0:T(8,128)(2,1)S(1)} %collective-permute-done.2.k_ref, ...), custom_call_target="tpu_custom_call" | custom-call | flops 268435456 | bytes 1572880 | tf_op jit(solution)/shard_map/pallas_call | solution.py:317
  142.3 0.0 copy-start.3
  142.3 7.7 %shard_map.92 = (f32[512,128]{1,0:T(8,128)S(1)}, f32[512,256]{1,0:T(8,128)S(1)}) custom-call(s32[4]{0:T(128)S(1)} %pad_add_fusion.place_ref, bf16[512,256]{1,0:T(8,128)(2,1)S(1)} %copy-done.2, f32[512,128]{1,0:T(8,128)S(1)} %get-tuple-element.25.stat_ref, f32[512,256]{1,0:T(8,128)S(1)} %get-tuple-element.26.acc_ref, ...), custom_call_target="tpu_custom_call" | custom-call | flops 536870912 | bytes 2097168 | tf_op jit(solution)/shard_map/pallas_call | solution.py:317
  150.0 0.0 collective-permute-done.7.k_ref
  150.0 0.0 collective-permute-done.8.v_ref
  150.0 7.1 %shard_map.93 = (bf16[512,256]{1,0:T(8,128)(2,1)}, f32[512,128]{1,0:T(8,128)S(1)}) custom-call(s32[4]{0:T(128)S(1)} %pad_add_fusion.place_ref, bf16[512,256]{1,0:T(8,128)(2,1)S(1)} %copy-done.2, f32[512,128]{1,0:T(8,128)S(1)} %get-tuple-element.30.stat_ref, f32[512,256]{1,0:T(8,128)S(1)} %get-tuple-element.31.acc_ref, ...), custom_call_target="tpu_custom_call" | custom-call | flops 268435456 | bytes 1572880 | tf_op jit(solution)/shard_map/pallas_call | solution.py:317
  157.0 3.7 %all-to-all-start.2 = ((bf16[4,128,256]{2,1,0:T(8,128)(2,1)}), bf16[4,128,256]{2,1,0:T(8,128)(2,1)S(1)}, u32[]{:S(2)}, u32[]{:S(2)}) async-start(bf16[4,128,256]{2,1,0:T(8,128)(2,1)} %bitcast.10), calls=%async_computation.2 | async-start | bytes 524288 | tf_op jit(solution)/shard_map/all_to_all | solution.py:460
  160.7 0.0 collective-permute-done.10.after_ref
  160.7 0.0 collective-permute-done.11.across_ref
  160.7 0.0 collective-permute-done.9.before_ref
  160.7 5.5 %all-to-all-done.2.att_ref = bf16[4,128,256]{2,1,0:T(8,128)(2,1)S(1)} async-done(((bf16[4,128,256]{2,1,0:T(8,128)(2,1)}), bf16[4,128,256]{2,1,0:T(8,128)(2,1)S(1)}, u32[]{:S(2)}, u32[]{:S(2)}) %all-to-all-start.2) | async-done | bytes 262176 | tf_op jit(solution)/shard_map/all_to_all | solution.py:460
  166.2 0.0 copy-done.3
  166.2 3.5 %shard_map.94 = (f32[64,2048]{1,0:T(8,128)S(1)}, bf16[64,2048]{1,0:T(8,128)(2,1)S(1)}) custom-call(s32[4]{0:T(128)S(1)} %pad_add_fusion.place_ref, bf16[4,128,256]{2,1,0:T(8,128)(2,1)S(1)} %all-to-all-done.2.att_ref, bf16[256,2048]{1,0:T(8,128)(2,1)S(1)} %copy-done.3, bf16[256,2048]{1,0:T(8,128)(2,1)} %collective-permute-done.9.before_ref, ...), custom_call_target="tpu_custom_call" | custom-call | flops 536870912 | bytes 4456464 | tf_op jit(solution)/shard_map/pallas_call | solution.py:317
  169.7 9.4 %collective-permute-start.12 = (bf16[64,2048]{1,0:T(8,128)(2,1)S(1)}, bf16[64,2048]{1,0:T(8,128)(2,1)S(1)}, u32[]{:S(2)}, u32[]{:S(2)}) collective-permute-start(bf16[64,2048]{1,0:T(8,128)(2,1)S(1)} %get-tuple-element.34), channel_id=1, source_target_pairs={{0,1},{1,0},{2,3},{3,2},{4,5},{5,4},{6,7},{7,6},{8,9},{9,8},{10,11... | collective-permute-start | bytes 786440 | tf_op jit(solution)/shard_map/ppermute | solution.py:475
  179.1 1.2 shard_map.96
  180.3 0.0 collective-permute-done.12.taken_ref
  180.3 0.9 shard_map.95
  (8 shorter events, 0.1 us)
Async XLA Ops:
  2.2 17.6 %copy-start = (bf16[512,2048]{1,0:T(8,128)(2,1)S(1)}, bf16[512,2048]{1,0:T(8,128)(2,1)}, u32[]{:S(2)}) copy-start(bf16[512,2048]{1,0:T(8,128)(2,1)} %hidden_ref.3) | copy-start | bytes 6291460
  2.2 17.6 %copy-start.7 = (f32[2048]{0:T(1024)S(1)}, f32[2048]{0:T(1024)}, u32[]{:S(2)}) copy-start(f32[2048]{0:T(1024)} %param.8) | copy-start | bytes 24580
  3.3 55.9 %all-to-all-start = ((bf16[32,32,512]{2,1,0:T(8,128)(2,1)}), bf16[32,32,512]{2,1,0:T(8,128)(2,1)S(1)}, u32[]{:S(2)}, u32[]{:S(2)}) async-start(bf16[32,32,512]{2,1,0:T(8,128)(2,1)} %pad_maximum_fusion), calls=%async_computation | async-start | bytes 2097152 | tf_op jit(solution)/shard_map/all_to_all | solution.py:343
  20.0 39.2 %collective-permute-start.6 = (bf16[64,2048]{1,0:T(8,128)(2,1)S(1)}, bf16[64,2048]{1,0:T(8,128)(2,1)S(1)}, u32[]{:S(2)}, u32[]{:S(2)}) collective-permute-start(bf16[64,2048]{1,0:T(8,128)(2,1)S(1)} %shard_map.90), channel_id=1, source_target_pairs={{0,32},{8,40},{16,48},{24,56},{32,64},{40,72},{48,80},{56,88},{64,... | collective-permute-start | bytes 786440 | tf_op jit(solution)/shard_map/ppermute | solution.py:361
  60.8 69.6 %all-to-all-start.1 = ((bf16[8,64,2048]{2,1,0:T(8,128)(2,1)}), bf16[8,64,2048]{2,1,0:T(8,128)(2,1)}, u32[]{:S(2)}, u32[]{:S(2)}) async-start(bf16[8,64,2048]{2,1,0:T(8,128)(2,1)} %broadcast_in_dim.16), calls=%async_computation.1 | async-start | bytes 4194304 | tf_op jit(solution)/shard_map/all_to_all | solution.py:328
  66.3 94.4 %collective-permute-start.10 = (bf16[256,2048]{1,0:T(8,128)(2,1)}, bf16[256,2048]{1,0:T(8,128)(2,1)}, u32[]{:S(2)}, u32[]{:S(2)}) collective-permute-start(bf16[256,2048]{1,0:T(8,128)(2,1)} %own_ref.1), channel_id=1, source_target_pairs={{0,6},{2,0},{4,2},{6,4},{1,7},{3,1},{5,3},{7,5},{8,14},{10,8},{12,... | collective-permute-start | bytes 3145736 | tf_op jit(solution)/shard_map/ppermute | solution.py:365
  70.8 89.9 %collective-permute-start.11 = (bf16[256,2048]{1,0:T(8,128)(2,1)}, bf16[256,2048]{1,0:T(8,128)(2,1)}, u32[]{:S(2)}, u32[]{:S(2)}) collective-permute-start(bf16[256,2048]{1,0:T(8,128)(2,1)} %own_ref.1), channel_id=1, source_target_pairs={{0,4},{2,6},{4,0},{6,2},{1,5},{3,7},{5,1},{7,3},{8,12},{10,14},{12... | collective-permute-start | bytes 3145736 | tf_op jit(solution)/shard_map/ppermute | solution.py:366
  73.3 87.4 %collective-permute-start.9 = (bf16[256,2048]{1,0:T(8,128)(2,1)}, bf16[256,2048]{1,0:T(8,128)(2,1)}, u32[]{:S(2)}, u32[]{:S(2)}) collective-permute-start(bf16[256,2048]{1,0:T(8,128)(2,1)} %own_ref.1), channel_id=1, source_target_pairs={{0,2},{2,4},{4,6},{6,0},{1,3},{3,5},{5,7},{7,1},{8,10},{10,12},{12... | collective-permute-start | bytes 3145736 | tf_op jit(solution)/shard_map/ppermute | solution.py:364
  75.8 7.4 %copy-start.4 = (bf16[2048,256]{1,0:T(8,128)(2,1)S(1)}, bf16[2048,256]{1,0:T(8,128)(2,1)}, u32[]{:S(2)}) copy-start(bf16[2048,256]{1,0:T(8,128)(2,1)} %weight_ref.1) | copy-start | bytes 3145732
  75.9 15.6 %collective-permute-start = (bf16[2,256,512]{2,1,0:T(8,128)(2,1)S(1)}, bf16[2,256,512]{2,1,0:T(8,128)(2,1)S(1)}, u32[]{:S(2)}, u32[]{:S(2)}) collective-permute-start(bf16[2,256,512]{2,1,0:T(8,128)(2,1)S(1)} %bitcast.17), channel_id=1, source_target_pairs={{0,64},{64,128},{128,192},{192,256},{256,320},{320,384},{384,448},... | collective-permute-start | bytes 1572872 | tf_op jit(solution)/shard_map/ppermute | solution.py:345
  78.0 14.3 %collective-permute-start.1 = (bf16[2,256,512]{2,1,0:T(8,128)(2,1)S(1)}, bf16[2,256,512]{2,1,0:T(8,128)(2,1)S(1)}, u32[]{:S(2)}, u32[]{:S(2)}) collective-permute-start(bf16[2,256,512]{2,1,0:T(8,128)(2,1)S(1)} %bitcast.16), channel_id=1, source_target_pairs={{0,448},{64,0},{128,64},{192,128},{256,192},{320,256},{384,320},{4... | collective-permute-start | bytes 1572872 | tf_op jit(solution)/shard_map/ppermute | solution.py:346
  85.8 40.3 %copy-start.1 = (bf16[512,256]{1,0:T(8,128)(2,1)}, bf16[512,256]{1,0:T(8,128)(2,1)S(1)}, u32[]{:S(2)}) copy-start(bf16[512,256]{1,0:T(8,128)(2,1)S(1)} %get-tuple-element.19.q_ref) | copy-start | bytes 786436
  95.9 8.5 %collective-permute-start.2 = (bf16[512,256]{1,0:T(8,128)(2,1)S(1)}, bf16[512,256]{1,0:T(8,128)(2,1)S(1)}, u32[]{:S(2)}, u32[]{:S(2)}) collective-permute-start(bf16[512,256]{1,0:T(8,128)(2,1)S(1)} %get-tuple-element.21.k_ref), channel_id=1, source_target_pairs={{0,8},{8,16},{16,24},{24,32},{32,40},{40,48},{48,56},{56,64},{64,7... | collective-permute-start | bytes 786440 | tf_op jit(solution)/shard_map/ppermute | solution.py:403
  101.1 8.9 %collective-permute-start.3 = (bf16[512,256]{1,0:T(8,128)(2,1)S(1)}, bf16[512,256]{1,0:T(8,128)(2,1)S(1)}, u32[]{:S(2)}, u32[]{:S(2)}) collective-permute-start(bf16[512,256]{1,0:T(8,128)(2,1)S(1)} %get-tuple-element.22.v_ref), channel_id=1, source_target_pairs={{0,8},{8,16},{16,24},{24,32},{32,40},{40,48},{48,56},{56,64},{64,7... | collective-permute-start | bytes 786440 | tf_op jit(solution)/shard_map/ppermute | solution.py:404
  104.4 11.2 %collective-permute-start.4 = (bf16[512,256]{1,0:T(8,128)(2,1)S(1)}, bf16[512,256]{1,0:T(8,128)(2,1)}, u32[]{:S(2)}, u32[]{:S(2)}) collective-permute-start(bf16[512,256]{1,0:T(8,128)(2,1)S(1)} %collective-permute-done.2.k_ref), channel_id=1, source_target_pairs={{0,8},{8,16},{16,24},{24,32},{32,40},{40,48},{48,56},{56,64},{64,7... | collective-permute-start | bytes 786440 | tf_op jit(solution)/shard_map/ppermute | solution.py:403
  110.0 11.2 %collective-permute-start.5 = (bf16[512,256]{1,0:T(8,128)(2,1)S(1)}, bf16[512,256]{1,0:T(8,128)(2,1)}, u32[]{:S(2)}, u32[]{:S(2)}) collective-permute-start(bf16[512,256]{1,0:T(8,128)(2,1)S(1)} %collective-permute-done.3.v_ref), channel_id=1, source_target_pairs={{0,8},{8,16},{16,24},{24,32},{32,40},{40,48},{48,56},{56,64},{64,7... | collective-permute-start | bytes 786440 | tf_op jit(solution)/shard_map/ppermute | solution.py:404
  115.6 34.3 %collective-permute-start.7 = (bf16[512,256]{1,0:T(8,128)(2,1)}, bf16[512,256]{1,0:T(8,128)(2,1)}, u32[]{:S(2)}, u32[]{:S(2)}) collective-permute-start(bf16[512,256]{1,0:T(8,128)(2,1)} %collective-permute-done.4.refs_0_), channel_id=1, source_target_pairs={{0,8},{8,16},{16,24},{24,32},{32,40},{40,48},{48,56},{56,64},{64,7... | collective-permute-start | bytes 786440 | tf_op jit(solution)/shard_map/ppermute | solution.py:403
  121.2 28.7 %collective-permute-start.8 = (bf16[512,256]{1,0:T(8,128)(2,1)}, bf16[512,256]{1,0:T(8,128)(2,1)}, u32[]{:S(2)}, u32[]{:S(2)}) collective-permute-start(bf16[512,256]{1,0:T(8,128)(2,1)} %collective-permute-done.5.refs_1_), channel_id=1, source_target_pairs={{0,8},{8,16},{16,24},{24,32},{32,40},{40,48},{48,56},{56,64},{64,7... | collective-permute-start | bytes 786440 | tf_op jit(solution)/shard_map/ppermute | solution.py:404
  129.6 0.7 copy-start.5
  130.4 4.5 %copy-start.2 = (bf16[512,256]{1,0:T(8,128)(2,1)S(1)}, bf16[512,256]{1,0:T(8,128)(2,1)}, u32[]{:S(2)}) copy-start(bf16[512,256]{1,0:T(8,128)(2,1)} %copy-done.1) | copy-start | bytes 786436
  130.4 4.5 %copy-start.6 = (f32[512,128]{1,0:T(8,128)S(1)}, f32[512,128]{1,0:T(8,128)}, u32[]{:S(2)}) copy-start(f32[512,128]{1,0:T(8,128)} %copy-done.5) | copy-start | bytes 786436
  142.3 24.0 %copy-start.3 = (bf16[256,2048]{1,0:T(8,128)(2,1)S(1)}, bf16[256,2048]{1,0:T(8,128)(2,1)}, u32[]{:S(2)}) copy-start(bf16[256,2048]{1,0:T(8,128)(2,1)} %own_ref.1) | copy-start | bytes 3145732
  157.0 9.2 %all-to-all-start.2 = ((bf16[4,128,256]{2,1,0:T(8,128)(2,1)}), bf16[4,128,256]{2,1,0:T(8,128)(2,1)S(1)}, u32[]{:S(2)}, u32[]{:S(2)}) async-start(bf16[4,128,256]{2,1,0:T(8,128)(2,1)} %bitcast.10), calls=%async_computation.2 | async-start | bytes 524288 | tf_op jit(solution)/shard_map/all_to_all | solution.py:460
  160.7 19.6 %copy-start.8 = (f32[2048]{0:T(1024)S(1)}, f32[2048]{0:T(1024)}, u32[]{:S(2)}) copy-start(f32[2048]{0:T(1024)} %param.13) | copy-start | bytes 24580
  169.7 10.6 %collective-permute-start.12 = (bf16[64,2048]{1,0:T(8,128)(2,1)S(1)}, bf16[64,2048]{1,0:T(8,128)(2,1)S(1)}, u32[]{:S(2)}, u32[]{:S(2)}) collective-permute-start(bf16[64,2048]{1,0:T(8,128)(2,1)S(1)} %get-tuple-element.34), channel_id=1, source_target_pairs={{0,1},{1,0},{2,3},{3,2},{4,5},{5,4},{6,7},{7,6},{8,9},{9,8},{10,11... | collective-permute-start | bytes 786440 | tf_op jit(solution)/shard_map/ppermute | solution.py:475

commit v7 on v5

--- a/solution.py
+++ b/solution.py
@@ -88,31 +88,41 @@
     query_ref[...] = permuted(to_residue(rows), query)
 
 
-def project(normed, weight_ref, cos, sin, key_ref, value_ref):
+def project(normed_ref, turn_ref, weight_ref, key_ref, value_ref, both_ref):
     rows, width = key_ref.shape
-    perm = to_residue(rows)
-    key = jnp.dot(normed, weight_ref[:, :width], preferred_element_type=F32)
-    key_ref[...] = permuted(perm, rotated(key, cos, sin).astype(BF16))
-    value = jnp.dot(normed, weight_ref[:, width:], preferred_element_type=F32).astype(BF16)
-    value_ref[...] = permuted(perm, value)
-
-
-def key_value_kernel(place_ref, normed_ref, mine_ref, below_ref, above_ref, turn_ref, key_ref, value_ref, weight_ref):
-    rows = normed_ref.shape[0]
-    low = place_ref[1]
-    slabs = []
-    for k in range(4):
-        slabs.append((2 * k + low, mine_ref, k))
-    for k in range(2):
-        slabs.append((2 * k + 1 - low, below_ref, k))
-        slabs.append((2 * (k + 2) + 1 - low, above_ref, k))
-    for place, ref, k in slabs:
-        weight_ref[pl.ds(pl.multiple_of(place * 256, 256), 256), :] = ref[k]
-    project(normed_ref[...], weight_ref, *spread(turn_ref, slice(rows, 2 * rows)), key_ref, value_ref)
-
-
-def far_key_value_kernel(normed_ref, weight_ref, turn_ref, key_ref, value_ref):
-    project(normed_ref[...], weight_ref, *spread(turn_ref, slice(0, normed_ref.shape[0])), key_ref, value_ref)
+    block = normed_ref.shape[0]
+    n = pl.program_id(0)
+    cos, sin = spread(turn_ref, slice(0, block))
+    both = jnp.dot(normed_ref[...], weight_ref[...], preferred_element_type=F32)
+    part = pl.ds(pl.multiple_of(n * block, block), block)
+    both_ref[part, :width] = rotated(both[:, :width], cos, sin).astype(BF16)
+    both_ref[part, width:] = both[:, width:].astype(BF16)
+
+    @pl.when(n == pl.num_programs(0) - 1)
+    def _():
+        ordered = permuted(to_residue(rows), both_ref[...])
+        key_ref[...] = ordered[:, :width]
+        value_ref[...] = ordered[:, width:]
+
+
+def key_value_kernel(place_ref, normed_ref, turn_ref, mine_ref, below_ref, above_ref, key_ref, value_ref, weight_ref, both_ref):
+    @pl.when(pl.program_id(0) == 0)
+    def _():
+        low = place_ref[1]
+        slabs = []
+        for k in range(4):
+            slabs.append((2 * k + low, mine_ref, k))
+        for k in range(2):
+            slabs.append((2 * k + 1 - low, below_ref, k))
+            slabs.append((2 * (k + 2) + 1 - low, above_ref, k))
+        for place, ref, k in slabs:
+            weight_ref[pl.ds(pl.multiple_of(place * 256, 256), 256), :] = ref[k]
+
+    project(normed_ref, turn_ref, weight_ref, key_ref, value_ref, both_ref)
+
+
+def far_key_value_kernel(normed_ref, turn_ref, weight_ref, key_ref, value_ref, both_ref):
+    project(normed_ref, turn_ref, weight_ref, key_ref, value_ref, both_ref)
 
 
 def stack_heads(q):
@@ -174,11 +184,12 @@
     acc_ref[...] = own_heads(pv)
 
 
-def merged(scores, bias, count, value, max_ref, sum_ref, acc_ref, p_ref, stat_ref):
+def merged(q, key, value, bias, count, max_ref, sum_ref, acc_ref, s_ref, p_ref, stat_ref):
     width = max_ref.shape[1]
+    s_ref[...] = lax.dot_general(stack_heads(q), key, NT, preferred_element_type=F32)
     for h in range(width // HEAD_DIM):
         part = slice(h * 128, (h + 1) * 128)
-        s = scores[part] + bias
+        s = s_ref[part, :] + bias
         m = jnp.maximum(jnp.max(s, axis=1, keepdims=True), max_ref[:, h * HEAD_DIM : h * HEAD_DIM + 1])
         p = jnp.exp(s - m)
         if count is not None:
@@ -193,7 +204,7 @@
     return m, total, acc_ref[...] * alpha + own_heads(pv)
 
 
-def before_kernel(place_ref, q_ref, max_ref, sum_ref, acc_ref, k_ref, v_ref, new_max, new_sum, new_acc, p_ref, stat_ref, tail_ref):
+def before_kernel(place_ref, q_ref, max_ref, sum_ref, acc_ref, k_ref, v_ref, new_max, new_sum, new_acc, s_ref, p_ref, stat_ref, tail_ref):
     cls = pl.program_id(0)
     keys = k_ref.shape[0]
     mine = pl.ds(pl.multiple_of(cls * 128, 128), 128)
@@ -216,8 +227,7 @@
     bias = jnp.where(count > 0, 0.0, LOW).astype(F32)
     key = jnp.concatenate([k_ref[mine, :], tail_ref[0]], axis=0)
     value = jnp.concatenate([v_ref[mine, :], tail_ref[1]], axis=0)
-    scores = lax.dot_general(stack_heads(q_ref[...]), key, NT, preferred_element_type=F32)
-    state = merged(scores, bias, count, value, max_ref, sum_ref, acc_ref, p_ref, stat_ref)
+    state = merged(q_ref[...], key, value, bias, count, max_ref, sum_ref, acc_ref, s_ref, p_ref, stat_ref)
     for ref, part in zip((new_max, new_sum, new_acc), state):
         ref[...] = part
 
@@ -225,12 +235,11 @@
 def far_kernel(backs, last, place_ref, q_ref, max_ref, sum_ref, acc_ref, *refs):
     count = len(backs)
     sources, outs = refs[: 2 * count], refs[2 * count :]
-    p_ref, stat_ref = outs[-2:]
+    s_ref, p_ref, stat_ref = outs[-3:]
     bias = jnp.concatenate([far_bias(place_ref[0], back) for back in backs], axis=1)
     key = jnp.concatenate([ref[...] for ref in sources[0::2]], axis=0)
     value = jnp.concatenate([ref[...] for ref in sources[1::2]], axis=0)
-    scores = lax.dot_general(stack_heads(q_ref[...]), key, NT, preferred_element_type=F32)
-    m, total, acc = merged(scores, bias, None, value, max_ref, sum_ref, acc_ref, p_ref, stat_ref)
+    m, total, acc = merged(q_ref[...], key, value, bias, None, max_ref, sum_ref, acc_ref, s_ref, p_ref, stat_ref)
     if last:
         cls = pl.program_id(0)
         out_ref, log_ref, att_ref = outs[:3]
@@ -262,13 +271,12 @@
 def out_kernel(place_ref, att_ref, own_ref, before_ref, after_ref, across_ref, keep_ref, give_ref, sum_ref):
     x, core = place_ref[2], place_ref[3]
     rows = keep_ref.shape[0]
+    total = None
     for n, ref in enumerate((own_ref, before_ref, after_ref, across_ref)):
         part = jnp.dot(att_ref[lax.rem(x + HOPS[n], 4)], ref[...], preferred_element_type=F32)
         part = part.astype(BF16).astype(F32)
-        if n == 0:
-            sum_ref[...] = part
-        else:
-            sum_ref[...] += part
+        total = part if total is None else total + part
+    sum_ref[...] = total
     keep_ref[...] = sum_ref[pl.ds(pl.multiple_of(core * rows, rows), rows), :]
     give_ref[...] = sum_ref[pl.ds(pl.multiple_of((1 - core) * rows, rows), rows), :].astype(BF16)
 
@@ -315,8 +323,9 @@
     gain = pre_gain[None]
     row = (rows, width)
 
-    shard = jnp.concatenate([key_proj, value_proj], axis=1)
-    mine = spread_to(shard, ("zh", "y"), 32).reshape(4, 256, 2 * width)
+    copies = [jnp.broadcast_to(shard[None], (32,) + shard.shape) for shard in (key_proj, value_proj)]
+    mine = lax.all_to_all(jnp.concatenate(copies, axis=2), ("zh", "y"), split_axis=0, concat_axis=0, tiled=True)
+    mine = mine.reshape(4, 256, 2 * width)
     below = lax.ppermute(mine[:2], Z, ring(8, 1))
     above = lax.ppermute(mine[2:], Z, ring(8, -1))
 
@@ -350,12 +359,27 @@
     normed, query = kernel_call(
         query_kernel, [((rows, depth), BF16), (row, BF16)], (hidden_in, gain, query_proj, turns), 2 * rows * depth * width, 12
     )
+    block_rows = rows // 4
+    row_part = pl.BlockSpec((block_rows, depth), lambda n: (n, 0))
+    whole = pl.BlockSpec(row, lambda c: (0, 0))
+    weight_spec = pl.BlockSpec((depth, 2 * width), lambda n: (0, 0))
     key, value, weights = kernel_call(
         key_value_kernel,
         [(row, BF16), (row, BF16), ((depth, 2 * width), BF16)],
-        (place, normed, mine, below, above, turns),
+        (place, normed, turns, mine, below, above),
         4 * rows * depth * width,
-        12,
+        14,
+        [((rows, 2 * width), BF16)],
+        grid=(4,),
+        in_specs=[
+            SMEM,
+            row_part,
+            pl.BlockSpec((2, HEAD_DIM // 2, block_rows), lambda n: (0, 0, 4 + n)),
+            pl.BlockSpec((4, 256, 2 * width), lambda n: (0, 0, 0)),
+            pl.BlockSpec((2, 256, 2 * width), lambda n: (0, 0, 0)),
+            pl.BlockSpec((2, 256, 2 * width), lambda n: (0, 0, 0)),
+        ],
+        out_specs=(whole, whole, weight_spec),
     )
     forward = [(i, i + 1) for i in range(63)]
     keys, values = [key], [value]
@@ -363,12 +387,19 @@
         keys.append(lax.ppermute(keys[-1], SP, forward))
         values.append(lax.ppermute(values[-1], SP, forward))
     key4, value4 = kernel_call(
-        far_key_value_kernel, [(row, BF16)] * 2, (far_rows, weights, turns), 4 * rows * depth * width, 10
-    )
-
-    whole = pl.BlockSpec(row, lambda c: (0, 0))
+        far_key_value_kernel,
+        [(row, BF16)] * 2,
+        (far_rows, turns, weights),
+        4 * rows * depth * width,
+        14,
+        [((rows, 2 * width), BF16)],
+        grid=(4,),
+        in_specs=[row_part, pl.BlockSpec((2, HEAD_DIM // 2, block_rows), lambda n: (0, 0, n)), weight_spec],
+        out_specs=(whole, whole),
+    )
+
     part = pl.BlockSpec((128, width), lambda c: (c, 0))
-    pair = ((512, 256), BF16), ((2, 512, width), F32)
+    pair = ((512, 256), F32), ((512, 256), BF16), ((2, 512, width), F32)
     state = kernel_call(
         own_kernel,
         [(row, F32)] * 3,
@@ -400,7 +431,7 @@
             (place, query, *state, *(array for back in backs for array in sources[back])),
             4 * rows * 512 * width * len(backs),
             10,
-            ([(row, BF16)] if last else []) + [((512, 128 * len(backs)), BF16), ((2, 512, width), F32)],
+            ([(row, BF16)] if last else []) + [((512, 128 * len(backs)), t) for t in (F32, BF16)] + [((2, 512, width), F32)],
             grid=(rows // 128,),
             in_specs=[SMEM] + [part] * (4 + 2 * len(backs)),
             out_specs=(whole, part) if last else (part,) * 3,
@@ -409,13 +440,18 @@
 
     arrived = lax.all_to_all(attended.reshape(4, rows // 4, width), "x", split_axis=0, concat_axis=0, tiled=True)
     (log_weight,) = kernel_call(log_kernel, [((heads, rows), F32)], (logs,), 6 * rows * rows * width, 8)
+    columns = depth // 4
+    piece_spec = pl.BlockSpec((piece, columns), lambda n: (0, n))
     keep, give = kernel_call(
         out_kernel,
         [((piece, depth), F32), ((piece, depth), BF16)],
         (place, arrived, out_proj, before, after, across),
         2 * rows // 8 * depth * depth,
         12,
-        [((2 * piece, depth), F32)],
+        [((2 * piece, columns), F32)],
+        grid=(4,),
+        in_specs=[SMEM, pl.BlockSpec((4, rows // 4, width), lambda n: (0, 0, 0))] + [pl.BlockSpec((width, columns), lambda n: (0, n))] * 4,
+        out_specs=(piece_spec, piece_spec),
     )
     taken = lax.ppermute(give, "c", ring(2, 1))
     (layer_out,) = kernel_call(end_kernel, [((piece, depth), BF16)], (keep, taken, post_gain[None]), 10 * piece * depth, 8)

time: 173 us -> 174 us (level)
    all_to_all x0 -> x1, starting transfers between devices: none -> 16.5 us  [layer(): lax.all_to_all(jnp.concatenate(copies, axis=2), ('zh', 'y'), split_axis=0...]
    all_to_all x2 -> x1, starting transfers between devices: 22 us -> 5.53 us  [spread_to(): return lax.all_to_all(copies, axis, split_axis=0, concat_axis=0, tiled=True)]
where the time goes in v7:
time: 174 us; the launch traced here: 173 us
  starting transfers between devices  85.2 us (49%)
  waiting for transfers between devices  45.8 us (26%)
  Pallas kernels  33.6 us (19%)
  local copies, waits for them, and re-layouts  5.53 us (3%)
  other arithmetic  1.74 us (1%)
    pallas_call x11, Pallas kernels, kernel_call(): pl.pallas_call(body, out_shape=tuple((jax.ShapeDtypeStruct(s, t) for s, t...  33.6 us
    ppermute x1, waiting for transfers between devices, layer(): fourth = lax.ppermute(eighth, SP, ring(64, 4))  32.2 us
    all_to_all x1, starting transfers between devices, layer(): lax.all_to_all(jnp.concatenate(copies, axis=2), ('zh', 'y'), split_axis=0...  16.5 us
    ppermute x3, starting transfers between devices, layer(): keys.append(lax.ppermute(keys[-1], SP, forward))  15.1 us
    ppermute x3, starting transfers between devices, layer(): values.append(lax.ppermute(values[-1], SP, forward))  12 us
    ppermute x1, starting transfers between devices, layer(): taken = lax.ppermute(give, 'c', ring(2, 1))  9.37 us
    ppermute x1, starting transfers between devices, layer(): fourth = lax.ppermute(eighth, SP, ring(64, 4))  7.05 us
    ppermute x1, waiting for transfers between devices, layer(): below = lax.ppermute(mine[:2], Z, ring(8, 1))  5.58 us
  transfers between devices with their start and end apart: 16, of which 6 were waited for; matrix products, arithmetic and copies ran while one was open for 0% of the time, Pallas kernels for 17%

profile of v7, /device:TPU:1, one launch (start us, length us, event | category | flops | bytes accessed | tf_op | source)
XLA Modules:
  0.0 172.9 jit_solution(14849999005069325389)
XLA Ops:
  0.6 0.8 broadcast_in_dim.13
  1.4 0.8 broadcast_in_dim.14
  2.2 0.0 copy-start
  2.2 0.0 copy-start.11
  2.2 1.1 pad_maximum_fusion
  3.3 16.5 %all-to-all-start = ((bf16[32,32,512]{2,1,0:T(8,128)(2,1)}), bf16[32,32,512]{2,1,0:T(8,128)(2,1)S(1)}, u32[]{:S(2)}, u32[]{:S(2)}) async-start(bf16[32,32,512]{2,1,0:T(8,128)(2,1)} %pad_maximum_fusion), calls=%async_computation | async-start | bytes 2097152 | tf_op jit(solution)/shard_map/all_to_all | solution.py:327
  19.8 0.0 copy-done
  19.8 0.0 copy-done.11
  19.8 0.2 shard_map.90
  20.0 7.0 %collective-permute-start.6 = (bf16[64,2048]{1,0:T(8,128)(2,1)S(1)}, bf16[64,2048]{1,0:T(8,128)(2,1)S(1)}, u32[]{:S(2)}, u32[]{:S(2)}) collective-permute-start(bf16[64,2048]{1,0:T(8,128)(2,1)S(1)} %shard_map.90), channel_id=1, source_target_pairs={{0,32},{8,40},{16,48},{24,56},{32,64},{40,72},{48,80},{56,88},{64,... | collective-permute-start | bytes 786440 | tf_op jit(solution)/shard_map/ppermute | solution.py:345
  27.0 32.2 %collective-permute-done.6 = bf16[64,2048]{1,0:T(8,128)(2,1)S(1)} collective-permute-done((bf16[64,2048]{1,0:T(8,128)(2,1)S(1)}, bf16[64,2048]{1,0:T(8,128)(2,1)S(1)}, u32[]{:S(2)}, u32[]{:S(2)}) %collective-permute-start.6) | collective-permute-done | bytes 262176 | tf_op jit(solution)/shard_map/ppermute | solution.py:345
  59.2 0.0 all-to-all-done
  59.2 1.6 broadcast_in_dim.16
  60.8 5.5 %all-to-all-start.1 = ((bf16[8,64,2048]{2,1,0:T(8,128)(2,1)}), bf16[8,64,2048]{2,1,0:T(8,128)(2,1)}, u32[]{:S(2)}, u32[]{:S(2)}) async-start(bf16[8,64,2048]{2,1,0:T(8,128)(2,1)} %broadcast_in_dim.16), calls=%async_computation.1 | async-start | bytes 4194304 | tf_op jit(solution)/shard_map/all_to_all | solution.py:312
  66.3 4.5 %collective-permute-start.10 = (bf16[256,2048]{1,0:T(8,128)(2,1)}, bf16[256,2048]{1,0:T(8,128)(2,1)}, u32[]{:S(2)}, u32[]{:S(2)}) collective-permute-start(bf16[256,2048]{1,0:T(8,128)(2,1)} %own_ref.1), channel_id=1, source_target_pairs={{0,6},{2,0},{4,2},{6,4},{1,7},{3,1},{5,3},{7,5},{8,14},{10,8},{12,... | collective-permute-start | bytes 3145736 | tf_op jit(solution)/shard_map/ppermute | solution.py:349
  70.8 2.5 %collective-permute-start.11 = (bf16[256,2048]{1,0:T(8,128)(2,1)}, bf16[256,2048]{1,0:T(8,128)(2,1)}, u32[]{:S(2)}, u32[]{:S(2)}) collective-permute-start(bf16[256,2048]{1,0:T(8,128)(2,1)} %own_ref.1), channel_id=1, source_target_pairs={{0,4},{2,6},{4,0},{6,2},{1,5},{3,7},{5,1},{7,3},{8,12},{10,14},{12... | collective-permute-start | bytes 3145736 | tf_op jit(solution)/shard_map/ppermute | solution.py:350
  73.3 2.5 %collective-permute-start.9 = (bf16[256,2048]{1,0:T(8,128)(2,1)}, bf16[256,2048]{1,0:T(8,128)(2,1)}, u32[]{:S(2)}, u32[]{:S(2)}) collective-permute-start(bf16[256,2048]{1,0:T(8,128)(2,1)} %own_ref.1), channel_id=1, source_target_pairs={{0,2},{2,4},{4,6},{6,0},{1,3},{3,5},{5,7},{7,1},{8,10},{10,12},{12... | collective-permute-start | bytes 3145736 | tf_op jit(solution)/shard_map/ppermute | solution.py:348
  75.8 0.0 copy-start.4
  75.8 0.1 fusion
  75.9 2.1 %collective-permute-start = (bf16[2,256,512]{2,1,0:T(8,128)(2,1)S(1)}, bf16[2,256,512]{2,1,0:T(8,128)(2,1)S(1)}, u32[]{:S(2)}, u32[]{:S(2)}) collective-permute-start(bf16[2,256,512]{2,1,0:T(8,128)(2,1)S(1)} %bitcast.17), channel_id=1, source_target_pairs={{0,64},{64,128},{128,192},{192,256},{256,320},{320,384},{384,448},... | collective-permute-start | bytes 1572872 | tf_op jit(solution)/shard_map/ppermute | solution.py:329
  78.0 4.6 %collective-permute-start.1 = (bf16[2,256,512]{2,1,0:T(8,128)(2,1)S(1)}, bf16[2,256,512]{2,1,0:T(8,128)(2,1)S(1)}, u32[]{:S(2)}, u32[]{:S(2)}) collective-permute-start(bf16[2,256,512]{2,1,0:T(8,128)(2,1)S(1)} %bitcast.16), channel_id=1, source_target_pairs={{0,448},{64,0},{128,64},{192,128},{256,192},{320,256},{384,320},{4... | collective-permute-start | bytes 1572872 | tf_op jit(solution)/shard_map/ppermute | solution.py:330
  82.6 0.5 multiply_cosine_fusion
  83.2 0.0 copy-done.4
  83.2 2.7 %shard_map.86 = (bf16[512,2048]{1,0:T(8,128)(2,1)S(1)}, bf16[512,256]{1,0:T(8,128)(2,1)S(1)}) custom-call(bf16[512,2048]{1,0:T(8,128)(2,1)S(1)} %copy-done, f32[1,2048]{1,0:T(1,128)S(1)} %bitcast.14, bf16[2048,256]{1,0:T(8,128)(2,1)S(1)} %copy-done.4, f32[2,32,1024]{2,1,0:T(8,128)S(1)} %pad_maximum_fusion.1.turn_ref), custom_call_target="tpu_custom_call" | custom-call | flops 536870912 | bytes 3416064 | tf_op jit(solution)/shard_map/pallas_call | solution.py:301
  85.9 0.0 copy-start.1
  85.9 0.1 pad_add_fusion.place_ref
  86.0 5.6 %collective-permute-done.below_ref = bf16[2,256,512]{2,1,0:T(8,128)(2,1)S(1)} collective-permute-done((bf16[2,256,512]{2,1,0:T(8,128)(2,1)S(1)}, bf16[2,256,512]{2,1,0:T(8,128)(2,1)S(1)}, u32[]{:S(2)}, u32[]{:S(2)}) %collective-permute-start) | collective-permute-done | bytes 524320 | tf_op jit(solution)/shard_map/ppermute | solution.py:329
  91.5 0.8 collective-permute-done.1.above_ref
  92.3 3.6 %shard_map.87 = (bf16[512,256]{1,0:T(8,128)(2,1)S(1)}, bf16[512,256]{1,0:T(8,128)(2,1)S(1)}, bf16[2048,512]{1,0:T(8,128)(2,1)S(1)}) custom-call(s32[4]{0:T(128)S(1)} %pad_add_fusion.place_ref, bf16[512,2048]{1,0:T(8,128)(2,1)S(1)} %get-tuple-element.23.normed_ref, f32[2,32,1024]{2,1,0:T(8,128)S(1)} %pad_maximum_fusion.1.turn_ref, ...), custom_call_target="tpu_custom_call" | custom-call | flops 1073741824 | bytes 4456464 | tf_op jit(solution)/shard_map/pallas_call | solution.py:301
  95.9 5.2 %collective-permute-start.2 = (bf16[512,256]{1,0:T(8,128)(2,1)S(1)}, bf16[512,256]{1,0:T(8,128)(2,1)S(1)}, u32[]{:S(2)}, u32[]{:S(2)}) collective-permute-start(bf16[512,256]{1,0:T(8,128)(2,1)S(1)} %get-tuple-element.24.k_ref), channel_id=1, source_target_pairs={{0,8},{8,16},{16,24},{24,32},{32,40},{40,48},{48,56},{56,64},{64,7... | collective-permute-start | bytes 786440 | tf_op jit(solution)/shard_map/ppermute | solution.py:387
  101.2 2.2 %collective-permute-start.3 = (bf16[512,256]{1,0:T(8,128)(2,1)S(1)}, bf16[512,256]{1,0:T(8,128)(2,1)S(1)}, u32[]{:S(2)}, u32[]{:S(2)}) collective-permute-start(bf16[512,256]{1,0:T(8,128)(2,1)S(1)} %get-tuple-element.25.v_ref), channel_id=1, source_target_pairs={{0,8},{8,16},{16,24},{24,32},{32,40},{40,48},{48,56},{56,64},{64,7... | collective-permute-start | bytes 786440 | tf_op jit(solution)/shard_map/ppermute | solution.py:388
  103.4 1.1 collective-permute-done.2.k_ref
  104.5 5.0 %collective-permute-start.4 = (bf16[512,256]{1,0:T(8,128)(2,1)S(1)}, bf16[512,256]{1,0:T(8,128)(2,1)}, u32[]{:S(2)}, u32[]{:S(2)}) collective-permute-start(bf16[512,256]{1,0:T(8,128)(2,1)S(1)} %collective-permute-done.2.k_ref), channel_id=1, source_target_pairs={{0,8},{8,16},{16,24},{24,32},{32,40},{40,48},{48,56},{56,64},{64,7... | collective-permute-start | bytes 786440 | tf_op jit(solution)/shard_map/ppermute | solution.py:387
  109.4 0.7 copy-done.7
  110.1 0.0 collective-permute-done.3.v_ref
  110.1 4.8 %collective-permute-start.5 = (bf16[512,256]{1,0:T(8,128)(2,1)S(1)}, bf16[512,256]{1,0:T(8,128)(2,1)}, u32[]{:S(2)}, u32[]{:S(2)}) collective-permute-start(bf16[512,256]{1,0:T(8,128)(2,1)S(1)} %collective-permute-done.3.v_ref), channel_id=1, source_target_pairs={{0,8},{8,16},{16,24},{24,32},{32,40},{40,48},{48,56},{56,64},{64,7... | collective-permute-start | bytes 786440 | tf_op jit(solution)/shard_map/ppermute | solution.py:388
  115.0 0.7 copy-done.9
  115.7 0.0 collective-permute-done.4.refs_0_
  115.7 4.9 %collective-permute-start.7 = (bf16[512,256]{1,0:T(8,128)(2,1)}, bf16[512,256]{1,0:T(8,128)(2,1)}, u32[]{:S(2)}, u32[]{:S(2)}) collective-permute-start(bf16[512,256]{1,0:T(8,128)(2,1)} %collective-permute-done.4.refs_0_), channel_id=1, source_target_pairs={{0,8},{8,16},{16,24},{24,32},{32,40},{40,48},{48,56},{56,64},{64,7... | collective-permute-start | bytes 786440 | tf_op jit(solution)/shard_map/ppermute | solution.py:387
  120.6 0.7 collective-permute-done.5.refs_1_
  121.3 4.9 %collective-permute-start.8 = (bf16[512,256]{1,0:T(8,128)(2,1)}, bf16[512,256]{1,0:T(8,128)(2,1)}, u32[]{:S(2)}, u32[]{:S(2)}) collective-permute-start(bf16[512,256]{1,0:T(8,128)(2,1)} %collective-permute-done.5.refs_1_), channel_id=1, source_target_pairs={{0,8},{8,16},{16,24},{24,32},{32,40},{40,48},{48,56},{56,64},{64,7... | collective-permute-start | bytes 786440 | tf_op jit(solution)/shard_map/ppermute | solution.py:388
  126.2 0.0 copy-done.1
  126.2 3.5 %shard_map.88 = (f32[512,256]{1,0:T(8,128)S(1)}, f32[512,256]{1,0:T(8,128)S(1)}, f32[512,256]{1,0:T(8,128)S(1)}) custom-call(bf16[512,256]{1,0:T(8,128)(2,1)S(1)} %get-tuple-element.22.q_ref, bf16[512,256]{1,0:T(8,128)(2,1)S(1)} %get-tuple-element.24.k_ref, bf16[512,256]{1,0:T(8,128)(2,1)S(1)} %get-tuple-element.25.v_ref), custom_call_target="tpu_custom_call" | custom-call | flops 536870912 | bytes 786432 | tf_op jit(solution)/shard_map/pallas_call | solution.py:301
  129.7 0.0 copy-start.5
  129.7 0.8 copy-done.5
  130.6 0.0 all-to-all-done.1
  130.6 0.0 copy-start.10
  130.6 4.5 %shard_map.91 = (bf16[512,256]{1,0:T(8,128)(2,1)S(1)}, bf16[512,256]{1,0:T(8,128)(2,1)S(1)}) custom-call(bf16[512,2048]{1,0:T(8,128)(2,1)} %bitcast.9.normed_ref, f32[2,32,1024]{2,1,0:T(8,128)S(1)} %pad_maximum_fusion.1.turn_ref, bf16[2048,512]{1,0:T(8,128)(2,1)S(1)} %get-tuple-element.32.weight_ref), custom_call_target="tpu_custom_call" | custom-call | flops 1073741824 | bytes 4456448 | tf_op jit(solution)/shard_map/pallas_call | solution.py:301
  135.1 4.1 %shard_map.89 = (f32[512,256]{1,0:T(8,128)S(1)}, f32[512,256]{1,0:T(8,128)S(1)}, f32[512,256]{1,0:T(8,128)S(1)}) custom-call(s32[4]{0:T(128)S(1)} %pad_add_fusion.place_ref, bf16[512,256]{1,0:T(8,128)(2,1)S(1)} %copy-done.2, f32[512,256]{1,0:T(8,128)S(1)} %get-tuple-element.26.max_ref, f32[512,256]{1,0:T(8,128)S(1)} %get-tuple-element.27.sum_ref, ...), custom_call_target="tpu_custom_call" | custom-call | flops 268435456 | bytes 2359312 | tf_op jit(solution)/shard_map/pallas_call | solution.py:301
  139.3 4.3 %shard_map.92 = (f32[512,256]{1,0:T(8,128)S(1)}, f32[512,256]{1,0:T(8,128)S(1)}, f32[512,256]{1,0:T(8,128)S(1)}) custom-call(s32[4]{0:T(128)S(1)} %pad_add_fusion.place_ref, bf16[512,256]{1,0:T(8,128)(2,1)S(1)} %copy-done.2, f32[512,256]{1,0:T(8,128)S(1)} %get-tuple-element.29.max_ref, f32[512,256]{1,0:T(8,128)S(1)} %get-tuple-element.30.sum_ref, ...), custom_call_target="tpu_custom_call" | custom-call | flops 536870912 | bytes 2883600 | tf_op jit(solution)/shard_map/pallas_call | solution.py:301
  143.5 0.0 copy-start.3
  143.5 0.0 collective-permute-done.7.refs_0_
  143.6 0.0 collective-permute-done.8.refs_1_
  143.6 5.2 %shard_map.93 = (bf16[512,256]{1,0:T(8,128)(2,1)}, f32[512,256]{1,0:T(8,128)S(1)}) custom-call(s32[4]{0:T(128)S(1)} %pad_add_fusion.place_ref, bf16[512,256]{1,0:T(8,128)(2,1)S(1)} %copy-done.2, f32[512,256]{1,0:T(8,128)S(1)} %get-tuple-element.35.max_ref, f32[512,256]{1,0:T(8,128)S(1)} %get-tuple-element.36.sum_ref, ...), custom_call_target="tpu_custom_call" | custom-call | flops 268435456 | bytes 2359312 | tf_op jit(solution)/shard_map/pallas_call | solution.py:301
  148.7 3.7 %all-to-all-start.2 = ((bf16[4,128,256]{2,1,0:T(8,128)(2,1)}), bf16[4,128,256]{2,1,0:T(8,128)(2,1)S(1)}, u32[]{:S(2)}, u32[]{:S(2)}) async-start(bf16[4,128,256]{2,1,0:T(8,128)(2,1)} %bitcast.10), calls=%async_computation.2 | async-start | bytes 524288 | tf_op jit(solution)/shard_map/all_to_all | solution.py:441
  152.4 0.0 collective-permute-done.10.after_ref
  152.4 0.0 collective-permute-done.11.across_ref
  152.4 0.0 collective-permute-done.9.before_ref
  152.4 5.5 %all-to-all-done.2.att_ref = bf16[4,128,256]{2,1,0:T(8,128)(2,1)S(1)} async-done(((bf16[4,128,256]{2,1,0:T(8,128)(2,1)}), bf16[4,128,256]{2,1,0:T(8,128)(2,1)S(1)}, u32[]{:S(2)}, u32[]{:S(2)}) %all-to-all-start.2) | async-done | bytes 262176 | tf_op jit(solution)/shard_map/all_to_all | solution.py:441
  157.9 3.5 %shard_map.94 = (f32[64,2048]{1,0:T(8,128)S(1)}, bf16[64,2048]{1,0:T(8,128)(2,1)S(1)}) custom-call(s32[4]{0:T(128)S(1)} %pad_add_fusion.place_ref, bf16[4,128,256]{2,1,0:T(8,128)(2,1)S(1)} %all-to-all-done.2.att_ref, bf16[256,2048]{1,0:T(8,128)(2,1)S(1)} %copy-done.3, bf16[256,2048]{1,0:T(8,128)(2,1)} %collective-permute-done.9.before_ref, ...), custom_call_target="tpu_custom_call" | custom-call | flops 536870912 | bytes 4456464 | tf_op jit(solution)/shard_map/pallas_call | solution.py:301
  161.4 9.4 %collective-permute-start.12 = (bf16[64,2048]{1,0:T(8,128)(2,1)S(1)}, bf16[64,2048]{1,0:T(8,128)(2,1)S(1)}, u32[]{:S(2)}, u32[]{:S(2)}) collective-permute-start(bf16[64,2048]{1,0:T(8,128)(2,1)S(1)} %get-tuple-element.40), channel_id=1, source_target_pairs={{0,1},{1,0},{2,3},{3,2},{4,5},{5,4},{6,7},{7,6},{8,9},{9,8},{10,11... | collective-permute-start | bytes 786440 | tf_op jit(solution)/shard_map/ppermute | solution.py:456
  170.8 1.3 shard_map.96
  172.1 0.0 collective-permute-done.12.taken_ref
  172.1 0.9 shard_map.95
  (16 shorter events, 0.1 us)
Async XLA Ops:
  2.2 17.6 %copy-start = (bf16[512,2048]{1,0:T(8,128)(2,1)S(1)}, bf16[512,2048]{1,0:T(8,128)(2,1)}, u32[]{:S(2)}) copy-start(bf16[512,2048]{1,0:T(8,128)(2,1)} %hidden_ref.3) | copy-start | bytes 6291460
  2.2 17.6 %copy-start.11 = (f32[2048]{0:T(1024)S(1)}, f32[2048]{0:T(1024)}, u32[]{:S(2)}) copy-start(f32[2048]{0:T(1024)} %param.8) | copy-start | bytes 24580
  3.3 55.9 %all-to-all-start = ((bf16[32,32,512]{2,1,0:T(8,128)(2,1)}), bf16[32,32,512]{2,1,0:T(8,128)(2,1)S(1)}, u32[]{:S(2)}, u32[]{:S(2)}) async-start(bf16[32,32,512]{2,1,0:T(8,128)(2,1)} %pad_maximum_fusion), calls=%async_computation | async-start | bytes 2097152 | tf_op jit(solution)/shard_map/all_to_all | solution.py:327
  20.0 39.2 %collective-permute-start.6 = (bf16[64,2048]{1,0:T(8,128)(2,1)S(1)}, bf16[64,2048]{1,0:T(8,128)(2,1)S(1)}, u32[]{:S(2)}, u32[]{:S(2)}) collective-permute-start(bf16[64,2048]{1,0:T(8,128)(2,1)S(1)} %shard_map.90), channel_id=1, source_target_pairs={{0,32},{8,40},{16,48},{24,56},{32,64},{40,72},{48,80},{56,88},{64,... | collective-permute-start | bytes 786440 | tf_op jit(solution)/shard_map/ppermute | solution.py:345
  60.8 69.8 %all-to-all-start.1 = ((bf16[8,64,2048]{2,1,0:T(8,128)(2,1)}), bf16[8,64,2048]{2,1,0:T(8,128)(2,1)}, u32[]{:S(2)}, u32[]{:S(2)}) async-start(bf16[8,64,2048]{2,1,0:T(8,128)(2,1)} %broadcast_in_dim.16), calls=%async_computation.1 | async-start | bytes 4194304 | tf_op jit(solution)/shard_map/all_to_all | solution.py:312
  66.3 86.1 %collective-permute-start.10 = (bf16[256,2048]{1,0:T(8,128)(2,1)}, bf16[256,2048]{1,0:T(8,128)(2,1)}, u32[]{:S(2)}, u32[]{:S(2)}) collective-permute-start(bf16[256,2048]{1,0:T(8,128)(2,1)} %own_ref.1), channel_id=1, source_target_pairs={{0,6},{2,0},{4,2},{6,4},{1,7},{3,1},{5,3},{7,5},{8,14},{10,8},{12,... | collective-permute-start | bytes 3145736 | tf_op jit(solution)/shard_map/ppermute | solution.py:349
  70.8 81.6 %collective-permute-start.11 = (bf16[256,2048]{1,0:T(8,128)(2,1)}, bf16[256,2048]{1,0:T(8,128)(2,1)}, u32[]{:S(2)}, u32[]{:S(2)}) collective-permute-start(bf16[256,2048]{1,0:T(8,128)(2,1)} %own_ref.1), channel_id=1, source_target_pairs={{0,4},{2,6},{4,0},{6,2},{1,5},{3,7},{5,1},{7,3},{8,12},{10,14},{12... | collective-permute-start | bytes 3145736 | tf_op jit(solution)/shard_map/ppermute | solution.py:350
  73.3 79.1 %collective-permute-start.9 = (bf16[256,2048]{1,0:T(8,128)(2,1)}, bf16[256,2048]{1,0:T(8,128)(2,1)}, u32[]{:S(2)}, u32[]{:S(2)}) collective-permute-start(bf16[256,2048]{1,0:T(8,128)(2,1)} %own_ref.1), channel_id=1, source_target_pairs={{0,2},{2,4},{4,6},{6,0},{1,3},{3,5},{5,7},{7,1},{8,10},{10,12},{12... | collective-permute-start | bytes 3145736 | tf_op jit(solution)/shard_map/ppermute | solution.py:348
  75.8 7.4 %copy-start.4 = (bf16[2048,256]{1,0:T(8,128)(2,1)S(1)}, bf16[2048,256]{1,0:T(8,128)(2,1)}, u32[]{:S(2)}) copy-start(bf16[2048,256]{1,0:T(8,128)(2,1)} %weight_ref.1) | copy-start | bytes 3145732
  75.9 15.6 %collective-permute-start = (bf16[2,256,512]{2,1,0:T(8,128)(2,1)S(1)}, bf16[2,256,512]{2,1,0:T(8,128)(2,1)S(1)}, u32[]{:S(2)}, u32[]{:S(2)}) collective-permute-start(bf16[2,256,512]{2,1,0:T(8,128)(2,1)S(1)} %bitcast.17), channel_id=1, source_target_pairs={{0,64},{64,128},{128,192},{192,256},{256,320},{320,384},{384,448},... | collective-permute-start | bytes 1572872 | tf_op jit(solution)/shard_map/ppermute | solution.py:329
  78.0 14.3 %collective-permute-start.1 = (bf16[2,256,512]{2,1,0:T(8,128)(2,1)S(1)}, bf16[2,256,512]{2,1,0:T(8,128)(2,1)S(1)}, u32[]{:S(2)}, u32[]{:S(2)}) collective-permute-start(bf16[2,256,512]{2,1,0:T(8,128)(2,1)S(1)} %bitcast.16), channel_id=1, source_target_pairs={{0,448},{64,0},{128,64},{192,128},{256,192},{320,256},{384,320},{4... | collective-permute-start | bytes 1572872 | tf_op jit(solution)/shard_map/ppermute | solution.py:330
  85.9 40.3 %copy-start.1 = (bf16[512,256]{1,0:T(8,128)(2,1)}, bf16[512,256]{1,0:T(8,128)(2,1)S(1)}, u32[]{:S(2)}) copy-start(bf16[512,256]{1,0:T(8,128)(2,1)S(1)} %get-tuple-element.22.q_ref) | copy-start | bytes 786436
  95.9 8.5 %collective-permute-start.2 = (bf16[512,256]{1,0:T(8,128)(2,1)S(1)}, bf16[512,256]{1,0:T(8,128)(2,1)S(1)}, u32[]{:S(2)}, u32[]{:S(2)}) collective-permute-start(bf16[512,256]{1,0:T(8,128)(2,1)S(1)} %get-tuple-element.24.k_ref), channel_id=1, source_target_pairs={{0,8},{8,16},{16,24},{24,32},{32,40},{40,48},{48,56},{56,64},{64,7... | collective-permute-start | bytes 786440 | tf_op jit(solution)/shard_map/ppermute | solution.py:387
  101.2 8.9 %collective-permute-start.3 = (bf16[512,256]{1,0:T(8,128)(2,1)S(1)}, bf16[512,256]{1,0:T(8,128)(2,1)S(1)}, u32[]{:S(2)}, u32[]{:S(2)}) collective-permute-start(bf16[512,256]{1,0:T(8,128)(2,1)S(1)} %get-tuple-element.25.v_ref), channel_id=1, source_target_pairs={{0,8},{8,16},{16,24},{24,32},{32,40},{40,48},{48,56},{56,64},{64,7... | collective-permute-start | bytes 786440 | tf_op jit(solution)/shard_map/ppermute | solution.py:388
  104.5 11.2 %collective-permute-start.4 = (bf16[512,256]{1,0:T(8,128)(2,1)S(1)}, bf16[512,256]{1,0:T(8,128)(2,1)}, u32[]{:S(2)}, u32[]{:S(2)}) collective-permute-start(bf16[512,256]{1,0:T(8,128)(2,1)S(1)} %collective-permute-done.2.k_ref), channel_id=1, source_target_pairs={{0,8},{8,16},{16,24},{24,32},{32,40},{40,48},{48,56},{56,64},{64,7... | collective-permute-start | bytes 786440 | tf_op jit(solution)/shard_map/ppermute | solution.py:387
  109.4 0.7 copy-start.7
  110.1 11.2 %collective-permute-start.5 = (bf16[512,256]{1,0:T(8,128)(2,1)S(1)}, bf16[512,256]{1,0:T(8,128)(2,1)}, u32[]{:S(2)}, u32[]{:S(2)}) collective-permute-start(bf16[512,256]{1,0:T(8,128)(2,1)S(1)} %collective-permute-done.3.v_ref), channel_id=1, source_target_pairs={{0,8},{8,16},{16,24},{24,32},{32,40},{40,48},{48,56},{56,64},{64,7... | collective-permute-start | bytes 786440 | tf_op jit(solution)/shard_map/ppermute | solution.py:388
  115.0 0.7 copy-start.9
  115.7 27.9 %collective-permute-start.7 = (bf16[512,256]{1,0:T(8,128)(2,1)}, bf16[512,256]{1,0:T(8,128)(2,1)}, u32[]{:S(2)}, u32[]{:S(2)}) collective-permute-start(bf16[512,256]{1,0:T(8,128)(2,1)} %collective-permute-done.4.refs_0_), channel_id=1, source_target_pairs={{0,8},{8,16},{16,24},{24,32},{32,40},{40,48},{48,56},{56,64},{64,7... | collective-permute-start | bytes 786440 | tf_op jit(solution)/shard_map/ppermute | solution.py:387
  121.3 22.3 %collective-permute-start.8 = (bf16[512,256]{1,0:T(8,128)(2,1)}, bf16[512,256]{1,0:T(8,128)(2,1)}, u32[]{:S(2)}, u32[]{:S(2)}) collective-permute-start(bf16[512,256]{1,0:T(8,128)(2,1)} %collective-permute-done.5.refs_1_), channel_id=1, source_target_pairs={{0,8},{8,16},{16,24},{24,32},{32,40},{40,48},{48,56},{56,64},{64,7... | collective-permute-start | bytes 786440 | tf_op jit(solution)/shard_map/ppermute | solution.py:388
  129.7 0.9 copy-start.5
  130.6 4.5 %copy-start.2 = (bf16[512,256]{1,0:T(8,128)(2,1)S(1)}, bf16[512,256]{1,0:T(8,128)(2,1)}, u32[]{:S(2)}) copy-start(bf16[512,256]{1,0:T(8,128)(2,1)} %copy-done.1) | copy-start | bytes 786436
  130.6 4.5 %copy-start.6 = (f32[512,256]{1,0:T(8,128)S(1)}, f32[512,256]{1,0:T(8,128)}, u32[]{:S(2)}) copy-start(f32[512,256]{1,0:T(8,128)} %copy-done.5) | copy-start | bytes 1572868
  130.6 4.5 %copy-start.8 = (bf16[512,256]{1,0:T(8,128)(2,1)S(1)}, bf16[512,256]{1,0:T(8,128)(2,1)}, u32[]{:S(2)}) copy-start(bf16[512,256]{1,0:T(8,128)(2,1)} %copy-done.7) | copy-start | bytes 786436
  130.6 4.5 %copy-start.10 = (bf16[512,256]{1,0:T(8,128)(2,1)S(1)}, bf16[512,256]{1,0:T(8,128)(2,1)}, u32[]{:S(2)}) copy-start(bf16[512,256]{1,0:T(8,128)(2,1)} %copy-done.9) | copy-start | bytes 786436
  143.5 14.4 %copy-start.3 = (bf16[256,2048]{1,0:T(8,128)(2,1)S(1)}, bf16[256,2048]{1,0:T(8,128)(2,1)}, u32[]{:S(2)}) copy-start(bf16[256,2048]{1,0:T(8,128)(2,1)} %own_ref.1) | copy-start | bytes 3145732
  148.7 9.2 %all-to-all-start.2 = ((bf16[4,128,256]{2,1,0:T(8,128)(2,1)}), bf16[4,128,256]{2,1,0:T(8,128)(2,1)S(1)}, u32[]{:S(2)}, u32[]{:S(2)}) async-start(bf16[4,128,256]{2,1,0:T(8,128)(2,1)} %bitcast.10), calls=%async_computation.2 | async-start | bytes 524288 | tf_op jit(solution)/shard_map/all_to_all | solution.py:441
  152.4 19.7 %copy-start.12 = (f32[2048]{0:T(1024)S(1)}, f32[2048]{0:T(1024)}, u32[]{:S(2)}) copy-start(f32[2048]{0:T(1024)} %param.13) | copy-start | bytes 24580
  161.4 10.6 %collective-permute-start.12 = (bf16[64,2048]{1,0:T(8,128)(2,1)S(1)}, bf16[64,2048]{1,0:T(8,128)(2,1)S(1)}, u32[]{:S(2)}, u32[]{:S(2)}) collective-permute-start(bf16[64,2048]{1,0:T(8,128)(2,1)S(1)} %get-tuple-element.40), channel_id=1, source_target_pairs={{0,1},{1,0},{2,3},{3,2},{4,5},{5,4},{6,7},{7,6},{8,9},{9,8},{10,11... | collective-permute-start | bytes 786440 | tf_op jit(solution)/shard_map/ppermute | solution.py:456

commit v8 on v7

--- a/solution.py
+++ b/solution.py
@@ -68,10 +68,6 @@
     return jnp.concatenate([cos, cos], axis=1), jnp.concatenate([sin, sin], axis=1)
 
 
-def slice_kernel(place_ref, hidden_ref, gain_ref, out_ref):
-    out_ref[...] = normed_rows(hidden_ref[...], gain_ref[...])
-
-
 def query_kernel(hidden_ref, gain_ref, weight_ref, turn_ref, normed_ref, query_ref):
     rows = hidden_ref.shape[0]
     gain = gain_ref[...]
@@ -83,7 +79,7 @@
 
     lax.fori_loop(0, rows // 64, step, 0)
     query = jnp.dot(normed_ref[...], weight_ref[...], preferred_element_type=F32)
-    cos, sin = spread(turn_ref, slice(rows, 2 * rows))
+    cos, sin = spread(turn_ref, slice(0, rows))
     query = rotated(query, cos, sin).astype(BF16) * 0.125
     query_ref[...] = permuted(to_residue(rows), query)
 
@@ -118,10 +114,6 @@
         for place, ref, k in slabs:
             weight_ref[pl.ds(pl.multiple_of(place * 256, 256), 256), :] = ref[k]
 
-    project(normed_ref, turn_ref, weight_ref, key_ref, value_ref, both_ref)
-
-
-def far_key_value_kernel(normed_ref, turn_ref, weight_ref, key_ref, value_ref, both_ref):
     project(normed_ref, turn_ref, weight_ref, key_ref, value_ref, both_ref)
 
 
@@ -268,23 +260,25 @@
         log_ref[head : head + 1, :] = flipped[head * HEAD_DIM : head * HEAD_DIM + 1, :]
 
 
-def out_kernel(place_ref, att_ref, own_ref, before_ref, after_ref, across_ref, keep_ref, give_ref, sum_ref):
+def out_kernel(place_ref, att_ref, *refs):
+    weights, (gain_ref, out_ref, sum_ref) = refs[:8], refs[8:]
     x, core = place_ref[2], place_ref[3]
-    rows = keep_ref.shape[0]
+    n = pl.program_id(0)
+    columns = weights[0].shape[1]
     total = None
-    for n, ref in enumerate((own_ref, before_ref, after_ref, across_ref)):
-        part = jnp.dot(att_ref[lax.rem(x + HOPS[n], 4)], ref[...], preferred_element_type=F32)
-        part = part.astype(BF16).astype(F32)
-        total = part if total is None else total + part
-    sum_ref[...] = total
-    keep_ref[...] = sum_ref[pl.ds(pl.multiple_of(core * rows, rows), rows), :]
-    give_ref[...] = sum_ref[pl.ds(pl.multiple_of((1 - core) * rows, rows), rows), :].astype(BF16)
-
-
-def end_kernel(keep_ref, taken_ref, gain_ref, out_ref):
-    summed = keep_ref[...] + taken_ref[...].astype(F32)
-    scale = lax.rsqrt(jnp.mean(summed * summed, axis=1, keepdims=True) + EPS)
-    out_ref[...] = (summed * scale * gain_ref[...]).astype(BF16)
+    for half, c in enumerate((core, 1 - core)):
+        for k, hop in enumerate(HOPS):
+            group = lax.rem(x + hop, 4) * 2 + c
+            part = jnp.dot(att_ref[group], weights[half * 4 + k][...], preferred_element_type=F32)
+            part = part.astype(BF16).astype(F32)
+            total = part if total is None else total + part
+    sum_ref[:, pl.ds(pl.multiple_of(n * columns, columns), columns)] = total
+
+    @pl.when(n == pl.num_programs(0) - 1)
+    def _():
+        summed = sum_ref[...]
+        scale = lax.rsqrt(jnp.mean(summed * summed, axis=1, keepdims=True) + EPS)
+        out_ref[...] = (summed * scale * gain_ref[...]).astype(BF16)
 
 
 SMEM = pl.BlockSpec(memory_space=pltpu.SMEM)
@@ -307,11 +301,6 @@
     )(*args)
 
 
-def spread_to(value, axis, count):
-    copies = jnp.broadcast_to(value[None], (count,) + value.shape)
-    return lax.all_to_all(copies, axis, split_axis=0, concat_axis=0, tiled=True)
-
-
 def layer(hidden_in, pre_gain, query_proj, key_proj, value_proj, out_proj, post_gain):
     rows, depth = hidden_in.shape
     width = query_proj.shape[1]
@@ -319,7 +308,6 @@
     piece = rows // 8
     sp, x, core = lax.axis_index(SP), lax.axis_index("x"), lax.axis_index("c")
     place = jnp.stack([sp, lax.axis_index("zl"), x, core]).astype(jnp.int32)
-    member = (x * 2 + core)[None].astype(jnp.int32)
     gain = pre_gain[None]
     row = (rows, width)
 
@@ -329,30 +317,15 @@
     below = lax.ppermute(mine[:2], Z, ring(8, 1))
     above = lax.ppermute(mine[2:], Z, ring(8, -1))
 
-    (eighth,) = kernel_call(
-        slice_kernel,
-        [((piece, depth), BF16)],
-        (member, hidden_in, gain),
-        10 * piece * depth,
-        12,
-        grid_spec=pltpu.PrefetchScalarGridSpec(
-            num_scalar_prefetch=1,
-            grid=(1,),
-            in_specs=[pl.BlockSpec((piece, depth), lambda i, t: (t[0], 0)), pl.BlockSpec((1, depth), lambda i, t: (0, 0))],
-            out_specs=[pl.BlockSpec((piece, depth), lambda i, t: (0, 0))],
-        ),
-    )
-    fourth = lax.ppermute(eighth, SP, ring(64, 4))
-    far_rows = spread_to(fourth, TP, 8).reshape(rows, depth)
-
-    before = lax.ppermute(out_proj, "x", ring(4, 1))
-    after = lax.ppermute(out_proj, "x", ring(4, -1))
-    across = lax.ppermute(out_proj, "x", ring(4, 2))
+    groups = [out_proj]
+    for steps in (1, -1, 2):
+        groups.append(lax.ppermute(out_proj, "x", ring(4, steps)))
+    for n in range(4):
+        groups.append(lax.ppermute(groups[n], "c", ring(2, 1)))
 
     quarter = HEAD_DIM // 2
     frequency = ROPE_BASE ** (-(jnp.arange(quarter, dtype=F32) * 2.0 / HEAD_DIM))
-    local = jnp.arange(rows, dtype=jnp.int32)
-    positions = jnp.concatenate([(sp - 4) * rows + local, sp * rows + local]).astype(F32)
+    positions = (sp * rows + jnp.arange(rows, dtype=jnp.int32)).astype(F32)
     angles = positions[None, :] * frequency[:, None]
     turns = jnp.stack([jnp.cos(angles), jnp.sin(angles)])
 
@@ -362,42 +335,29 @@
     block_rows = rows // 4
     row_part = pl.BlockSpec((block_rows, depth), lambda n: (n, 0))
     whole = pl.BlockSpec(row, lambda c: (0, 0))
-    weight_spec = pl.BlockSpec((depth, 2 * width), lambda n: (0, 0))
-    key, value, weights = kernel_call(
+    key, value = kernel_call(
         key_value_kernel,
-        [(row, BF16), (row, BF16), ((depth, 2 * width), BF16)],
+        [(row, BF16)] * 2,
         (place, normed, turns, mine, below, above),
         4 * rows * depth * width,
         14,
-        [((rows, 2 * width), BF16)],
+        [((depth, 2 * width), BF16), ((rows, 2 * width), BF16)],
         grid=(4,),
         in_specs=[
             SMEM,
             row_part,
-            pl.BlockSpec((2, HEAD_DIM // 2, block_rows), lambda n: (0, 0, 4 + n)),
+            pl.BlockSpec((2, HEAD_DIM // 2, block_rows), lambda n: (0, 0, n)),
             pl.BlockSpec((4, 256, 2 * width), lambda n: (0, 0, 0)),
             pl.BlockSpec((2, 256, 2 * width), lambda n: (0, 0, 0)),
             pl.BlockSpec((2, 256, 2 * width), lambda n: (0, 0, 0)),
         ],
-        out_specs=(whole, whole, weight_spec),
+        out_specs=(whole, whole),
     )
     forward = [(i, i + 1) for i in range(63)]
     keys, values = [key], [value]
-    for _ in range(1, 4):
+    for _ in range(1, 5):
         keys.append(lax.ppermute(keys[-1], SP, forward))
         values.append(lax.ppermute(values[-1], SP, forward))
-    key4, value4 = kernel_call(
-        far_key_value_kernel,
-        [(row, BF16)] * 2,
-        (far_rows, turns, weights),
-        4 * rows * depth * width,
-        14,
-        [((rows, 2 * width), BF16)],
-        grid=(4,),
-        in_specs=[row_part, pl.BlockSpec((2, HEAD_DIM // 2, block_rows), lambda n: (0, 0, n)), weight_spec],
-        out_specs=(whole, whole),
-    )
-
     part = pl.BlockSpec((128, width), lambda c: (c, 0))
     pair = ((512, 256), F32), ((512, 256), BF16), ((2, 512, width), F32)
     state = kernel_call(
@@ -422,39 +382,37 @@
         in_specs=[SMEM] + [part] * 4 + [whole, whole],
         out_specs=(part,) * 3,
     )
-    sources = {2: (keys[2], values[2]), 3: (keys[3], values[3]), 4: (key4, value4)}
-    for backs in ((2, 4), (3,)):
-        last = backs == (3,)
+    for back in (2, 3, 4):
+        last = back == 4
         state = kernel_call(
-            functools.partial(far_kernel, backs, last),
+            functools.partial(far_kernel, (back,), last),
             [(row, BF16), (row, F32)] if last else [(row, F32)] * 3,
-            (place, query, *state, *(array for back in backs for array in sources[back])),
-            4 * rows * 512 * width * len(backs),
+            (place, query, *state, keys[back], values[back]),
+            4 * rows * 512 * width,
             10,
-            ([(row, BF16)] if last else []) + [((512, 128 * len(backs)), t) for t in (F32, BF16)] + [((2, 512, width), F32)],
+            ([(row, BF16)] if last else []) + [((512, 128), t) for t in (F32, BF16)] + [((2, 512, width), F32)],
             grid=(rows // 128,),
-            in_specs=[SMEM] + [part] * (4 + 2 * len(backs)),
+            in_specs=[SMEM] + [part] * 6,
             out_specs=(whole, part) if last else (part,) * 3,
         )
     attended, logs = state
 
-    arrived = lax.all_to_all(attended.reshape(4, rows // 4, width), "x", split_axis=0, concat_axis=0, tiled=True)
+    arrived = lax.all_to_all(attended.reshape(8, piece, width), TP, split_axis=0, concat_axis=0, tiled=True)
     (log_weight,) = kernel_call(log_kernel, [((heads, rows), F32)], (logs,), 6 * rows * rows * width, 8)
     columns = depth // 4
-    piece_spec = pl.BlockSpec((piece, columns), lambda n: (0, n))
-    keep, give = kernel_call(
+    (layer_out,) = kernel_call(
         out_kernel,
-        [((piece, depth), F32), ((piece, depth), BF16)],
-        (place, arrived, out_proj, before, after, across),
-        2 * rows // 8 * depth * depth,
+        [((piece, depth), BF16)],
+        (place, arrived, *groups, post_gain[None]),
+        2 * piece * depth * depth,
         12,
-        [((2 * piece, columns), F32)],
+        [((piece, depth), F32)],
         grid=(4,),
-        in_specs=[SMEM, pl.BlockSpec((4, rows // 4, width), lambda n: (0, 0, 0))] + [pl.BlockSpec((width, columns), lambda n: (0, n))] * 4,
-        out_specs=(piece_spec, piece_spec),
-    )
-    taken = lax.ppermute(give, "c", ring(2, 1))
-    (layer_out,) = kernel_call(end_kernel, [((piece, depth), BF16)], (keep, taken, post_gain[None]), 10 * piece * depth, 8)
+        in_specs=[SMEM, pl.BlockSpec((8, piece, width), lambda n: (0, 0, 0))]
+        + [pl.BlockSpec((width, columns), lambda n: (0, n))] * 8
+        + [pl.BlockSpec((1, depth), lambda n: (0, 0))],
+        out_specs=(pl.BlockSpec((piece, depth), lambda n: (0, 0)),),
+    )
     return layer_out, log_weight
 
 

time: 174 us -> 172 us (0.989)
  the two profiles are of different devices: /device:TPU:1 before, /device:TPU:24 now
where the time goes in v8:
time: 172 us; the launch traced here: 171 us
  starting transfers between devices  81.5 us (47%)
  waiting for transfers between devices  49 us (28%)
  Pallas kernels  31.9 us (19%)
  local copies, waits for them, and re-layouts  6.36 us (4%)
    pallas_call x9, Pallas kernels, kernel_call(): pl.pallas_call(body, out_shape=tuple((jax.ShapeDtypeStruct(s, t) for s, t...  31.9 us
    ppermute x4, starting transfers between devices, layer(): keys.append(lax.ppermute(keys[-1], SP, forward))  20.4 us
    all_to_all x1, waiting for transfers between devices, layer(): lax.all_to_all(jnp.concatenate(copies, axis=2), ('zh', 'y'), split_axis=0...  19.3 us
    all_to_all x1, starting transfers between devices, layer(): lax.all_to_all(jnp.concatenate(copies, axis=2), ('zh', 'y'), split_axis=0...  16.1 us
    ppermute x4, starting transfers between devices, layer(): values.append(lax.ppermute(values[-1], SP, forward))  14.1 us
    ppermute x4, waiting for transfers between devices, layer(): keys.append(lax.ppermute(keys[-1], SP, forward))  11.8 us
    ppermute x3, starting transfers between devices, layer(): groups.append(lax.ppermute(out_proj, 'x', ring(4, steps)))  10.8 us
    ppermute x4, starting transfers between devices, layer(): groups.append(lax.ppermute(groups[n], 'c', ring(2, 1)))  8.66 us
  transfers between devices with their start and end apart: 19, of which 8 were waited for; matrix products, arithmetic and copies ran while one was open for 1% of the time, Pallas kernels for 16%

profile of v8, /device:TPU:24, one launch (start us, length us, event | category | flops | bytes accessed | tf_op | source)
XLA Modules:
  0.0 171.1 jit_solution(15197599032695271133)
XLA Ops:
  0.6 0.8 broadcast_in_dim.10
  1.4 0.8 broadcast_in_dim.9
  2.2 1.1 pad_maximum_fusion
  3.2 0.0 copy-start
  3.2 16.1 %all-to-all-start = ((bf16[32,32,512]{2,1,0:T(8,128)(2,1)}), bf16[32,32,512]{2,1,0:T(8,128)(2,1)S(1)}, u32[]{:S(2)}, u32[]{:S(2)}) async-start(bf16[32,32,512]{2,1,0:T(8,128)(2,1)} %pad_maximum_fusion), calls=%async_computation | async-start | bytes 2097152 | tf_op jit(solution)/shard_map/all_to_all | solution.py:315
  19.3 3.4 %collective-permute-start.10 = (bf16[256,2048]{1,0:T(8,128)(2,1)}, bf16[256,2048]{1,0:T(8,128)(2,1)}, u32[]{:S(2)}, u32[]{:S(2)}) collective-permute-start(bf16[256,2048]{1,0:T(8,128)(2,1)} %refs_0_.1), channel_id=1, source_target_pairs={{0,2},{2,4},{4,6},{6,0},{1,3},{3,5},{5,7},{7,1},{8,10},{10,12},{12... | collective-permute-start | bytes 3145736 | tf_op jit(solution)/shard_map/ppermute | solution.py:322
  22.7 3.7 %collective-permute-start.11 = (bf16[256,2048]{1,0:T(8,128)(2,1)}, bf16[256,2048]{1,0:T(8,128)(2,1)}, u32[]{:S(2)}, u32[]{:S(2)}) collective-permute-start(bf16[256,2048]{1,0:T(8,128)(2,1)} %refs_0_.1), channel_id=1, source_target_pairs={{0,6},{2,0},{4,2},{6,4},{1,7},{3,1},{5,3},{7,5},{8,14},{10,8},{12,... | collective-permute-start | bytes 3145736 | tf_op jit(solution)/shard_map/ppermute | solution.py:322
  26.4 3.7 %collective-permute-start.12 = (bf16[256,2048]{1,0:T(8,128)(2,1)}, bf16[256,2048]{1,0:T(8,128)(2,1)}, u32[]{:S(2)}, u32[]{:S(2)}) collective-permute-start(bf16[256,2048]{1,0:T(8,128)(2,1)} %refs_0_.1), channel_id=1, source_target_pairs={{0,4},{2,6},{4,0},{6,2},{1,5},{3,7},{5,1},{7,3},{8,12},{10,14},{12... | collective-permute-start | bytes 3145736 | tf_op jit(solution)/shard_map/ppermute | solution.py:322
  30.2 19.3 %all-to-all-done = bf16[32,32,512]{2,1,0:T(8,128)(2,1)S(1)} async-done(((bf16[32,32,512]{2,1,0:T(8,128)(2,1)}), bf16[32,32,512]{2,1,0:T(8,128)(2,1)S(1)}, u32[]{:S(2)}, u32[]{:S(2)}) %all-to-all-start) | async-done | bytes 1048608 | tf_op jit(solution)/shard_map/all_to_all | solution.py:315
  49.5 1.0 fusion
  50.5 4.1 %collective-permute-start = (bf16[2,256,512]{2,1,0:T(8,128)(2,1)}, bf16[2,256,512]{2,1,0:T(8,128)(2,1)}, u32[]{:S(2)}, u32[]{:S(2)}) collective-permute-start(bf16[2,256,512]{2,1,0:T(8,128)(2,1)} %bitcast.6), channel_id=1, source_target_pairs={{0,64},{64,128},{128,192},{192,256},{256,320},{320,384},{384,448},... | collective-permute-start | bytes 1572872 | tf_op jit(solution)/shard_map/ppermute | solution.py:317
  54.6 3.0 %collective-permute-start.1 = (bf16[2,256,512]{2,1,0:T(8,128)(2,1)}, bf16[2,256,512]{2,1,0:T(8,128)(2,1)}, u32[]{:S(2)}, u32[]{:S(2)}) collective-permute-start(bf16[2,256,512]{2,1,0:T(8,128)(2,1)} %bitcast.7), channel_id=1, source_target_pairs={{0,448},{64,0},{128,64},{192,128},{256,192},{320,256},{384,320},{4... | collective-permute-start | bytes 1572872 | tf_op jit(solution)/shard_map/ppermute | solution.py:318
  57.6 0.3 multiply_cosine_fusion
  58.0 0.0 copy-done
  58.0 0.0 copy-done.3
  58.0 0.0 copy-start.1
  58.0 1.2 copy-done.1
  59.2 2.7 %shard_map.86 = (bf16[512,2048]{1,0:T(8,128)(2,1)S(1)}, bf16[512,256]{1,0:T(8,128)(2,1)S(1)}) custom-call(bf16[512,2048]{1,0:T(8,128)(2,1)S(1)} %copy-done, f32[1,2048]{1,0:T(1,128)S(1)} %bitcast.12, bf16[2048,256]{1,0:T(8,128)(2,1)S(1)} %copy-done.1, f32[2,32,512]{2,1,0:T(8,128)S(1)} %pad_maximum_fusion.1.turn_ref), custom_call_target="tpu_custom_call" | custom-call | flops 536870912 | bytes 3284992 | tf_op jit(solution)/shard_map/pallas_call | solution.py:295
  61.9 0.1 pad_add_fusion.place_ref
  62.0 2.6 %collective-permute-done.below_ref = bf16[2,256,512]{2,1,0:T(8,128)(2,1)} collective-permute-done((bf16[2,256,512]{2,1,0:T(8,128)(2,1)}, bf16[2,256,512]{2,1,0:T(8,128)(2,1)}, u32[]{:S(2)}, u32[]{:S(2)}) %collective-permute-start) | collective-permute-done | bytes 524320 | tf_op jit(solution)/shard_map/ppermute | solution.py:317
  64.5 1.8 %collective-permute-done.1.above_ref = bf16[2,256,512]{2,1,0:T(8,128)(2,1)} collective-permute-done((bf16[2,256,512]{2,1,0:T(8,128)(2,1)}, bf16[2,256,512]{2,1,0:T(8,128)(2,1)}, u32[]{:S(2)}, u32[]{:S(2)}) %collective-permute-start.1) | collective-permute-done | bytes 524320 | tf_op jit(solution)/shard_map/ppermute | solution.py:318
  66.4 4.2 %shard_map.87 = (bf16[512,256]{1,0:T(8,128)(2,1)S(1)}, bf16[512,256]{1,0:T(8,128)(2,1)S(1)}) custom-call(s32[4]{0:T(128)S(1)} %pad_add_fusion.place_ref, bf16[512,2048]{1,0:T(8,128)(2,1)S(1)} %get-tuple-element.21.normed_ref, f32[2,32,512]{2,1,0:T(8,128)S(1)} %pad_maximum_fusion.1.turn_ref, bf16[4,256,512]{2,1,0:T(8,128)(2,1)S(1)} %bitcast.10, ...), custom_call_target="tpu_custom_call" | custom-call | flops 1073741824 | bytes 4325392 | tf_op jit(solution)/shard_map/pallas_call | solution.py:295
  70.5 5.9 %collective-permute-start.2 = (bf16[512,256]{1,0:T(8,128)(2,1)S(1)}, bf16[512,256]{1,0:T(8,128)(2,1)S(1)}, u32[]{:S(2)}, u32[]{:S(2)}) collective-permute-start(bf16[512,256]{1,0:T(8,128)(2,1)S(1)} %get-tuple-element.22.k_ref), channel_id=1, source_target_pairs={{0,8},{8,16},{16,24},{24,32},{32,40},{40,48},{48,56},{56,64},{64,7... | collective-permute-start | bytes 786440 | tf_op jit(solution)/shard_map/ppermute | solution.py:359
  76.4 1.9 %collective-permute-start.3 = (bf16[512,256]{1,0:T(8,128)(2,1)S(1)}, bf16[512,256]{1,0:T(8,128)(2,1)S(1)}, u32[]{:S(2)}, u32[]{:S(2)}) collective-permute-start(bf16[512,256]{1,0:T(8,128)(2,1)S(1)} %get-tuple-element.23.v_ref), channel_id=1, source_target_pairs={{0,8},{8,16},{16,24},{24,32},{32,40},{40,48},{48,56},{56,64},{64,7... | collective-permute-start | bytes 786440 | tf_op jit(solution)/shard_map/ppermute | solution.py:360
  78.3 4.7 %collective-permute-done.2.k_ref = bf16[512,256]{1,0:T(8,128)(2,1)S(1)} collective-permute-done((bf16[512,256]{1,0:T(8,128)(2,1)S(1)}, bf16[512,256]{1,0:T(8,128)(2,1)S(1)}, u32[]{:S(2)}, u32[]{:S(2)}) %collective-permute-start.2) | collective-permute-done | bytes 262176 | tf_op jit(solution)/shard_map/ppermute | solution.py:359
  83.1 5.6 %collective-permute-start.4 = (bf16[512,256]{1,0:T(8,128)(2,1)S(1)}, bf16[512,256]{1,0:T(8,128)(2,1)S(1)}, u32[]{:S(2)}, u32[]{:S(2)}) collective-permute-start(bf16[512,256]{1,0:T(8,128)(2,1)S(1)} %collective-permute-done.2.k_ref), channel_id=1, source_target_pairs={{0,8},{8,16},{16,24},{24,32},{32,40},{40,48},{48,56},{56,64},{64,7... | collective-permute-start | bytes 786440 | tf_op jit(solution)/shard_map/ppermute | solution.py:359
  88.7 0.0 collective-permute-done.3.v_ref
  88.7 5.4 %collective-permute-start.5 = (bf16[512,256]{1,0:T(8,128)(2,1)S(1)}, bf16[512,256]{1,0:T(8,128)(2,1)S(1)}, u32[]{:S(2)}, u32[]{:S(2)}) collective-permute-start(bf16[512,256]{1,0:T(8,128)(2,1)S(1)} %collective-permute-done.3.v_ref), channel_id=1, source_target_pairs={{0,8},{8,16},{16,24},{24,32},{32,40},{40,48},{48,56},{56,64},{64,7... | collective-permute-start | bytes 786440 | tf_op jit(solution)/shard_map/ppermute | solution.py:360
  94.1 1.2 collective-permute-done.4.refs_0_
  95.4 5.6 %collective-permute-start.6 = (bf16[512,256]{1,0:T(8,128)(2,1)S(1)}, bf16[512,256]{1,0:T(8,128)(2,1)S(1)}, u32[]{:S(2)}, u32[]{:S(2)}) collective-permute-start(bf16[512,256]{1,0:T(8,128)(2,1)S(1)} %collective-permute-done.4.refs_0_), channel_id=1, source_target_pairs={{0,8},{8,16},{16,24},{24,32},{32,40},{40,48},{48,56},{56,64},{64,7... | collective-permute-start | bytes 786440 | tf_op jit(solution)/shard_map/ppermute | solution.py:359
  101.0 0.0 collective-permute-done.10.refs_1_
  101.0 1.9 %collective-permute-start.13 = (bf16[256,2048]{1,0:T(8,128)(2,1)}, bf16[256,2048]{1,0:T(8,128)(2,1)S(1)}, u32[]{:S(2)}, u32[]{:S(2)}) collective-permute-start(bf16[256,2048]{1,0:T(8,128)(2,1)} %refs_0_.1), channel_id=1, source_target_pairs={{0,1},{1,0},{2,3},{3,2},{4,5},{5,4},{6,7},{7,6},{8,9},{9,8},{10,11... | collective-permute-start | bytes 3145736 | tf_op jit(solution)/shard_map/ppermute | solution.py:324
  102.9 0.0 collective-permute-done.11.refs_2_
  102.9 2.4 %collective-permute-start.14 = (bf16[256,2048]{1,0:T(8,128)(2,1)}, bf16[256,2048]{1,0:T(8,128)(2,1)S(1)}, u32[]{:S(2)}, u32[]{:S(2)}) collective-permute-start(bf16[256,2048]{1,0:T(8,128)(2,1)} %collective-permute-done.10.refs_1_), channel_id=1, source_target_pairs={{0,1},{1,0},{2,3},{3,2},{4,5},{5,4},{6,7},{7,6},{8,9},{9,8},{10,11... | collective-permute-start | bytes 3145736 | tf_op jit(solution)/shard_map/ppermute | solution.py:324
  105.3 0.0 collective-permute-done.12.refs_3_
  105.3 1.9 %collective-permute-start.15 = (bf16[256,2048]{1,0:T(8,128)(2,1)}, bf16[256,2048]{1,0:T(8,128)(2,1)S(1)}, u32[]{:S(2)}, u32[]{:S(2)}) collective-permute-start(bf16[256,2048]{1,0:T(8,128)(2,1)} %collective-permute-done.11.refs_2_), channel_id=1, source_target_pairs={{0,1},{1,0},{2,3},{3,2},{4,5},{5,4},{6,7},{7,6},{8,9},{9,8},{10,11... | collective-permute-start | bytes 3145736 | tf_op jit(solution)/shard_map/ppermute | solution.py:324
  107.3 0.0 collective-permute-done.5.refs_1_
  107.3 2.4 %collective-permute-start.16 = (bf16[256,2048]{1,0:T(8,128)(2,1)}, bf16[256,2048]{1,0:T(8,128)(2,1)}, u32[]{:S(2)}, u32[]{:S(2)}) collective-permute-start(bf16[256,2048]{1,0:T(8,128)(2,1)} %collective-permute-done.12.refs_3_), channel_id=1, source_target_pairs={{0,1},{1,0},{2,3},{3,2},{4,5},{5,4},{6,7},{7,6},{8,9},{9,8},{10,11... | collective-permute-start | bytes 3145736 | tf_op jit(solution)/shard_map/ppermute | solution.py:324
  109.7 0.0 collective-permute-done.6.refs_0_
  109.7 1.9 %collective-permute-start.7 = (bf16[512,256]{1,0:T(8,128)(2,1)S(1)}, bf16[512,256]{1,0:T(8,128)(2,1)S(1)}, u32[]{:S(2)}, u32[]{:S(2)}) collective-permute-start(bf16[512,256]{1,0:T(8,128)(2,1)S(1)} %collective-permute-done.5.refs_1_), channel_id=1, source_target_pairs={{0,8},{8,16},{16,24},{24,32},{32,40},{40,48},{48,56},{56,64},{64,7... | collective-permute-start | bytes 786440 | tf_op jit(solution)/shard_map/ppermute | solution.py:360
  111.6 8.2 %collective-permute-done.7.refs_1_ = bf16[512,256]{1,0:T(8,128)(2,1)S(1)} collective-permute-done((bf16[512,256]{1,0:T(8,128)(2,1)S(1)}, bf16[512,256]{1,0:T(8,128)(2,1)S(1)}, u32[]{:S(2)}, u32[]{:S(2)}) %collective-permute-start.7) | collective-permute-done | bytes 262176 | tf_op jit(solution)/shard_map/ppermute | solution.py:360
  119.8 3.4 %collective-permute-start.8 = (bf16[512,256]{1,0:T(8,128)(2,1)S(1)}, bf16[512,256]{1,0:T(8,128)(2,1)S(1)}, u32[]{:S(2)}, u32[]{:S(2)}) collective-permute-start(bf16[512,256]{1,0:T(8,128)(2,1)S(1)} %collective-permute-done.6.refs_0_), channel_id=1, source_target_pairs={{0,8},{8,16},{16,24},{24,32},{32,40},{40,48},{48,56},{56,64},{64,7... | collective-permute-start | bytes 786440 | tf_op jit(solution)/shard_map/ppermute | solution.py:359
  123.2 5.8 %collective-permute-done.8.refs_0_ = bf16[512,256]{1,0:T(8,128)(2,1)S(1)} collective-permute-done((bf16[512,256]{1,0:T(8,128)(2,1)S(1)}, bf16[512,256]{1,0:T(8,128)(2,1)S(1)}, u32[]{:S(2)}, u32[]{:S(2)}) %collective-permute-start.8) | collective-permute-done | bytes 262176 | tf_op jit(solution)/shard_map/ppermute | solution.py:359
  129.1 4.9 %collective-permute-start.9 = (bf16[512,256]{1,0:T(8,128)(2,1)S(1)}, bf16[512,256]{1,0:T(8,128)(2,1)S(1)}, u32[]{:S(2)}, u32[]{:S(2)}) collective-permute-start(bf16[512,256]{1,0:T(8,128)(2,1)S(1)} %collective-permute-done.7.refs_1_), channel_id=1, source_target_pairs={{0,8},{8,16},{16,24},{24,32},{32,40},{40,48},{48,56},{56,64},{64,7... | collective-permute-start | bytes 786440 | tf_op jit(solution)/shard_map/ppermute | solution.py:360
  134.0 3.5 %shard_map.88 = (f32[512,256]{1,0:T(8,128)S(1)}, f32[512,256]{1,0:T(8,128)S(1)}, f32[512,256]{1,0:T(8,128)S(1)}) custom-call(bf16[512,256]{1,0:T(8,128)(2,1)S(1)} %get-tuple-element.20.q_ref, bf16[512,256]{1,0:T(8,128)(2,1)S(1)} %get-tuple-element.22.k_ref, bf16[512,256]{1,0:T(8,128)(2,1)S(1)} %get-tuple-element.23.v_ref), custom_call_target="tpu_custom_call" | custom-call | flops 536870912 | bytes 786432 | tf_op jit(solution)/shard_map/pallas_call | solution.py:295
  137.5 4.1 %shard_map.89 = (f32[512,256]{1,0:T(8,128)S(1)}, f32[512,256]{1,0:T(8,128)S(1)}, f32[512,256]{1,0:T(8,128)S(1)}) custom-call(s32[4]{0:T(128)S(1)} %pad_add_fusion.place_ref, bf16[512,256]{1,0:T(8,128)(2,1)S(1)} %get-tuple-element.20.q_ref, f32[512,256]{1,0:T(8,128)S(1)} %get-tuple-element.24.max_ref, f32[512,256]{1,0:T(8,128)S(1)} %get-tuple-element.25.sum_ref, ...), custom_call_target="tpu_custom_call" | custom-call | flops 268435456 | bytes 2359312 | tf_op jit(solution)/shard_map/pallas_call | solution.py:295
  141.6 3.6 %shard_map.90 = (f32[512,256]{1,0:T(8,128)S(1)}, f32[512,256]{1,0:T(8,128)S(1)}, f32[512,256]{1,0:T(8,128)S(1)}) custom-call(s32[4]{0:T(128)S(1)} %pad_add_fusion.place_ref, bf16[512,256]{1,0:T(8,128)(2,1)S(1)} %get-tuple-element.20.q_ref, f32[512,256]{1,0:T(8,128)S(1)} %get-tuple-element.27.max_ref, f32[512,256]{1,0:T(8,128)S(1)} %get-tuple-element.28.sum_ref, ...), custom_call_target="tpu_custom_call" | custom-call | flops 268435456 | bytes 2359312 | tf_op jit(solution)/shard_map/pallas_call | solution.py:295
  145.2 3.6 %shard_map.91 = (f32[512,256]{1,0:T(8,128)S(1)}, f32[512,256]{1,0:T(8,128)S(1)}, f32[512,256]{1,0:T(8,128)S(1)}) custom-call(s32[4]{0:T(128)S(1)} %pad_add_fusion.place_ref, bf16[512,256]{1,0:T(8,128)(2,1)S(1)} %get-tuple-element.20.q_ref, f32[512,256]{1,0:T(8,128)S(1)} %get-tuple-element.30.max_ref, f32[512,256]{1,0:T(8,128)S(1)} %get-tuple-element.31.sum_ref, ...), custom_call_target="tpu_custom_call" | custom-call | flops 268435456 | bytes 2359312 | tf_op jit(solution)/shard_map/pallas_call | solution.py:295
  148.7 0.0 collective-permute-done.9.refs_1_
  148.8 0.0 copy-start.4
  148.8 3.9 %shard_map.92 = (bf16[512,256]{1,0:T(8,128)(2,1)S(1)}, f32[512,256]{1,0:T(8,128)S(1)}) custom-call(s32[4]{0:T(128)S(1)} %pad_add_fusion.place_ref, bf16[512,256]{1,0:T(8,128)(2,1)S(1)} %get-tuple-element.20.q_ref, f32[512,256]{1,0:T(8,128)S(1)} %get-tuple-element.33.max_ref, f32[512,256]{1,0:T(8,128)S(1)} %get-tuple-element.34.sum_ref, ...), custom_call_target="tpu_custom_call" | custom-call | flops 268435456 | bytes 2359312 | tf_op jit(solution)/shard_map/pallas_call | solution.py:295
  152.7 0.0 copy-start.2
  152.7 0.7 copy-done.2
  153.4 0.8 copy-done.5
  154.2 4.3 %all-to-all-start.1 = ((bf16[8,64,256]{2,1,0:T(8,128)(2,1)}), bf16[8,64,256]{2,1,0:T(8,128)(2,1)S(1)}, u32[]{:S(2)}, u32[]{:S(2)}) async-start(bf16[8,64,256]{2,1,0:T(8,128)(2,1)} %bitcast.11), calls=%async_computation.1 | async-start | bytes 524288 | tf_op jit(solution)/shard_map/all_to_all | solution.py:400
  158.5 1.0 copy-done.6
  159.5 1.3 shard_map.94
  160.8 0.0 collective-permute-done.13.refs_4_
  160.8 0.0 collective-permute-done.14.refs_5_
  160.8 0.0 collective-permute-done.15.refs_6_
  160.8 0.0 collective-permute-done.16.refs_7_
  160.8 5.2 %all-to-all-done.1.att_ref = bf16[8,64,256]{2,1,0:T(8,128)(2,1)S(1)} async-done(((bf16[8,64,256]{2,1,0:T(8,128)(2,1)}), bf16[8,64,256]{2,1,0:T(8,128)(2,1)S(1)}, u32[]{:S(2)}, u32[]{:S(2)}) %all-to-all-start.1) | async-done | bytes 262176 | tf_op jit(solution)/shard_map/all_to_all | solution.py:400
  166.0 0.0 copy-done.4
  166.0 5.1 %shard_map.93 = bf16[64,2048]{1,0:T(8,128)(2,1)} custom-call(s32[4]{0:T(128)S(1)} %pad_add_fusion.place_ref, bf16[8,64,256]{2,1,0:T(8,128)(2,1)S(1)} %all-to-all-done.1.att_ref, bf16[256,2048]{1,0:T(8,128)(2,1)} %refs_0_.1, bf16[256,2048]{1,0:T(8,128)(2,1)} %collective-permute-done.10.refs_1_, bf16[256,2048]{1,0:T(8,128)(2,1)} %collective-permute-done.11.refs_2_, ...), custom_call_target="tpu_custom_call" | custom-call | flops 536870912 | bytes 8658960 | tf_op jit(solution)/shard_map/pallas_call | solution.py:295
  (6 shorter events, 0.0 us)
Async XLA Ops:
  3.2 54.7 %copy-start = (bf16[512,2048]{1,0:T(8,128)(2,1)S(1)}, bf16[512,2048]{1,0:T(8,128)(2,1)}, u32[]{:S(2)}) copy-start(bf16[512,2048]{1,0:T(8,128)(2,1)} %hidden_ref.1) | copy-start | bytes 6291460
  3.2 54.7 %copy-start.3 = (f32[2048]{0:T(1024)S(1)}, f32[2048]{0:T(1024)}, u32[]{:S(2)}) copy-start(f32[2048]{0:T(1024)} %param.8) | copy-start | bytes 24580
  3.2 46.3 %all-to-all-start = ((bf16[32,32,512]{2,1,0:T(8,128)(2,1)}), bf16[32,32,512]{2,1,0:T(8,128)(2,1)S(1)}, u32[]{:S(2)}, u32[]{:S(2)}) async-start(bf16[32,32,512]{2,1,0:T(8,128)(2,1)} %pad_maximum_fusion), calls=%async_computation | async-start | bytes 2097152 | tf_op jit(solution)/shard_map/all_to_all | solution.py:315
  19.3 81.6 %collective-permute-start.10 = (bf16[256,2048]{1,0:T(8,128)(2,1)}, bf16[256,2048]{1,0:T(8,128)(2,1)}, u32[]{:S(2)}, u32[]{:S(2)}) collective-permute-start(bf16[256,2048]{1,0:T(8,128)(2,1)} %refs_0_.1), channel_id=1, source_target_pairs={{0,2},{2,4},{4,6},{6,0},{1,3},{3,5},{5,7},{7,1},{8,10},{10,12},{12... | collective-permute-start | bytes 3145736 | tf_op jit(solution)/shard_map/ppermute | solution.py:322
  22.7 80.2 %collective-permute-start.11 = (bf16[256,2048]{1,0:T(8,128)(2,1)}, bf16[256,2048]{1,0:T(8,128)(2,1)}, u32[]{:S(2)}, u32[]{:S(2)}) collective-permute-start(bf16[256,2048]{1,0:T(8,128)(2,1)} %refs_0_.1), channel_id=1, source_target_pairs={{0,6},{2,0},{4,2},{6,4},{1,7},{3,1},{5,3},{7,5},{8,14},{10,8},{12,... | collective-permute-start | bytes 3145736 | tf_op jit(solution)/shard_map/ppermute | solution.py:322
  26.4 78.9 %collective-permute-start.12 = (bf16[256,2048]{1,0:T(8,128)(2,1)}, bf16[256,2048]{1,0:T(8,128)(2,1)}, u32[]{:S(2)}, u32[]{:S(2)}) collective-permute-start(bf16[256,2048]{1,0:T(8,128)(2,1)} %refs_0_.1), channel_id=1, source_target_pairs={{0,4},{2,6},{4,0},{6,2},{1,5},{3,7},{5,1},{7,3},{8,12},{10,14},{12... | collective-permute-start | bytes 3145736 | tf_op jit(solution)/shard_map/ppermute | solution.py:322
  50.5 14.0 %collective-permute-start = (bf16[2,256,512]{2,1,0:T(8,128)(2,1)}, bf16[2,256,512]{2,1,0:T(8,128)(2,1)}, u32[]{:S(2)}, u32[]{:S(2)}) collective-permute-start(bf16[2,256,512]{2,1,0:T(8,128)(2,1)} %bitcast.6), channel_id=1, source_target_pairs={{0,64},{64,128},{128,192},{192,256},{256,320},{320,384},{384,448},... | collective-permute-start | bytes 1572872 | tf_op jit(solution)/shard_map/ppermute | solution.py:317
  54.6 11.7 %collective-permute-start.1 = (bf16[2,256,512]{2,1,0:T(8,128)(2,1)}, bf16[2,256,512]{2,1,0:T(8,128)(2,1)}, u32[]{:S(2)}, u32[]{:S(2)}) collective-permute-start(bf16[2,256,512]{2,1,0:T(8,128)(2,1)} %bitcast.7), channel_id=1, source_target_pairs={{0,448},{64,0},{128,64},{192,128},{256,192},{320,256},{384,320},{4... | collective-permute-start | bytes 1572872 | tf_op jit(solution)/shard_map/ppermute | solution.py:318
  58.0 1.2 copy-start.1
  70.5 12.5 %collective-permute-start.2 = (bf16[512,256]{1,0:T(8,128)(2,1)S(1)}, bf16[512,256]{1,0:T(8,128)(2,1)S(1)}, u32[]{:S(2)}, u32[]{:S(2)}) collective-permute-start(bf16[512,256]{1,0:T(8,128)(2,1)S(1)} %get-tuple-element.22.k_ref), channel_id=1, source_target_pairs={{0,8},{8,16},{16,24},{24,32},{32,40},{40,48},{48,56},{56,64},{64,7... | collective-permute-start | bytes 786440 | tf_op jit(solution)/shard_map/ppermute | solution.py:359
  76.4 12.3 %collective-permute-start.3 = (bf16[512,256]{1,0:T(8,128)(2,1)S(1)}, bf16[512,256]{1,0:T(8,128)(2,1)S(1)}, u32[]{:S(2)}, u32[]{:S(2)}) collective-permute-start(bf16[512,256]{1,0:T(8,128)(2,1)S(1)} %get-tuple-element.23.v_ref), channel_id=1, source_target_pairs={{0,8},{8,16},{16,24},{24,32},{32,40},{40,48},{48,56},{56,64},{64,7... | collective-permute-start | bytes 786440 | tf_op jit(solution)/shard_map/ppermute | solution.py:360
  83.1 12.3 %collective-permute-start.4 = (bf16[512,256]{1,0:T(8,128)(2,1)S(1)}, bf16[512,256]{1,0:T(8,128)(2,1)S(1)}, u32[]{:S(2)}, u32[]{:S(2)}) collective-permute-start(bf16[512,256]{1,0:T(8,128)(2,1)S(1)} %collective-permute-done.2.k_ref), channel_id=1, source_target_pairs={{0,8},{8,16},{16,24},{24,32},{32,40},{40,48},{48,56},{56,64},{64,7... | collective-permute-start | bytes 786440 | tf_op jit(solution)/shard_map/ppermute | solution.py:359
  88.7 18.6 %collective-permute-start.5 = (bf16[512,256]{1,0:T(8,128)(2,1)S(1)}, bf16[512,256]{1,0:T(8,128)(2,1)S(1)}, u32[]{:S(2)}, u32[]{:S(2)}) collective-permute-start(bf16[512,256]{1,0:T(8,128)(2,1)S(1)} %collective-permute-done.3.v_ref), channel_id=1, source_target_pairs={{0,8},{8,16},{16,24},{24,32},{32,40},{40,48},{48,56},{56,64},{64,7... | collective-permute-start | bytes 786440 | tf_op jit(solution)/shard_map/ppermute | solution.py:360
  95.4 14.3 %collective-permute-start.6 = (bf16[512,256]{1,0:T(8,128)(2,1)S(1)}, bf16[512,256]{1,0:T(8,128)(2,1)S(1)}, u32[]{:S(2)}, u32[]{:S(2)}) collective-permute-start(bf16[512,256]{1,0:T(8,128)(2,1)S(1)} %collective-permute-done.4.refs_0_), channel_id=1, source_target_pairs={{0,8},{8,16},{16,24},{24,32},{32,40},{40,48},{48,56},{56,64},{64,7... | collective-permute-start | bytes 786440 | tf_op jit(solution)/shard_map/ppermute | solution.py:359
  101.0 59.8 %collective-permute-start.13 = (bf16[256,2048]{1,0:T(8,128)(2,1)}, bf16[256,2048]{1,0:T(8,128)(2,1)S(1)}, u32[]{:S(2)}, u32[]{:S(2)}) collective-permute-start(bf16[256,2048]{1,0:T(8,128)(2,1)} %refs_0_.1), channel_id=1, source_target_pairs={{0,1},{1,0},{2,3},{3,2},{4,5},{5,4},{6,7},{7,6},{8,9},{9,8},{10,11... | collective-permute-start | bytes 3145736 | tf_op jit(solution)/shard_map/ppermute | solution.py:324
  102.9 57.9 %collective-permute-start.14 = (bf16[256,2048]{1,0:T(8,128)(2,1)}, bf16[256,2048]{1,0:T(8,128)(2,1)S(1)}, u32[]{:S(2)}, u32[]{:S(2)}) collective-permute-start(bf16[256,2048]{1,0:T(8,128)(2,1)} %collective-permute-done.10.refs_1_), channel_id=1, source_target_pairs={{0,1},{1,0},{2,3},{3,2},{4,5},{5,4},{6,7},{7,6},{8,9},{9,8},{10,11... | collective-permute-start | bytes 3145736 | tf_op jit(solution)/shard_map/ppermute | solution.py:324
  105.3 55.5 %collective-permute-start.15 = (bf16[256,2048]{1,0:T(8,128)(2,1)}, bf16[256,2048]{1,0:T(8,128)(2,1)S(1)}, u32[]{:S(2)}, u32[]{:S(2)}) collective-permute-start(bf16[256,2048]{1,0:T(8,128)(2,1)} %collective-permute-done.11.refs_2_), channel_id=1, source_target_pairs={{0,1},{1,0},{2,3},{3,2},{4,5},{5,4},{6,7},{7,6},{8,9},{9,8},{10,11... | collective-permute-start | bytes 3145736 | tf_op jit(solution)/shard_map/ppermute | solution.py:324
  107.3 53.5 %collective-permute-start.16 = (bf16[256,2048]{1,0:T(8,128)(2,1)}, bf16[256,2048]{1,0:T(8,128)(2,1)}, u32[]{:S(2)}, u32[]{:S(2)}) collective-permute-start(bf16[256,2048]{1,0:T(8,128)(2,1)} %collective-permute-done.12.refs_3_), channel_id=1, source_target_pairs={{0,1},{1,0},{2,3},{3,2},{4,5},{5,4},{6,7},{7,6},{8,9},{9,8},{10,11... | collective-permute-start | bytes 3145736 | tf_op jit(solution)/shard_map/ppermute | solution.py:324
  109.7 10.1 %collective-permute-start.7 = (bf16[512,256]{1,0:T(8,128)(2,1)S(1)}, bf16[512,256]{1,0:T(8,128)(2,1)S(1)}, u32[]{:S(2)}, u32[]{:S(2)}) collective-permute-start(bf16[512,256]{1,0:T(8,128)(2,1)S(1)} %collective-permute-done.5.refs_1_), channel_id=1, source_target_pairs={{0,8},{8,16},{16,24},{24,32},{32,40},{40,48},{48,56},{56,64},{64,7... | collective-permute-start | bytes 786440 | tf_op jit(solution)/shard_map/ppermute | solution.py:360
  119.8 9.2 %collective-permute-start.8 = (bf16[512,256]{1,0:T(8,128)(2,1)S(1)}, bf16[512,256]{1,0:T(8,128)(2,1)S(1)}, u32[]{:S(2)}, u32[]{:S(2)}) collective-permute-start(bf16[512,256]{1,0:T(8,128)(2,1)S(1)} %collective-permute-done.6.refs_0_), channel_id=1, source_target_pairs={{0,8},{8,16},{16,24},{24,32},{32,40},{40,48},{48,56},{56,64},{64,7... | collective-permute-start | bytes 786440 | tf_op jit(solution)/shard_map/ppermute | solution.py:359
  129.1 19.7 %collective-permute-start.9 = (bf16[512,256]{1,0:T(8,128)(2,1)S(1)}, bf16[512,256]{1,0:T(8,128)(2,1)S(1)}, u32[]{:S(2)}, u32[]{:S(2)}) collective-permute-start(bf16[512,256]{1,0:T(8,128)(2,1)S(1)} %collective-permute-done.7.refs_1_), channel_id=1, source_target_pairs={{0,8},{8,16},{16,24},{24,32},{32,40},{40,48},{48,56},{56,64},{64,7... | collective-permute-start | bytes 786440 | tf_op jit(solution)/shard_map/ppermute | solution.py:360
  148.8 17.2 %copy-start.4 = (f32[2048]{0:T(1024)S(1)}, f32[2048]{0:T(1024)}, u32[]{:S(2)}) copy-start(f32[2048]{0:T(1024)} %param.13) | copy-start | bytes 24580
  152.7 0.7 copy-start.2
  153.4 0.8 copy-start.5
  154.2 11.8 %all-to-all-start.1 = ((bf16[8,64,256]{2,1,0:T(8,128)(2,1)}), bf16[8,64,256]{2,1,0:T(8,128)(2,1)S(1)}, u32[]{:S(2)}, u32[]{:S(2)}) async-start(bf16[8,64,256]{2,1,0:T(8,128)(2,1)} %bitcast.11), calls=%async_computation.1 | async-start | bytes 524288 | tf_op jit(solution)/shard_map/all_to_all | solution.py:400
  158.5 1.0 copy-start.6
